TPU v7x, 128 devices: a whole 4x4x4 slice. The times are simulated.
128 devices in a mesh: sp: 32 (over z, y, core), tp: 4 (over x).
Axes of the slice: x: 4, y: 4, z: 4, core: 2. Of those that a mesh axis runs over, the one named last changes fastest.
Arguments:
- queries: bfloat16 [12288, 2048], P('sp', 'tp'), may hold values from -6 to 6
- keys: bfloat16 [12288, 2048], P('sp', 'tp'), may hold values from -6 to 6
- values: bfloat16 [12288, 2048], P('sp', 'tp'), may hold values from -6 to 6
- gates: bfloat16 [12288, 2048], P('sp', 'tp'), may hold values from -8 to 8
- decay_pre: float32 [32, 12288], P('tp', 'sp'), may hold values from -18 to 3
- beta_pre: float32 [32, 12288], P('tp', 'sp'), may hold values from -10 to 3
- out_gain: float32 [64], replicated, may hold values from 0.1 to 1.9
- w_out: bfloat16 [2048, 2048], P('tp'), may hold values from -0.125 to 0.125
- stream: bfloat16 [12288, 2048], P(('sp', 'tp')), may hold values from -6 to 6
- norm_gain: float32 [2048], replicated, may hold values from 0.1 to 1.9
- w_gate: bfloat16 [2048, 5632], P('sp', 'tp'), may hold values from -0.125 to 0.125
- w_up: bfloat16 [2048, 5632], P('sp', 'tp'), may hold values from -0.125 to 0.125
- w_down: bfloat16 [5632, 2048], P('tp', 'sp'), may hold values from -0.078125 to 0.078125
Outputs:
- updated: bfloat16 [12288, 2048], P(('sp', 'tp'))
All inputs are finite; a program needn't handle non-finite values.
Results may differ from a plain program's by a relative error of at most 0.019.
Values may be sent and summed in bfloat16 or wider, within the bound.
No kernel may reach another device: no remote copies, remote signals or barrier semaphores. Data moves between devices by JAX's collectives and lax.ppermute only.
A program may use at most 128 MiB of HBM per device.

v0:
```python
import jax
import jax.numpy as jnp
from jax import lax
from jax.sharding import Mesh
from jax.sharding import PartitionSpec as P

HEAD_DIM = 64
BLOCK = 64
SP = ("sp_0", "sp_1", "sp_2")
SP_TP = ("sp_0", "sp_1", "sp_2", "tp")


EPSILON = 1e-06


def turned_gather(arrays, axis, dims):
    turned = [jnp.moveaxis(a, dim, 0) for a, dim in zip(arrays, dims)]
    widths = [t[0].size for t in turned]
    both = jnp.concatenate([t.reshape(-1, w) for t, w in zip(turned, widths)], axis=1)
    whole = lax.all_gather(both, axis, axis=0, tiled=True)
    pieces = jnp.split(whole, [sum(widths[:k]) for k in range(1, len(widths))], axis=1)
    return tuple(
        (
            jnp.moveaxis(b.reshape(-1, *t.shape[1:]), 0, dim)
            for b, t, dim in zip(pieces, turned, dims)
        )
    )


def filled_with(x, identity):
    return jax.tree.map(
        lambda part, zero: jnp.zeros_like(part) + jnp.asarray(zero, part.dtype), x, identity
    )


def carried_in(x, axes, combine, identity):
    before = start = filled_with(x, identity)
    subtotal = x
    for axis in reversed(axes):
        size, index = (lax.axis_size(axis), lax.axis_index(axis))
        pieces = jax.tree.map(
            lambda part, kind: lax.all_gather(part.astype(kind), axis),
            subtotal,
            (jnp.bfloat16, jnp.bfloat16),
        )
        inside, subtotal = (start, start)
        for k in range(size):
            passed = k < index
            subtotal = combine(
                subtotal, jax.tree.map(lambda part, own: part[k].astype(own.dtype), pieces, x)
            )
            inside = jax.tree.map(lambda new, old: jnp.where(passed, new, old), subtotal, inside)
        before = combine(inside, before)
    return before


def laid_out(pieces, dim):
    lengths = list(pieces.shape[1:])
    lengths[dim] *= pieces.shape[0]
    return jnp.moveaxis(pieces, 0, dim).reshape(lengths)


def sent_to_all(x, axis):
    size = lax.axis_size(axis)
    return lax.all_to_all(jnp.broadcast_to(x[None], (size, *x.shape)), axis, 0, 0, tiled=True)


def collect(x, axis, dim):
    return laid_out(sent_to_all(x, axis), dim)


def split_up(x, dim, size):
    lengths = x.shape
    pieces = x.reshape(*lengths[:dim], size, lengths[dim] // size, *lengths[dim + 1 :])
    return jnp.moveaxis(pieces, dim, 0)


def summed_on_arrival(x, axis, dim):
    pieces = split_up(x, dim, lax.axis_size(axis))
    arrived = lax.all_to_all(pieces, axis, split_axis=0, concat_axis=0, tiled=True)
    return arrived.astype(jnp.float32).sum(axis=0)


def unit_lower_inverse(lower_mat):
    span_len = lower_mat.shape[-1]
    identity = jnp.eye(span_len, dtype=jnp.float32)
    power = -lower_mat
    inverse = identity + power
    steps = 1
    while 1 << steps < span_len:
        power = jnp.einsum("...ij,...jk->...ik", power, power)
        inverse = jnp.einsum("...ij,...jk->...ik", inverse, identity + power)
        steps = steps + 1
    return inverse


def prepare(queries, keys, values, beta_pre, decay_pre):
    length = queries.shape[0]
    heads = queries.shape[1] // HEAD_DIM

    def split_heads(arr):
        return arr.astype(jnp.float32).reshape(length, heads, HEAD_DIM)

    query_unit = jax.nn.silu(split_heads(queries))
    query_unit = query_unit * lax.rsqrt(
        jnp.sum(query_unit * query_unit, axis=-1, keepdims=True) + EPSILON
    )
    query_unit = (query_unit * HEAD_DIM ** (-0.5)).astype(jnp.bfloat16)
    key_unit = jax.nn.silu(split_heads(keys))
    key_unit = (
        key_unit * lax.rsqrt(jnp.sum(key_unit * key_unit, axis=-1, keepdims=True) + EPSILON)
    ).astype(jnp.bfloat16)
    value_act = jax.nn.silu(split_heads(values))
    strength = jax.nn.sigmoid(beta_pre)
    log_decay = -jax.nn.softplus(decay_pre)
    nblocks = length // BLOCK

    def blocked(arr):
        return arr.reshape(nblocks, BLOCK, heads, HEAD_DIM).transpose(0, 2, 1, 3)

    def blocked_rates(arr):
        return arr.reshape(heads, nblocks, BLOCK).transpose(1, 0, 2)

    return (
        blocked(query_unit),
        blocked(key_unit),
        blocked(value_act),
        blocked_rates(strength),
        blocked_rates(log_decay),
    )


def block_terms(query_blk, key_blk, value_blk, strength_blk, decay_blk):
    span_len = query_blk.shape[-2]
    query_f = query_blk.astype(jnp.float32)
    key_f = key_blk.astype(jnp.float32)
    cumulative = jnp.cumsum(decay_blk, axis=-1)
    row_ids = jnp.arange(span_len)[:, None]
    col_ids = jnp.arange(span_len)[None, :]
    inclusive = row_ids >= col_ids
    strict = row_ids > col_ids
    decay_mat = jnp.exp(
        jnp.where(inclusive, cumulative[..., :, None] - cumulative[..., None, :], -jnp.inf)
    )
    key_inner = jnp.einsum(
        "...id,...jd->...ij", key_blk, key_blk, preferred_element_type=jnp.float32
    )
    lower_mat = jnp.where(strict, strength_blk[..., :, None] * key_inner * decay_mat, 0.0)
    key_strong = key_f * strength_blk[..., None]
    right_side = jnp.concatenate(
        [value_blk * strength_blk[..., None], key_strong * jnp.exp(cumulative)[..., None]], axis=-1
    )
    solved = jnp.einsum("...ij,...jk->...ik", unit_lower_inverse(lower_mat), right_side)
    width = value_blk.shape[-1]
    update_values = solved[..., :width]
    update_keys = solved[..., width:]
    query_inner = jnp.einsum(
        "...id,...jd->...ij", query_blk, key_blk, preferred_element_type=jnp.float32
    )
    inside_span = jnp.where(inclusive, query_inner * decay_mat, 0.0)
    final_decay = cumulative[..., -1:]
    key_attenuated = key_f * jnp.exp(final_decay - cumulative)[..., None]
    query_attenuated = query_f * jnp.exp(cumulative)[..., None]
    return (update_values, update_keys, inside_span, query_attenuated, key_attenuated, final_decay)


def advance(matrix_state, terms):
    update_values, update_keys, inside_span, query_attenuated, key_attenuated, final_decay = terms
    value_corrected = update_values - jnp.einsum("jod,jdg->jog", update_keys, matrix_state)
    output_result = jnp.einsum("jod,jdg->jog", query_attenuated, matrix_state) + jnp.einsum(
        "oyn,onk->oyk", inside_span, value_corrected
    )
    matrix_state = matrix_state * jnp.exp(final_decay)[..., None] + jnp.einsum(
        "lyq,lyf->lqf", key_attenuated, value_corrected
    )
    return (matrix_state, output_result)


def compose(carry, items):
    trans_mat, offset_mat = carry
    update_keys, update_values, key_attenuated, final_decay = items
    heads = update_keys.shape[0]
    identity = jnp.broadcast_to(jnp.eye(HEAD_DIM, dtype=jnp.float32), (heads, HEAD_DIM, HEAD_DIM))
    step_trans = jnp.exp(final_decay)[..., None] * identity - jnp.einsum(
        "hck,hcl->hkl", key_attenuated, update_keys
    )
    stride_displacement = jnp.einsum("lyq,lyf->lqf", key_attenuated, update_values)
    new_trans = jnp.einsum("hkl,hlm->hkm", step_trans, trans_mat)
    new_offset = jnp.einsum("hkl,hlm->hkm", step_trans, offset_mat) + stride_displacement
    return ((new_trans, new_offset), None)


def chain(earlier, later):
    joined_trans = jnp.einsum("hkl,hlm->hkm", later[0], earlier[0])
    joined_offset = jnp.einsum("hkl,hlm->hkm", later[0], earlier[1]) + later[1]
    return (joined_trans, joined_offset)


def finish(outputs, gates, out_gain):
    length = gates.shape[0]
    heads = gates.shape[1] // HEAD_DIM
    heads_out = outputs.transpose(0, 2, 1, 3).reshape(length, heads, HEAD_DIM)
    heads_out = heads_out * lax.rsqrt(
        jnp.mean(heads_out * heads_out, axis=-1, keepdims=True) + EPSILON
    )
    heads_out = heads_out * out_gain
    gated = heads_out * jax.nn.silu(gates.astype(jnp.float32).reshape(length, heads, HEAD_DIM))
    return gated.reshape(length, heads * HEAD_DIM).astype(jnp.bfloat16)


def per_device(
    queries,
    keys,
    values,
    gates,
    decay_pre,
    beta_pre,
    out_gain,
    w_out,
    stream,
    norm_gain,
    w_gate,
    w_up,
    w_down,
):
    gate_whole, up_whole, down_whole = turned_gather((w_gate, w_up, w_down), SP, (0, 0, 1))
    blocks = prepare(queries, keys, values, beta_pre, decay_pre)
    terms = block_terms(*blocks)
    update_values, update_keys, inside_span, query_attenuated, key_attenuated, final_decay = terms
    heads = update_keys.shape[1]
    identity = jnp.broadcast_to(jnp.eye(HEAD_DIM, dtype=jnp.float32), (heads, HEAD_DIM, HEAD_DIM))
    zero_state = jnp.zeros((heads, HEAD_DIM, HEAD_DIM), jnp.float32)
    (trans_mat, offset_mat), _ = lax.scan(
        compose, (identity, zero_state), (update_keys, update_values, key_attenuated, final_decay)
    )
    earlier_part = carried_in((trans_mat, offset_mat), SP, chain, (identity, zero_state))
    _, outputs = lax.scan(advance, earlier_part[1], terms)
    mixed_heads = finish(outputs, gates, out_gain)
    head_block = lax.all_to_all(mixed_heads, "tp", split_axis=0, concat_axis=1, tiled=True)
    out_whole = lax.all_gather(w_out, "tp", axis=0, tiled=True)
    projected = jnp.dot(head_block, out_whole, preferred_element_type=jnp.float32)
    middle = (stream.astype(jnp.float32) + projected).astype(jnp.bfloat16)
    middle_f = middle.astype(jnp.float32)
    normed = middle_f * lax.rsqrt(jnp.mean(middle_f * middle_f, axis=-1, keepdims=True) + EPSILON)
    normed = (normed * norm_gain).astype(jnp.bfloat16)
    span_rows = collect(normed, "tp", 0)
    gate_hidden = jnp.dot(span_rows, gate_whole, preferred_element_type=jnp.float32)
    up_hidden = jnp.dot(span_rows, up_whole, preferred_element_type=jnp.float32)
    hidden = (jax.nn.silu(gate_hidden) * up_hidden).astype(jnp.bfloat16)
    channel_term = jnp.dot(hidden, down_whole, preferred_element_type=jnp.float32)
    channel_sum = summed_on_arrival(channel_term.astype(jnp.bfloat16), "tp", 0)
    return (middle_f + 0.5 * channel_sum).astype(jnp.bfloat16)


def solution(mesh):
    finer = Mesh(mesh.devices.reshape(4, 4, 2, mesh.shape["tp"]), ("sp_0", "sp_1", "sp_2", "tp"))
    placed = (
        P(SP, "tp"),
        P(SP, "tp"),
        P(SP, "tp"),
        P(SP, "tp"),
        P("tp", SP),
        P("tp", SP),
        P(),
        P("tp", None),
        P(SP_TP, None),
        P(),
        P(SP, "tp"),
        P(SP, "tp"),
        P("tp", SP),
    )
    return jax.shard_map(
        per_device, mesh=finer, in_specs=placed, out_specs=P(SP_TP, None), check_vma=False
    )
```

profile of v0, /device:TPU:0, one launch (start us, length us, event | category | flops | bytes accessed | tf_op | source)
XLA Modules:
  0.0 222.9 jit_solution(13525093395992439991)
XLA Ops:
  9.4 1.6 copy.76
  12.1 1.7 copy.66
  14.2 1.5 reshape.165
  15.7 1.3 reduce_window_sum.11
  18.4 4.7 %fusion.54 = (bf16[6,8,64,64]{3,2,1,0:T(8,128)(2,1)}, bf16[6,64,8,64]{3,1,2,0:T(8,128)(2,1)S(1)}, bf16[6,8,64,64]{3,2,1,0:T(8,128)(2,1)}, bf16[6,8,64,64]{3,2,1,0:T(8,128)(2,1)}) fusion(f32[6,8,64]{2,1,0:T(8,128)S(1)} %get-tuple-element.220, f32[6,8,64]{2,1,0:T(8,128)S(1)} %copy.68, f32[6,64,8]{1,2,0:T(8,128)S(1)} %copy.67, f32[6,64,8,64]{3,1,2,0:T(8,128)} %copy.66, ...), kind=kLoop, calls=%fused_computation.58 | loop fusion | flops 5111808 | bytes 3981312 | tf_op jit(solution)/shard_map/mul | solution.py:151
  24.4 1.3 fusion.71
  26.5 1.2 copy-done
  28.0 3.1 %fusion.65 = bf16[6,8,64,64]{3,2,1,0:T(8,128)(2,1)} fusion(f32[6,8,64,64]{3,2,1,0:T(8,128)} %copy-done, bf16[6,8,64,64]{3,2,1,0:T(8,128)(2,1)} %fusion.71, f32[6,8,64,64]{3,2,1,0:T(8,128)S(1)} %fusion.154, f32[64,64]{1,0:T(8,128)S(1)} %fusion.142), kind=kOutput, calls=%fused_computation.72 | convolution fusion | flops 50724864 | bytes 2375680 | tf_op jit(solution)/shard_map/...ij,...jk->...ik/dot_general | solution.py:92
  31.1 1.9 fusion.59
  33.1 1.9 fusion.55
  36.2 1.4 convert_multiply_fusion.1
  37.6 1.5 copy.72
  39.2 1.7 fusion.151
  40.9 10.1 %while.28 = (s32[]{:T(128)}, bf16[8,64,64]{2,1,0:T(8,128)(2,1)S(1)}, bf16[8,64,64]{2,1,0:T(8,128)(2,1)S(1)}, f32[6,8,1]{1,2,0:T(1,128)S(1)}, bf16[6,8,64,64]{2,3...) while((s32[]{:T(128)}, ...), condition=%wide.region_3.4_spmd.clone.clone, body=%wide.region_2.3_spmd.clone.sunk.clone | while | flops 16982020 | bytes 1559195 | solution.py:233
  41.3 1.1 convolution_add_fusion.20
  44.7 1.1 convolution_add_fusion.20
  46.4 1.1 convolution_add_fusion.20
  51.0 2.0 all-gather
  53.0 2.0 all-gather.3
  55.3 13.4 %all-gather.4 = bf16[32,64,64]{2,1,0:T(8,128)(2,1)S(1)} all-gather(bf16[8,64,64]{2,1,0:T(8,128)(2,1)S(1)} %convolution_add_fusion.10), channel_id=6, replica_groups=mesh['sp_0'=4,'sp_1'=4,'sp_2'=2,'tp'=4] {'sp_1'}, dimensions={0}, use_global_device_ids=true | all-gather | bytes 327680 | tf_op jit(solution)/shard_map/all_gather | solution.py:42
  69.1 12.8 %all-gather.1 = bf16[32,64,64]{2,1,0:T(8,128)(2,1)S(1)} all-gather(bf16[8,64,64]{2,1,0:T(8,128)(2,1)S(1)} %fusion.157), channel_id=3, replica_groups=mesh['sp_0'=4,'sp_1'=4,'sp_2'=2,'tp'=4] {'sp_1'}, dimensions={0}, use_global_device_ids=true | all-gather | bytes 327680 | tf_op jit(solution)/shard_map/all_gather | solution.py:42
  82.6 14.8 %all-gather.5 = bf16[32,64,64]{2,1,0:T(8,128)(2,1)S(1)} all-gather(bf16[8,64,64]{2,1,0:T(8,128)(2,1)S(1)} %convolution_add_fusion.7), channel_id=7, replica_groups=mesh['sp_0'=4,'sp_1'=4,'sp_2'=2,'tp'=4] {'sp_0'}, dimensions={0}, use_global_device_ids=true | all-gather | bytes 327680 | tf_op jit(solution)/shard_map/all_gather | solution.py:42
  98.4 12.8 %all-gather.2 = bf16[32,64,64]{2,1,0:T(8,128)(2,1)S(1)} all-gather(bf16[8,64,64]{2,1,0:T(8,128)(2,1)S(1)} %fusion.160), channel_id=4, replica_groups=mesh['sp_0'=4,'sp_1'=4,'sp_2'=2,'tp'=4] {'sp_0'}, dimensions={0}, use_global_device_ids=true | all-gather | bytes 327680 | tf_op jit(solution)/shard_map/all_gather | solution.py:42
  113.0 1.2 fusion.77
  114.5 3.5 %multiply_select_fusion = bf16[6,8,64,64]{3,2,1,0:T(8,128)(2,1)} fusion(bf16[6,64,8,64]{3,1,2,0:T(8,128)(2,1)} %copy-done.6, f32[6,8,64]{2,1,0:T(8,128)S(1)} %copy-done.13, pred[64,64]{1,0:T(8,128)(4,1)S(1)} %get-tuple-element.225, f32[6,64,8,64]{3,1,2,0:T(8,128)} %copy.76, f32[6,64,8]{1,2,0:T(8,128)S(1)} %copy-done.25), kind=kOutput, calls=%fused_computation.65 | convolution fusion | flops 27328512 | bytes 1601536 | tf_op jit(solution)/shard_map/...id,...jd->...ij/dot_general | solution.py:157
  118.0 21.3 %while.27 = (s32[]{:T(128)}, f32[8,64,64]{2,1,0:T(8,128)S(1)}, f32[6,8,64,64]{3,2,1,0:T(8,128)S(1)}, f32[6,8,1]{1,2,0:T(1,128)S(1)}, bf16[6,8,64,64]{2,3,1,0:T(8...) while((s32[]{:T(128)}, f32[8,64,64]{2,1,0:T(8,128)S(1)}, ...), condition=%wide.region_6.7_spmd.clone, body=%wide.region_5.6_spmd.sunk.clone | while | flops 16941056 | bytes 2559141 | solution.py:237
  118.0 1.1 convolution_subtract_fusion.6
  119.2 1.1 fusion.270
  120.2 1.1 fusion.271
  121.6 1.1 convolution_subtract_fusion.6
  123.8 1.1 fusion.271
  125.1 1.1 convolution_subtract_fusion.6
  126.3 1.1 fusion.270
  127.3 1.1 fusion.271
  128.7 1.1 convolution_subtract_fusion.6
  130.9 1.1 fusion.271
  132.3 1.1 convolution_subtract_fusion.6
  134.5 1.1 fusion.271
  135.8 1.1 convolution_subtract_fusion.6
  138.0 1.1 fusion.271
  139.4 2.1 copy.80
  141.4 2.0 reshape.161
  145.2 12.2 %all_to_all.29 = bf16[4,96,512]{2,1,0:T(8,128)(2,1)S(1)} all-to-all(bf16[4,96,512]{2,1,0:T(8,128)(2,1)S(1)} %bitcast.192), channel_id=1, replica_groups=mesh['sp_0'=4,'sp_1'=4,'sp_2'=2,'tp'=4] {'tp'}, dimensions={0} | all-to-all | bytes 786432 | tf_op jit(solution)/shard_map/all_to_all | solution.py:239
  157.5 5.3 %multiply_reduce_fusion.1 = (f32[96]{0:T(128)S(1)}, f32[96,2048]{1,0:T(8,128)S(1)}) fusion(bf16[96,2048]{1,0:T(8,128)(2,1)S(1)} %bitcast.187, bf16[2048,2048]{1,0:T(8,128)(2,1)} %all-gather.9.cloned.1.call-done, bf16[96,2048]{1,0:T(8,128)(2,1)S(1)} %copy-done.11), kind=kOutput, calls=%fused_computation.110 | convolution fusion | flops 806485888 | bytes 9961856 | tf_op jit(solution)/shard_map/dot_general | solution.py:241
  163.2 16.1 %all_to_all.30 = bf16[4,96,2048]{2,1,0:T(8,128)(2,1)S(1)} all-to-all(bf16[4,96,2048]{2,1,0:T(8,128)(2,1)S(1)} %broadcast_in_dim.80), channel_id=1, replica_groups=mesh['sp_0'=4,'sp_1'=4,'sp_2'=2,'tp'=4] {'tp'}, dimensions={0} | all-to-all | bytes 3145728 | tf_op jit(solution)/shard_map/all_to_all | solution.py:65
  179.4 6.6 %fusion.39 = f32[384,1408]{1,0:T(8,128)} fusion(bf16[384,2048]{1,0:T(8,128)(2,1)S(1)} %bitcast.188, bf16[2048,4224]{1,0:T(8,128)(2,1)} %all-gather.11.cloned.1.call-done), kind=kOutput, calls=%fused_computation.47 | convolution fusion | flops 2214592512 | bytes 9502720 | tf_op jit(solution)/shard_map/dot_general | solution.py:247
  186.0 11.2 %fusion.47 = bf16[384,2048]{1,0:T(8,128)(2,1)} fusion(bf16[2048,4224]{1,0:T(8,128)(2,1)} %all-gather.11.cloned.1.call-done, bf16[384,2048]{1,0:T(8,128)(2,1)S(1)} %bitcast.189, f32[384,1408]{1,0:T(8,128)} %fusion.39), kind=kOutput, calls=%fused_computation.52 | convolution fusion | flops 4433215488 | bytes 16842752 | tf_op jit(solution)/shard_map/dot_general | solution.py:250
  197.1 17.8 %all_to_all.31 = bf16[4,96,2048]{2,1,0:T(8,128)(2,1)S(1)} all-to-all(bf16[4,96,2048]{2,1,0:T(8,128)(2,1)} %bitcast.190), channel_id=1, replica_groups=mesh['sp_0'=4,'sp_1'=4,'sp_2'=2,'tp'=4] {'tp'}, dimensions={0} | all-to-all | bytes 3145728 | tf_op jit(solution)/shard_map/all_to_all | solution.py:80
  (187 shorter events, 28.7 us)
Async XLA Ops:
  6.5 0.9 copy-start.14
  6.5 1.0 copy-start.16
  6.5 1.1 copy-start.15
  6.5 2.0 copy-start.26
  6.5 2.1 copy-start.8
  6.5 151.0 %all-gather.9.cloned.1.call-start = ((), (), s32[]{:S(2)}) async-start(), calls=%async_computation.3 | async-start | bytes 10485760 | tf_op jit(solution)/shard_map/all_gather | solution.py:240
  7.3 172.1 %all-gather.11.cloned.1.call-start = ((), (), s32[]{:S(2)}) async-start(), calls=%async_computation.4 | async-start | bytes 17842176 | tf_op jit(solution)/shard_map/all_gather | solution.py:20
  9.4 2.0 copy-start.9
  11.4 7.1 %copy-start.24 = (f32[6,64,8]{1,2,0:T(8,128)}, f32[6,64,8]{1,2,0:T(8,128)S(1)}, u32[]{:S(2)}) copy-start(f32[6,64,8]{1,2,0:T(8,128)S(1)} %copy.77) | copy-start | bytes 36868
  12.1 2.0 copy-start.27
  13.7 4.7 %copy-start.2 = (f32[6,64,8,64]{3,1,2,0:T(8,128)S(1)}, f32[6,64,8,64]{3,1,2,0:T(8,128)}, u32[]{:S(2)}) copy-start(f32[6,64,8,64]{3,1,2,0:T(8,128)} %copy.76) | copy-start | bytes 2359300
  17.0 6.1 %copy-start.12 = (f32[6,8,64]{2,1,0:T(8,128)}, f32[6,8,64]{2,1,0:T(8,128)S(1)}, u32[]{:S(2)}) copy-start(f32[6,8,64]{2,1,0:T(8,128)S(1)} %reduce_window_sum.11) | copy-start | bytes 36868
  17.1 14.1 %copy-start.3 = (f32[64,64]{1,0:T(8,128)}, f32[64,64]{1,0:T(8,128)S(1)}, u32[]{:S(2)}) copy-start(f32[64,64]{1,0:T(8,128)S(1)} %fusion.142) | copy-start | bytes 49156
  23.2 0.9 copy-start.6
  26.4 1.2 copy-start
  35.0 1.1 copy-start.7
  35.0 1.1 copy-start.23
  36.2 2.9 %copy-start.22 = (f32[6,8,1]{2,1,0:T(8,128)S(1)}, f32[6,8,1]{2,1,0:T(8,128)}, u32[]{:S(2)}) copy-start(f32[6,8,1]{2,1,0:T(8,128)} %get-tuple-element.222) | copy-start | bytes 580
  39.2 1.7 copy-start.4
  55.1 14.0 %copy-start.17 = (bf16[8,64,64]{2,1,0:T(8,128)(2,1)}, bf16[8,64,64]{2,1,0:T(8,128)(2,1)S(1)}, u32[]{:S(2)}) copy-start(bf16[8,64,64]{2,1,0:T(8,128)(2,1)S(1)} %convolution_add_fusion.11) | copy-start | bytes 196612
  97.6 13.7 %copy-start.19 = (bf16[8,64,64]{2,1,0:T(8,128)(2,1)}, bf16[8,64,64]{2,1,0:T(8,128)(2,1)S(1)}, u32[]{:S(2)}) copy-start(bf16[8,64,64]{2,1,0:T(8,128)(2,1)S(1)} %fusion.120) | copy-start | bytes 196612
  97.8 0.7 copy-start.20
  98.0 13.8 %copy-start.21 = (bf16[8,64,64]{2,1,0:T(8,128)(2,1)}, bf16[8,64,64]{2,1,0:T(8,128)(2,1)S(1)}, u32[]{:S(2)}) copy-start(bf16[8,64,64]{2,1,0:T(8,128)(2,1)S(1)} %fusion.159) | copy-start | bytes 196612
  111.9 2.3 %copy-start.5 = (f32[64,64]{1,0:T(8,128)S(1)}, f32[64,64]{1,0:T(8,128)}, u32[]{:S(2)}) copy-start(f32[64,64]{1,0:T(8,128)} %copy-done.3) | copy-start | bytes 49156
  112.0 2.3 %copy-start.18 = (bf16[8,64,64]{2,1,0:T(8,128)(2,1)S(1)}, bf16[8,64,64]{2,1,0:T(8,128)(2,1)}, u32[]{:S(2)}) copy-start(bf16[8,64,64]{2,1,0:T(8,128)(2,1)} %copy-done.17) | copy-start | bytes 196612
  112.2 2.3 %copy-start.13 = (f32[6,8,64]{2,1,0:T(8,128)S(1)}, f32[6,8,64]{2,1,0:T(8,128)}, u32[]{:S(2)}) copy-start(f32[6,8,64]{2,1,0:T(8,128)} %copy-done.12) | copy-start | bytes 36868
  112.2 2.3 %copy-start.25 = (f32[6,64,8]{1,2,0:T(8,128)S(1)}, f32[6,64,8]{1,2,0:T(8,128)}, u32[]{:S(2)}) copy-start(f32[6,64,8]{1,2,0:T(8,128)} %copy-done.24) | copy-start | bytes 36868
  114.5 3.6 %copy-start.1 = (f32[6,8,64,64]{3,2,1,0:T(8,128)S(1)}, f32[6,8,64,64]{3,2,1,0:T(8,128)}, u32[]{:S(2)}) copy-start(f32[6,8,64,64]{3,2,1,0:T(8,128)} %custom-call.1) | copy-start | bytes 2359300
  143.9 0.7 copy-start.29
  144.0 1.0 copy-start.10
  145.0 12.6 %copy-start.11 = (bf16[96,2048]{1,0:T(8,128)(2,1)S(1)}, bf16[96,2048]{1,0:T(8,128)(2,1)}, u32[]{:S(2)}) copy-start(bf16[96,2048]{1,0:T(8,128)(2,1)} %param.25) | copy-start | bytes 1179652
  157.5 5.4 %copy-start.28 = (f32[2048]{0:T(1024)S(1)}, f32[2048]{0:T(1024)}, u32[]{:S(2)}) copy-start(f32[2048]{0:T(1024)} %param.26) | copy-start | bytes 24580
Sparse Core Ops, SparseCore 0:
  9.0 85.5 all-gather.8
  96.8 74.9 all-gather.10
where the time goes:
time: 224 us; the launch traced here: 223 us
  blocking collectives  104 us (46%)
  matrix products  72.7 us (32%)
  local copies, waits for them, and re-layouts  17.2 us (8%)
  between operations  14.1 us (6%)
  other arithmetic  13.4 us (6%)
    all_gather x6, blocking collectives, carried_in(): lax.all_gather(part.astype(kind), axis)  57.8 us
    all_to_all x1, blocking collectives, summed_on_arrival(): lax.all_to_all(pieces, axis, split_axis=0, concat_axis=0, tiled=True)  17.8 us
    all_to_all x1, blocking collectives, sent_to_all(): lax.all_to_all(jnp.broadcast_to(x[None], (size, *x.shape)), axis, 0, 0, t...  16.1 us
    all_to_all x1, blocking collectives, per_device(): lax.all_to_all(mixed_heads, 'tp', split_axis=0, concat_axis=1, tiled=True)  12.2 us
    dot_general x1, matrix products, per_device(): jnp.dot(hidden, down_whole, preferred_element_type=jnp.float32)  11.2 us
    dot_general x6, matrix products, advance(): jnp.einsum('jod,jdg->jog', update_keys, matrix_state)  6.72 us
    dot_general x1, matrix products, per_device(): jnp.dot(span_rows, gate_whole, preferred_element_type=jnp.float32)  6.6 us
    dot_general x6, matrix products, advance(): jnp.einsum('oyn,onk->oyk', inside_span, value_corrected)  6.56 us
  transfers between devices with their start and end apart: 2, of which 0 were waited for; matrix products, arithmetic and copies ran while one was open for 36% of the time, Pallas kernels for 0%

commit v1 on v0

v1 whole, which is shorter than its diff:
```python
import jax
import jax.numpy as jnp
from jax import lax
from jax.experimental import pallas as pl
from jax.experimental.pallas import tpu as pltpu
from jax.sharding import Mesh
from jax.sharding import PartitionSpec as P

HEAD_DIM = 64
PAIR = 2 * HEAD_DIM
CHUNK = 128
SP = ("sp_0", "sp_1", "sp_2")
SP_TP = ("sp_0", "sp_1", "sp_2", "tp")
EPSILON = 1e-06
BF = jnp.bfloat16
F32 = jnp.float32
NT = (((1,), (1,)), ((), ()))
HIGH = lax.Precision.HIGHEST


def dot(a, b):
    return jnp.dot(a, b, preferred_element_type=F32)


def dot_nt(a, b, precision=None):
    return lax.dot_general(a, b, NT, precision=precision, preferred_element_type=F32)


def silu(x):
    return x / (1.0 + jnp.exp(-x))


def places():
    row = lax.broadcasted_iota(jnp.int32, (PAIR, PAIR), 0)
    col = lax.broadcasted_iota(jnp.int32, (PAIR, PAIR), 1)
    return row, col


def half_sums(squares, ones):
    high = squares.astype(BF)
    low = (squares - high.astype(F32)).astype(BF)
    return dot(high, ones) + dot(low, ones)


def softplus(x):
    small = jnp.exp(-jnp.abs(x))
    series = small * (1.0 - small * (0.5 - small * (1.0 / 3.0 - 0.25 * small)))
    return jnp.maximum(x, 0.0) + jnp.where(small < 0.015, series, jnp.log(1.0 + small))


def turned(z):
    return pltpu.roll(z, HEAD_DIM, 1)


def keys_kernel(
    k_ref, v_ref, beta_ref, decay_ref,
    before_ref, total_ref, y_ref, d_ref, kb_ref, ec_ref,
    run_ref, l_ref, x_ref, r_ref,
):
    chunk = pl.program_id(0)
    row, col = places()
    left = col < HEAD_DIM
    top = row < HEAD_DIM
    same = left == top
    ones = jnp.where(same, 1.0, 0.0).astype(BF)
    inclusive = row >= col
    strict = row > col
    differ = row ^ col
    eye = jnp.where(row == col, 1.0, 0.0)
    off_eye = differ == HEAD_DIM
    triangle = jnp.where(inclusive, 1.0, 0.0)
    pairs = k_ref.shape[1] // PAIR

    @pl.when(chunk == 0)
    def _():
        for p in range(pairs):
            run_ref[p] = jnp.where(off_eye, 1.0, 0.0).astype(BF)

    rates = -softplus(decay_ref[...])
    strength = 1.0 / (1.0 + jnp.exp(-beta_ref[...]))
    cum_row = dot_nt(rates, triangle, HIGH)
    cum_col = dot_nt(triangle, rates, HIGH)
    beta_col = dot_nt(eye, strength, HIGH)
    kept = []
    for p in range(pairs):
        lanes = slice(p * PAIR, (p + 1) * PAIR)
        key = silu(k_ref[:, lanes].astype(F32))
        key = (key * lax.rsqrt(half_sums(key * key, ones) + EPSILON)).astype(BF)
        kb_ref[:, lanes] = key
        key_f = key.astype(F32)
        cums = [cum_col[:, h : h + 1] for h in (2 * p, 2 * p + 1)]
        betas = [beta_col[:, h : h + 1] for h in (2 * p, 2 * p + 1)]
        cum = jnp.where(left, cums[0], cums[1])
        beta = jnp.where(left, betas[0], betas[1])
        grown = jnp.exp(cum)
        ec_ref[:, lanes] = grown
        strong = turned(key_f * (beta * grown))
        value = silu(v_ref[:, lanes].astype(F32)) * beta
        r_ref[2 * p] = jnp.where(left, value, strong).astype(BF)
        r_ref[2 * p + 1] = jnp.where(left, strong, value).astype(BF)
        fade = jnp.exp(cum[CHUNK - 1 : CHUNK, :] - cum)
        faded = (key_f * fade).T.astype(BF)
        ends = [jnp.exp(c[CHUNK - 1 : CHUNK, :]) for c in cums]
        kept.append((faded, jnp.where(off_eye, jnp.where(top, ends[0], ends[1]), 0.0)))
        for s in range(2):
            h = 2 * p + s
            mine = left if s == 0 else jnp.logical_not(left)
            own = jnp.where(mine, key_f, 0.0).astype(BF)
            inner = dot_nt(own, key)
            decay = jnp.where(inclusive, jnp.exp(cums[s] - cum_row[h : h + 1, :]), 0.0)
            d_ref[h] = decay.astype(BF)
            lower = jnp.where(strict, inner * decay * betas[s], 0.0)
            l_ref[h] = lower.astype(BF)
            x_ref[h] = (eye - jnp.where(differ == 1, lower, 0.0)).astype(BF)
    heads = 2 * pairs
    for level in range(1, 7):
        mask = jnp.where((differ >> level) == 1, 1.0, 0.0).astype(BF)
        parts = [dot(x_ref[h], l_ref[h] * mask).astype(BF) for h in range(heads)]
        for h in range(heads):
            x = x_ref[h]
            x_ref[h] = x - dot(parts[h], x).astype(BF)
    for p in range(pairs):
        faded, ends = kept[p]
        got = []
        for h in (2 * p, 2 * p + 1):
            y = dot(x_ref[h], r_ref[h]).astype(BF)
            y_ref[h] = y
            got.append(dot(faded, y))
        z = jnp.where(top, got[0], got[1])
        z = jnp.where(same, z, ends - z)
        step = jnp.where(same, turned(z), 0.0).astype(BF)
        run = run_ref[p]
        before_ref[p] = run
        run = (dot(step, run) + jnp.where(same, z, 0.0)).astype(BF)
        run_ref[p] = run
        total_ref[p] = run


def keys_side(keys, values, beta_pre, decay_pre):
    length, width = keys.shape
    heads = width // HEAD_DIM
    pairs = width // PAIR
    steps = length // CHUNK
    rows = pl.BlockSpec((CHUNK, width), lambda c: (c, 0))
    rates = pl.BlockSpec((heads, CHUNK), lambda c: (0, c))
    per_head = pl.BlockSpec((None, heads, CHUNK, PAIR), lambda c: (c, 0, 0, 0))
    return pl.pallas_call(
        keys_kernel,
        grid=(steps,),
        in_specs=[rows, rows, rates, rates],
        out_specs=[
            pl.BlockSpec((None, pairs, PAIR, PAIR), lambda c: (c, 0, 0, 0)),
            pl.BlockSpec((pairs, PAIR, PAIR), lambda c: (0, 0, 0)),
            per_head,
            per_head,
            rows,
            rows,
        ],
        out_shape=[
            jax.ShapeDtypeStruct((steps, pairs, PAIR, PAIR), BF),
            jax.ShapeDtypeStruct((pairs, PAIR, PAIR), BF),
            jax.ShapeDtypeStruct((steps, heads, CHUNK, PAIR), BF),
            jax.ShapeDtypeStruct((steps, heads, CHUNK, CHUNK), BF),
            jax.ShapeDtypeStruct((length, width), BF),
            jax.ShapeDtypeStruct((length, width), F32),
        ],
        scratch_shapes=[
            pltpu.VMEM((pairs, PAIR, PAIR), BF),
            pltpu.VMEM((heads, CHUNK, CHUNK), BF),
            pltpu.VMEM((heads, CHUNK, CHUNK), BF),
            pltpu.VMEM((heads, CHUNK, PAIR), BF),
        ],
        name="keys_side",
    )(keys, values, beta_pre, decay_pre)


def queries_kernel(q_ref, kb_ref, d_ref, y_ref, before_ref, ec_ref, o_ref, q1_ref):
    row, col = places()
    left = col < HEAD_DIM
    same = left == (row < HEAD_DIM)
    ones = jnp.where(same, 1.0, 0.0).astype(BF)
    for p in range(q_ref.shape[1] // PAIR):
        lanes = slice(p * PAIR, (p + 1) * PAIR)
        query = silu(q_ref[:, lanes].astype(F32))
        query = query * lax.rsqrt(half_sums(query * query, ones) + EPSILON)
        query = (query * HEAD_DIM ** (-0.5)).astype(BF)
        query_f = query.astype(F32)
        key = kb_ref[:, lanes]
        got = []
        for s in range(2):
            h = 2 * p + s
            mine = left if s == 0 else jnp.logical_not(left)
            own = jnp.where(mine, query_f, 0.0).astype(BF)
            inside = (dot_nt(own, key) * d_ref[h].astype(F32)).astype(BF)
            got.append(dot(inside, y_ref[h]))
        local = jnp.where(left, got[0], got[1])
        crossed = turned(jnp.where(left, got[1], got[0]))
        query = (query_f * ec_ref[:, lanes] - crossed).astype(BF)
        before = before_ref[p].astype(F32)
        offset = jnp.where(same, before, 0.0).astype(BF)
        trans = jnp.where(same, turned(before), 0.0).astype(BF)
        o_ref[:, lanes] = local + dot(query, offset)
        q1_ref[:, lanes] = dot(query, trans).astype(BF)


def queries_side(queries, key_unit, decay, solved, before, grown):
    length, width = queries.shape
    heads = width // HEAD_DIM
    pairs = width // PAIR
    rows = pl.BlockSpec((CHUNK, width), lambda c: (c, 0))
    per_head = pl.BlockSpec((None, heads, CHUNK, PAIR), lambda c: (c, 0, 0, 0))
    return pl.pallas_call(
        queries_kernel,
        grid=(length // CHUNK,),
        in_specs=[
            rows,
            rows,
            per_head,
            per_head,
            pl.BlockSpec((None, pairs, PAIR, PAIR), lambda c: (c, 0, 0, 0)),
            rows,
        ],
        out_specs=[rows, rows],
        out_shape=[
            jax.ShapeDtypeStruct((length, width), F32),
            jax.ShapeDtypeStruct((length, width), BF),
        ],
        name="queries_side",
    )(queries, key_unit, decay, solved, before, grown)


def mixed_kernel(me_ref, o_ref, q1_ref, state_ref, gates_ref, gain_ref, w_ref, *rest):
    out_refs, mixed_ref = rest[:-1], rest[-1]
    row, col = places()
    same = (col < HEAD_DIM) == (row < HEAD_DIM)
    ones = jnp.where(same, 1.0, 0.0).astype(BF)
    length, width = o_ref.shape
    for c in range(length // CHUNK):
        rows = slice(c * CHUNK, (c + 1) * CHUNK)
        for p in range(width // PAIR):
            lanes = slice(p * PAIR, (p + 1) * PAIR)
            out = o_ref[rows, lanes] + dot(q1_ref[rows, lanes], state_ref[p])
            mean = half_sums(out * out, ones) * (1.0 / HEAD_DIM)
            out = out * lax.rsqrt(mean + EPSILON) * gain_ref[...]
            mixed_ref[rows, lanes] = (out * silu(gates_ref[rows, lanes].astype(F32))).astype(BF)
    size = len(out_refs)
    block = length // size
    for k, out_ref in enumerate(out_refs):
        start = lax.rem(me_ref[0] + k, size) * block
        rows = mixed_ref[pl.ds(pl.multiple_of(start, 32), block), :]
        out_ref[...] = dot(rows, w_ref[...]).astype(out_ref.dtype)


def mixed_and_projected(me, size, local, query, state, gates, gain, w_out):
    length, width = local.shape
    block = length // size
    full = pl.BlockSpec(memory_space=pltpu.VMEM)
    return pl.pallas_call(
        mixed_kernel,
        in_specs=[pl.BlockSpec(memory_space=pltpu.SMEM)] + [full] * 6,
        out_specs=[full] * size,
        out_shape=[
            jax.ShapeDtypeStruct((block, w_out.shape[1]), F32 if k == 0 else BF)
            for k in range(size)
        ],
        scratch_shapes=[pltpu.VMEM((length, width), BF)],
        name="mixed_and_projected",
    )(me, local, query, state, gates, jnp.tile(gain, 2).reshape(1, PAIR), w_out)


def norm_kernel(stream_ref, gain_ref, *rest):
    parts, middle_ref, normed_ref = rest[:-2], rest[-2], rest[-1]
    total = stream_ref[...].astype(F32)
    projected = parts[0][...].astype(F32)
    for part in parts[1:]:
        projected = projected + part[...].astype(F32)
    middle = (total + projected).astype(BF)
    middle_ref[...] = middle
    middle = middle.astype(F32)
    mean = jnp.mean(middle * middle, axis=-1, keepdims=True)
    normed_ref[...] = (middle * lax.rsqrt(mean + EPSILON) * gain_ref[...]).astype(BF)


def normed_rows(stream, gain, parts):
    full = pl.BlockSpec(memory_space=pltpu.VMEM)
    return pl.pallas_call(
        norm_kernel,
        in_specs=[full] * (2 + len(parts)),
        out_specs=[full] * 2,
        out_shape=[jax.ShapeDtypeStruct(stream.shape, BF)] * 2,
        name="normed_rows",
    )(stream, gain.reshape(1, -1), *parts)


def hidden_kernel(wg_ref, wu_ref, *rest):
    parts, out_ref, rows_ref = rest[:-2], rest[-2], rest[-1]
    block = parts[0].shape[0]

    @pl.when(pl.program_id(0) == 0)
    def _():
        for k, part in enumerate(parts):
            rows_ref[k * block : (k + 1) * block, :] = part[...]

    both = jnp.concatenate([wg_ref[...], wu_ref[...]], axis=1)
    got = dot(rows_ref[...], both)
    width = out_ref.shape[1]
    out_ref[...] = (silu(got[:, :width]) * got[:, width:]).astype(BF)


def hidden_units(weights, parts, hidden):
    tile = 128
    steps = hidden // tile
    block, width = parts[0].shape
    length = block * len(parts)
    rows = pl.BlockSpec((block, width), lambda j: (0, 0))
    return pl.pallas_call(
        hidden_kernel,
        grid=(steps,),
        in_specs=[
            pl.BlockSpec((width, tile), lambda j: (0, j)),
            pl.BlockSpec((width, tile), lambda j: (0, steps + j)),
        ]
        + [rows] * len(parts),
        out_specs=pl.BlockSpec((length, tile), lambda j: (0, j)),
        out_shape=jax.ShapeDtypeStruct((length, hidden), BF),
        scratch_shapes=[pltpu.VMEM((length, width), BF)],
        name="hidden_units",
    )(weights, weights, *parts)


def down_kernel(h_ref, w_ref, *out_refs):
    got = dot_nt(h_ref[...], w_ref[...])
    block = out_refs[0].shape[0]
    for k, out_ref in enumerate(out_refs):
        out_ref[...] = got[k * block : (k + 1) * block, :].astype(BF)


def down_products(hidden, weights, size):
    tile = 256
    length, units = hidden.shape
    width = weights.shape[0]
    block = length // size
    return pl.pallas_call(
        down_kernel,
        grid=(width // tile,),
        in_specs=[
            pl.BlockSpec((length, units), lambda n: (0, 0)),
            pl.BlockSpec((tile, units), lambda n: (n, 2)),
        ],
        out_specs=[pl.BlockSpec((block, tile), lambda n: (0, n))] * size,
        out_shape=[jax.ShapeDtypeStruct((block, width), BF)] * size,
        name="down_products",
    )(hidden, weights)


def last_kernel(middle_ref, *rest):
    parts, out_ref = rest[:-1], rest[-1]
    total = parts[0][...].astype(F32)
    for part in parts[1:]:
        total = total + part[...].astype(F32)
    out_ref[...] = (middle_ref[...].astype(F32) + 0.5 * total).astype(BF)


def last_sum(middle, parts):
    full = pl.BlockSpec(memory_space=pltpu.VMEM)
    return pl.pallas_call(
        last_kernel,
        in_specs=[full] * (1 + len(parts)),
        out_specs=full,
        out_shape=jax.ShapeDtypeStruct(middle.shape, BF),
        name="last_sum",
    )(middle, *parts)


def blocks_same():
    half = jnp.arange(PAIR) // HEAD_DIM
    return half[:, None] == half[None, :]


def chain(earlier, later):
    same = blocks_same()
    step = jnp.where(same, jnp.roll(later, HEAD_DIM, axis=-1), 0.0).astype(BF)
    moved = jnp.einsum("pij,pjk->pik", step, earlier.astype(BF), preferred_element_type=F32)
    return moved + jnp.where(same, later, 0.0).astype(F32)


def carried_in(total, axes):
    shift = (jnp.arange(PAIR)[:, None] ^ jnp.arange(PAIR)[None, :]) == HEAD_DIM
    start = jnp.broadcast_to(jnp.where(shift, 1.0, 0.0).astype(F32), total.shape)
    before = start
    subtotal = total
    for axis in reversed(axes):
        size, index = lax.axis_size(axis), lax.axis_index(axis)
        pieces = lax.all_gather(subtotal.astype(BF), axis)
        inside, subtotal = start, start
        for k in range(size):
            subtotal = chain(subtotal, pieces[k])
            inside = jnp.where(k + 1 == index, subtotal, inside)
        before = chain(inside, before)
    return jnp.where(blocks_same(), before, 0.0).astype(BF)


def ring(size, k):
    return [(i, (i + k) % size) for i in range(size)]


def per_device(
    queries,
    keys,
    values,
    gates,
    decay_pre,
    beta_pre,
    out_gain,
    w_out,
    stream,
    norm_gain,
    w_gate,
    w_up,
    w_down,
):
    hidden = w_gate.shape[1]
    weights = jnp.concatenate([w_gate, w_up, w_down.T], axis=1)
    weights = lax.all_gather(weights, SP, axis=0, tiled=True)
    size = lax.axis_size("tp")
    me = lax.axis_index("tp").astype(jnp.int32).reshape(1)
    before, total, solved, decay, key_unit, grown = keys_side(keys, values, beta_pre, decay_pre)
    local, query = queries_side(queries, key_unit, decay, solved, before, grown)
    state = carried_in(total, SP)
    parts = mixed_and_projected(me, size, local, query, state, gates, out_gain, w_out)
    got = [lax.ppermute(parts[k], "tp", ring(size, k)) for k in range(1, size)]
    middle, normed = normed_rows(stream, norm_gain, [parts[0]] + got)
    rows = [normed] + [lax.ppermute(normed, "tp", ring(size, k)) for k in range(1, size)]
    sums = down_products(hidden_units(weights, rows, hidden), weights, size)
    back = [lax.ppermute(sums[k], "tp", ring(size, -k)) for k in range(1, size)]
    return last_sum(middle, [sums[0]] + back)


def solution(mesh):
    finer = Mesh(mesh.devices.reshape(4, 4, 2, mesh.shape["tp"]), SP_TP)
    placed = (
        P(SP, "tp"),
        P(SP, "tp"),
        P(SP, "tp"),
        P(SP, "tp"),
        P("tp", SP),
        P("tp", SP),
        P(),
        P("tp", None),
        P(SP_TP, None),
        P(),
        P(SP, "tp"),
        P(SP, "tp"),
        P("tp", SP),
    )
    return jax.shard_map(
        per_device, mesh=finer, in_specs=placed, out_specs=P(SP_TP, None), check_vma=False
    )
```

time: 224 us -> 172 us (0.77)
  blocking collectives: 104 us -> 32.2 us
  matrix products: 72.7 us -> 3.71 us
  Pallas kernels: 0 us -> 54.2 us
  waiting for transfers between devices: 0.72 us -> 46.3 us
  starting transfers between devices: 0.08 us -> 14.6 us
  local copies, waits for them, and re-layouts: 17.2 us -> 4.15 us
  other arithmetic: 13.4 us -> 2.06 us
    dot_general x81 -> x12, matrix products: 72.7 us -> 3.71 us  [chain(): jnp.einsum('pij,pjk->pik', step, earlier.astype(BF), preferred_element_ty...]
    pallas_call x0 -> x7, Pallas kernels: none -> 54.2 us  [the longest x1 13.5 us: keys_side(): pl.pallas_call(keys_kernel, grid=(steps,), in_specs=[rows, rows, rates, r...]
    ppermute x0 -> x9, waiting for transfers between devices: none -> 46.3 us  [the longest x3 18.9 us: per_device(): back = [lax.ppermute(sums[k], 'tp', ring(size, -k)) for k in range(1, size)]]
    all_to_all x3 -> x0, blocking collectives: 46.1 us -> none  [the longest x1 17.8 us: summed_on_arrival(): lax.all_to_all(pieces, axis, split_axis=0, concat_axis=0, tiled=True)]
    all_gather x6 -> x3, blocking collectives: 57.8 us -> 32.2 us  [carried_in(): pieces = lax.all_gather(subtotal.astype(BF), axis)]
    ppermute x0 -> x9, starting transfers between devices: none -> 14.6 us  [the longest x3 5.61 us: per_device(): got = [lax.ppermute(parts[k], 'tp', ring(size, k)) for k in range(1, size)]]
    reshape x8 -> x0, local copies, waits for them, and re-layouts: 7.84 us -> none  [the longest x5 5.65 us: split_heads(): return arr.astype(jnp.float32).reshape(length, heads, HEAD_DIM)]
    mul x2 -> x0, other arithmetic: 6.11 us -> none  [the longest x1 4.72 us: block_terms(): key_strong * jnp.exp(cumulative)[..., None]]
  transfers between devices with their start and end apart: 2 -> 10, of which waited for: 0 -> 6; matrix products, arithmetic and copies ran while one was open for 36% -> 3% of each run, Pallas kernels for 0% -> 18%
where the time goes in v1:
time: 172 us; the launch traced here: 171 us
  Pallas kernels  54.2 us (32%)
  waiting for transfers between devices  46.3 us (27%)
  blocking collectives  32.2 us (19%)
  starting transfers between devices  14.6 us (8%)
  between operations  13.6 us (8%)
  local copies, waits for them, and re-layouts  4.15 us (2%)
  matrix products  3.71 us (2%)
  other arithmetic  2.06 us (1%)
    all_gather x3, blocking collectives, carried_in(): pieces = lax.all_gather(subtotal.astype(BF), axis)  32.2 us
    ppermute x3, waiting for transfers between devices, per_device(): back = [lax.ppermute(sums[k], 'tp', ring(size, -k)) for k in range(1, size)]  18.9 us
    ppermute x3, waiting for transfers between devices, per_device(): lax.ppermute(normed, 'tp', ring(size, k))  14.6 us
    pallas_call x1, Pallas kernels, keys_side(): pl.pallas_call(keys_kernel, grid=(steps,), in_specs=[rows, rows, rates, r...  13.5 us
    ppermute x3, waiting for transfers between devices, per_device(): got = [lax.ppermute(parts[k], 'tp', ring(size, k)) for k in range(1, size)]  12.7 us
    pallas_call x1, Pallas kernels, hidden_units(): pl.pallas_call(hidden_kernel, grid=(steps,), in_specs=[pl.BlockSpec((widt...  12.5 us
    pallas_call x1, Pallas kernels, queries_side(): pl.pallas_call(queries_kernel, grid=(length // CHUNK,), in_specs=[rows, r...  8.75 us
    pallas_call x1, Pallas kernels, down_products(): pl.pallas_call(down_kernel, grid=(width // tile,), in_specs=[pl.BlockSpec...  8.29 us
  transfers between devices with their start and end apart: 10, of which 6 were waited for; matrix products, arithmetic and copies ran while one was open for 3% of the time, Pallas kernels for 18%

profile of v1, /device:TPU:0, one launch (start us, length us, event | category | flops | bytes accessed | tf_op | source)
XLA Modules:
  0.0 170.9 jit_solution(4282063701556198300)
XLA Ops:
  6.5 1.9 %pad_maximum_fusion = bf16[64,4224]{1,0:T(8,128)(2,1)} fusion(bf16[64,1408]{1,0:T(8,128)(2,1)} %bitcast.10, bf16[64,1408]{1,0:T(8,128)(2,1)} %param.24, bf16[64,1408]{1,0:T(8,128)(2,1)} %param.23), kind=kLoop, calls=%fused_computation.17 | loop fusion | flops 1622016 | bytes 1081344 | tf_op jit(solution)/shard_map/concatenate | solution.py:423
  8.6 0.7 reshape_tile.3.gain_ref
  9.2 13.5 %keys_side.1 = (bf16[3,4,128,128]{3,2,1,0:T(8,128)(2,1)}, bf16[4,128,128]{2,1,0:T(8,128)(2,1)}, bf16[3,8,128,128]{3,2,1,0:T(8,128)(2,1)}, bf16[3,8,128,128]{3,2,...) custom-call(bf16[384,512]{1,0:T(8,128)(2,1)} %k_ref.1, bf16[384,512]{1,0:T(8,128)(2,1)} %v_ref.1, ...), custom_call_target="tpu_custom_call" | custom-call | tf_op jit(solution)/shard_map/keys_side/pallas_call | solution.py:147
  22.8 8.8 %queries_side.1 = (f32[384,512]{1,0:T(8,128)}, bf16[384,512]{1,0:T(8,128)(2,1)}) custom-call(bf16[384,512]{1,0:T(8,128)(2,1)} %q_ref.1, bf16[384,512]{1,0:T(8,128)(2,1)} %get-tuple-element.23.kb_ref, bf16[3,8,128,128]{3,2,1,0:T(8,128)(2,1)} %get-tuple-element.24.d_ref, bf16[3,8,128,128]{3,2,1,0:T(8,128)(2,1)} %get-tuple-element.25.y_ref, ...), custom_call_target="tpu_custom_call" | custom-call | tf_op jit(solution)/shard_map/queries_side/pallas_call | solution.py:212
  31.5 2.0 %all-gather = bf16[8,128,128]{2,1,0:T(8,128)(2,1)S(1)} all-gather(bf16[4,128,128]{2,1,0:T(8,128)(2,1)S(1)} %copy-done.9), channel_id=2, replica_groups=mesh['sp_0'=4,'sp_1'=4,'sp_2'=2,'tp'=4] {'sp_2'}, dimensions={0}, use_global_device_ids=true | all-gather | bytes 393216 | tf_op jit(solution)/shard_map/all_gather | solution.py:394
  33.7 0.1 fusion.121
  33.8 0.2 convolution_add_fusion.12
  34.1 0.2 convolution_add_fusion.11
  34.3 13.6 %all-gather.1 = bf16[16,128,128]{2,1,0:T(8,128)(2,1)S(1)} all-gather(bf16[4,128,128]{2,1,0:T(8,128)(2,1)S(1)} %convolution_add_fusion.11), channel_id=3, replica_groups=mesh['sp_0'=4,'sp_1'=4,'sp_2'=2,'tp'=4] {'sp_1'}, dimensions={0}, use_global_device_ids=true | all-gather | bytes 655360 | tf_op jit(solution)/shard_map/all_gather | solution.py:394
  47.9 0.2 fusion.118
  48.1 0.2 convolution_add_fusion.9
  48.4 0.2 convolution_add_fusion.8
  48.6 0.2 convolution_add_fusion.7
  48.9 0.2 convolution_add_fusion.6
  49.1 16.7 %all-gather.2 = bf16[16,128,128]{2,1,0:T(8,128)(2,1)S(1)} all-gather(bf16[4,128,128]{2,1,0:T(8,128)(2,1)S(1)} %convolution_add_fusion.6), channel_id=4, replica_groups=mesh['sp_0'=4,'sp_1'=4,'sp_2'=2,'tp'=4] {'sp_0'}, dimensions={0}, use_global_device_ids=true | all-gather | bytes 655360 | tf_op jit(solution)/shard_map/all_gather | solution.py:394
  65.8 0.2 fusion.117
  66.1 0.2 convolution_add_fusion.4
  66.3 0.2 convolution_add_fusion.3
  66.6 0.2 convolution_add_fusion.2
  66.9 0.3 convolution_add_fusion.10
  67.2 0.3 convolution_add_fusion.5
  67.5 0.1 fusion.119
  67.6 1.1 fusion.3.state_ref
  68.7 5.9 %mixed_and_projected.1 = (f32[96,2048]{1,0:T(8,128)}, bf16[96,2048]{1,0:T(8,128)(2,1)}, bf16[96,2048]{1,0:T(8,128)(2,1)}, bf16[96,2048]{1,0:T(8,128)(2,1)}) custom-call(s32[1]{0:T(128)} %bitcast.1.me_ref, f32[384,512]{1,0:T(8,128)} %get-tuple-element.28.o_ref, bf16[384,512]{1,0:T(8,128)(2,1)} %get-tuple-element.29.q1_ref, ...), custom_call_target="tpu_custom_call" | custom-call | tf_op jit(solution)/shard_map/mixed_and_projected/pallas_call | solution.py:258
  74.6 1.5 collective-permute-start
  76.0 2.7 %collective-permute-start.1 = (bf16[96,2048]{1,0:T(8,128)(2,1)}, bf16[96,2048]{1,0:T(8,128)(2,1)S(1)}, u32[]{:S(2)}, u32[]{:S(2)}) collective-permute-start(bf16[96,2048]{1,0:T(8,128)(2,1)} %get-tuple-element.33), channel_id=1, source_target_pairs={{0,2},{1,3},{2,0},{3,1},{4,6},{5,7},{6,4},{7,5},{8,10},{9,11},{10,... | collective-permute-start | bytes 1179656 | tf_op jit(solution)/shard_map/ppermute | solution.py:431
  78.7 1.4 collective-permute-start.2
  80.2 7.3 %collective-permute-done.rest_1_ = bf16[96,2048]{1,0:T(8,128)(2,1)S(1)} collective-permute-done((bf16[96,2048]{1,0:T(8,128)(2,1)}, bf16[96,2048]{1,0:T(8,128)(2,1)S(1)}, u32[]{:S(2)}, u32[]{:S(2)}) %collective-permute-start) | collective-permute-done | bytes 393248 | tf_op jit(solution)/shard_map/ppermute | solution.py:431
  87.4 5.5 %collective-permute-done.1.rest_2_ = bf16[96,2048]{1,0:T(8,128)(2,1)S(1)} collective-permute-done((bf16[96,2048]{1,0:T(8,128)(2,1)}, bf16[96,2048]{1,0:T(8,128)(2,1)S(1)}, u32[]{:S(2)}, u32[]{:S(2)}) %collective-permute-start.1) | collective-permute-done | bytes 393248 | tf_op jit(solution)/shard_map/ppermute | solution.py:431
  92.9 0.7 copy-done.5
  93.7 0.2 copy-done.7
  93.8 2.8 %normed_rows.1 = (bf16[96,2048]{1,0:T(8,128)(2,1)}, bf16[96,2048]{1,0:T(8,128)(2,1)}) custom-call(bf16[96,2048]{1,0:T(8,128)(2,1)} %stream_ref.1, f32[1,2048]{1,0:T(1,128)} %bitcast.11, f32[96,2048]{1,0:T(8,128)} %get-tuple-element.31.rest_0_, bf16[96,2048]{1,0:T(8,128)(2,1)} %copy-done.3, bf16[96,2048]{1,0:T(8,128)(2,1)} %copy-done.5, ...), custom_call_target="tpu_custom_call" | custom-call | tf_op jit(solution)/shard_map/normed_rows/pallas_call | solution.py:286
  96.6 1.2 collective-permute-start.3
  97.8 2.4 %collective-permute-start.4 = (bf16[96,2048]{1,0:T(8,128)(2,1)}, bf16[96,2048]{1,0:T(8,128)(2,1)S(1)}, u32[]{:S(2)}, u32[]{:S(2)}) collective-permute-start(bf16[96,2048]{1,0:T(8,128)(2,1)} %get-tuple-element.36.rest_0_), channel_id=1, source_target_pairs={{0,2},{1,3},{2,0},{3,1},{4,6},{5,7},{6,4},{7,5},{8,10},{9,11},{10,... | collective-permute-start | bytes 1179656 | tf_op jit(solution)/shard_map/ppermute | solution.py:433
  100.2 1.6 collective-permute-start.5
  101.8 6.2 %collective-permute-done.3.rest_1_ = bf16[96,2048]{1,0:T(8,128)(2,1)S(1)} collective-permute-done((bf16[96,2048]{1,0:T(8,128)(2,1)}, bf16[96,2048]{1,0:T(8,128)(2,1)S(1)}, u32[]{:S(2)}, u32[]{:S(2)}) %collective-permute-start.3) | collective-permute-done | bytes 393248 | tf_op jit(solution)/shard_map/ppermute | solution.py:433
  108.0 8.4 %collective-permute-done.4.rest_2_ = bf16[96,2048]{1,0:T(8,128)(2,1)S(1)} collective-permute-done((bf16[96,2048]{1,0:T(8,128)(2,1)}, bf16[96,2048]{1,0:T(8,128)(2,1)S(1)}, u32[]{:S(2)}, u32[]{:S(2)}) %collective-permute-start.4) | collective-permute-done | bytes 393248 | tf_op jit(solution)/shard_map/ppermute | solution.py:433
  116.4 0.7 copy-done.1
  117.1 0.2 copy-done.2
  117.3 12.5 %hidden_units.1.h_ref = bf16[384,1408]{1,0:T(8,128)(2,1)} custom-call(bf16[2048,4224]{1,0:T(8,128)(2,1)} %all-gather.5.cloned.1.call-done.wg_ref.wu_ref.w_ref, bf16[2048,4224]{1,0:T(8,128)(2,1)} %all-gather.5.cloned.1.call-done.wg_ref.wu_ref.w_ref, bf16[96,2048]{1,0:T(8,128)(2,1)} %get-tuple-element.36.rest_0_, bf16[96,2048]{1,0:T(8,128)(2,1)} %copy-done, ...), custom_call_target="tpu_custom_call" | custom-call | tf_op jit(solution)/shard_map/hidden_units/pallas_call | solution.py:316
  129.8 8.3 %down_products.1 = (bf16[96,2048]{1,0:T(8,128)(2,1)}, bf16[96,2048]{1,0:T(8,128)(2,1)}, bf16[96,2048]{1,0:T(8,128)(2,1)}, bf16[96,2048]{1,0:T(8,128)(2,1)}) custom-call(bf16[384,1408]{1,0:T(8,128)(2,1)} %hidden_units.1.h_ref, bf16[2048,4224]{1,0:T(8,128)(2,1)} %all-gather.5.cloned.1.call-done.wg_ref.wu_ref.w_ref), custom_call_target="tpu_custom_call" | custom-call | tf_op jit(solution)/shard_map/down_products/pallas_call | solution.py:343
  138.1 1.9 %collective-permute-start.6 = (bf16[96,2048]{1,0:T(8,128)(2,1)}, bf16[96,2048]{1,0:T(8,128)(2,1)S(1)}, u32[]{:S(2)}, u32[]{:S(2)}) collective-permute-start(bf16[96,2048]{1,0:T(8,128)(2,1)} %get-tuple-element.38), channel_id=1, source_target_pairs={{0,3},{1,0},{2,1},{3,2},{4,7},{5,4},{6,5},{7,6},{8,11},{9,8},{10,9... | collective-permute-start | bytes 1179656 | tf_op jit(solution)/shard_map/ppermute | solution.py:435
  140.0 1.6 collective-permute-start.7
  141.6 0.3 collective-permute-start.8
  141.9 15.4 %collective-permute-done.6.rest_1_ = bf16[96,2048]{1,0:T(8,128)(2,1)S(1)} collective-permute-done((bf16[96,2048]{1,0:T(8,128)(2,1)}, bf16[96,2048]{1,0:T(8,128)(2,1)S(1)}, u32[]{:S(2)}, u32[]{:S(2)}) %collective-permute-start.6) | collective-permute-done | bytes 393248 | tf_op jit(solution)/shard_map/ppermute | solution.py:435
  157.3 3.6 %collective-permute-done.8.rest_3_ = bf16[96,2048]{1,0:T(8,128)(2,1)S(1)} collective-permute-done((bf16[96,2048]{1,0:T(8,128)(2,1)}, bf16[96,2048]{1,0:T(8,128)(2,1)S(1)}, u32[]{:S(2)}, u32[]{:S(2)}) %collective-permute-start.8) | collective-permute-done | bytes 393248 | tf_op jit(solution)/shard_map/ppermute | solution.py:435
  160.8 0.8 copy-done.8
  161.6 2.5 %last_sum.1 = bf16[96,2048]{1,0:T(8,128)(2,1)} custom-call(bf16[96,2048]{1,0:T(8,128)(2,1)} %get-tuple-element.35.middle_ref, bf16[96,2048]{1,0:T(8,128)(2,1)} %get-tuple-element.37.rest_0_, bf16[96,2048]{1,0:T(8,128)(2,1)} %copy-done.4, bf16[96,2048]{1,0:T(8,128)(2,1)} %copy-done.6, bf16[96,2048]{1,0:T(8,128)(2,1)} %copy-done.8), custom_call_target="tpu_custom_call" | custom-call | tf_op jit(solution)/shard_map/last_sum/pallas_call | solution.py:366
  (32 shorter events, 0.4 us)
Async XLA Ops:
  6.5 2.0 %copy-start.10 = (f32[64]{0:T(128)S(1)}, f32[64]{0:T(128)}, u32[]{:S(2)}) copy-start(f32[64]{0:T(128)} %param.19) | copy-start | bytes 772
  6.5 109.8 %all-gather.5.cloned.1.call-start = ((), (), s32[]{:S(2)}) async-start(), calls=%async_computation | async-start | bytes 17842176 | tf_op jit(solution)/shard_map/all_gather | solution.py:424
  22.8 8.8 %copy-start.9 = (bf16[4,128,128]{2,1,0:T(8,128)(2,1)S(1)}, bf16[4,128,128]{2,1,0:T(8,128)(2,1)}, u32[]{:S(2)}) copy-start(bf16[4,128,128]{2,1,0:T(8,128)(2,1)} %get-tuple-element.30) | copy-start | bytes 393220
  74.6 12.9 %collective-permute-start = (bf16[96,2048]{1,0:T(8,128)(2,1)}, bf16[96,2048]{1,0:T(8,128)(2,1)S(1)}, u32[]{:S(2)}, u32[]{:S(2)}) collective-permute-start(bf16[96,2048]{1,0:T(8,128)(2,1)} %get-tuple-element.32), channel_id=1, source_target_pairs={{0,1},{1,2},{2,3},{3,0},{4,5},{5,6},{6,7},{7,4},{8,9},{9,10},{10,1... | collective-permute-start | bytes 1179656 | tf_op jit(solution)/shard_map/ppermute | solution.py:431
  76.0 16.9 %collective-permute-start.1 = (bf16[96,2048]{1,0:T(8,128)(2,1)}, bf16[96,2048]{1,0:T(8,128)(2,1)S(1)}, u32[]{:S(2)}, u32[]{:S(2)}) collective-permute-start(bf16[96,2048]{1,0:T(8,128)(2,1)} %get-tuple-element.33), channel_id=1, source_target_pairs={{0,2},{1,3},{2,0},{3,1},{4,6},{5,7},{6,4},{7,5},{8,10},{9,11},{10,... | collective-permute-start | bytes 1179656 | tf_op jit(solution)/shard_map/ppermute | solution.py:431
  78.7 14.2 %collective-permute-start.2 = (bf16[96,2048]{1,0:T(8,128)(2,1)}, bf16[96,2048]{1,0:T(8,128)(2,1)S(1)}, u32[]{:S(2)}, u32[]{:S(2)}) collective-permute-start(bf16[96,2048]{1,0:T(8,128)(2,1)} %get-tuple-element.34), channel_id=1, source_target_pairs={{0,3},{1,0},{2,1},{3,2},{4,7},{5,4},{6,5},{7,6},{8,11},{9,8},{10,9... | collective-permute-start | bytes 1179656 | tf_op jit(solution)/shard_map/ppermute | solution.py:431
  87.4 5.5 %copy-start.3 = (bf16[96,2048]{1,0:T(8,128)(2,1)}, bf16[96,2048]{1,0:T(8,128)(2,1)S(1)}, u32[]{:S(2)}) copy-start(bf16[96,2048]{1,0:T(8,128)(2,1)S(1)} %collective-permute-done.rest_1_) | copy-start | bytes 1179652
  92.9 0.8 copy-start.5
  92.9 0.9 copy-start.7
  96.6 11.4 %collective-permute-start.3 = (bf16[96,2048]{1,0:T(8,128)(2,1)}, bf16[96,2048]{1,0:T(8,128)(2,1)S(1)}, u32[]{:S(2)}, u32[]{:S(2)}) collective-permute-start(bf16[96,2048]{1,0:T(8,128)(2,1)} %get-tuple-element.36.rest_0_), channel_id=1, source_target_pairs={{0,1},{1,2},{2,3},{3,0},{4,5},{5,6},{6,7},{7,4},{8,9},{9,10},{10,1... | collective-permute-start | bytes 1179656 | tf_op jit(solution)/shard_map/ppermute | solution.py:433
  97.8 18.6 %collective-permute-start.4 = (bf16[96,2048]{1,0:T(8,128)(2,1)}, bf16[96,2048]{1,0:T(8,128)(2,1)S(1)}, u32[]{:S(2)}, u32[]{:S(2)}) collective-permute-start(bf16[96,2048]{1,0:T(8,128)(2,1)} %get-tuple-element.36.rest_0_), channel_id=1, source_target_pairs={{0,2},{1,3},{2,0},{3,1},{4,6},{5,7},{6,4},{7,5},{8,10},{9,11},{10,... | collective-permute-start | bytes 1179656 | tf_op jit(solution)/shard_map/ppermute | solution.py:433
  100.2 16.2 %collective-permute-start.5 = (bf16[96,2048]{1,0:T(8,128)(2,1)}, bf16[96,2048]{1,0:T(8,128)(2,1)S(1)}, u32[]{:S(2)}, u32[]{:S(2)}) collective-permute-start(bf16[96,2048]{1,0:T(8,128)(2,1)} %get-tuple-element.36.rest_0_), channel_id=1, source_target_pairs={{0,3},{1,0},{2,1},{3,2},{4,7},{5,4},{6,5},{7,6},{8,11},{9,8},{10,9... | collective-permute-start | bytes 1179656 | tf_op jit(solution)/shard_map/ppermute | solution.py:433
  108.0 8.4 %copy-start = (bf16[96,2048]{1,0:T(8,128)(2,1)}, bf16[96,2048]{1,0:T(8,128)(2,1)S(1)}, u32[]{:S(2)}) copy-start(bf16[96,2048]{1,0:T(8,128)(2,1)S(1)} %collective-permute-done.3.rest_1_) | copy-start | bytes 1179652
  116.4 0.7 copy-start.1
  116.4 0.9 copy-start.2
  138.1 19.2 %collective-permute-start.6 = (bf16[96,2048]{1,0:T(8,128)(2,1)}, bf16[96,2048]{1,0:T(8,128)(2,1)S(1)}, u32[]{:S(2)}, u32[]{:S(2)}) collective-permute-start(bf16[96,2048]{1,0:T(8,128)(2,1)} %get-tuple-element.38), channel_id=1, source_target_pairs={{0,3},{1,0},{2,1},{3,2},{4,7},{5,4},{6,5},{7,6},{8,11},{9,8},{10,9... | collective-permute-start | bytes 1179656 | tf_op jit(solution)/shard_map/ppermute | solution.py:435
  140.0 17.3 %collective-permute-start.7 = (bf16[96,2048]{1,0:T(8,128)(2,1)}, bf16[96,2048]{1,0:T(8,128)(2,1)S(1)}, u32[]{:S(2)}, u32[]{:S(2)}) collective-permute-start(bf16[96,2048]{1,0:T(8,128)(2,1)} %get-tuple-element.39), channel_id=1, source_target_pairs={{0,2},{1,3},{2,0},{3,1},{4,6},{5,7},{6,4},{7,5},{8,10},{9,11},{10,... | collective-permute-start | bytes 1179656 | tf_op jit(solution)/shard_map/ppermute | solution.py:435
  141.6 19.2 %collective-permute-start.8 = (bf16[96,2048]{1,0:T(8,128)(2,1)}, bf16[96,2048]{1,0:T(8,128)(2,1)S(1)}, u32[]{:S(2)}, u32[]{:S(2)}) collective-permute-start(bf16[96,2048]{1,0:T(8,128)(2,1)} %get-tuple-element.40), channel_id=1, source_target_pairs={{0,1},{1,2},{2,3},{3,0},{4,5},{5,6},{6,7},{7,4},{8,9},{9,10},{10,1... | collective-permute-start | bytes 1179656 | tf_op jit(solution)/shard_map/ppermute | solution.py:435
  157.3 3.6 %copy-start.4 = (bf16[96,2048]{1,0:T(8,128)(2,1)}, bf16[96,2048]{1,0:T(8,128)(2,1)S(1)}, u32[]{:S(2)}) copy-start(bf16[96,2048]{1,0:T(8,128)(2,1)S(1)} %collective-permute-done.6.rest_1_) | copy-start | bytes 1179652
  157.3 3.6 %copy-start.6 = (bf16[96,2048]{1,0:T(8,128)(2,1)}, bf16[96,2048]{1,0:T(8,128)(2,1)S(1)}, u32[]{:S(2)}) copy-start(bf16[96,2048]{1,0:T(8,128)(2,1)S(1)} %collective-permute-done.7.rest_2_) | copy-start | bytes 1179652
  160.8 0.8 copy-start.8
Sparse Core Ops, SparseCore 0:
  9.6 80.7 all-gather.4

commit v2 on v1

v2 whole, which is shorter than its diff:
```python
import jax
import jax.numpy as jnp
from jax import lax
from jax.experimental import pallas as pl
from jax.experimental.pallas import tpu as pltpu
from jax.sharding import Mesh
from jax.sharding import PartitionSpec as P

HEAD_DIM = 64
PAIR = 2 * HEAD_DIM
CHUNK = 128
SP = ("sp_0", "sp_1", "sp_2")
SP_TP = ("sp_0", "sp_1", "sp_2", "tp")
EPSILON = 1e-06
BF = jnp.bfloat16
F32 = jnp.float32
NT = (((1,), (1,)), ((), ()))


def ring(size, k):
    return [(i, (i + k) % size) for i in range(size)]


def dot(a, b):
    return jnp.dot(a, b, preferred_element_type=F32)


def dot_nt(a, b):
    return lax.dot_general(a, b, NT, preferred_element_type=F32)


def silu(x):
    return x / (1.0 + jnp.exp(-x))


def places():
    row = lax.broadcasted_iota(jnp.int32, (PAIR, PAIR), 0)
    col = lax.broadcasted_iota(jnp.int32, (PAIR, PAIR), 1)
    return row, col


def half_sums(squares, ones):
    high = squares.astype(BF)
    low = (squares - high.astype(F32)).astype(BF)
    return dot(high, ones) + dot(low, ones)


def softplus(x):
    small = jnp.exp(-jnp.abs(x))
    series = small * (1.0 - small * (0.5 - small * (1.0 / 3.0 - 0.25 * small)))
    return jnp.maximum(x, 0.0) + jnp.where(small < 0.015, series, jnp.log(1.0 + small))


def turned(z):
    return pltpu.roll(z, HEAD_DIM, 1)


def split_three(x):
    high = x.astype(BF)
    rest = x - high.astype(F32)
    middle = rest.astype(BF)
    return jnp.concatenate([high, middle], axis=1), (rest - middle.astype(F32)).astype(BF)


def side_by_side(pair):
    zero = jnp.zeros_like(pair[0])
    upper = jnp.concatenate([pair[0], zero], axis=1)
    lower = jnp.concatenate([zero, pair[1]], axis=1)
    return jnp.concatenate([upper, lower], axis=0)


def halves(x):
    return x[:, :CHUNK], x[:, CHUNK:]


def keys_kernel(
    k_ref, v_ref, beta_ref, decay_ref,
    before_ref, total_ref, y_ref, d_ref, kb_ref, ec_ref,
    l_ref, x_ref, r_ref, f_ref,
):
    row, col = places()
    left = col < HEAD_DIM
    top = row < HEAD_DIM
    same = left == top
    ones = jnp.where(same, 1.0, 0.0).astype(BF)
    inclusive = row >= col
    strict = row > col
    differ = row ^ col
    eye = jnp.where(row == col, 1.0, 0.0)
    off_eye = differ == HEAD_DIM
    length, width = k_ref.shape
    pairs = width // PAIR
    heads = 2 * pairs
    steps = length // CHUNK

    def stacked(x):
        return jnp.concatenate([x[:, c * CHUNK : (c + 1) * CHUNK] for c in range(steps)], axis=0)

    rates = split_three(stacked(-softplus(decay_ref[...])))
    strength = split_three(stacked(1.0 / (1.0 + jnp.exp(-beta_ref[...]))))
    triangle = jnp.where(inclusive, 1.0, 0.0).astype(BF)
    eye_bf = eye.astype(BF)
    triangle_two = jnp.concatenate([triangle, triangle], axis=1)
    cum_row = dot_nt(rates[0], triangle_two) + dot_nt(rates[1], triangle)
    cum_col = dot_nt(triangle_two, rates[0]) + dot_nt(triangle, rates[1])
    beta_col = dot_nt(jnp.concatenate([eye_bf, eye_bf], axis=1), strength[0])
    beta_col = beta_col + dot_nt(eye_bf, strength[1])

    ends = []
    for c in range(steps):
        rows = slice(c * CHUNK, (c + 1) * CHUNK)
        for p in range(pairs):
            lanes = slice(p * PAIR, (p + 1) * PAIR)
            item = c * pairs + p
            key = silu(k_ref[rows, lanes].astype(F32))
            key = (key * lax.rsqrt(half_sums(key * key, ones) + EPSILON)).astype(BF)
            kb_ref[rows, lanes] = key
            key_f = key.astype(F32)
            first = c * heads + 2 * p
            cums = [cum_col[:, h : h + 1] for h in (first, first + 1)]
            betas = [beta_col[:, h : h + 1] for h in (first, first + 1)]
            cum = jnp.where(left, cums[0], cums[1])
            beta = jnp.where(left, betas[0], betas[1])
            grown = jnp.exp(cum)
            ec_ref[rows, lanes] = grown
            strong = turned(key_f * (beta * grown))
            value = silu(v_ref[rows, lanes].astype(F32)) * beta
            r_ref[item, :, :CHUNK] = jnp.where(left, value, strong).astype(BF)
            r_ref[item, :, CHUNK:] = jnp.where(left, strong, value).astype(BF)
            fade = jnp.exp(cum[CHUNK - 1 : CHUNK, :] - cum)
            f_ref[item] = (key_f * fade).T.astype(BF)
            last = [jnp.exp(x[CHUNK - 1 : CHUNK, :]) for x in cums]
            ends.append(jnp.where(off_eye, jnp.where(top, last[0], last[1]), 0.0))
            owns = [jnp.where(left, key_f, 0.0), jnp.where(left, 0.0, key_f)]
            inner = dot_nt(key, jnp.concatenate(owns, axis=0).astype(BF))
            for s in range(2):
                part = slice(s * CHUNK, (s + 1) * CHUNK)
                gap = cums[s] - cum_row[first + s : first + s + 1, :]
                decay = jnp.where(inclusive, jnp.exp(gap), 0.0)
                d_ref[item, :, part] = decay.astype(BF)
                lower = jnp.where(strict, inner[:, part] * decay * betas[s], 0.0)
                l_ref[item, :, part] = lower.astype(BF)
                x_ref[item, :, part] = (eye - jnp.where(differ == 1, lower, 0.0)).astype(BF)

    items = steps * pairs

    def level(power, carry):
        mask = jnp.where((differ >> power) == 1, 1.0, 0.0).astype(BF)
        parts = []
        for i in range(items):
            block = side_by_side([part * mask for part in halves(l_ref[i])])
            parts.append(dot(x_ref[i], block).astype(BF))
        for i in range(items):
            x = x_ref[i]
            x_ref[i] = x - dot(parts[i], side_by_side(halves(x))).astype(BF)
        return carry

    lax.fori_loop(1, 7, level, 0)

    runs = [None] * pairs
    for c in range(steps):
        for p in range(pairs):
            item = c * pairs + p
            y = dot(x_ref[item], side_by_side(halves(r_ref[item]))).astype(BF)
            y_ref[item] = y
            z = jnp.where(top, *halves(dot(f_ref[item], y)))
            z = jnp.where(same, z, ends[item] - z)
            if c == 0:
                before_ref[c, p] = jnp.where(off_eye, 1.0, 0.0).astype(BF)
                runs[p] = z.astype(BF)
            else:
                before_ref[c, p] = runs[p]
                step = jnp.where(same, turned(z), 0.0).astype(BF)
                runs[p] = (dot(step, runs[p]) + jnp.where(same, z, 0.0)).astype(BF)
    for p in range(pairs):
        total_ref[p] = runs[p]


def keys_side(keys, values, beta_pre, decay_pre):
    length, width = keys.shape
    pairs = width // PAIR
    steps = length // CHUNK
    items = steps * pairs
    full = pl.BlockSpec(memory_space=pltpu.VMEM)
    return pl.pallas_call(
        keys_kernel,
        in_specs=[full] * 4,
        out_specs=[full] * 6,
        out_shape=[
            jax.ShapeDtypeStruct((steps, pairs, PAIR, PAIR), BF),
            jax.ShapeDtypeStruct((pairs, PAIR, PAIR), BF),
            jax.ShapeDtypeStruct((items, CHUNK, 2 * PAIR), BF),
            jax.ShapeDtypeStruct((items, CHUNK, 2 * CHUNK), BF),
            jax.ShapeDtypeStruct((length, width), BF),
            jax.ShapeDtypeStruct((length, width), F32),
        ],
        scratch_shapes=[
            pltpu.VMEM((items, CHUNK, 2 * CHUNK), BF),
            pltpu.VMEM((items, CHUNK, 2 * CHUNK), BF),
            pltpu.VMEM((items, CHUNK, 2 * PAIR), BF),
            pltpu.VMEM((items, PAIR, CHUNK), BF),
        ],
        name="keys_side",
    )(keys, values, beta_pre, decay_pre)


def queries_kernel(
    q_ref, kb_ref, d_ref, y_ref, before_ref, ec_ref, gates_ref, gain_ref, o_ref, q1_ref, gate_ref
):
    row, col = places()
    left = col < HEAD_DIM
    same = left == (row < HEAD_DIM)
    ones = jnp.where(same, 1.0, 0.0).astype(BF)
    gain = jnp.concatenate([gain_ref[...], gain_ref[...]], axis=1)
    for p in range(q_ref.shape[1] // PAIR):
        lanes = slice(p * PAIR, (p + 1) * PAIR)
        gate_ref[:, lanes] = silu(gates_ref[:, lanes].astype(F32)) * gain
        query = silu(q_ref[:, lanes].astype(F32))
        query = query * lax.rsqrt(half_sums(query * query, ones) + EPSILON)
        query = (query * HEAD_DIM ** (-0.5)).astype(BF)
        key_f = kb_ref[:, lanes].astype(F32)
        owns = [jnp.where(left, key_f, 0.0), jnp.where(left, 0.0, key_f)]
        inside = dot_nt(query, jnp.concatenate(owns, axis=0).astype(BF))
        inside = (inside * d_ref[p].astype(F32)).astype(BF)
        got = halves(dot(inside, side_by_side(halves(y_ref[p]))))
        local = jnp.where(left, got[0], got[1])
        crossed = turned(jnp.where(left, got[1], got[0]))
        query = (query.astype(F32) * ec_ref[:, lanes] - crossed).astype(BF)
        before = before_ref[p].astype(F32)
        both = [jnp.where(same, before, 0.0), jnp.where(same, turned(before), 0.0)]
        moved = halves(dot(query, jnp.concatenate(both, axis=1).astype(BF)))
        o_ref[:, lanes] = local + moved[0]
        q1_ref[:, lanes] = moved[1].astype(BF)


def queries_side(queries, key_unit, decay, solved, before, grown, gates, gain):
    length, width = queries.shape
    pairs = width // PAIR
    rows = pl.BlockSpec((CHUNK, width), lambda c: (c, 0))
    per_pair = pl.BlockSpec((pairs, CHUNK, 2 * PAIR), lambda c: (c, 0, 0))
    return pl.pallas_call(
        queries_kernel,
        grid=(length // CHUNK,),
        in_specs=[
            rows,
            rows,
            per_pair,
            per_pair,
            pl.BlockSpec((None, pairs, PAIR, PAIR), lambda c: (c, 0, 0, 0)),
            rows,
            rows,
            pl.BlockSpec((1, HEAD_DIM), lambda c: (0, 0)),
        ],
        out_specs=[rows] * 3,
        out_shape=[
            jax.ShapeDtypeStruct((length, width), F32),
            jax.ShapeDtypeStruct((length, width), BF),
            jax.ShapeDtypeStruct((length, width), F32),
        ],
        name="queries_side",
    )(queries, key_unit, decay, solved, before, grown, gates, gain.reshape(1, HEAD_DIM))


def chained(earlier, later, same):
    later = later.astype(F32)
    step = jnp.where(same, turned(later), 0.0).astype(BF)
    return dot(step, earlier.astype(BF)) + jnp.where(same, later, 0.0)


def chip_kernel(at_ref, own_ref, other_ref, out_ref):
    row, col = places()
    same = (col < HEAD_DIM) == (row < HEAD_DIM)
    core = at_ref[1]
    count = out_ref.shape[0]
    for p in range(count):
        mine = own_ref[core * count + p]
        theirs = other_ref[core * count + p]
        first = jnp.where(core == 0, mine, theirs)
        second = jnp.where(core == 0, theirs, mine)
        out_ref[p] = chained(first, second, same).astype(BF)


def row_kernel(at_ref, *rest):
    parts, (total_ref, before_ref, all_ref) = rest[:-3], rest[-3:]
    row, col = places()
    same = (col < HEAD_DIM) == (row < HEAD_DIM)
    place = at_ref[2]
    size = len(parts)
    for k, part in enumerate(parts):
        all_ref[lax.rem(place - k + size, size)] = part[...]
    for p in range(total_ref.shape[0]):
        run = all_ref[0, p].astype(F32)
        inside = jnp.where(place == 0, jnp.where((row ^ col) == HEAD_DIM, 1.0, 0.0), run)
        for k in range(1, size):
            run = chained(run, all_ref[k, p], same)
            inside = jnp.where(k < place, run, inside)
        before_ref[p] = inside.astype(BF)
        total_ref[p] = run.astype(BF)


def plane_kernel(at_ref, before_ref, *rest):
    parts, out_ref = rest[:-1], rest[-1]
    row, col = places()
    same = (col < HEAD_DIM) == (row < HEAD_DIM)
    place = at_ref[3]
    for p in range(out_ref.shape[0]):
        state = jnp.zeros((PAIR, PAIR), F32)
        for k in range(len(parts), 0, -1):
            later = jnp.where(same, chained(state, parts[k - 1][p], same), 0.0)
            state = jnp.where(k <= place, later, state)
        state = chained(state, before_ref[p], same)
        out_ref[p] = jnp.where(same, state, 0.0).astype(BF)


def small_call(kernel, name, at, arrays, shapes, scratch=()):
    full = pl.BlockSpec(memory_space=pltpu.VMEM)
    return pl.pallas_call(
        kernel,
        in_specs=[pl.BlockSpec(memory_space=pltpu.SMEM)] + [full] * len(arrays),
        out_specs=[full] * len(shapes),
        out_shape=[jax.ShapeDtypeStruct(shape, BF) for shape in shapes],
        scratch_shapes=[pltpu.VMEM(shape, BF) for shape in scratch],
        name=name,
    )(at, *arrays)


def state_ahead(at, total):
    plane, line, core = SP
    swap = [(0, 1), (1, 0)]
    half = (total.shape[0] // 2, PAIR, PAIR)
    other = lax.ppermute(total, core, swap)
    (chip,) = small_call(chip_kernel, "chip_total", at, [total, other], [half])
    size = lax.axis_size(line)
    lines = [chip] + [lax.ppermute(chip, line, ring(size, k)) for k in range(1, size)]
    whole, before = small_call(
        row_kernel, "line_total", at, lines, [half, half], [(size, *half)]
    )
    size = lax.axis_size(plane)
    planes = [lax.ppermute(whole, plane, ring(size, k)) for k in range(1, size)]
    (state,) = small_call(plane_kernel, "plane_state", at, [before] + planes, [half])
    return other, state, lax.ppermute(state, core, swap)


def mixed_kernel(
    at_ref, o_ref, q1_ref, first_ref, mine_ref, theirs_ref, gate_ref, w_ref, *rest
):
    out_refs, (mixed_ref, state_ref) = rest[:-2], rest[-2:]
    row, col = places()
    same = (col < HEAD_DIM) == (row < HEAD_DIM)
    ones = jnp.where(same, 1.0, 0.0).astype(BF)
    length, width = o_ref.shape
    core = at_ref[1]
    half = mine_ref.shape[0]
    state_ref[pl.ds(core * half, half)] = mine_ref[...]
    state_ref[pl.ds((1 - core) * half, half)] = theirs_ref[...]
    for p in range(width // PAIR):
        lanes = slice(p * PAIR, (p + 1) * PAIR)
        state = state_ref[p].astype(F32)
        later = jnp.where(same, chained(state, first_ref[p], same), 0.0)
        state = jnp.where(core == 0, state, later).astype(BF)
        out = o_ref[:, lanes] + dot(q1_ref[:, lanes], state)
        mean = half_sums(out * out, ones) * (1.0 / HEAD_DIM)
        out = out * lax.rsqrt(mean + EPSILON) * gate_ref[:, lanes]
        mixed_ref[:, lanes] = out.astype(BF)
    size = len(out_refs)
    block = length // size
    for k, out_ref in enumerate(out_refs):
        start = lax.rem(at_ref[0] + k, size) * block
        rows = mixed_ref[pl.ds(pl.multiple_of(start, 32), block), :]
        out_ref[...] = dot(rows, w_ref[...]).astype(out_ref.dtype)


def mixed_and_projected(at, size, local, query, states, gate, w_out):
    length, width = local.shape
    block = length // size
    full = pl.BlockSpec(memory_space=pltpu.VMEM)
    return pl.pallas_call(
        mixed_kernel,
        in_specs=[pl.BlockSpec(memory_space=pltpu.SMEM)] + [full] * 7,
        out_specs=[full] * size,
        out_shape=[
            jax.ShapeDtypeStruct((block, w_out.shape[1]), F32 if k == 0 else BF)
            for k in range(size)
        ],
        scratch_shapes=[
            pltpu.VMEM((length, width), BF),
            pltpu.VMEM((width // PAIR, PAIR, PAIR), BF),
        ],
        name="mixed_and_projected",
    )(at, local, query, *states, gate, w_out)


def norm_kernel(stream_ref, gain_ref, *rest):
    parts, middle_ref, normed_ref = rest[:-2], rest[-2], rest[-1]
    total = stream_ref[...].astype(F32)
    projected = parts[0][...].astype(F32)
    for part in parts[1:]:
        projected = projected + part[...].astype(F32)
    middle = (total + projected).astype(BF)
    middle_ref[...] = middle
    middle = middle.astype(F32)
    mean = jnp.mean(middle * middle, axis=-1, keepdims=True)
    normed_ref[...] = (middle * lax.rsqrt(mean + EPSILON) * gain_ref[...]).astype(BF)


def normed_rows(stream, gain, parts):
    full = pl.BlockSpec(memory_space=pltpu.VMEM)
    return pl.pallas_call(
        norm_kernel,
        in_specs=[full] * (2 + len(parts)),
        out_specs=[full] * 2,
        out_shape=[jax.ShapeDtypeStruct(stream.shape, BF)] * 2,
        name="normed_rows",
    )(stream, gain.reshape(1, -1), *parts)


def channels_kernel(w_ref, *rest):
    size = (len(rest) - 7) // 2
    parts, out_refs = rest[:size], rest[size : 2 * size]
    gate_ref, up_ref, down_ref, rows_ref, hidden_ref, in_sems, down_sems = rest[2 * size :]
    width, hidden = gate_ref.shape
    block = parts[0].shape[0]
    tile, strip = 128, 256
    tiles, strips = hidden // tile, width // strip
    copies, downs = [], []
    for j in range(tiles):
        here = pl.ds(j * tile, tile)
        for k, ref in enumerate((gate_ref, up_ref)):
            from_ref = w_ref.at[:, pl.ds(k * hidden + j * tile, tile)]
            copies.append(pltpu.make_async_copy(from_ref, ref.at[:, here], in_sems.at[k, j]))
    for n in range(strips):
        here = pl.ds(n * strip, strip)
        from_ref = w_ref.at[here, pl.ds(2 * hidden, hidden)]
        downs.append(pltpu.make_async_copy(from_ref, down_ref.at[here, :], down_sems.at[n]))
    for copy in copies + downs:
        copy.start()
    for k, part in enumerate(parts):
        rows_ref[k * block : (k + 1) * block, :] = part[...]
    for j in range(tiles):
        copies[2 * j].wait()
        copies[2 * j + 1].wait()
        here = slice(j * tile, (j + 1) * tile)
        both = jnp.concatenate([gate_ref[:, here], up_ref[:, here]], axis=1)
        got = dot(rows_ref[...], both)
        hidden_ref[:, here] = (silu(got[:, :tile]) * got[:, tile:]).astype(BF)
    for n in range(strips):
        downs[n].wait()
        here = slice(n * strip, (n + 1) * strip)
        got = dot_nt(hidden_ref[...], down_ref[here, :])
        for k, out_ref in enumerate(out_refs):
            out_ref[:, here] = got[k * block : (k + 1) * block, :].astype(BF)


def channel_sums(weights, parts, hidden):
    block, width = parts[0].shape
    size = len(parts)
    length = block * size
    full = pl.BlockSpec(memory_space=pltpu.VMEM)
    return pl.pallas_call(
        channels_kernel,
        in_specs=[pl.BlockSpec(memory_space=pl.ANY)] + [full] * size,
        out_specs=[full] * size,
        out_shape=[jax.ShapeDtypeStruct((block, width), BF)] * size,
        scratch_shapes=[
            pltpu.VMEM((width, hidden), BF),
            pltpu.VMEM((width, hidden), BF),
            pltpu.VMEM((width, hidden), BF),
            pltpu.VMEM((length, width), BF),
            pltpu.VMEM((length, hidden), BF),
            pltpu.SemaphoreType.DMA((2, hidden // 128)),
            pltpu.SemaphoreType.DMA((width // 256,)),
        ],
        name="channel_sums",
    )(weights, *parts)


def last_kernel(middle_ref, *rest):
    parts, out_ref = rest[:-1], rest[-1]
    total = parts[0][...].astype(F32)
    for part in parts[1:]:
        total = total + part[...].astype(F32)
    out_ref[...] = (middle_ref[...].astype(F32) + 0.5 * total).astype(BF)


def last_sum(middle, parts):
    full = pl.BlockSpec(memory_space=pltpu.VMEM)
    return pl.pallas_call(
        last_kernel,
        in_specs=[full] * (1 + len(parts)),
        out_specs=full,
        out_shape=jax.ShapeDtypeStruct(middle.shape, BF),
        name="last_sum",
    )(middle, *parts)


def per_device(
    queries,
    keys,
    values,
    gates,
    decay_pre,
    beta_pre,
    out_gain,
    w_out,
    stream,
    norm_gain,
    w_gate,
    w_up,
    w_down,
):
    hidden = w_gate.shape[1]
    weights = jnp.concatenate([w_gate, w_up, w_down.T], axis=1)
    weights = lax.all_gather(weights, SP, axis=0, tiled=True)
    size = lax.axis_size("tp")
    at = jnp.stack([lax.axis_index(a).astype(jnp.int32) for a in ("tp", *reversed(SP))])
    before, total, solved, decay, key_unit, grown = keys_side(keys, values, beta_pre, decay_pre)
    local, query, gate = queries_side(
        queries, key_unit, decay, solved, before, grown, gates, out_gain
    )
    states = state_ahead(at, total)
    parts = mixed_and_projected(at, size, local, query, states, gate, w_out)
    got = [lax.ppermute(parts[k], "tp", ring(size, k)) for k in range(1, size)]
    middle, normed = normed_rows(stream, norm_gain, [parts[0]] + got)
    rows = [normed] + [lax.ppermute(normed, "tp", ring(size, k)) for k in range(1, size)]
    sums = channel_sums(weights, rows, hidden)
    back = [lax.ppermute(sums[k], "tp", ring(size, -k)) for k in range(1, size)]
    return last_sum(middle, [sums[0]] + back)


def solution(mesh):
    finer = Mesh(mesh.devices.reshape(4, 4, 2, mesh.shape["tp"]), SP_TP)
    placed = (
        P(SP, "tp"),
        P(SP, "tp"),
        P(SP, "tp"),
        P(SP, "tp"),
        P("tp", SP),
        P("tp", SP),
        P(),
        P("tp", None),
        P(SP_TP, None),
        P(),
        P(SP, "tp"),
        P(SP, "tp"),
        P("tp", SP),
    )
    return jax.shard_map(
        per_device, mesh=finer, in_specs=placed, out_specs=P(SP_TP, None), check_vma=False
    )
```

time: 172 us -> 170 us (0.988)
  blocking collectives: 32.2 us -> 0 us
  waiting for transfers between devices: 46.3 us -> 61.9 us
  starting transfers between devices: 14.6 us -> 27.1 us
  matrix products: 3.71 us -> 0 us
  Pallas kernels: 54.2 us -> 57.7 us
    all_gather x3 -> x0, blocking collectives: 32.2 us -> none  [carried_in(): pieces = lax.all_gather(subtotal.astype(BF), axis)]
    ppermute x0 -> x8, starting transfers between devices: none -> 13.1 us  [the longest x3 7.13 us: state_ahead(): planes = [lax.ppermute(whole, plane, ring(size, k)) for k in range(1, size)]]
    ppermute x0 -> x8, waiting for transfers between devices: none -> 9.47 us  [the longest x3 4.94 us: state_ahead(): lax.ppermute(chip, line, ring(size, k))]
    pallas_call x3 -> x5, Pallas kernels: 34.3 us -> 38.4 us  [the longest x1 20.8 us: channel_sums(): pl.pallas_call(channels_kernel, in_specs=[pl.BlockSpec(memory_space=pl.AN...]
    ppermute x3, waiting for transfers between devices: 12.7 us -> 16.5 us  [per_device(): got = [lax.ppermute(parts[k], 'tp', ring(size, k)) for k in range(1, size)]]
    dot_general x12 -> x0, matrix products: 3.71 us -> none  [chain(): jnp.einsum('pij,pjk->pik', step, earlier.astype(BF), preferred_element_ty...]
    unnamed x22 -> x34, local copies, waits for them, and re-layouts: 2.55 us -> 5.61 us
  transfers between devices with their start and end apart: 10 -> 18, of which waited for: 6 -> 12; matrix products, arithmetic and copies ran while one was open for 3% -> 0% of each run, Pallas kernels for 18% -> 20%
where the time goes in v2:
time: 170 us; the launch traced here: 168 us
  waiting for transfers between devices  61.9 us (36%)
  Pallas kernels  57.7 us (34%)
  starting transfers between devices  27.1 us (16%)
  between operations  13.5 us (8%)
  local copies, waits for them, and re-layouts  5.61 us (3%)
  other arithmetic  2.52 us (1%)
    pallas_call x1, Pallas kernels, channel_sums(): pl.pallas_call(channels_kernel, in_specs=[pl.BlockSpec(memory_space=pl.AN...  20.8 us
    ppermute x3, waiting for transfers between devices, per_device(): back = [lax.ppermute(sums[k], 'tp', ring(size, -k)) for k in range(1, size)]  19.8 us
    ppermute x3, waiting for transfers between devices, per_device(): got = [lax.ppermute(parts[k], 'tp', ring(size, k)) for k in range(1, size)]  16.5 us
    ppermute x3, waiting for transfers between devices, per_device(): lax.ppermute(normed, 'tp', ring(size, k))  16.1 us
    pallas_call x1, Pallas kernels, keys_side(): pl.pallas_call(keys_kernel, in_specs=[full] * 4, out_specs=[full] * 6, ou...  11 us
    pallas_call x1, Pallas kernels, queries_side(): pl.pallas_call(queries_kernel, grid=(length // CHUNK,), in_specs=[rows, r...  8.1 us
    ppermute x3, starting transfers between devices, state_ahead(): planes = [lax.ppermute(whole, plane, ring(size, k)) for k in range(1, size)]  7.13 us
    pallas_call x3, Pallas kernels, small_call(): pl.pallas_call(kernel, in_specs=[pl.BlockSpec(memory_space=pltpu.SMEM)] +...  6.55 us
  transfers between devices with their start and end apart: 18, of which 12 were waited for; matrix products, arithmetic and copies ran while one was open for 0% of the time, Pallas kernels for 20%

profile of v2, /device:TPU:0, one launch (start us, length us, event | category | flops | bytes accessed | tf_op | source)
XLA Modules:
  0.0 168.3 jit_solution(13702041769897950654)
XLA Ops:
  6.5 1.9 %pad_maximum_fusion = bf16[64,4224]{1,0:T(8,128)(2,1)} fusion(bf16[64,1408]{1,0:T(8,128)(2,1)} %bitcast.7, bf16[64,1408]{1,0:T(8,128)(2,1)} %param.24, bf16[64,1408]{1,0:T(8,128)(2,1)} %param.23), kind=kLoop, calls=%fused_computation | loop fusion | flops 1622016 | bytes 1081344 | tf_op jit(solution)/shard_map/concatenate | solution.py:512
  8.5 0.0 all-gather.2.cloned.1.call-update
  8.5 11.0 %keys_side.1 = (bf16[3,4,128,128]{3,2,1,0:T(8,128)(2,1)}, bf16[4,128,128]{2,1,0:T(8,128)(2,1)}, bf16[12,128,256]{2,1,0:T(8,128)(2,1)}, bf16[12,128,256]{2,1,0:T(...) custom-call(bf16[384,512]{1,0:T(8,128)(2,1)} %k_ref.1, bf16[384,512]{1,0:T(8,128)(2,1)} %v_ref.1, ...), custom_call_target="tpu_custom_call" | custom-call | tf_op jit(solution)/shard_map/keys_side/pallas_call | solution.py:185
  19.5 0.6 pad_add_fusion.at_ref
  20.1 1.0 collective-permute-done.other_ref.first_ref
  21.1 0.6 copy-done
  21.7 1.9 %chip_total.1.rest_0_ = bf16[2,128,128]{2,1,0:T(8,128)(2,1)} custom-call(s32[4]{0:T(128)} %pad_add_fusion.at_ref, bf16[4,128,128]{2,1,0:T(8,128)(2,1)} %get-tuple-element.33.own_ref, bf16[4,128,128]{2,1,0:T(8,128)(2,1)} %copy-done), custom_call_target="tpu_custom_call" | custom-call | tf_op jit(solution)/shard_map/chip_total/pallas_call | solution.py:317
  23.6 1.7 %collective-permute-start.1 = (bf16[2,128,128]{2,1,0:T(8,128)(2,1)}, bf16[2,128,128]{2,1,0:T(8,128)(2,1)S(1)}, u32[]{:S(2)}, u32[]{:S(2)}) collective-permute-start(bf16[2,128,128]{2,1,0:T(8,128)(2,1)} %chip_total.1.rest_0_), channel_id=1, source_target_pairs={{0,8},{8,16},{16,24},{24,0},{1,9},{9,17},{17,25},{25,1},{2,10},{10... | collective-permute-start | bytes 196616 | tf_op jit(solution)/shard_map/ppermute | solution.py:334
  25.3 2.9 %collective-permute-start.2 = (bf16[2,128,128]{2,1,0:T(8,128)(2,1)}, bf16[2,128,128]{2,1,0:T(8,128)(2,1)S(1)}, u32[]{:S(2)}, u32[]{:S(2)}) collective-permute-start(bf16[2,128,128]{2,1,0:T(8,128)(2,1)} %chip_total.1.rest_0_), channel_id=1, source_target_pairs={{0,16},{8,24},{16,0},{24,8},{1,17},{9,25},{17,1},{25,9},{2,18},{10... | collective-permute-start | bytes 196616 | tf_op jit(solution)/shard_map/ppermute | solution.py:334
  28.1 1.4 collective-permute-start.3
  29.5 1.6 collective-permute-done.1.rest_1_
  31.1 3.4 %collective-permute-done.2.rest_2_ = bf16[2,128,128]{2,1,0:T(8,128)(2,1)S(1)} collective-permute-done((bf16[2,128,128]{2,1,0:T(8,128)(2,1)}, bf16[2,128,128]{2,1,0:T(8,128)(2,1)S(1)}, u32[]{:S(2)}, u32[]{:S(2)}) %collective-permute-start.2) | collective-permute-done | bytes 65568 | tf_op jit(solution)/shard_map/ppermute | solution.py:334
  34.5 0.6 copy-done.15
  35.1 0.6 copy-done.16
  35.7 2.2 %line_total.1 = (bf16[2,128,128]{2,1,0:T(8,128)(2,1)}, bf16[2,128,128]{2,1,0:T(8,128)(2,1)}) custom-call(s32[4]{0:T(128)} %pad_add_fusion.at_ref, bf16[2,128,128]{2,1,0:T(8,128)(2,1)} %chip_total.1.rest_0_, bf16[2,128,128]{2,1,0:T(8,128)(2,1)} %copy-done.14, bf16[2,128,128]{2,1,0:T(8,128)(2,1)} %copy-done.15, bf16[2,128,128]{2,1,0:T(8,128)(2,1)} %copy-done.16), custom_call_target="tpu_custom_call" | custom-call | tf_op jit(solution)/shard_map/line_total/pallas_call | solution.py:317
  37.9 2.4 %collective-permute-start.4 = (bf16[2,128,128]{2,1,0:T(8,128)(2,1)}, bf16[2,128,128]{2,1,0:T(8,128)(2,1)S(1)}, u32[]{:S(2)}, u32[]{:S(2)}) collective-permute-start(bf16[2,128,128]{2,1,0:T(8,128)(2,1)} %get-tuple-element.35), channel_id=1, source_target_pairs={{0,32},{32,64},{64,96},{96,0},{1,33},{33,65},{65,97},{97,1},{2,34}... | collective-permute-start | bytes 196616 | tf_op jit(solution)/shard_map/ppermute | solution.py:339
  40.4 3.8 %collective-permute-start.5 = (bf16[2,128,128]{2,1,0:T(8,128)(2,1)}, bf16[2,128,128]{2,1,0:T(8,128)(2,1)S(1)}, u32[]{:S(2)}, u32[]{:S(2)}) collective-permute-start(bf16[2,128,128]{2,1,0:T(8,128)(2,1)} %get-tuple-element.35), channel_id=1, source_target_pairs={{0,64},{32,96},{64,0},{96,32},{1,65},{33,97},{65,1},{97,33},{2,66}... | collective-permute-start | bytes 196616 | tf_op jit(solution)/shard_map/ppermute | solution.py:339
  44.1 0.9 collective-permute-start.6
  45.1 0.8 collective-permute-done.4.rest_0_
  45.8 1.5 collective-permute-done.5.rest_1_
  47.3 1.3 collective-permute-done.6.rest_2_
  48.6 0.6 copy-done.13
  49.2 2.5 %plane_state.1.mine_ref = bf16[2,128,128]{2,1,0:T(8,128)(2,1)} custom-call(s32[4]{0:T(128)} %pad_add_fusion.at_ref, bf16[2,128,128]{2,1,0:T(8,128)(2,1)} %get-tuple-element.34.before_ref, bf16[2,128,128]{2,1,0:T(8,128)(2,1)} %copy-done.11, bf16[2,128,128]{2,1,0:T(8,128)(2,1)} %copy-done.12, bf16[2,128,128]{2,1,0:T(8,128)(2,1)} %copy-done.13), custom_call_target="tpu_custom_call" | custom-call | tf_op jit(solution)/shard_map/plane_state/pallas_call | solution.py:317
  51.7 8.1 %queries_side.1 = (f32[384,512]{1,0:T(8,128)}, bf16[384,512]{1,0:T(8,128)(2,1)}, f32[384,512]{1,0:T(8,128)}) custom-call(bf16[384,512]{1,0:T(8,128)(2,1)} %q_ref.1, bf16[384,512]{1,0:T(8,128)(2,1)} %get-tuple-element.26.kb_ref, bf16[12,128,256]{2,1,0:T(8,128)(2,1)} %get-tuple-element.27.d_ref, bf16[12,128,256]{2,1,0:T(8,128)(2,1)} %get-tuple-element.28.y_ref, ...), custom_call_target="tpu_custom_call" | custom-call | tf_op jit(solution)/shard_map/queries_side/pallas_call | solution.py:241
  59.8 0.6 copy-done.10
  60.4 6.0 %mixed_and_projected.1 = (f32[96,2048]{1,0:T(8,128)}, bf16[96,2048]{1,0:T(8,128)(2,1)}, bf16[96,2048]{1,0:T(8,128)(2,1)}, bf16[96,2048]{1,0:T(8,128)(2,1)}) custom-call(s32[4]{0:T(128)} %pad_add_fusion.at_ref, f32[384,512]{1,0:T(8,128)} %get-tuple-element.31.o_ref, bf16[384,512]{1,0:T(8,128)(2,1)} %get-tuple-element.32.q1_ref, bf16[4,128,128]{2,1,0:T(8,128)(2,1)} %copy-done, ...), custom_call_target="tpu_custom_call" | custom-call | tf_op jit(solution)/shard_map/mixed_and_projected/pallas_call | solution.py:377
  66.4 1.5 collective-permute-start.8
  67.9 2.7 %collective-permute-start.9 = (bf16[96,2048]{1,0:T(8,128)(2,1)}, bf16[96,2048]{1,0:T(8,128)(2,1)S(1)}, u32[]{:S(2)}, u32[]{:S(2)}) collective-permute-start(bf16[96,2048]{1,0:T(8,128)(2,1)} %get-tuple-element.39), channel_id=1, source_target_pairs={{0,2},{1,3},{2,0},{3,1},{4,6},{5,7},{6,4},{7,5},{8,10},{9,11},{10,... | collective-permute-start | bytes 1179656 | tf_op jit(solution)/shard_map/ppermute | solution.py:522
  70.7 1.4 collective-permute-start.10
  72.1 7.1 %collective-permute-done.8.rest_1_ = bf16[96,2048]{1,0:T(8,128)(2,1)S(1)} collective-permute-done((bf16[96,2048]{1,0:T(8,128)(2,1)}, bf16[96,2048]{1,0:T(8,128)(2,1)S(1)}, u32[]{:S(2)}, u32[]{:S(2)}) %collective-permute-start.8) | collective-permute-done | bytes 393248 | tf_op jit(solution)/shard_map/ppermute | solution.py:522
  79.2 9.4 %collective-permute-done.9.rest_2_ = bf16[96,2048]{1,0:T(8,128)(2,1)S(1)} collective-permute-done((bf16[96,2048]{1,0:T(8,128)(2,1)}, bf16[96,2048]{1,0:T(8,128)(2,1)S(1)}, u32[]{:S(2)}, u32[]{:S(2)}) %collective-permute-start.9) | collective-permute-done | bytes 393248 | tf_op jit(solution)/shard_map/ppermute | solution.py:522
  88.6 0.7 copy-done.3
  89.3 0.1 copy-done.5
  89.4 2.8 %normed_rows.1 = (bf16[96,2048]{1,0:T(8,128)(2,1)}, bf16[96,2048]{1,0:T(8,128)(2,1)}) custom-call(bf16[96,2048]{1,0:T(8,128)(2,1)} %stream_ref.1, f32[1,2048]{1,0:T(1,128)} %bitcast.8, f32[96,2048]{1,0:T(8,128)} %get-tuple-element.37.rest_0_, bf16[96,2048]{1,0:T(8,128)(2,1)} %copy-done.1, bf16[96,2048]{1,0:T(8,128)(2,1)} %copy-done.3, bf16[96,2048]{1,0:T(8,128)(2,1)} %copy-done.5), custom_call_target="tpu_custom_call" | custom-call | tf_op jit(solution)/shard_map/normed_rows/pallas_call | solution.py:408
  92.2 1.2 collective-permute-start.11
  93.4 2.4 %collective-permute-start.12 = (bf16[96,2048]{1,0:T(8,128)(2,1)}, bf16[96,2048]{1,0:T(8,128)(2,1)S(1)}, u32[]{:S(2)}, u32[]{:S(2)}) collective-permute-start(bf16[96,2048]{1,0:T(8,128)(2,1)} %get-tuple-element.42.rest_0_), channel_id=1, source_target_pairs={{0,2},{1,3},{2,0},{3,1},{4,6},{5,7},{6,4},{7,5},{8,10},{9,11},{10,... | collective-permute-start | bytes 1179656 | tf_op jit(solution)/shard_map/ppermute | solution.py:524
  95.8 1.5 collective-permute-start.13
  97.3 6.7 %collective-permute-done.11.rest_1_ = bf16[96,2048]{1,0:T(8,128)(2,1)S(1)} collective-permute-done((bf16[96,2048]{1,0:T(8,128)(2,1)}, bf16[96,2048]{1,0:T(8,128)(2,1)S(1)}, u32[]{:S(2)}, u32[]{:S(2)}) %collective-permute-start.11) | collective-permute-done | bytes 393248 | tf_op jit(solution)/shard_map/ppermute | solution.py:524
  104.0 9.4 %collective-permute-done.12.rest_2_ = bf16[96,2048]{1,0:T(8,128)(2,1)S(1)} collective-permute-done((bf16[96,2048]{1,0:T(8,128)(2,1)}, bf16[96,2048]{1,0:T(8,128)(2,1)S(1)}, u32[]{:S(2)}, u32[]{:S(2)}) %collective-permute-start.12) | collective-permute-done | bytes 393248 | tf_op jit(solution)/shard_map/ppermute | solution.py:524
  113.5 0.7 copy-done.8
  114.2 0.1 copy-done.9
  114.3 20.8 %channel_sums.1 = (bf16[96,2048]{1,0:T(8,128)(2,1)}, bf16[96,2048]{1,0:T(8,128)(2,1)}, bf16[96,2048]{1,0:T(8,128)(2,1)}, bf16[96,2048]{1,0:T(8,128)(2,1)}) custom-call(bf16[2048,4224]{1,0:T(8,128)(2,1)} %all-gather.2.cloned.1.call-done.w_ref, bf16[96,2048]{1,0:T(8,128)(2,1)} %get-tuple-element.42.rest_0_, bf16[96,2048]{1,0:T(8,128)(2,1)} %copy-done.7, ...), custom_call_target="tpu_custom_call" | custom-call | tf_op jit(solution)/shard_map/channel_sums/pallas_call | solution.py:459
  135.1 2.2 %collective-permute-start.14 = (bf16[96,2048]{1,0:T(8,128)(2,1)}, bf16[96,2048]{1,0:T(8,128)(2,1)S(1)}, u32[]{:S(2)}, u32[]{:S(2)}) collective-permute-start(bf16[96,2048]{1,0:T(8,128)(2,1)} %get-tuple-element.44), channel_id=1, source_target_pairs={{0,3},{1,0},{2,1},{3,2},{4,7},{5,4},{6,5},{7,6},{8,11},{9,8},{10,9... | collective-permute-start | bytes 1179656 | tf_op jit(solution)/shard_map/ppermute | solution.py:526
  137.3 1.0 collective-permute-start.15
  138.4 16.3 %collective-permute-done.14.rest_1_ = bf16[96,2048]{1,0:T(8,128)(2,1)S(1)} collective-permute-done((bf16[96,2048]{1,0:T(8,128)(2,1)}, bf16[96,2048]{1,0:T(8,128)(2,1)S(1)}, u32[]{:S(2)}, u32[]{:S(2)}) %collective-permute-start.14) | collective-permute-done | bytes 393248 | tf_op jit(solution)/shard_map/ppermute | solution.py:526
  154.7 3.6 %collective-permute-done.16.rest_3_ = bf16[96,2048]{1,0:T(8,128)(2,1)S(1)} collective-permute-done((bf16[96,2048]{1,0:T(8,128)(2,1)}, bf16[96,2048]{1,0:T(8,128)(2,1)S(1)}, u32[]{:S(2)}, u32[]{:S(2)}) %collective-permute-start.16) | collective-permute-done | bytes 393248 | tf_op jit(solution)/shard_map/ppermute | solution.py:526
  158.2 0.8 copy-done.6
  159.0 2.5 %last_sum.1 = bf16[96,2048]{1,0:T(8,128)(2,1)} custom-call(bf16[96,2048]{1,0:T(8,128)(2,1)} %get-tuple-element.41.middle_ref, bf16[96,2048]{1,0:T(8,128)(2,1)} %get-tuple-element.43.rest_0_, bf16[96,2048]{1,0:T(8,128)(2,1)} %copy-done.2, bf16[96,2048]{1,0:T(8,128)(2,1)} %copy-done.4, bf16[96,2048]{1,0:T(8,128)(2,1)} %copy-done.6), custom_call_target="tpu_custom_call" | custom-call | tf_op jit(solution)/shard_map/last_sum/pallas_call | solution.py:487
  (34 shorter events, 0.1 us)
Async XLA Ops:
  6.5 106.9 %all-gather.2.cloned.1.call-start = ((), (), s32[]{:S(2)}) async-start(), calls=%async_computation | async-start | bytes 17842176 | tf_op jit(solution)/shard_map/all_gather | solution.py:513
  19.5 1.6 collective-permute-start
  21.1 0.6 copy-start
  23.6 7.5 %collective-permute-start.1 = (bf16[2,128,128]{2,1,0:T(8,128)(2,1)}, bf16[2,128,128]{2,1,0:T(8,128)(2,1)S(1)}, u32[]{:S(2)}, u32[]{:S(2)}) collective-permute-start(bf16[2,128,128]{2,1,0:T(8,128)(2,1)} %chip_total.1.rest_0_), channel_id=1, source_target_pairs={{0,8},{8,16},{16,24},{24,0},{1,9},{9,17},{17,25},{25,1},{2,10},{10... | collective-permute-start | bytes 196616 | tf_op jit(solution)/shard_map/ppermute | solution.py:334
  25.3 9.2 %collective-permute-start.2 = (bf16[2,128,128]{2,1,0:T(8,128)(2,1)}, bf16[2,128,128]{2,1,0:T(8,128)(2,1)S(1)}, u32[]{:S(2)}, u32[]{:S(2)}) collective-permute-start(bf16[2,128,128]{2,1,0:T(8,128)(2,1)} %chip_total.1.rest_0_), channel_id=1, source_target_pairs={{0,16},{8,24},{16,0},{24,8},{1,17},{9,25},{17,1},{25,9},{2,18},{10... | collective-permute-start | bytes 196616 | tf_op jit(solution)/shard_map/ppermute | solution.py:334
  28.1 6.3 %collective-permute-start.3 = (bf16[2,128,128]{2,1,0:T(8,128)(2,1)}, bf16[2,128,128]{2,1,0:T(8,128)(2,1)S(1)}, u32[]{:S(2)}, u32[]{:S(2)}) collective-permute-start(bf16[2,128,128]{2,1,0:T(8,128)(2,1)} %chip_total.1.rest_0_), channel_id=1, source_target_pairs={{0,24},{8,0},{16,8},{24,16},{1,25},{9,1},{17,9},{25,17},{2,26},{10... | collective-permute-start | bytes 196616 | tf_op jit(solution)/shard_map/ppermute | solution.py:334
  31.1 3.4 %copy-start.14 = (bf16[2,128,128]{2,1,0:T(8,128)(2,1)}, bf16[2,128,128]{2,1,0:T(8,128)(2,1)S(1)}, u32[]{:S(2)}) copy-start(bf16[2,128,128]{2,1,0:T(8,128)(2,1)S(1)} %collective-permute-done.1.rest_1_) | copy-start | bytes 196612
  34.4 0.6 copy-start.15
  35.1 0.6 copy-start.16
  37.9 7.9 %collective-permute-start.4 = (bf16[2,128,128]{2,1,0:T(8,128)(2,1)}, bf16[2,128,128]{2,1,0:T(8,128)(2,1)S(1)}, u32[]{:S(2)}, u32[]{:S(2)}) collective-permute-start(bf16[2,128,128]{2,1,0:T(8,128)(2,1)} %get-tuple-element.35), channel_id=1, source_target_pairs={{0,32},{32,64},{64,96},{96,0},{1,33},{33,65},{65,97},{97,1},{2,34}... | collective-permute-start | bytes 196616 | tf_op jit(solution)/shard_map/ppermute | solution.py:339
  40.4 6.9 %collective-permute-start.5 = (bf16[2,128,128]{2,1,0:T(8,128)(2,1)}, bf16[2,128,128]{2,1,0:T(8,128)(2,1)S(1)}, u32[]{:S(2)}, u32[]{:S(2)}) collective-permute-start(bf16[2,128,128]{2,1,0:T(8,128)(2,1)} %get-tuple-element.35), channel_id=1, source_target_pairs={{0,64},{32,96},{64,0},{96,32},{1,65},{33,97},{65,1},{97,33},{2,66}... | collective-permute-start | bytes 196616 | tf_op jit(solution)/shard_map/ppermute | solution.py:339
  44.1 4.5 %collective-permute-start.6 = (bf16[2,128,128]{2,1,0:T(8,128)(2,1)}, bf16[2,128,128]{2,1,0:T(8,128)(2,1)S(1)}, u32[]{:S(2)}, u32[]{:S(2)}) collective-permute-start(bf16[2,128,128]{2,1,0:T(8,128)(2,1)} %get-tuple-element.35), channel_id=1, source_target_pairs={{0,96},{32,0},{64,32},{96,64},{1,97},{33,1},{65,33},{97,65},{2,98}... | collective-permute-start | bytes 196616 | tf_op jit(solution)/shard_map/ppermute | solution.py:339
  45.8 2.8 %copy-start.11 = (bf16[2,128,128]{2,1,0:T(8,128)(2,1)}, bf16[2,128,128]{2,1,0:T(8,128)(2,1)S(1)}, u32[]{:S(2)}) copy-start(bf16[2,128,128]{2,1,0:T(8,128)(2,1)S(1)} %collective-permute-done.4.rest_0_) | copy-start | bytes 196612
  47.3 1.3 copy-start.12
  48.6 0.6 copy-start.13
  51.7 8.1 %collective-permute-start.7 = (bf16[2,128,128]{2,1,0:T(8,128)(2,1)}, bf16[2,128,128]{2,1,0:T(8,128)(2,1)S(1)}, u32[]{:S(2)}, u32[]{:S(2)}) collective-permute-start(bf16[2,128,128]{2,1,0:T(8,128)(2,1)} %plane_state.1.mine_ref), channel_id=1, source_target_pairs={{0,4},{4,0},{1,5},{5,1},{2,6},{6,2},{3,7},{7,3},{8,12},{12,8},{9,1... | collective-permute-start | bytes 196616 | tf_op jit(solution)/shard_map/ppermute | solution.py:341
  59.8 0.6 copy-start.10
  66.4 12.7 %collective-permute-start.8 = (bf16[96,2048]{1,0:T(8,128)(2,1)}, bf16[96,2048]{1,0:T(8,128)(2,1)S(1)}, u32[]{:S(2)}, u32[]{:S(2)}) collective-permute-start(bf16[96,2048]{1,0:T(8,128)(2,1)} %get-tuple-element.38), channel_id=1, source_target_pairs={{0,1},{1,2},{2,3},{3,0},{4,5},{5,6},{6,7},{7,4},{8,9},{9,10},{10,1... | collective-permute-start | bytes 1179656 | tf_op jit(solution)/shard_map/ppermute | solution.py:522
  67.9 20.6 %collective-permute-start.9 = (bf16[96,2048]{1,0:T(8,128)(2,1)}, bf16[96,2048]{1,0:T(8,128)(2,1)S(1)}, u32[]{:S(2)}, u32[]{:S(2)}) collective-permute-start(bf16[96,2048]{1,0:T(8,128)(2,1)} %get-tuple-element.39), channel_id=1, source_target_pairs={{0,2},{1,3},{2,0},{3,1},{4,6},{5,7},{6,4},{7,5},{8,10},{9,11},{10,... | collective-permute-start | bytes 1179656 | tf_op jit(solution)/shard_map/ppermute | solution.py:522
  70.7 17.9 %collective-permute-start.10 = (bf16[96,2048]{1,0:T(8,128)(2,1)}, bf16[96,2048]{1,0:T(8,128)(2,1)S(1)}, u32[]{:S(2)}, u32[]{:S(2)}) collective-permute-start(bf16[96,2048]{1,0:T(8,128)(2,1)} %get-tuple-element.40), channel_id=1, source_target_pairs={{0,3},{1,0},{2,1},{3,2},{4,7},{5,4},{6,5},{7,6},{8,11},{9,8},{10,9... | collective-permute-start | bytes 1179656 | tf_op jit(solution)/shard_map/ppermute | solution.py:522
  79.2 9.4 %copy-start.1 = (bf16[96,2048]{1,0:T(8,128)(2,1)}, bf16[96,2048]{1,0:T(8,128)(2,1)S(1)}, u32[]{:S(2)}) copy-start(bf16[96,2048]{1,0:T(8,128)(2,1)S(1)} %collective-permute-done.8.rest_1_) | copy-start | bytes 1179652
  88.5 0.8 copy-start.3
  88.6 0.9 copy-start.5
  92.2 11.8 %collective-permute-start.11 = (bf16[96,2048]{1,0:T(8,128)(2,1)}, bf16[96,2048]{1,0:T(8,128)(2,1)S(1)}, u32[]{:S(2)}, u32[]{:S(2)}) collective-permute-start(bf16[96,2048]{1,0:T(8,128)(2,1)} %get-tuple-element.42.rest_0_), channel_id=1, source_target_pairs={{0,1},{1,2},{2,3},{3,0},{4,5},{5,6},{6,7},{7,4},{8,9},{9,10},{10,1... | collective-permute-start | bytes 1179656 | tf_op jit(solution)/shard_map/ppermute | solution.py:524
  93.4 20.0 %collective-permute-start.12 = (bf16[96,2048]{1,0:T(8,128)(2,1)}, bf16[96,2048]{1,0:T(8,128)(2,1)S(1)}, u32[]{:S(2)}, u32[]{:S(2)}) collective-permute-start(bf16[96,2048]{1,0:T(8,128)(2,1)} %get-tuple-element.42.rest_0_), channel_id=1, source_target_pairs={{0,2},{1,3},{2,0},{3,1},{4,6},{5,7},{6,4},{7,5},{8,10},{9,11},{10,... | collective-permute-start | bytes 1179656 | tf_op jit(solution)/shard_map/ppermute | solution.py:524
  95.8 17.7 %collective-permute-start.13 = (bf16[96,2048]{1,0:T(8,128)(2,1)}, bf16[96,2048]{1,0:T(8,128)(2,1)S(1)}, u32[]{:S(2)}, u32[]{:S(2)}) collective-permute-start(bf16[96,2048]{1,0:T(8,128)(2,1)} %get-tuple-element.42.rest_0_), channel_id=1, source_target_pairs={{0,3},{1,0},{2,1},{3,2},{4,7},{5,4},{6,5},{7,6},{8,11},{9,8},{10,9... | collective-permute-start | bytes 1179656 | tf_op jit(solution)/shard_map/ppermute | solution.py:524
  104.0 9.4 %copy-start.7 = (bf16[96,2048]{1,0:T(8,128)(2,1)}, bf16[96,2048]{1,0:T(8,128)(2,1)S(1)}, u32[]{:S(2)}) copy-start(bf16[96,2048]{1,0:T(8,128)(2,1)S(1)} %collective-permute-done.11.rest_1_) | copy-start | bytes 1179652
  113.4 0.8 copy-start.8
  113.4 0.9 copy-start.9
  135.1 19.5 %collective-permute-start.14 = (bf16[96,2048]{1,0:T(8,128)(2,1)}, bf16[96,2048]{1,0:T(8,128)(2,1)S(1)}, u32[]{:S(2)}, u32[]{:S(2)}) collective-permute-start(bf16[96,2048]{1,0:T(8,128)(2,1)} %get-tuple-element.44), channel_id=1, source_target_pairs={{0,3},{1,0},{2,1},{3,2},{4,7},{5,4},{6,5},{7,6},{8,11},{9,8},{10,9... | collective-permute-start | bytes 1179656 | tf_op jit(solution)/shard_map/ppermute | solution.py:526
  137.3 17.3 %collective-permute-start.15 = (bf16[96,2048]{1,0:T(8,128)(2,1)}, bf16[96,2048]{1,0:T(8,128)(2,1)S(1)}, u32[]{:S(2)}, u32[]{:S(2)}) collective-permute-start(bf16[96,2048]{1,0:T(8,128)(2,1)} %get-tuple-element.45), channel_id=1, source_target_pairs={{0,2},{1,3},{2,0},{3,1},{4,6},{5,7},{6,4},{7,5},{8,10},{9,11},{10,... | collective-permute-start | bytes 1179656 | tf_op jit(solution)/shard_map/ppermute | solution.py:526
  138.4 19.8 %collective-permute-start.16 = (bf16[96,2048]{1,0:T(8,128)(2,1)}, bf16[96,2048]{1,0:T(8,128)(2,1)S(1)}, u32[]{:S(2)}, u32[]{:S(2)}) collective-permute-start(bf16[96,2048]{1,0:T(8,128)(2,1)} %get-tuple-element.46), channel_id=1, source_target_pairs={{0,1},{1,2},{2,3},{3,0},{4,5},{5,6},{6,7},{7,4},{8,9},{9,10},{10,1... | collective-permute-start | bytes 1179656 | tf_op jit(solution)/shard_map/ppermute | solution.py:526
  154.7 3.6 %copy-start.2 = (bf16[96,2048]{1,0:T(8,128)(2,1)}, bf16[96,2048]{1,0:T(8,128)(2,1)S(1)}, u32[]{:S(2)}) copy-start(bf16[96,2048]{1,0:T(8,128)(2,1)S(1)} %collective-permute-done.14.rest_1_) | copy-start | bytes 1179652
  154.7 3.6 %copy-start.4 = (bf16[96,2048]{1,0:T(8,128)(2,1)}, bf16[96,2048]{1,0:T(8,128)(2,1)S(1)}, u32[]{:S(2)}) copy-start(bf16[96,2048]{1,0:T(8,128)(2,1)S(1)} %collective-permute-done.15.rest_2_) | copy-start | bytes 1179652
  158.2 0.8 copy-start.6
Sparse Core Ops, SparseCore 0:
  9.6 78.8 all-gather.1

commit v3 on v2

--- a/solution.py
+++ b/solution.py
@@ -15,6 +15,25 @@
 BF = jnp.bfloat16
 F32 = jnp.float32
 NT = (((1,), (1,)), ((), ()))
+
+
+FULL = pl.BlockSpec(memory_space=pltpu.VMEM)
+FAR = pl.BlockSpec(memory_space=pl.ANY)
+TABLE = pl.BlockSpec(memory_space=pltpu.SMEM)
+
+
+def call(kernel, name, arrays, shapes, scratch=(), table=None, far=(), mib=16):
+    near = [pltpu.with_memory_space_constraint(x, pltpu.VMEM) for x in arrays]
+    tables = [] if table is None else [table]
+    return pl.pallas_call(
+        kernel,
+        in_specs=[TABLE] * len(tables) + [FAR] * len(far) + [FULL] * len(near),
+        out_specs=[FULL] * len(shapes),
+        out_shape=[pltpu.VMEM(shape, dtype) for shape, dtype in shapes],
+        scratch_shapes=scratch,
+        compiler_params=pltpu.CompilerParams(vmem_limit_bytes=mib << 20),
+        name=name,
+    )(*tables, *far, *near)
 
 
 def ring(size, k):
@@ -166,10 +185,10 @@
             z = jnp.where(top, *halves(dot(f_ref[item], y)))
             z = jnp.where(same, z, ends[item] - z)
             if c == 0:
-                before_ref[c, p] = jnp.where(off_eye, 1.0, 0.0).astype(BF)
+                before_ref[item] = jnp.where(off_eye, 1.0, 0.0).astype(BF)
                 runs[p] = z.astype(BF)
             else:
-                before_ref[c, p] = runs[p]
+                before_ref[item] = runs[p]
                 step = jnp.where(same, turned(z), 0.0).astype(BF)
                 runs[p] = (dot(step, runs[p]) + jnp.where(same, z, 0.0)).astype(BF)
     for p in range(pairs):
@@ -181,84 +200,78 @@
     pairs = width // PAIR
     steps = length // CHUNK
     items = steps * pairs
-    full = pl.BlockSpec(memory_space=pltpu.VMEM)
-    return pl.pallas_call(
+    wide = pltpu.VMEM((items, CHUNK, 2 * CHUNK), BF)
+    return call(
         keys_kernel,
-        in_specs=[full] * 4,
-        out_specs=[full] * 6,
-        out_shape=[
-            jax.ShapeDtypeStruct((steps, pairs, PAIR, PAIR), BF),
-            jax.ShapeDtypeStruct((pairs, PAIR, PAIR), BF),
-            jax.ShapeDtypeStruct((items, CHUNK, 2 * PAIR), BF),
-            jax.ShapeDtypeStruct((items, CHUNK, 2 * CHUNK), BF),
-            jax.ShapeDtypeStruct((length, width), BF),
-            jax.ShapeDtypeStruct((length, width), F32),
+        "keys_side",
+        [keys, values, beta_pre, decay_pre],
+        [
+            ((items, PAIR, PAIR), BF),
+            ((pairs, PAIR, PAIR), BF),
+            ((items, CHUNK, 2 * PAIR), BF),
+            ((items, CHUNK, 2 * CHUNK), BF),
+            ((length, width), BF),
+            ((length, width), F32),
         ],
-        scratch_shapes=[
-            pltpu.VMEM((items, CHUNK, 2 * CHUNK), BF),
-            pltpu.VMEM((items, CHUNK, 2 * CHUNK), BF),
-            pltpu.VMEM((items, CHUNK, 2 * PAIR), BF),
-            pltpu.VMEM((items, PAIR, CHUNK), BF),
-        ],
-        name="keys_side",
-    )(keys, values, beta_pre, decay_pre)
-
-
-def queries_kernel(
-    q_ref, kb_ref, d_ref, y_ref, before_ref, ec_ref, gates_ref, gain_ref, o_ref, q1_ref, gate_ref
-):
+        [wide, wide, wide, pltpu.VMEM((items, PAIR, CHUNK), BF)],
+    )
+
+
+def gates_kernel(gates_ref, gain_ref, gate_ref):
+    gain = jnp.concatenate([gain_ref[...], gain_ref[...]], axis=1)
+    for p in range(gates_ref.shape[1] // PAIR):
+        lanes = slice(p * PAIR, (p + 1) * PAIR)
+        gate_ref[:, lanes] = silu(gates_ref[:, lanes].astype(F32)) * gain
+
+
+def queries_kernel(after_ref, q_ref, kb_ref, d_ref, y_ref, before_ref, ec_ref, o_ref, q1_ref):
     row, col = places()
     left = col < HEAD_DIM
     same = left == (row < HEAD_DIM)
     ones = jnp.where(same, 1.0, 0.0).astype(BF)
-    gain = jnp.concatenate([gain_ref[...], gain_ref[...]], axis=1)
-    for p in range(q_ref.shape[1] // PAIR):
-        lanes = slice(p * PAIR, (p + 1) * PAIR)
-        gate_ref[:, lanes] = silu(gates_ref[:, lanes].astype(F32)) * gain
-        query = silu(q_ref[:, lanes].astype(F32))
-        query = query * lax.rsqrt(half_sums(query * query, ones) + EPSILON)
-        query = (query * HEAD_DIM ** (-0.5)).astype(BF)
-        key_f = kb_ref[:, lanes].astype(F32)
-        owns = [jnp.where(left, key_f, 0.0), jnp.where(left, 0.0, key_f)]
-        inside = dot_nt(query, jnp.concatenate(owns, axis=0).astype(BF))
-        inside = (inside * d_ref[p].astype(F32)).astype(BF)
-        got = halves(dot(inside, side_by_side(halves(y_ref[p]))))
-        local = jnp.where(left, got[0], got[1])
-        crossed = turned(jnp.where(left, got[1], got[0]))
-        query = (query.astype(F32) * ec_ref[:, lanes] - crossed).astype(BF)
-        before = before_ref[p].astype(F32)
-        both = [jnp.where(same, before, 0.0), jnp.where(same, turned(before), 0.0)]
-        moved = halves(dot(query, jnp.concatenate(both, axis=1).astype(BF)))
-        o_ref[:, lanes] = local + moved[0]
-        q1_ref[:, lanes] = moved[1].astype(BF)
-
-
-def queries_side(queries, key_unit, decay, solved, before, grown, gates, gain):
-    length, width = queries.shape
+    length, width = q_ref.shape
     pairs = width // PAIR
-    rows = pl.BlockSpec((CHUNK, width), lambda c: (c, 0))
-    per_pair = pl.BlockSpec((pairs, CHUNK, 2 * PAIR), lambda c: (c, 0, 0))
-    return pl.pallas_call(
+
+    def chunk(c, carry):
+        rows = pl.ds(pl.multiple_of(c * CHUNK, CHUNK), CHUNK)
+        for p in range(pairs):
+            lanes = slice(p * PAIR, (p + 1) * PAIR)
+            item = c * pairs + p
+            query = silu(q_ref[rows, lanes].astype(F32))
+            query = query * lax.rsqrt(half_sums(query * query, ones) + EPSILON)
+            query = (query * HEAD_DIM ** (-0.5)).astype(BF)
+            key_f = kb_ref[rows, lanes].astype(F32)
+            owns = [jnp.where(left, key_f, 0.0), jnp.where(left, 0.0, key_f)]
+            inside = dot_nt(query, jnp.concatenate(owns, axis=0).astype(BF))
+            inside = (inside * d_ref[item].astype(F32)).astype(BF)
+            got = halves(dot(inside, side_by_side(halves(y_ref[item]))))
+            local = jnp.where(left, got[0], got[1])
+            crossed = turned(jnp.where(left, got[1], got[0]))
+            query = (query.astype(F32) * ec_ref[rows, lanes] - crossed).astype(BF)
+            before = before_ref[item].astype(F32)
+            both = [jnp.where(same, before, 0.0), jnp.where(same, turned(before), 0.0)]
+            moved = halves(dot(query, jnp.concatenate(both, axis=1).astype(BF)))
+            o_ref[rows, lanes] = local + moved[0]
+            q1_ref[rows, lanes] = moved[1].astype(BF)
+        return carry
+
+    lax.fori_loop(0, length // CHUNK, chunk, 0)
+
+
+def gates_side(gates, gain):
+    return call(
+        gates_kernel, "gates_side", [gates, gain.reshape(1, HEAD_DIM)], [(gates.shape, F32)]
+    )[0]
+
+
+def queries_side(after, queries, key_unit, decay, solved, before, grown):
+    return call(
         queries_kernel,
-        grid=(length // CHUNK,),
-        in_specs=[
-            rows,
-            rows,
-            per_pair,
-            per_pair,
-            pl.BlockSpec((None, pairs, PAIR, PAIR), lambda c: (c, 0, 0, 0)),
-            rows,
-            rows,
-            pl.BlockSpec((1, HEAD_DIM), lambda c: (0, 0)),
-        ],
-        out_specs=[rows] * 3,
-        out_shape=[
-            jax.ShapeDtypeStruct((length, width), F32),
-            jax.ShapeDtypeStruct((length, width), BF),
-            jax.ShapeDtypeStruct((length, width), F32),
-        ],
-        name="queries_side",
-    )(queries, key_unit, decay, solved, before, grown, gates, gain.reshape(1, HEAD_DIM))
+        "queries_side",
+        [queries, key_unit, decay, solved, before, grown],
+        [(queries.shape, F32), (queries.shape, BF)],
+        far=[after],
+    )
 
 
 def chained(earlier, later, same):
@@ -280,7 +293,7 @@
         out_ref[p] = chained(first, second, same).astype(BF)
 
 
-def row_kernel(at_ref, *rest):
+def row_kernel(at_ref, after_ref, *rest):
     parts, (total_ref, before_ref, all_ref) = rest[:-3], rest[-3:]
     row, col = places()
     same = (col < HEAD_DIM) == (row < HEAD_DIM)
@@ -298,7 +311,7 @@
         total_ref[p] = run.astype(BF)
 
 
-def plane_kernel(at_ref, before_ref, *rest):
+def plane_kernel(at_ref, after_ref, before_ref, *rest):
     parts, out_ref = rest[:-1], rest[-1]
     row, col = places()
     same = (col < HEAD_DIM) == (row < HEAD_DIM)
@@ -312,33 +325,31 @@
         out_ref[p] = jnp.where(same, state, 0.0).astype(BF)
 
 
-def small_call(kernel, name, at, arrays, shapes, scratch=()):
-    full = pl.BlockSpec(memory_space=pltpu.VMEM)
-    return pl.pallas_call(
-        kernel,
-        in_specs=[pl.BlockSpec(memory_space=pltpu.SMEM)] + [full] * len(arrays),
-        out_specs=[full] * len(shapes),
-        out_shape=[jax.ShapeDtypeStruct(shape, BF) for shape in shapes],
-        scratch_shapes=[pltpu.VMEM(shape, BF) for shape in scratch],
-        name=name,
-    )(at, *arrays)
-
-
-def state_ahead(at, total):
+def state_ahead(at, total, meanwhile, then):
     plane, line, core = SP
     swap = [(0, 1), (1, 0)]
     half = (total.shape[0] // 2, PAIR, PAIR)
     other = lax.ppermute(total, core, swap)
-    (chip,) = small_call(chip_kernel, "chip_total", at, [total, other], [half])
+    (chip,) = call(chip_kernel, "chip_total", [total, other], [(half, BF)], table=at)
     size = lax.axis_size(line)
     lines = [chip] + [lax.ppermute(chip, line, ring(size, k)) for k in range(1, size)]
-    whole, before = small_call(
-        row_kernel, "line_total", at, lines, [half, half], [(size, *half)]
+    local, query = meanwhile(chip)
+    whole, before = call(
+        row_kernel,
+        "line_total",
+        lines,
+        [(half, BF), (half, BF)],
+        [pltpu.VMEM((size, *half), BF)],
+        table=at,
+        far=[query],
     )
     size = lax.axis_size(plane)
     planes = [lax.ppermute(whole, plane, ring(size, k)) for k in range(1, size)]
-    (state,) = small_call(plane_kernel, "plane_state", at, [before] + planes, [half])
-    return other, state, lax.ppermute(state, core, swap)
+    gate = then()
+    (state,) = call(
+        plane_kernel, "plane_state", [before] + planes, [(half, BF)], table=at, far=[gate]
+    )
+    return local, query, gate, (other, state, lax.ppermute(state, core, swap))
 
 
 def mixed_kernel(
@@ -372,22 +383,15 @@
 
 def mixed_and_projected(at, size, local, query, states, gate, w_out):
     length, width = local.shape
-    block = length // size
-    full = pl.BlockSpec(memory_space=pltpu.VMEM)
-    return pl.pallas_call(
+    block = (length // size, w_out.shape[1])
+    return call(
         mixed_kernel,
-        in_specs=[pl.BlockSpec(memory_space=pltpu.SMEM)] + [full] * 7,
-        out_specs=[full] * size,
-        out_shape=[
-            jax.ShapeDtypeStruct((block, w_out.shape[1]), F32 if k == 0 else BF)
-            for k in range(size)
-        ],
-        scratch_shapes=[
-            pltpu.VMEM((length, width), BF),
-            pltpu.VMEM((width // PAIR, PAIR, PAIR), BF),
-        ],
-        name="mixed_and_projected",
-    )(at, local, query, *states, gate, w_out)
+        "mixed_and_projected",
+        [local, query, *states, gate, w_out],
+        [(block, F32 if k == 0 else BF) for k in range(size)],
+        [pltpu.VMEM((length, width), BF), pltpu.VMEM((width // PAIR, PAIR, PAIR), BF)],
+        table=at,
+    )
 
 
 def norm_kernel(stream_ref, gain_ref, *rest):
@@ -404,14 +408,12 @@
 
 
 def normed_rows(stream, gain, parts):
-    full = pl.BlockSpec(memory_space=pltpu.VMEM)
-    return pl.pallas_call(
+    return call(
         norm_kernel,
-        in_specs=[full] * (2 + len(parts)),
-        out_specs=[full] * 2,
-        out_shape=[jax.ShapeDtypeStruct(stream.shape, BF)] * 2,
-        name="normed_rows",
-    )(stream, gain.reshape(1, -1), *parts)
+        "normed_rows",
+        [stream, gain.reshape(1, -1), *parts],
+        [(stream.shape, BF), (stream.shape, BF)],
+    )
 
 
 def channels_kernel(w_ref, *rest):
@@ -422,6 +424,7 @@
     block = parts[0].shape[0]
     tile, strip = 128, 256
     tiles, strips = hidden // tile, width // strip
+    even = hidden // strip * strip
     copies, downs = [], []
     for j in range(tiles):
         here = pl.ds(j * tile, tile)
@@ -446,7 +449,8 @@
     for n in range(strips):
         downs[n].wait()
         here = slice(n * strip, (n + 1) * strip)
-        got = dot_nt(hidden_ref[...], down_ref[here, :])
+        got = dot_nt(hidden_ref[:, :even], down_ref[here, :even])
+        got = got + dot_nt(hidden_ref[:, even:], down_ref[here, even:])
         for k, out_ref in enumerate(out_refs):
             out_ref[:, here] = got[k * block : (k + 1) * block, :].astype(BF)
 
@@ -454,24 +458,24 @@
 def channel_sums(weights, parts, hidden):
     block, width = parts[0].shape
     size = len(parts)
-    length = block * size
-    full = pl.BlockSpec(memory_space=pltpu.VMEM)
-    return pl.pallas_call(
+    weight = pltpu.VMEM((width, hidden), BF)
+    return call(
         channels_kernel,
-        in_specs=[pl.BlockSpec(memory_space=pl.ANY)] + [full] * size,
-        out_specs=[full] * size,
-        out_shape=[jax.ShapeDtypeStruct((block, width), BF)] * size,
-        scratch_shapes=[
-            pltpu.VMEM((width, hidden), BF),
-            pltpu.VMEM((width, hidden), BF),
-            pltpu.VMEM((width, hidden), BF),
-            pltpu.VMEM((length, width), BF),
-            pltpu.VMEM((length, hidden), BF),
+        "channel_sums",
+        parts,
+        [((block, width), BF)] * size,
+        [
+            weight,
+            weight,
+            weight,
+            pltpu.VMEM((block * size, width), BF),
+            pltpu.VMEM((block * size, hidden), BF),
             pltpu.SemaphoreType.DMA((2, hidden // 128)),
             pltpu.SemaphoreType.DMA((width // 256,)),
         ],
-        name="channel_sums",
-    )(weights, *parts)
+        far=[weights],
+        mib=32,
+    )
 
 
 def last_kernel(middle_ref, *rest):
@@ -483,14 +487,15 @@
 
 
 def last_sum(middle, parts):
-    full = pl.BlockSpec(memory_space=pltpu.VMEM)
+    near = [pltpu.with_memory_space_constraint(x, pltpu.VMEM) for x in [middle, *parts]]
     return pl.pallas_call(
         last_kernel,
-        in_specs=[full] * (1 + len(parts)),
-        out_specs=full,
+        in_specs=[FULL] * len(near),
+        out_specs=FULL,
         out_shape=jax.ShapeDtypeStruct(middle.shape, BF),
+        compiler_params=pltpu.CompilerParams(vmem_limit_bytes=16 << 20),
         name="last_sum",
-    )(middle, *parts)
+    )(*near)
 
 
 def per_device(
@@ -514,10 +519,12 @@
     size = lax.axis_size("tp")
     at = jnp.stack([lax.axis_index(a).astype(jnp.int32) for a in ("tp", *reversed(SP))])
     before, total, solved, decay, key_unit, grown = keys_side(keys, values, beta_pre, decay_pre)
-    local, query, gate = queries_side(
-        queries, key_unit, decay, solved, before, grown, gates, out_gain
-    )
-    states = state_ahead(at, total)
+    local, query, gate, states = state_ahead(
+        at,
+        total,
+        lambda chip: queries_side(chip, queries, key_unit, decay, solved, before, grown),
+        lambda: gates_side(gates, out_gain),
+    )
     parts = mixed_and_projected(at, size, local, query, states, gate, w_out)
     got = [lax.ppermute(parts[k], "tp", ring(size, k)) for k in range(1, size)]
     middle, normed = normed_rows(stream, norm_gain, [parts[0]] + got)

time: 170 us -> 153 us (0.900)
  Pallas kernels: 57.7 us -> 42.5 us
  waiting for transfers between devices: 61.9 us -> 57.4 us
  local copies, waits for them, and re-layouts: 5.61 us -> 9.73 us
    pallas_call x9 -> x10, Pallas kernels: 57.7 us -> 42.5 us  [the longest x9 41.5 us: call(): pl.pallas_call(kernel, in_specs=[TABLE] * len(tables) + [FAR] * len(far)...]
    ppermute x3, waiting for transfers between devices: 4.94 us -> 0.01 us  [state_ahead(): lax.ppermute(chip, line, ring(size, k))]
    unnamed x34 -> x26, local copies, waits for them, and re-layouts: 5.61 us -> 9.73 us
  transfers between devices with their start and end apart: 18 -> 18, of which waited for: 12 -> 11; matrix products, arithmetic and copies ran while one was open for 0% -> 0% of each run, Pallas kernels for 20% -> 15%
where the time goes in v3:
time: 153 us; the launch traced here: 152 us
  waiting for transfers between devices  57.4 us (38%)
  Pallas kernels  42.5 us (28%)
  starting transfers between devices  27 us (18%)
  between operations  13.5 us (9%)
  local copies, waits for them, and re-layouts  9.73 us (6%)
  other arithmetic  2.05 us (1%)
    pallas_call x9, Pallas kernels, call(): pl.pallas_call(kernel, in_specs=[TABLE] * len(tables) + [FAR] * len(far)...  41.5 us
    ppermute x3, waiting for transfers between devices, per_device(): back = [lax.ppermute(sums[k], 'tp', ring(size, -k)) for k in range(1, size)]  19.7 us
    ppermute x3, waiting for transfers between devices, per_device(): got = [lax.ppermute(parts[k], 'tp', ring(size, k)) for k in range(1, size)]  16.1 us
    ppermute x3, waiting for transfers between devices, per_device(): lax.ppermute(normed, 'tp', ring(size, k))  16 us
    unnamed x26, local copies, waits for them, and re-layouts  9.73 us
    ppermute x3, starting transfers between devices, state_ahead(): planes = [lax.ppermute(whole, plane, ring(size, k)) for k in range(1, size)]  6.58 us
    ppermute x3, starting transfers between devices, state_ahead(): lax.ppermute(chip, line, ring(size, k))  6 us
    ppermute x3, starting transfers between devices, per_device(): got = [lax.ppermute(parts[k], 'tp', ring(size, k)) for k in range(1, size)]  5.73 us
  transfers between devices with their start and end apart: 18, of which 11 were waited for; matrix products, arithmetic and copies ran while one was open for 0% of the time, Pallas kernels for 15%

profile of v3, /device:TPU:0, one launch (start us, length us, event | category | flops | bytes accessed | tf_op | source)
XLA Modules:
  0.0 152.3 jit_solution(17255001845586121498)
XLA Ops:
  6.5 2.0 %pad_maximum_fusion = bf16[64,4224]{1,0:T(8,128)(2,1)} fusion(bf16[64,1408]{1,0:T(8,128)(2,1)} %bitcast.9, bf16[64,1408]{1,0:T(8,128)(2,1)} %param.24, bf16[64,1408]{1,0:T(8,128)(2,1)} %param.23), kind=kLoop, calls=%fused_computation | loop fusion | flops 1622016 | bytes 1081344 | tf_op jit(solution)/shard_map/concatenate | solution.py:517
  8.5 0.0 all-gather.2.cloned.1.call-update
  8.6 0.0 copy-start.6
  8.6 1.0 copy-done.6
  9.6 1.0 copy-done.7
  10.6 8.9 %keys_side.1 = (bf16[12,128,128]{2,1,0:T(8,128)(2,1)S(1)}, bf16[4,128,128]{2,1,0:T(8,128)(2,1)S(1)}, bf16[12,128,256]{2,1,0:T(8,128)(2,1)S(1)}, bf16[12,128,256]...) custom-call(bf16[384,512]{1,0:T(8,128)(2,1)S(1)} %copy-done.6, ...), custom_call_target="tpu_custom_call" | custom-call | tf_op jit(solution)/shard_map/keys_side/pallas_call | solution.py:28
  19.5 0.7 copy-done.4
  20.3 0.0 collective-permute-start
  20.3 0.1 pad_add_fusion.at_ref
  20.4 1.3 collective-permute-done.other_ref.first_ref
  21.6 0.8 chip_total.1.after_ref.rest_0_
  22.4 1.8 %collective-permute-start.1 = (bf16[2,128,128]{2,1,0:T(8,128)(2,1)S(1)}, bf16[2,128,128]{2,1,0:T(8,128)(2,1)S(1)}, u32[]{:S(2)}, u32[]{:S(2)}) collective-permute-start(bf16[2,128,128]{2,1,0:T(8,128)(2,1)S(1)} %chip_total.1.after_ref.rest_0_), channel_id=1, source_target_pairs={{0,8},{8,16},{16,24},{24,0},{1,9},{9,17},{17,25},{25,1},{2,10},{10... | collective-permute-start | bytes 196616 | tf_op jit(solution)/shard_map/ppermute | solution.py:335
  24.1 2.9 %collective-permute-start.2 = (bf16[2,128,128]{2,1,0:T(8,128)(2,1)S(1)}, bf16[2,128,128]{2,1,0:T(8,128)(2,1)S(1)}, u32[]{:S(2)}, u32[]{:S(2)}) collective-permute-start(bf16[2,128,128]{2,1,0:T(8,128)(2,1)S(1)} %chip_total.1.after_ref.rest_0_), channel_id=1, source_target_pairs={{0,16},{8,24},{16,0},{24,8},{1,17},{9,25},{17,1},{25,9},{2,18},{10... | collective-permute-start | bytes 196616 | tf_op jit(solution)/shard_map/ppermute | solution.py:335
  27.0 1.3 collective-permute-start.3
  28.4 1.0 copy-done.5
  29.4 5.8 %queries_side.1 = (f32[384,512]{1,0:T(8,128)S(1)}, bf16[384,512]{1,0:T(8,128)(2,1)S(1)}) custom-call(bf16[2,128,128]{2,1,0:T(8,128)(2,1)S(1)} %chip_total.1.after_ref.rest_0_, bf16[384,512]{1,0:T(8,128)(2,1)S(1)} %copy-done.2, bf16[384,512]{1,0:T(8,128)(2,1)S(1)} %copy-done.5, bf16[12,128,256]{2,1,0:T(8,128)(2,1)S(1)} %get-tuple-element.27.d_ref, ...), custom_call_target="tpu_custom_call" | custom-call | tf_op jit(solution)/shard_map/queries_side/pallas_call | solution.py:28
  35.2 0.0 collective-permute-done.1.rest_1_
  35.3 0.0 collective-permute-done.2.rest_2_
  35.3 1.2 line_total.1
  36.5 2.0 %collective-permute-start.4 = (bf16[2,128,128]{2,1,0:T(8,128)(2,1)S(1)}, bf16[2,128,128]{2,1,0:T(8,128)(2,1)S(1)}, u32[]{:S(2)}, u32[]{:S(2)}) collective-permute-start(bf16[2,128,128]{2,1,0:T(8,128)(2,1)S(1)} %get-tuple-element.34), channel_id=1, source_target_pairs={{0,32},{32,64},{64,96},{96,0},{1,33},{33,65},{65,97},{97,1},{2,34}... | collective-permute-start | bytes 196616 | tf_op jit(solution)/shard_map/ppermute | solution.py:347
  38.4 3.6 %collective-permute-start.5 = (bf16[2,128,128]{2,1,0:T(8,128)(2,1)S(1)}, bf16[2,128,128]{2,1,0:T(8,128)(2,1)S(1)}, u32[]{:S(2)}, u32[]{:S(2)}) collective-permute-start(bf16[2,128,128]{2,1,0:T(8,128)(2,1)S(1)} %get-tuple-element.34), channel_id=1, source_target_pairs={{0,64},{32,96},{64,0},{96,32},{1,65},{33,97},{65,1},{97,33},{2,66}... | collective-permute-start | bytes 196616 | tf_op jit(solution)/shard_map/ppermute | solution.py:347
  42.0 1.0 collective-permute-start.6
  43.1 0.3 gates_side.1.after_ref.gate_ref
  43.3 0.2 collective-permute-done.4.rest_0_
  43.5 1.5 collective-permute-done.5.rest_1_
  45.0 1.3 collective-permute-done.6.rest_2_
  46.3 1.4 plane_state.1.mine_ref
  47.7 0.1 collective-permute-start.7
  47.8 1.3 collective-permute-done.7.theirs_ref
  49.2 3.3 %mixed_and_projected.1 = (f32[96,2048]{1,0:T(8,128)S(1)}, bf16[96,2048]{1,0:T(8,128)(2,1)S(1)}, bf16[96,2048]{1,0:T(8,128)(2,1)S(1)}, bf16[96,2048]{1,0:T(8,128)(2,1)S(1)}) custom-call(s32[4]{0:T(128)S(1)} %pad_add_fusion.at_ref, f32[384,512]{1,0:T(8,128)S(1)} %get-tuple-element.31.o_ref, bf16[384,512]{1,0:T(8,128)(2,1)S(1)} %get-tuple-element.32.after_ref.q1_ref, ...), custom_call_target="tpu_custom_call" | custom-call | tf_op jit(solution)/shard_map/mixed_and_projected/pallas_call | solution.py:28
  52.5 1.6 %collective-permute-start.8 = (bf16[96,2048]{1,0:T(8,128)(2,1)S(1)}, bf16[96,2048]{1,0:T(8,128)(2,1)S(1)}, u32[]{:S(2)}, u32[]{:S(2)}) collective-permute-start(bf16[96,2048]{1,0:T(8,128)(2,1)S(1)} %get-tuple-element.36), channel_id=1, source_target_pairs={{0,1},{1,2},{2,3},{3,0},{4,5},{5,6},{6,7},{7,4},{8,9},{9,10},{10,1... | collective-permute-start | bytes 1179656 | tf_op jit(solution)/shard_map/ppermute | solution.py:529
  54.0 2.7 %collective-permute-start.9 = (bf16[96,2048]{1,0:T(8,128)(2,1)S(1)}, bf16[96,2048]{1,0:T(8,128)(2,1)S(1)}, u32[]{:S(2)}, u32[]{:S(2)}) collective-permute-start(bf16[96,2048]{1,0:T(8,128)(2,1)S(1)} %get-tuple-element.37), channel_id=1, source_target_pairs={{0,2},{1,3},{2,0},{3,1},{4,6},{5,7},{6,4},{7,5},{8,10},{9,11},{10,... | collective-permute-start | bytes 1179656 | tf_op jit(solution)/shard_map/ppermute | solution.py:529
  56.8 1.4 collective-permute-start.10
  58.2 6.7 %collective-permute-done.8.rest_1_ = bf16[96,2048]{1,0:T(8,128)(2,1)S(1)} collective-permute-done((bf16[96,2048]{1,0:T(8,128)(2,1)S(1)}, bf16[96,2048]{1,0:T(8,128)(2,1)S(1)}, u32[]{:S(2)}, u32[]{:S(2)}) %collective-permute-start.8) | collective-permute-done | bytes 393248 | tf_op jit(solution)/shard_map/ppermute | solution.py:529
  64.9 9.4 %collective-permute-done.9.rest_2_ = bf16[96,2048]{1,0:T(8,128)(2,1)S(1)} collective-permute-done((bf16[96,2048]{1,0:T(8,128)(2,1)S(1)}, bf16[96,2048]{1,0:T(8,128)(2,1)S(1)}, u32[]{:S(2)}, u32[]{:S(2)}) %collective-permute-start.9) | collective-permute-done | bytes 393248 | tf_op jit(solution)/shard_map/ppermute | solution.py:529
  74.3 0.4 normed_rows.1
  74.8 1.5 collective-permute-start.11
  76.3 2.4 %collective-permute-start.12 = (bf16[96,2048]{1,0:T(8,128)(2,1)S(1)}, bf16[96,2048]{1,0:T(8,128)(2,1)S(1)}, u32[]{:S(2)}, u32[]{:S(2)}) collective-permute-start(bf16[96,2048]{1,0:T(8,128)(2,1)S(1)} %get-tuple-element.40.rest_0_), channel_id=1, source_target_pairs={{0,2},{1,3},{2,0},{3,1},{4,6},{5,7},{6,4},{7,5},{8,10},{9,11},{10,... | collective-permute-start | bytes 1179656 | tf_op jit(solution)/shard_map/ppermute | solution.py:531
  78.6 1.5 collective-permute-start.13
  80.1 6.4 %collective-permute-done.11.rest_1_ = bf16[96,2048]{1,0:T(8,128)(2,1)S(1)} collective-permute-done((bf16[96,2048]{1,0:T(8,128)(2,1)S(1)}, bf16[96,2048]{1,0:T(8,128)(2,1)S(1)}, u32[]{:S(2)}, u32[]{:S(2)}) %collective-permute-start.11) | collective-permute-done | bytes 393248 | tf_op jit(solution)/shard_map/ppermute | solution.py:531
  86.6 9.6 %collective-permute-done.12.rest_2_ = bf16[96,2048]{1,0:T(8,128)(2,1)S(1)} collective-permute-done((bf16[96,2048]{1,0:T(8,128)(2,1)S(1)}, bf16[96,2048]{1,0:T(8,128)(2,1)S(1)}, u32[]{:S(2)}, u32[]{:S(2)}) %collective-permute-start.12) | collective-permute-done | bytes 393248 | tf_op jit(solution)/shard_map/ppermute | solution.py:531
  96.2 5.9 %copy-done = bf16[2048,4224]{1,0:T(8,128)(2,1)S(1)} copy-done((bf16[2048,4224]{1,0:T(8,128)(2,1)S(1)}, bf16[2048,4224]{1,0:T(8,128)(2,1)}, u32[]{:S(2)}) %copy-start) | copy-done | bytes 17301528
  102.1 19.4 %channel_sums.1 = (bf16[96,2048]{1,0:T(8,128)(2,1)S(1)}, bf16[96,2048]{1,0:T(8,128)(2,1)S(1)}, bf16[96,2048]{1,0:T(8,128)(2,1)S(1)}, bf16[96,2048]{1,0:T(8,128)(2,1)S(1)}) custom-call(bf16[2048,4224]{1,0:T(8,128)(2,1)S(1)} %copy-done, bf16[96,2048]{1,0:T(8,128)(2,1)S(1)} %get-tuple-element.40.rest_0_, bf16[96,2048]{1,0:T(8,128)(2,1)S(1)} %collective-permute-done.11.rest_1_, ...), custom_call_target="tpu_custom_call" | custom-call | tf_op jit(solution)/shard_map/channel_sums/pallas_call | solution.py:28
  121.5 2.2 %collective-permute-start.14 = (bf16[96,2048]{1,0:T(8,128)(2,1)S(1)}, bf16[96,2048]{1,0:T(8,128)(2,1)S(1)}, u32[]{:S(2)}, u32[]{:S(2)}) collective-permute-start(bf16[96,2048]{1,0:T(8,128)(2,1)S(1)} %get-tuple-element.42), channel_id=1, source_target_pairs={{0,3},{1,0},{2,1},{3,2},{4,7},{5,4},{6,5},{7,6},{8,11},{9,8},{10,9... | collective-permute-start | bytes 1179656 | tf_op jit(solution)/shard_map/ppermute | solution.py:533
  123.8 1.0 collective-permute-start.15
  124.8 16.0 %collective-permute-done.14.rest_1_ = bf16[96,2048]{1,0:T(8,128)(2,1)S(1)} collective-permute-done((bf16[96,2048]{1,0:T(8,128)(2,1)S(1)}, bf16[96,2048]{1,0:T(8,128)(2,1)S(1)}, u32[]{:S(2)}, u32[]{:S(2)}) %collective-permute-start.14) | collective-permute-done | bytes 393248 | tf_op jit(solution)/shard_map/ppermute | solution.py:533
  140.7 3.7 %collective-permute-done.16.rest_3_ = bf16[96,2048]{1,0:T(8,128)(2,1)S(1)} collective-permute-done((bf16[96,2048]{1,0:T(8,128)(2,1)S(1)}, bf16[96,2048]{1,0:T(8,128)(2,1)S(1)}, u32[]{:S(2)}, u32[]{:S(2)}) %collective-permute-start.16) | collective-permute-done | bytes 393248 | tf_op jit(solution)/shard_map/ppermute | solution.py:533
  144.4 1.0 last_sum.1
  (27 shorter events, 0.1 us)
Async XLA Ops:
  6.5 2.0 %copy-start.9 = (f32[8,384]{1,0:T(8,128)S(1)}, f32[8,384]{1,0:T(8,128)}, u32[]{:S(2)}) copy-start(f32[8,384]{1,0:T(8,128)} %beta_ref.1) | copy-start | bytes 36868
  6.5 2.0 %copy-start.10 = (f32[8,384]{1,0:T(8,128)S(1)}, f32[8,384]{1,0:T(8,128)}, u32[]{:S(2)}) copy-start(f32[8,384]{1,0:T(8,128)} %decay_ref.1) | copy-start | bytes 36868
  6.5 89.7 %all-gather.2.cloned.1.call-start = ((), (), s32[]{:S(2)}) async-start(), calls=%async_computation | async-start | bytes 17842176 | tf_op jit(solution)/shard_map/all_gather | solution.py:518
  8.5 19.9 %copy-start.2 = (bf16[384,512]{1,0:T(8,128)(2,1)S(1)}, bf16[384,512]{1,0:T(8,128)(2,1)}, u32[]{:S(2)}) copy-start(bf16[384,512]{1,0:T(8,128)(2,1)} %q_ref.1) | copy-start | bytes 1179652
  8.6 1.0 copy-start.6
  9.6 1.0 copy-start.7
  19.5 0.7 copy-start.4
  20.3 1.3 collective-permute-start
  22.4 12.9 %collective-permute-start.1 = (bf16[2,128,128]{2,1,0:T(8,128)(2,1)S(1)}, bf16[2,128,128]{2,1,0:T(8,128)(2,1)S(1)}, u32[]{:S(2)}, u32[]{:S(2)}) collective-permute-start(bf16[2,128,128]{2,1,0:T(8,128)(2,1)S(1)} %chip_total.1.after_ref.rest_0_), channel_id=1, source_target_pairs={{0,8},{8,16},{16,24},{24,0},{1,9},{9,17},{17,25},{25,1},{2,10},{10... | collective-permute-start | bytes 196616 | tf_op jit(solution)/shard_map/ppermute | solution.py:335
  24.1 11.1 %collective-permute-start.2 = (bf16[2,128,128]{2,1,0:T(8,128)(2,1)S(1)}, bf16[2,128,128]{2,1,0:T(8,128)(2,1)S(1)}, u32[]{:S(2)}, u32[]{:S(2)}) collective-permute-start(bf16[2,128,128]{2,1,0:T(8,128)(2,1)S(1)} %chip_total.1.after_ref.rest_0_), channel_id=1, source_target_pairs={{0,16},{8,24},{16,0},{24,8},{1,17},{9,25},{17,1},{25,9},{2,18},{10... | collective-permute-start | bytes 196616 | tf_op jit(solution)/shard_map/ppermute | solution.py:335
  27.0 8.2 %collective-permute-start.3 = (bf16[2,128,128]{2,1,0:T(8,128)(2,1)S(1)}, bf16[2,128,128]{2,1,0:T(8,128)(2,1)S(1)}, u32[]{:S(2)}, u32[]{:S(2)}) collective-permute-start(bf16[2,128,128]{2,1,0:T(8,128)(2,1)S(1)} %chip_total.1.after_ref.rest_0_), channel_id=1, source_target_pairs={{0,24},{8,0},{16,8},{24,16},{1,25},{9,1},{17,9},{25,17},{2,26},{10... | collective-permute-start | bytes 196616 | tf_op jit(solution)/shard_map/ppermute | solution.py:335
  28.4 1.0 copy-start.5
  29.4 13.7 %copy-start.8 = (bf16[384,512]{1,0:T(8,128)(2,1)S(1)}, bf16[384,512]{1,0:T(8,128)(2,1)}, u32[]{:S(2)}) copy-start(bf16[384,512]{1,0:T(8,128)(2,1)} %gates_ref.1) | copy-start | bytes 1179652
  29.4 13.7 %copy-start.12 = (f32[64]{0:T(128)S(1)}, f32[64]{0:T(128)}, u32[]{:S(2)}) copy-start(f32[64]{0:T(128)} %param.19) | copy-start | bytes 772
  36.5 7.0 %collective-permute-start.4 = (bf16[2,128,128]{2,1,0:T(8,128)(2,1)S(1)}, bf16[2,128,128]{2,1,0:T(8,128)(2,1)S(1)}, u32[]{:S(2)}, u32[]{:S(2)}) collective-permute-start(bf16[2,128,128]{2,1,0:T(8,128)(2,1)S(1)} %get-tuple-element.34), channel_id=1, source_target_pairs={{0,32},{32,64},{64,96},{96,0},{1,33},{33,65},{65,97},{97,1},{2,34}... | collective-permute-start | bytes 196616 | tf_op jit(solution)/shard_map/ppermute | solution.py:347
  38.4 6.5 %collective-permute-start.5 = (bf16[2,128,128]{2,1,0:T(8,128)(2,1)S(1)}, bf16[2,128,128]{2,1,0:T(8,128)(2,1)S(1)}, u32[]{:S(2)}, u32[]{:S(2)}) collective-permute-start(bf16[2,128,128]{2,1,0:T(8,128)(2,1)S(1)} %get-tuple-element.34), channel_id=1, source_target_pairs={{0,64},{32,96},{64,0},{96,32},{1,65},{33,97},{65,1},{97,33},{2,66}... | collective-permute-start | bytes 196616 | tf_op jit(solution)/shard_map/ppermute | solution.py:347
  42.0 4.3 %collective-permute-start.6 = (bf16[2,128,128]{2,1,0:T(8,128)(2,1)S(1)}, bf16[2,128,128]{2,1,0:T(8,128)(2,1)S(1)}, u32[]{:S(2)}, u32[]{:S(2)}) collective-permute-start(bf16[2,128,128]{2,1,0:T(8,128)(2,1)S(1)} %get-tuple-element.34), channel_id=1, source_target_pairs={{0,96},{32,0},{64,32},{96,64},{1,97},{33,1},{65,33},{97,65},{2,98}... | collective-permute-start | bytes 196616 | tf_op jit(solution)/shard_map/ppermute | solution.py:347
  43.1 6.1 %copy-start.1 = (bf16[512,2048]{1,0:T(8,128)(2,1)S(1)}, bf16[512,2048]{1,0:T(8,128)(2,1)}, u32[]{:S(2)}) copy-start(bf16[512,2048]{1,0:T(8,128)(2,1)} %w_ref.1) | copy-start | bytes 6291460
  47.7 1.4 collective-permute-start.7
  49.2 25.2 %copy-start.3 = (bf16[96,2048]{1,0:T(8,128)(2,1)S(1)}, bf16[96,2048]{1,0:T(8,128)(2,1)}, u32[]{:S(2)}) copy-start(bf16[96,2048]{1,0:T(8,128)(2,1)} %stream_ref.1) | copy-start | bytes 1179652
  49.2 25.2 %copy-start.11 = (f32[2048]{0:T(1024)S(1)}, f32[2048]{0:T(1024)}, u32[]{:S(2)}) copy-start(f32[2048]{0:T(1024)} %param.22) | copy-start | bytes 24580
  52.5 12.4 %collective-permute-start.8 = (bf16[96,2048]{1,0:T(8,128)(2,1)S(1)}, bf16[96,2048]{1,0:T(8,128)(2,1)S(1)}, u32[]{:S(2)}, u32[]{:S(2)}) collective-permute-start(bf16[96,2048]{1,0:T(8,128)(2,1)S(1)} %get-tuple-element.36), channel_id=1, source_target_pairs={{0,1},{1,2},{2,3},{3,0},{4,5},{5,6},{6,7},{7,4},{8,9},{9,10},{10,1... | collective-permute-start | bytes 1179656 | tf_op jit(solution)/shard_map/ppermute | solution.py:529
  54.0 20.3 %collective-permute-start.9 = (bf16[96,2048]{1,0:T(8,128)(2,1)S(1)}, bf16[96,2048]{1,0:T(8,128)(2,1)S(1)}, u32[]{:S(2)}, u32[]{:S(2)}) collective-permute-start(bf16[96,2048]{1,0:T(8,128)(2,1)S(1)} %get-tuple-element.37), channel_id=1, source_target_pairs={{0,2},{1,3},{2,0},{3,1},{4,6},{5,7},{6,4},{7,5},{8,10},{9,11},{10,... | collective-permute-start | bytes 1179656 | tf_op jit(solution)/shard_map/ppermute | solution.py:529
  56.8 17.6 %collective-permute-start.10 = (bf16[96,2048]{1,0:T(8,128)(2,1)S(1)}, bf16[96,2048]{1,0:T(8,128)(2,1)S(1)}, u32[]{:S(2)}, u32[]{:S(2)}) collective-permute-start(bf16[96,2048]{1,0:T(8,128)(2,1)S(1)} %get-tuple-element.38), channel_id=1, source_target_pairs={{0,3},{1,0},{2,1},{3,2},{4,7},{5,4},{6,5},{7,6},{8,11},{9,8},{10,9... | collective-permute-start | bytes 1179656 | tf_op jit(solution)/shard_map/ppermute | solution.py:529
  74.8 11.8 %collective-permute-start.11 = (bf16[96,2048]{1,0:T(8,128)(2,1)S(1)}, bf16[96,2048]{1,0:T(8,128)(2,1)S(1)}, u32[]{:S(2)}, u32[]{:S(2)}) collective-permute-start(bf16[96,2048]{1,0:T(8,128)(2,1)S(1)} %get-tuple-element.40.rest_0_), channel_id=1, source_target_pairs={{0,1},{1,2},{2,3},{3,0},{4,5},{5,6},{6,7},{7,4},{8,9},{9,10},{10,1... | collective-permute-start | bytes 1179656 | tf_op jit(solution)/shard_map/ppermute | solution.py:531
  76.3 19.9 %collective-permute-start.12 = (bf16[96,2048]{1,0:T(8,128)(2,1)S(1)}, bf16[96,2048]{1,0:T(8,128)(2,1)S(1)}, u32[]{:S(2)}, u32[]{:S(2)}) collective-permute-start(bf16[96,2048]{1,0:T(8,128)(2,1)S(1)} %get-tuple-element.40.rest_0_), channel_id=1, source_target_pairs={{0,2},{1,3},{2,0},{3,1},{4,6},{5,7},{6,4},{7,5},{8,10},{9,11},{10,... | collective-permute-start | bytes 1179656 | tf_op jit(solution)/shard_map/ppermute | solution.py:531
  78.6 17.5 %collective-permute-start.13 = (bf16[96,2048]{1,0:T(8,128)(2,1)S(1)}, bf16[96,2048]{1,0:T(8,128)(2,1)S(1)}, u32[]{:S(2)}, u32[]{:S(2)}) collective-permute-start(bf16[96,2048]{1,0:T(8,128)(2,1)S(1)} %get-tuple-element.40.rest_0_), channel_id=1, source_target_pairs={{0,3},{1,0},{2,1},{3,2},{4,7},{5,4},{6,5},{7,6},{8,11},{9,8},{10,9... | collective-permute-start | bytes 1179656 | tf_op jit(solution)/shard_map/ppermute | solution.py:531
  96.2 5.9 %copy-start = (bf16[2048,4224]{1,0:T(8,128)(2,1)S(1)}, bf16[2048,4224]{1,0:T(8,128)(2,1)}, u32[]{:S(2)}) copy-start(bf16[2048,4224]{1,0:T(8,128)(2,1)} %all-gather.2.cloned.1.call-done.w_ref) | copy-start | bytes 51904516
  121.5 19.2 %collective-permute-start.14 = (bf16[96,2048]{1,0:T(8,128)(2,1)S(1)}, bf16[96,2048]{1,0:T(8,128)(2,1)S(1)}, u32[]{:S(2)}, u32[]{:S(2)}) collective-permute-start(bf16[96,2048]{1,0:T(8,128)(2,1)S(1)} %get-tuple-element.42), channel_id=1, source_target_pairs={{0,3},{1,0},{2,1},{3,2},{4,7},{5,4},{6,5},{7,6},{8,11},{9,8},{10,9... | collective-permute-start | bytes 1179656 | tf_op jit(solution)/shard_map/ppermute | solution.py:533
  123.8 17.0 %collective-permute-start.15 = (bf16[96,2048]{1,0:T(8,128)(2,1)S(1)}, bf16[96,2048]{1,0:T(8,128)(2,1)S(1)}, u32[]{:S(2)}, u32[]{:S(2)}) collective-permute-start(bf16[96,2048]{1,0:T(8,128)(2,1)S(1)} %get-tuple-element.43), channel_id=1, source_target_pairs={{0,2},{1,3},{2,0},{3,1},{4,6},{5,7},{6,4},{7,5},{8,10},{9,11},{10,... | collective-permute-start | bytes 1179656 | tf_op jit(solution)/shard_map/ppermute | solution.py:533
  124.8 19.7 %collective-permute-start.16 = (bf16[96,2048]{1,0:T(8,128)(2,1)S(1)}, bf16[96,2048]{1,0:T(8,128)(2,1)S(1)}, u32[]{:S(2)}, u32[]{:S(2)}) collective-permute-start(bf16[96,2048]{1,0:T(8,128)(2,1)S(1)} %get-tuple-element.44), channel_id=1, source_target_pairs={{0,1},{1,2},{2,3},{3,0},{4,5},{5,6},{6,7},{7,4},{8,9},{9,10},{10,1... | collective-permute-start | bytes 1179656 | tf_op jit(solution)/shard_map/ppermute | solution.py:533
Sparse Core Ops, SparseCore 0:
  9.6 78.0 all-gather.1

commit v4 on v3

--- a/solution.py
+++ b/solution.py
@@ -1,3 +1,5 @@
+import functools
+
 import jax
 import jax.numpy as jnp
 from jax import lax
@@ -22,8 +24,8 @@
 TABLE = pl.BlockSpec(memory_space=pltpu.SMEM)
 
 
-def call(kernel, name, arrays, shapes, scratch=(), table=None, far=(), mib=16):
-    near = [pltpu.with_memory_space_constraint(x, pltpu.VMEM) for x in arrays]
+def call(kernel, name, arrays, shapes, scratch=(), table=None, far=(), mib=16, pinned=True):
+    near = [pltpu.with_memory_space_constraint(x, pltpu.VMEM) if pinned else x for x in arrays]
     tables = [] if table is None else [table]
     return pl.pallas_call(
         kernel,
@@ -94,7 +96,7 @@
 
 def keys_kernel(
     k_ref, v_ref, beta_ref, decay_ref,
-    before_ref, total_ref, y_ref, d_ref, kb_ref, ec_ref,
+    before_ref, total_ref, y_ref, d_ref, ec_ref,
     l_ref, x_ref, r_ref, f_ref,
 ):
     row, col = places()
@@ -133,7 +135,7 @@
             item = c * pairs + p
             key = silu(k_ref[rows, lanes].astype(F32))
             key = (key * lax.rsqrt(half_sums(key * key, ones) + EPSILON)).astype(BF)
-            kb_ref[rows, lanes] = key
+            y_ref[item, :, 2 * PAIR :] = key
             key_f = key.astype(F32)
             first = c * heads + 2 * p
             cums = [cum_col[:, h : h + 1] for h in (first, first + 1)]
@@ -181,7 +183,7 @@
         for p in range(pairs):
             item = c * pairs + p
             y = dot(x_ref[item], side_by_side(halves(r_ref[item]))).astype(BF)
-            y_ref[item] = y
+            y_ref[item, :, : 2 * PAIR] = y
             z = jnp.where(top, *halves(dot(f_ref[item], y)))
             z = jnp.where(same, z, ends[item] - z)
             if c == 0:
@@ -208,12 +210,12 @@
         [
             ((items, PAIR, PAIR), BF),
             ((pairs, PAIR, PAIR), BF),
-            ((items, CHUNK, 2 * PAIR), BF),
+            ((items, CHUNK, 3 * PAIR), BF),
             ((items, CHUNK, 2 * CHUNK), BF),
-            ((length, width), BF),
             ((length, width), F32),
         ],
         [wide, wide, wide, pltpu.VMEM((items, PAIR, CHUNK), BF)],
+        pinned=False,
     )
 
 
@@ -224,35 +226,36 @@
         gate_ref[:, lanes] = silu(gates_ref[:, lanes].astype(F32)) * gain
 
 
-def queries_kernel(after_ref, q_ref, kb_ref, d_ref, y_ref, before_ref, ec_ref, o_ref, q1_ref):
+def queries_kernel(first, after_ref, q_ref, d_ref, y_ref, before_ref, ec_ref, o_ref, q1_ref):
     row, col = places()
     left = col < HEAD_DIM
     same = left == (row < HEAD_DIM)
     ones = jnp.where(same, 1.0, 0.0).astype(BF)
-    length, width = q_ref.shape
-    pairs = width // PAIR
+    length, width = o_ref.shape
+    pairs = q_ref.shape[1] // PAIR
 
     def chunk(c, carry):
         rows = pl.ds(pl.multiple_of(c * CHUNK, CHUNK), CHUNK)
-        for p in range(pairs):
+        for p in range(first, first + width // PAIR):
             lanes = slice(p * PAIR, (p + 1) * PAIR)
+            place = slice((p - first) * PAIR, (p - first + 1) * PAIR)
             item = c * pairs + p
             query = silu(q_ref[rows, lanes].astype(F32))
             query = query * lax.rsqrt(half_sums(query * query, ones) + EPSILON)
             query = (query * HEAD_DIM ** (-0.5)).astype(BF)
-            key_f = kb_ref[rows, lanes].astype(F32)
+            key_f = y_ref[item, :, 2 * PAIR :].astype(F32)
             owns = [jnp.where(left, key_f, 0.0), jnp.where(left, 0.0, key_f)]
             inside = dot_nt(query, jnp.concatenate(owns, axis=0).astype(BF))
             inside = (inside * d_ref[item].astype(F32)).astype(BF)
-            got = halves(dot(inside, side_by_side(halves(y_ref[item]))))
+            got = halves(dot(inside, side_by_side(halves(y_ref[item, :, : 2 * PAIR]))))
             local = jnp.where(left, got[0], got[1])
             crossed = turned(jnp.where(left, got[1], got[0]))
             query = (query.astype(F32) * ec_ref[rows, lanes] - crossed).astype(BF)
             before = before_ref[item].astype(F32)
             both = [jnp.where(same, before, 0.0), jnp.where(same, turned(before), 0.0)]
             moved = halves(dot(query, jnp.concatenate(both, axis=1).astype(BF)))
-            o_ref[rows, lanes] = local + moved[0]
-            q1_ref[rows, lanes] = moved[1].astype(BF)
+            o_ref[rows, place] = local + moved[0]
+            q1_ref[rows, place] = moved[1].astype(BF)
         return carry
 
     lax.fori_loop(0, length // CHUNK, chunk, 0)
@@ -264,12 +267,14 @@
     )[0]
 
 
-def queries_side(after, queries, key_unit, decay, solved, before, grown):
+def queries_side(first, after, queries, decay, solved, before, grown):
+    length, width = queries.shape
+    shape = (length, width // 2)
     return call(
-        queries_kernel,
+        functools.partial(queries_kernel, first),
         "queries_side",
-        [queries, key_unit, decay, solved, before, grown],
-        [(queries.shape, F32), (queries.shape, BF)],
+        [queries, decay, solved, before, grown],
+        [(shape, F32), (shape, BF)],
         far=[after],
     )
 
@@ -333,7 +338,7 @@
     (chip,) = call(chip_kernel, "chip_total", [total, other], [(half, BF)], table=at)
     size = lax.axis_size(line)
     lines = [chip] + [lax.ppermute(chip, line, ring(size, k)) for k in range(1, size)]
-    local, query = meanwhile(chip)
+    early = meanwhile(chip)
     whole, before = call(
         row_kernel,
         "line_total",
@@ -341,25 +346,26 @@
         [(half, BF), (half, BF)],
         [pltpu.VMEM((size, *half), BF)],
         table=at,
-        far=[query],
+        far=[early[1]],
     )
     size = lax.axis_size(plane)
     planes = [lax.ppermute(whole, plane, ring(size, k)) for k in range(1, size)]
-    gate = then()
+    late = then(whole)
     (state,) = call(
-        plane_kernel, "plane_state", [before] + planes, [(half, BF)], table=at, far=[gate]
-    )
-    return local, query, gate, (other, state, lax.ppermute(state, core, swap))
+        plane_kernel, "plane_state", [before] + planes, [(half, BF)], table=at, far=[late[1]]
+    )
+    return early, late, (other, state, lax.ppermute(state, core, swap))
 
 
 def mixed_kernel(
-    at_ref, o_ref, q1_ref, first_ref, mine_ref, theirs_ref, gate_ref, w_ref, *rest
+    at_ref, o0_ref, q0_ref, o1_ref, q1_ref,
+    first_ref, mine_ref, theirs_ref, gate_ref, w_ref, *rest,
 ):
     out_refs, (mixed_ref, state_ref) = rest[:-2], rest[-2:]
     row, col = places()
     same = (col < HEAD_DIM) == (row < HEAD_DIM)
     ones = jnp.where(same, 1.0, 0.0).astype(BF)
-    length, width = o_ref.shape
+    length, width = gate_ref.shape
     core = at_ref[1]
     half = mine_ref.shape[0]
     state_ref[pl.ds(core * half, half)] = mine_ref[...]
@@ -369,7 +375,9 @@
         state = state_ref[p].astype(F32)
         later = jnp.where(same, chained(state, first_ref[p], same), 0.0)
         state = jnp.where(core == 0, state, later).astype(BF)
-        out = o_ref[:, lanes] + dot(q1_ref[:, lanes], state)
+        o_ref, q_ref = ((o0_ref, q0_ref), (o1_ref, q1_ref))[p // half]
+        place = slice((p % half) * PAIR, (p % half + 1) * PAIR)
+        out = o_ref[:, place] + dot(q_ref[:, place], state)
         mean = half_sums(out * out, ones) * (1.0 / HEAD_DIM)
         out = out * lax.rsqrt(mean + EPSILON) * gate_ref[:, lanes]
         mixed_ref[:, lanes] = out.astype(BF)
@@ -381,13 +389,13 @@
         out_ref[...] = dot(rows, w_ref[...]).astype(out_ref.dtype)
 
 
-def mixed_and_projected(at, size, local, query, states, gate, w_out):
-    length, width = local.shape
+def mixed_and_projected(at, size, early, late, states, gate, w_out):
+    length, width = gate.shape
     block = (length // size, w_out.shape[1])
     return call(
         mixed_kernel,
         "mixed_and_projected",
-        [local, query, *states, gate, w_out],
+        [*early, *late, *states, gate, w_out],
         [(block, F32 if k == 0 else BF) for k in range(size)],
         [pltpu.VMEM((length, width), BF), pltpu.VMEM((width // PAIR, PAIR, PAIR), BF)],
         table=at,
@@ -416,66 +424,89 @@
     )
 
 
-def channels_kernel(w_ref, *rest):
-    size = (len(rest) - 7) // 2
-    parts, out_refs = rest[:size], rest[size : 2 * size]
-    gate_ref, up_ref, down_ref, rows_ref, hidden_ref, in_sems, down_sems = rest[2 * size :]
+def activated(rows, gate, up):
+    got = dot(rows, jnp.concatenate([gate, up], axis=1))
+    width = gate.shape[1]
+    return (silu(got[:, :width]) * got[:, width:]).astype(BF)
+
+
+def product_nt(a, b):
+    even = a.shape[1] // 256 * 256
+    return dot_nt(a[:, :even], b[:, :even]) + dot_nt(a[:, even:], b[:, even:])
+
+
+TILE = 128
+STRIP = 256
+
+
+def first_channels_kernel(count, w_ref, *rest):
+    parts, out_refs = rest[:count], rest[count : 2 * count]
+    gate_ref, up_ref, down_ref, rows_ref, hidden_ref, in_sems, down_sems = rest[2 * count :]
     width, hidden = gate_ref.shape
     block = parts[0].shape[0]
-    tile, strip = 128, 256
-    tiles, strips = hidden // tile, width // strip
-    even = hidden // strip * strip
     copies, downs = [], []
-    for j in range(tiles):
-        here = pl.ds(j * tile, tile)
+    for j in range(hidden // TILE):
+        here = pl.ds(j * TILE, TILE)
         for k, ref in enumerate((gate_ref, up_ref)):
-            from_ref = w_ref.at[:, pl.ds(k * hidden + j * tile, tile)]
+            from_ref = w_ref.at[:, pl.ds(k * hidden + j * TILE, TILE)]
             copies.append(pltpu.make_async_copy(from_ref, ref.at[:, here], in_sems.at[k, j]))
-    for n in range(strips):
-        here = pl.ds(n * strip, strip)
+    for n in range(width // STRIP):
+        here = pl.ds(n * STRIP, STRIP)
         from_ref = w_ref.at[here, pl.ds(2 * hidden, hidden)]
         downs.append(pltpu.make_async_copy(from_ref, down_ref.at[here, :], down_sems.at[n]))
     for copy in copies + downs:
         copy.start()
     for k, part in enumerate(parts):
         rows_ref[k * block : (k + 1) * block, :] = part[...]
-    for j in range(tiles):
+    for j in range(hidden // TILE):
         copies[2 * j].wait()
         copies[2 * j + 1].wait()
-        here = slice(j * tile, (j + 1) * tile)
-        both = jnp.concatenate([gate_ref[:, here], up_ref[:, here]], axis=1)
-        got = dot(rows_ref[...], both)
-        hidden_ref[:, here] = (silu(got[:, :tile]) * got[:, tile:]).astype(BF)
-    for n in range(strips):
+        here = slice(j * TILE, (j + 1) * TILE)
+        hidden_ref[:, here] = activated(rows_ref[...], gate_ref[:, here], up_ref[:, here])
+    for n in range(width // STRIP):
         downs[n].wait()
-        here = slice(n * strip, (n + 1) * strip)
-        got = dot_nt(hidden_ref[:, :even], down_ref[here, :even])
-        got = got + dot_nt(hidden_ref[:, even:], down_ref[here, even:])
+        here = slice(n * STRIP, (n + 1) * STRIP)
+        got = product_nt(hidden_ref[...], down_ref[here, :])
         for k, out_ref in enumerate(out_refs):
             out_ref[:, here] = got[k * block : (k + 1) * block, :].astype(BF)
 
 
-def channel_sums(weights, parts, hidden):
+def first_channels(weights, parts, hidden):
     block, width = parts[0].shape
-    size = len(parts)
-    weight = pltpu.VMEM((width, hidden), BF)
+    count = len(parts)
+    out = call(
+        functools.partial(first_channels_kernel, count),
+        "first_channels",
+        parts,
+        [((block, width), BF)] * count + [((width, hidden), BF)] * 3,
+        [
+            pltpu.VMEM((block * count, width), BF),
+            pltpu.VMEM((block * count, hidden), BF),
+            pltpu.SemaphoreType.DMA((2, hidden // TILE)),
+            pltpu.SemaphoreType.DMA((width // STRIP,)),
+        ],
+        far=[pltpu.with_memory_space_constraint(weights, pltpu.HBM)],
+    )
+    return out[:count], out[count:]
+
+
+def more_channels_kernel(rows_ref, gate_ref, up_ref, down_ref, out_ref, hidden_ref):
+    for j in range(gate_ref.shape[1] // TILE):
+        here = slice(j * TILE, (j + 1) * TILE)
+        hidden_ref[:, here] = activated(rows_ref[...], gate_ref[:, here], up_ref[:, here])
+    for n in range(down_ref.shape[0] // STRIP):
+        here = slice(n * STRIP, (n + 1) * STRIP)
+        out_ref[:, here] = product_nt(hidden_ref[...], down_ref[here, :]).astype(BF)
+
+
+def more_channels(rows, projections):
     return call(
-        channels_kernel,
-        "channel_sums",
-        parts,
-        [((block, width), BF)] * size,
-        [
-            weight,
-            weight,
-            weight,
-            pltpu.VMEM((block * size, width), BF),
-            pltpu.VMEM((block * size, hidden), BF),
-            pltpu.SemaphoreType.DMA((2, hidden // 128)),
-            pltpu.SemaphoreType.DMA((width // 256,)),
-        ],
-        far=[weights],
-        mib=32,
-    )
+        more_channels_kernel,
+        "more_channels",
+        [rows, *projections],
+        [(rows.shape, BF)],
+        [pltpu.VMEM((rows.shape[0], projections[0].shape[1]), BF)],
+    )[0]
 
 
 def last_kernel(middle_ref, *rest):
@@ -518,19 +549,25 @@
     weights = lax.all_gather(weights, SP, axis=0, tiled=True)
     size = lax.axis_size("tp")
     at = jnp.stack([lax.axis_index(a).astype(jnp.int32) for a in ("tp", *reversed(SP))])
-    before, total, solved, decay, key_unit, grown = keys_side(keys, values, beta_pre, decay_pre)
-    local, query, gate, states = state_ahead(
+    before, total, solved, decay, grown = keys_side(keys, values, beta_pre, decay_pre)
+    gate = gates_side(gates, out_gain)
+    pairs = queries.shape[1] // PAIR
+    early, late, states = state_ahead(
         at,
         total,
-        lambda chip: queries_side(chip, queries, key_unit, decay, solved, before, grown),
-        lambda: gates_side(gates, out_gain),
-    )
-    parts = mixed_and_projected(at, size, local, query, states, gate, w_out)
+        lambda x: queries_side(0, x, queries, decay, solved, before, grown),
+        lambda x: queries_side(pairs // 2, x, queries, decay, solved, before, grown),
+    )
+    parts = mixed_and_projected(at, size, early, late, states, gate, w_out)
     got = [lax.ppermute(parts[k], "tp", ring(size, k)) for k in range(1, size)]
     middle, normed = normed_rows(stream, norm_gain, [parts[0]] + got)
-    rows = [normed] + [lax.ppermute(normed, "tp", ring(size, k)) for k in range(1, size)]
-    sums = channel_sums(weights, rows, hidden)
-    back = [lax.ppermute(sums[k], "tp", ring(size, -k)) for k in range(1, size)]
+    right = lax.ppermute(normed, "tp", ring(size, 1))
+    left = lax.ppermute(normed, "tp", ring(size, -1))
+    across = lax.ppermute(normed, "tp", ring(size, 2))
+    sums, projections = first_channels(weights, [normed, right, left], hidden)
+    back = [lax.ppermute(sums[1], "tp", ring(size, -1)), lax.ppermute(sums[2], "tp", ring(size, 1))]
+    last = more_channels(across, projections)
+    back.append(lax.ppermute(last, "tp", ring(size, 2)))
     return last_sum(middle, [sums[0]] + back)
 
 

time: 153 us -> 136 us (0.89)
  waiting for transfers between devices: 57.4 us -> 44.9 us
  local copies, waits for them, and re-layouts: 9.73 us -> 2.72 us
  starting transfers between devices: 27 us -> 29.1 us
    ppermute x7, waiting for transfers between devices: 37.1 us -> 24.8 us  [the longest x1 7.8 us: per_device(): left = lax.ppermute(normed, 'tp', ring(size, -1))]
    unnamed x26 -> x20, local copies, waits for them, and re-layouts: 9.73 us -> 2.72 us
    ppermute x3, waiting for transfers between devices: 2.95 us -> 0.4 us  [state_ahead(): planes = [lax.ppermute(whole, plane, ring(size, k)) for k in range(1, size)]]
    ppermute x3, waiting for transfers between devices: 0.01 us -> 1.86 us  [state_ahead(): lax.ppermute(chip, line, ring(size, k))]
    pallas_call x9 -> x11, Pallas kernels: 41.5 us -> 42.3 us  [call(): pl.pallas_call(kernel, in_specs=[TABLE] * len(tables) + [FAR] * len(far)...]
  transfers between devices with their start and end apart: 18 -> 18, of which waited for: 11 -> 10; matrix products, arithmetic and copies ran while one was open for 0% -> 0% of each run, Pallas kernels for 15% -> 31%
where the time goes in v4:
time: 136 us
  waiting for transfers between devices  44.9 us (33%)
  Pallas kernels  43.3 us (32%)
  starting transfers between devices  29.1 us (21%)
  between operations  13.6 us (10%)
  local copies, waits for them, and re-layouts  2.72 us (2%)
  other arithmetic  2.07 us (2%)
    pallas_call x11, Pallas kernels, call(): pl.pallas_call(kernel, in_specs=[TABLE] * len(tables) + [FAR] * len(far)...  42.3 us
    ppermute x3, waiting for transfers between devices, per_device(): got = [lax.ppermute(parts[k], 'tp', ring(size, k)) for k in range(1, size)]  16.1 us
    ppermute x1, waiting for transfers between devices, per_device(): left = lax.ppermute(normed, 'tp', ring(size, -1))  7.8 us
    ppermute x1, waiting for transfers between devices, per_device(): lax.ppermute(sums[1], 'tp', ring(size, -1))  7.76 us
    ppermute x3, starting transfers between devices, state_ahead(): planes = [lax.ppermute(whole, plane, ring(size, k)) for k in range(1, size)]  7.16 us
    ppermute x1, waiting for transfers between devices, per_device(): right = lax.ppermute(normed, 'tp', ring(size, 1))  7.05 us
    ppermute x3, starting transfers between devices, state_ahead(): lax.ppermute(chip, line, ring(size, k))  6.02 us
    ppermute x3, starting transfers between devices, per_device(): got = [lax.ppermute(parts[k], 'tp', ring(size, k)) for k in range(1, size)]  5.75 us
  transfers between devices with their start and end apart: 18, of which 10 were waited for; matrix products, arithmetic and copies ran while one was open for 0% of the time, Pallas kernels for 31%

profile of v4, /device:TPU:0, one launch (start us, length us, event | category | flops | bytes accessed | tf_op | source)
XLA Modules:
  0.0 135.6 jit_solution(7588029961317325037)
XLA Ops:
  6.5 2.0 %pad_maximum_fusion = bf16[64,4224]{1,0:T(8,128)(2,1)} fusion(bf16[64,1408]{1,0:T(8,128)(2,1)} %bitcast.9, bf16[64,1408]{1,0:T(8,128)(2,1)} %param.24, bf16[64,1408]{1,0:T(8,128)(2,1)} %param.23), kind=kLoop, calls=%fused_computation | loop fusion | flops 1622016 | bytes 1081344 | tf_op jit(solution)/shard_map/concatenate | solution.py:548
  8.5 0.0 all-gather.2.cloned.1.call-update
  8.6 0.0 copy-start.3
  8.6 1.0 copy-done.3
  9.6 1.0 copy-done.4
  10.6 0.7 copy-done.7
  11.3 9.6 %keys_side.1 = (bf16[12,128,128]{2,1,0:T(8,128)(2,1)S(1)}, bf16[4,128,128]{2,1,0:T(8,128)(2,1)}, bf16[12,128,384]{2,1,0:T(8,128)(2,1)S(1)}, bf16[12,128,256]{2,1,0:T(8,128)(2,1)S(1)}, f32[384,512]{1,0:T(8,128)S(1)}) custom-call(bf16[384,512]{1,0:T(8,128)(2,1)S(1)} %copy-done.3, bf16[384,512]{1,0:T(8,128)(2,1)S(1)} %copy-done.4, f32[8,384]{1,0:T(8,128)S(1)} %copy-done.6, ...), custom_call_target="tpu_custom_call" | custom-call | tf_op jit(solution)/shard_map/keys_side/pallas_call | solution.py:30
  20.9 0.1 pad_add_fusion.at_ref
  20.9 1.6 %collective-permute-done.other_ref.first_ref = bf16[4,128,128]{2,1,0:T(8,128)(2,1)} collective-permute-done((bf16[4,128,128]{2,1,0:T(8,128)(2,1)}, bf16[4,128,128]{2,1,0:T(8,128)(2,1)}, u32[]{:S(2)}, u32[]{:S(2)}) %collective-permute-start) | collective-permute-done | bytes 131104 | tf_op jit(solution)/shard_map/ppermute | solution.py:337
  22.5 1.2 chip_total.1.after_ref.rest_0_
  23.7 1.8 %collective-permute-start.1 = (bf16[2,128,128]{2,1,0:T(8,128)(2,1)S(1)}, bf16[2,128,128]{2,1,0:T(8,128)(2,1)S(1)}, u32[]{:S(2)}, u32[]{:S(2)}) collective-permute-start(bf16[2,128,128]{2,1,0:T(8,128)(2,1)S(1)} %chip_total.1.after_ref.rest_0_), channel_id=1, source_target_pairs={{0,8},{8,16},{16,24},{24,0},{1,9},{9,17},{17,25},{25,1},{2,10},{10... | collective-permute-start | bytes 196616 | tf_op jit(solution)/shard_map/ppermute | solution.py:340
  25.5 2.9 %collective-permute-start.2 = (bf16[2,128,128]{2,1,0:T(8,128)(2,1)S(1)}, bf16[2,128,128]{2,1,0:T(8,128)(2,1)S(1)}, u32[]{:S(2)}, u32[]{:S(2)}) collective-permute-start(bf16[2,128,128]{2,1,0:T(8,128)(2,1)S(1)} %chip_total.1.after_ref.rest_0_), channel_id=1, source_target_pairs={{0,16},{8,24},{16,0},{24,8},{1,17},{9,25},{17,1},{25,9},{2,18},{10... | collective-permute-start | bytes 196616 | tf_op jit(solution)/shard_map/ppermute | solution.py:340
  28.4 1.3 collective-permute-start.3
  29.8 2.9 %queries_side.2 = (f32[384,256]{1,0:T(8,128)S(1)}, bf16[384,256]{1,0:T(8,128)(2,1)S(1)}) custom-call(bf16[2,128,128]{2,1,0:T(8,128)(2,1)S(1)} %chip_total.1.after_ref.rest_0_, bf16[384,512]{1,0:T(8,128)(2,1)S(1)} %copy-done.1, bf16[12,128,256]{2,1,0:T(8,128)(2,1)S(1)} %get-tuple-element.29.d_ref, bf16[12,128,384]{2,1,0:T(8,128)(2,1)S(1)} %get-tuple-element.30.y_ref, ...), custom_call_target="tpu_custom_call" | custom-call | tf_op jit(solution)/shard_map/queries_side/pallas_call | solution.py:30
  32.7 1.9 %collective-permute-done.2.rest_2_ = bf16[2,128,128]{2,1,0:T(8,128)(2,1)S(1)} collective-permute-done((bf16[2,128,128]{2,1,0:T(8,128)(2,1)S(1)}, bf16[2,128,128]{2,1,0:T(8,128)(2,1)S(1)}, u32[]{:S(2)}, u32[]{:S(2)}) %collective-permute-start.2) | collective-permute-done | bytes 65568 | tf_op jit(solution)/shard_map/ppermute | solution.py:340
  34.5 0.0 collective-permute-done.3.rest_3_
  34.6 1.2 line_total.1
  35.7 0.0 copy-start.5
  35.8 0.0 copy-start.9
  35.8 2.5 %collective-permute-start.4 = (bf16[2,128,128]{2,1,0:T(8,128)(2,1)S(1)}, bf16[2,128,128]{2,1,0:T(8,128)(2,1)S(1)}, u32[]{:S(2)}, u32[]{:S(2)}) collective-permute-start(bf16[2,128,128]{2,1,0:T(8,128)(2,1)S(1)} %get-tuple-element.35.after_ref), channel_id=1, source_target_pairs={{0,32},{32,64},{64,96},{96,0},{1,33},{33,65},{65,97},{97,1},{2,34}... | collective-permute-start | bytes 196616 | tf_op jit(solution)/shard_map/ppermute | solution.py:352
  38.3 3.7 %collective-permute-start.5 = (bf16[2,128,128]{2,1,0:T(8,128)(2,1)S(1)}, bf16[2,128,128]{2,1,0:T(8,128)(2,1)S(1)}, u32[]{:S(2)}, u32[]{:S(2)}) collective-permute-start(bf16[2,128,128]{2,1,0:T(8,128)(2,1)S(1)} %get-tuple-element.35.after_ref), channel_id=1, source_target_pairs={{0,64},{32,96},{64,0},{96,32},{1,65},{33,97},{65,1},{97,33},{2,66}... | collective-permute-start | bytes 196616 | tf_op jit(solution)/shard_map/ppermute | solution.py:352
  42.0 0.9 collective-permute-start.6
  42.9 2.9 %queries_side.3 = (f32[384,256]{1,0:T(8,128)S(1)}, bf16[384,256]{1,0:T(8,128)(2,1)S(1)}) custom-call(bf16[2,128,128]{2,1,0:T(8,128)(2,1)S(1)} %get-tuple-element.35.after_ref, bf16[384,512]{1,0:T(8,128)(2,1)S(1)} %copy-done.1, bf16[12,128,256]{2,1,0:T(8,128)(2,1)S(1)} %get-tuple-element.29.d_ref, bf16[12,128,384]{2,1,0:T(8,128)(2,1)S(1)} %get-tuple-element.30.y_ref, ...), custom_call_target="tpu_custom_call" | custom-call | tf_op jit(solution)/shard_map/queries_side/pallas_call | solution.py:30
  45.9 0.0 collective-permute-done.5.rest_1_
  45.9 0.4 collective-permute-done.6.rest_2_
  46.3 1.4 %plane_state.1.mine_ref = bf16[2,128,128]{2,1,0:T(8,128)(2,1)S(1)} custom-call(s32[4]{0:T(128)S(1)} %pad_add_fusion.at_ref, bf16[384,256]{1,0:T(8,128)(2,1)S(1)} %get-tuple-element.37.after_ref.q1_ref, bf16[2,128,128]{2,1,0:T(8,128)(2,1)S(1)} %get-tuple-element.38.before_ref, bf16[2,128,128]{2,1,0:T(8,128)(2,1)S(1)} %collective-permute-done.4.rest_0_, ...), custom_call_target="tpu_custom_call" | custom-call | tf_op jit(solution)/shard_map/plane_state/pallas_call | solution.py:30
  47.7 0.1 collective-permute-start.7
  47.8 0.3 gates_side.1.gate_ref
  48.1 1.1 collective-permute-done.7.theirs_ref
  49.1 3.7 %mixed_and_projected.1 = (f32[96,2048]{1,0:T(8,128)S(1)}, bf16[96,2048]{1,0:T(8,128)(2,1)S(1)}, bf16[96,2048]{1,0:T(8,128)(2,1)S(1)}, bf16[96,2048]{1,0:T(8,128)(2,1)S(1)}) custom-call(s32[4]{0:T(128)S(1)} %pad_add_fusion.at_ref, f32[384,256]{1,0:T(8,128)S(1)} %get-tuple-element.33.o0_ref, bf16[384,256]{1,0:T(8,128)(2,1)S(1)} %get-tuple-element.34.after_ref.q0_ref, ...), custom_call_target="tpu_custom_call" | custom-call | tf_op jit(solution)/shard_map/mixed_and_projected/pallas_call | solution.py:30
  52.9 1.6 %collective-permute-start.8 = (bf16[96,2048]{1,0:T(8,128)(2,1)S(1)}, bf16[96,2048]{1,0:T(8,128)(2,1)S(1)}, u32[]{:S(2)}, u32[]{:S(2)}) collective-permute-start(bf16[96,2048]{1,0:T(8,128)(2,1)S(1)} %get-tuple-element.40), channel_id=1, source_target_pairs={{0,1},{1,2},{2,3},{3,0},{4,5},{5,6},{6,7},{7,4},{8,9},{9,10},{10,1... | collective-permute-start | bytes 1179656 | tf_op jit(solution)/shard_map/ppermute | solution.py:562
  54.5 2.7 %collective-permute-start.9 = (bf16[96,2048]{1,0:T(8,128)(2,1)S(1)}, bf16[96,2048]{1,0:T(8,128)(2,1)S(1)}, u32[]{:S(2)}, u32[]{:S(2)}) collective-permute-start(bf16[96,2048]{1,0:T(8,128)(2,1)S(1)} %get-tuple-element.41), channel_id=1, source_target_pairs={{0,2},{1,3},{2,0},{3,1},{4,6},{5,7},{6,4},{7,5},{8,10},{9,11},{10,... | collective-permute-start | bytes 1179656 | tf_op jit(solution)/shard_map/ppermute | solution.py:562
  57.2 1.4 %collective-permute-start.10 = (bf16[96,2048]{1,0:T(8,128)(2,1)S(1)}, bf16[96,2048]{1,0:T(8,128)(2,1)S(1)}, u32[]{:S(2)}, u32[]{:S(2)}) collective-permute-start(bf16[96,2048]{1,0:T(8,128)(2,1)S(1)} %get-tuple-element.42), channel_id=1, source_target_pairs={{0,3},{1,0},{2,1},{3,2},{4,7},{5,4},{6,5},{7,6},{8,11},{9,8},{10,9... | collective-permute-start | bytes 1179656 | tf_op jit(solution)/shard_map/ppermute | solution.py:562
  58.6 6.7 %collective-permute-done.8.rest_1_ = bf16[96,2048]{1,0:T(8,128)(2,1)S(1)} collective-permute-done((bf16[96,2048]{1,0:T(8,128)(2,1)S(1)}, bf16[96,2048]{1,0:T(8,128)(2,1)S(1)}, u32[]{:S(2)}, u32[]{:S(2)}) %collective-permute-start.8) | collective-permute-done | bytes 393248 | tf_op jit(solution)/shard_map/ppermute | solution.py:562
  65.3 9.4 %collective-permute-done.9.rest_2_ = bf16[96,2048]{1,0:T(8,128)(2,1)S(1)} collective-permute-done((bf16[96,2048]{1,0:T(8,128)(2,1)S(1)}, bf16[96,2048]{1,0:T(8,128)(2,1)S(1)}, u32[]{:S(2)}, u32[]{:S(2)}) %collective-permute-start.9) | collective-permute-done | bytes 393248 | tf_op jit(solution)/shard_map/ppermute | solution.py:562
  74.8 0.4 normed_rows.1
  75.2 1.5 %collective-permute-start.11 = (bf16[96,2048]{1,0:T(8,128)(2,1)S(1)}, bf16[96,2048]{1,0:T(8,128)(2,1)S(1)}, u32[]{:S(2)}, u32[]{:S(2)}) collective-permute-start(bf16[96,2048]{1,0:T(8,128)(2,1)S(1)} %get-tuple-element.44.rest_0_), channel_id=1, source_target_pairs={{0,1},{1,2},{2,3},{3,0},{4,5},{5,6},{6,7},{7,4},{8,9},{9,10},{10,1... | collective-permute-start | bytes 1179656 | tf_op jit(solution)/shard_map/ppermute | solution.py:564
  76.7 1.8 %collective-permute-start.12 = (bf16[96,2048]{1,0:T(8,128)(2,1)S(1)}, bf16[96,2048]{1,0:T(8,128)(2,1)S(1)}, u32[]{:S(2)}, u32[]{:S(2)}) collective-permute-start(bf16[96,2048]{1,0:T(8,128)(2,1)S(1)} %get-tuple-element.44.rest_0_), channel_id=1, source_target_pairs={{0,3},{1,0},{2,1},{3,2},{4,7},{5,4},{6,5},{7,6},{8,11},{9,8},{10,9... | collective-permute-start | bytes 1179656 | tf_op jit(solution)/shard_map/ppermute | solution.py:565
  78.5 1.4 %collective-permute-start.15 = (bf16[96,2048]{1,0:T(8,128)(2,1)S(1)}, bf16[96,2048]{1,0:T(8,128)(2,1)S(1)}, u32[]{:S(2)}, u32[]{:S(2)}) collective-permute-start(bf16[96,2048]{1,0:T(8,128)(2,1)S(1)} %get-tuple-element.44.rest_0_), channel_id=1, source_target_pairs={{0,2},{1,3},{2,0},{3,1},{4,6},{5,7},{6,4},{7,5},{8,10},{9,11},{10,... | collective-permute-start | bytes 1179656 | tf_op jit(solution)/shard_map/ppermute | solution.py:566
  80.0 7.1 %collective-permute-done.11.rest_1_ = bf16[96,2048]{1,0:T(8,128)(2,1)S(1)} collective-permute-done((bf16[96,2048]{1,0:T(8,128)(2,1)S(1)}, bf16[96,2048]{1,0:T(8,128)(2,1)S(1)}, u32[]{:S(2)}, u32[]{:S(2)}) %collective-permute-start.11) | collective-permute-done | bytes 393248 | tf_op jit(solution)/shard_map/ppermute | solution.py:564
  87.0 7.8 %collective-permute-done.12.rest_2_ = bf16[96,2048]{1,0:T(8,128)(2,1)S(1)} collective-permute-done((bf16[96,2048]{1,0:T(8,128)(2,1)S(1)}, bf16[96,2048]{1,0:T(8,128)(2,1)S(1)}, u32[]{:S(2)}, u32[]{:S(2)}) %collective-permute-start.12) | collective-permute-done | bytes 393248 | tf_op jit(solution)/shard_map/ppermute | solution.py:565
  94.8 14.7 %first_channels.1 = (bf16[96,2048]{1,0:T(8,128)(2,1)S(1)}, bf16[96,2048]{1,0:T(8,128)(2,1)S(1)}, bf16[96,2048]{1,0:T(8,128)(2,1)S(1)}, bf16[2048,1408]{1,0:T(8,1...) custom-call(bf16[2048,4224]{1,0:T(8,128)(2,1)} %all-gather.2.cloned.1.call-done.w_ref, ...), custom_call_target="tpu_custom_call" | custom-call | tf_op jit(solution)/shard_map/first_channels/pallas_call | solution.py:30
  109.5 3.7 %collective-permute-start.13 = (bf16[96,2048]{1,0:T(8,128)(2,1)S(1)}, bf16[96,2048]{1,0:T(8,128)(2,1)S(1)}, u32[]{:S(2)}, u32[]{:S(2)}) collective-permute-start(bf16[96,2048]{1,0:T(8,128)(2,1)S(1)} %get-tuple-element.46), channel_id=1, source_target_pairs={{0,3},{1,0},{2,1},{3,2},{4,7},{5,4},{6,5},{7,6},{8,11},{9,8},{10,9... | collective-permute-start | bytes 1179656 | tf_op jit(solution)/shard_map/ppermute | solution.py:568
  113.3 4.0 %more_channels.1 = bf16[96,2048]{1,0:T(8,128)(2,1)S(1)} custom-call(bf16[96,2048]{1,0:T(8,128)(2,1)S(1)} %collective-permute-done.15.rows_ref, bf16[2048,1408]{1,0:T(8,128)(2,1)S(1)} %get-tuple-element.48.gate_ref, bf16[2048,1408]{1,0:T(8,128)(2,1)S(1)} %get-tuple-element.49.up_ref, bf16[2048,1408]{1,0:T(8,128)(2,1)S(1)} %get-tuple-element.50.down_ref), custom_call_target="tpu_custom_call" | custom-call | tf_op jit(solution)/shard_map/more_channels/pallas_call | solution.py:30
  117.2 1.6 %collective-permute-start.16 = (bf16[96,2048]{1,0:T(8,128)(2,1)S(1)}, bf16[96,2048]{1,0:T(8,128)(2,1)S(1)}, u32[]{:S(2)}, u32[]{:S(2)}) collective-permute-start(bf16[96,2048]{1,0:T(8,128)(2,1)S(1)} %more_channels.1), channel_id=1, source_target_pairs={{0,2},{1,3},{2,0},{3,1},{4,6},{5,7},{6,4},{7,5},{8,10},{9,11},{10,... | collective-permute-start | bytes 1179656 | tf_op jit(solution)/shard_map/ppermute | solution.py:570
  118.9 7.8 %collective-permute-done.13.rest_1_ = bf16[96,2048]{1,0:T(8,128)(2,1)S(1)} collective-permute-done((bf16[96,2048]{1,0:T(8,128)(2,1)S(1)}, bf16[96,2048]{1,0:T(8,128)(2,1)S(1)}, u32[]{:S(2)}, u32[]{:S(2)}) %collective-permute-start.13) | collective-permute-done | bytes 393248 | tf_op jit(solution)/shard_map/ppermute | solution.py:568
  126.6 1.2 collective-permute-done.14.rest_2_
  127.8 1.0 last_sum.1
  (23 shorter events, 0.0 us)
Async XLA Ops:
  6.5 2.0 %copy-start.6 = (f32[8,384]{1,0:T(8,128)S(1)}, f32[8,384]{1,0:T(8,128)}, u32[]{:S(2)}) copy-start(f32[8,384]{1,0:T(8,128)} %beta_ref.1) | copy-start | bytes 36868
  6.5 88.3 %all-gather.2.cloned.1.call-start = ((), (), s32[]{:S(2)}) async-start(), calls=%async_computation | async-start | bytes 17842176 | tf_op jit(solution)/shard_map/all_gather | solution.py:549
  6.5 23.2 %copy-start.1 = (bf16[384,512]{1,0:T(8,128)(2,1)S(1)}, bf16[384,512]{1,0:T(8,128)(2,1)}, u32[]{:S(2)}) copy-start(bf16[384,512]{1,0:T(8,128)(2,1)} %q_ref.3) | copy-start | bytes 1179652
  8.6 1.0 copy-start.3
  9.6 1.0 copy-start.4
  10.6 0.7 copy-start.7
  20.8 1.7 %collective-permute-start = (bf16[4,128,128]{2,1,0:T(8,128)(2,1)}, bf16[4,128,128]{2,1,0:T(8,128)(2,1)}, u32[]{:S(2)}, u32[]{:S(2)}) collective-permute-start(bf16[4,128,128]{2,1,0:T(8,128)(2,1)} %get-tuple-element.28.own_ref), channel_id=1, source_target_pairs={{0,4},{4,0},{1,5},{5,1},{2,6},{6,2},{3,7},{7,3},{8,12},{12,8},{9,1... | collective-permute-start | bytes 393224 | tf_op jit(solution)/shard_map/ppermute | solution.py:337
  23.7 8.9 %collective-permute-start.1 = (bf16[2,128,128]{2,1,0:T(8,128)(2,1)S(1)}, bf16[2,128,128]{2,1,0:T(8,128)(2,1)S(1)}, u32[]{:S(2)}, u32[]{:S(2)}) collective-permute-start(bf16[2,128,128]{2,1,0:T(8,128)(2,1)S(1)} %chip_total.1.after_ref.rest_0_), channel_id=1, source_target_pairs={{0,8},{8,16},{16,24},{24,0},{1,9},{9,17},{17,25},{25,1},{2,10},{10... | collective-permute-start | bytes 196616 | tf_op jit(solution)/shard_map/ppermute | solution.py:340
  25.5 9.0 %collective-permute-start.2 = (bf16[2,128,128]{2,1,0:T(8,128)(2,1)S(1)}, bf16[2,128,128]{2,1,0:T(8,128)(2,1)S(1)}, u32[]{:S(2)}, u32[]{:S(2)}) collective-permute-start(bf16[2,128,128]{2,1,0:T(8,128)(2,1)S(1)} %chip_total.1.after_ref.rest_0_), channel_id=1, source_target_pairs={{0,16},{8,24},{16,0},{24,8},{1,17},{9,25},{17,1},{25,9},{2,18},{10... | collective-permute-start | bytes 196616 | tf_op jit(solution)/shard_map/ppermute | solution.py:340
  28.4 6.1 %collective-permute-start.3 = (bf16[2,128,128]{2,1,0:T(8,128)(2,1)S(1)}, bf16[2,128,128]{2,1,0:T(8,128)(2,1)S(1)}, u32[]{:S(2)}, u32[]{:S(2)}) collective-permute-start(bf16[2,128,128]{2,1,0:T(8,128)(2,1)S(1)} %chip_total.1.after_ref.rest_0_), channel_id=1, source_target_pairs={{0,24},{8,0},{16,8},{24,16},{1,25},{9,1},{17,9},{25,17},{2,26},{10... | collective-permute-start | bytes 196616 | tf_op jit(solution)/shard_map/ppermute | solution.py:340
  35.7 12.1 %copy-start.5 = (bf16[384,512]{1,0:T(8,128)(2,1)S(1)}, bf16[384,512]{1,0:T(8,128)(2,1)}, u32[]{:S(2)}) copy-start(bf16[384,512]{1,0:T(8,128)(2,1)} %gates_ref.1) | copy-start | bytes 1179652
  35.8 12.0 %copy-start.9 = (f32[64]{0:T(128)S(1)}, f32[64]{0:T(128)}, u32[]{:S(2)}) copy-start(f32[64]{0:T(128)} %param.19) | copy-start | bytes 772
  35.8 10.1 %collective-permute-start.4 = (bf16[2,128,128]{2,1,0:T(8,128)(2,1)S(1)}, bf16[2,128,128]{2,1,0:T(8,128)(2,1)S(1)}, u32[]{:S(2)}, u32[]{:S(2)}) collective-permute-start(bf16[2,128,128]{2,1,0:T(8,128)(2,1)S(1)} %get-tuple-element.35.after_ref), channel_id=1, source_target_pairs={{0,32},{32,64},{64,96},{96,0},{1,33},{33,65},{65,97},{97,1},{2,34}... | collective-permute-start | bytes 196616 | tf_op jit(solution)/shard_map/ppermute | solution.py:352
  38.3 7.6 %collective-permute-start.5 = (bf16[2,128,128]{2,1,0:T(8,128)(2,1)S(1)}, bf16[2,128,128]{2,1,0:T(8,128)(2,1)S(1)}, u32[]{:S(2)}, u32[]{:S(2)}) collective-permute-start(bf16[2,128,128]{2,1,0:T(8,128)(2,1)S(1)} %get-tuple-element.35.after_ref), channel_id=1, source_target_pairs={{0,64},{32,96},{64,0},{96,32},{1,65},{33,97},{65,1},{97,33},{2,66}... | collective-permute-start | bytes 196616 | tf_op jit(solution)/shard_map/ppermute | solution.py:352
  42.0 4.3 %collective-permute-start.6 = (bf16[2,128,128]{2,1,0:T(8,128)(2,1)S(1)}, bf16[2,128,128]{2,1,0:T(8,128)(2,1)S(1)}, u32[]{:S(2)}, u32[]{:S(2)}) collective-permute-start(bf16[2,128,128]{2,1,0:T(8,128)(2,1)S(1)} %get-tuple-element.35.after_ref), channel_id=1, source_target_pairs={{0,96},{32,0},{64,32},{96,64},{1,97},{33,1},{65,33},{97,65},{2,98}... | collective-permute-start | bytes 196616 | tf_op jit(solution)/shard_map/ppermute | solution.py:352
  42.9 6.2 %copy-start = (bf16[512,2048]{1,0:T(8,128)(2,1)S(1)}, bf16[512,2048]{1,0:T(8,128)(2,1)}, u32[]{:S(2)}) copy-start(bf16[512,2048]{1,0:T(8,128)(2,1)} %w_ref.1) | copy-start | bytes 6291460
  47.7 1.4 %collective-permute-start.7 = (bf16[2,128,128]{2,1,0:T(8,128)(2,1)S(1)}, bf16[2,128,128]{2,1,0:T(8,128)(2,1)S(1)}, u32[]{:S(2)}, u32[]{:S(2)}) collective-permute-start(bf16[2,128,128]{2,1,0:T(8,128)(2,1)S(1)} %plane_state.1.mine_ref), channel_id=1, source_target_pairs={{0,4},{4,0},{1,5},{5,1},{2,6},{6,2},{3,7},{7,3},{8,12},{12,8},{9,1... | collective-permute-start | bytes 196616 | tf_op jit(solution)/shard_map/ppermute | solution.py:357
  49.1 25.6 %copy-start.2 = (bf16[96,2048]{1,0:T(8,128)(2,1)S(1)}, bf16[96,2048]{1,0:T(8,128)(2,1)}, u32[]{:S(2)}) copy-start(bf16[96,2048]{1,0:T(8,128)(2,1)} %stream_ref.1) | copy-start | bytes 1179652
  49.1 25.6 %copy-start.8 = (f32[2048]{0:T(1024)S(1)}, f32[2048]{0:T(1024)}, u32[]{:S(2)}) copy-start(f32[2048]{0:T(1024)} %param.22) | copy-start | bytes 24580
  52.9 12.4 %collective-permute-start.8 = (bf16[96,2048]{1,0:T(8,128)(2,1)S(1)}, bf16[96,2048]{1,0:T(8,128)(2,1)S(1)}, u32[]{:S(2)}, u32[]{:S(2)}) collective-permute-start(bf16[96,2048]{1,0:T(8,128)(2,1)S(1)} %get-tuple-element.40), channel_id=1, source_target_pairs={{0,1},{1,2},{2,3},{3,0},{4,5},{5,6},{6,7},{7,4},{8,9},{9,10},{10,1... | collective-permute-start | bytes 1179656 | tf_op jit(solution)/shard_map/ppermute | solution.py:562
  54.5 20.2 %collective-permute-start.9 = (bf16[96,2048]{1,0:T(8,128)(2,1)S(1)}, bf16[96,2048]{1,0:T(8,128)(2,1)S(1)}, u32[]{:S(2)}, u32[]{:S(2)}) collective-permute-start(bf16[96,2048]{1,0:T(8,128)(2,1)S(1)} %get-tuple-element.41), channel_id=1, source_target_pairs={{0,2},{1,3},{2,0},{3,1},{4,6},{5,7},{6,4},{7,5},{8,10},{9,11},{10,... | collective-permute-start | bytes 1179656 | tf_op jit(solution)/shard_map/ppermute | solution.py:562
  57.2 17.6 %collective-permute-start.10 = (bf16[96,2048]{1,0:T(8,128)(2,1)S(1)}, bf16[96,2048]{1,0:T(8,128)(2,1)S(1)}, u32[]{:S(2)}, u32[]{:S(2)}) collective-permute-start(bf16[96,2048]{1,0:T(8,128)(2,1)S(1)} %get-tuple-element.42), channel_id=1, source_target_pairs={{0,3},{1,0},{2,1},{3,2},{4,7},{5,4},{6,5},{7,6},{8,11},{9,8},{10,9... | collective-permute-start | bytes 1179656 | tf_op jit(solution)/shard_map/ppermute | solution.py:562
  75.2 11.8 %collective-permute-start.11 = (bf16[96,2048]{1,0:T(8,128)(2,1)S(1)}, bf16[96,2048]{1,0:T(8,128)(2,1)S(1)}, u32[]{:S(2)}, u32[]{:S(2)}) collective-permute-start(bf16[96,2048]{1,0:T(8,128)(2,1)S(1)} %get-tuple-element.44.rest_0_), channel_id=1, source_target_pairs={{0,1},{1,2},{2,3},{3,0},{4,5},{5,6},{6,7},{7,4},{8,9},{9,10},{10,1... | collective-permute-start | bytes 1179656 | tf_op jit(solution)/shard_map/ppermute | solution.py:564
  76.7 18.1 %collective-permute-start.12 = (bf16[96,2048]{1,0:T(8,128)(2,1)S(1)}, bf16[96,2048]{1,0:T(8,128)(2,1)S(1)}, u32[]{:S(2)}, u32[]{:S(2)}) collective-permute-start(bf16[96,2048]{1,0:T(8,128)(2,1)S(1)} %get-tuple-element.44.rest_0_), channel_id=1, source_target_pairs={{0,3},{1,0},{2,1},{3,2},{4,7},{5,4},{6,5},{7,6},{8,11},{9,8},{10,9... | collective-permute-start | bytes 1179656 | tf_op jit(solution)/shard_map/ppermute | solution.py:565
  78.5 34.7 %collective-permute-start.15 = (bf16[96,2048]{1,0:T(8,128)(2,1)S(1)}, bf16[96,2048]{1,0:T(8,128)(2,1)S(1)}, u32[]{:S(2)}, u32[]{:S(2)}) collective-permute-start(bf16[96,2048]{1,0:T(8,128)(2,1)S(1)} %get-tuple-element.44.rest_0_), channel_id=1, source_target_pairs={{0,2},{1,3},{2,0},{3,1},{4,6},{5,7},{6,4},{7,5},{8,10},{9,11},{10,... | collective-permute-start | bytes 1179656 | tf_op jit(solution)/shard_map/ppermute | solution.py:566
  109.5 17.1 %collective-permute-start.13 = (bf16[96,2048]{1,0:T(8,128)(2,1)S(1)}, bf16[96,2048]{1,0:T(8,128)(2,1)S(1)}, u32[]{:S(2)}, u32[]{:S(2)}) collective-permute-start(bf16[96,2048]{1,0:T(8,128)(2,1)S(1)} %get-tuple-element.46), channel_id=1, source_target_pairs={{0,3},{1,0},{2,1},{3,2},{4,7},{5,4},{6,5},{7,6},{8,11},{9,8},{10,9... | collective-permute-start | bytes 1179656 | tf_op jit(solution)/shard_map/ppermute | solution.py:568
  113.2 14.5 %collective-permute-start.14 = (bf16[96,2048]{1,0:T(8,128)(2,1)S(1)}, bf16[96,2048]{1,0:T(8,128)(2,1)S(1)}, u32[]{:S(2)}, u32[]{:S(2)}) collective-permute-start(bf16[96,2048]{1,0:T(8,128)(2,1)S(1)} %get-tuple-element.47), channel_id=1, source_target_pairs={{0,1},{1,2},{2,3},{3,0},{4,5},{5,6},{6,7},{7,4},{8,9},{9,10},{10,1... | collective-permute-start | bytes 1179656 | tf_op jit(solution)/shard_map/ppermute | solution.py:568
  117.2 10.6 %collective-permute-start.16 = (bf16[96,2048]{1,0:T(8,128)(2,1)S(1)}, bf16[96,2048]{1,0:T(8,128)(2,1)S(1)}, u32[]{:S(2)}, u32[]{:S(2)}) collective-permute-start(bf16[96,2048]{1,0:T(8,128)(2,1)S(1)} %more_channels.1), channel_id=1, source_target_pairs={{0,2},{1,3},{2,0},{3,1},{4,6},{5,7},{6,4},{7,5},{8,10},{9,11},{10,... | collective-permute-start | bytes 1179656 | tf_op jit(solution)/shard_map/ppermute | solution.py:570
Sparse Core Ops, SparseCore 0:
  9.6 79.0 all-gather.1

commit v5 on v4

--- a/solution.py
+++ b/solution.py
@@ -24,8 +24,8 @@
 TABLE = pl.BlockSpec(memory_space=pltpu.SMEM)
 
 
-def call(kernel, name, arrays, shapes, scratch=(), table=None, far=(), mib=16, pinned=True):
-    near = [pltpu.with_memory_space_constraint(x, pltpu.VMEM) if pinned else x for x in arrays]
+def call(kernel, name, arrays, shapes, scratch=(), table=None, far=(), mib=16):
+    near = [pltpu.with_memory_space_constraint(x, pltpu.VMEM) for x in arrays]
     tables = [] if table is None else [table]
     return pl.pallas_call(
         kernel,
@@ -95,10 +95,23 @@
 
 
 def keys_kernel(
-    k_ref, v_ref, beta_ref, decay_ref,
+    k_far_ref, v_far_ref, beta_far_ref, decay_far_ref,
     before_ref, total_ref, y_ref, d_ref, ec_ref,
-    l_ref, x_ref, r_ref, f_ref,
+    l_ref, x_ref, r_ref, f_ref, k_ref, v_ref, beta_ref, decay_ref, sems,
 ):
+    length, width = k_ref.shape
+    rate_copies = [
+        pltpu.make_async_copy(decay_far_ref, decay_ref, sems.at[0]),
+        pltpu.make_async_copy(beta_far_ref, beta_ref, sems.at[1]),
+    ]
+    row_copies = []
+    for c in range(length // CHUNK):
+        rows = pl.ds(c * CHUNK, CHUNK)
+        for k, (far_ref, ref) in enumerate(((k_far_ref, k_ref), (v_far_ref, v_ref))):
+            sem = sems.at[2 + 2 * c + k]
+            row_copies.append(pltpu.make_async_copy(far_ref.at[rows], ref.at[rows], sem))
+    for copy in rate_copies + row_copies:
+        copy.start()
     row, col = places()
     left = col < HEAD_DIM
     top = row < HEAD_DIM
@@ -109,7 +122,6 @@
     differ = row ^ col
     eye = jnp.where(row == col, 1.0, 0.0)
     off_eye = differ == HEAD_DIM
-    length, width = k_ref.shape
     pairs = width // PAIR
     heads = 2 * pairs
     steps = length // CHUNK
@@ -117,6 +129,8 @@
     def stacked(x):
         return jnp.concatenate([x[:, c * CHUNK : (c + 1) * CHUNK] for c in range(steps)], axis=0)
 
+    for copy in rate_copies:
+        copy.wait()
     rates = split_three(stacked(-softplus(decay_ref[...])))
     strength = split_three(stacked(1.0 / (1.0 + jnp.exp(-beta_ref[...]))))
     triangle = jnp.where(inclusive, 1.0, 0.0).astype(BF)
@@ -130,6 +144,8 @@
     ends = []
     for c in range(steps):
         rows = slice(c * CHUNK, (c + 1) * CHUNK)
+        row_copies[2 * c].wait()
+        row_copies[2 * c + 1].wait()
         for p in range(pairs):
             lanes = slice(p * PAIR, (p + 1) * PAIR)
             item = c * pairs + p
@@ -206,7 +222,7 @@
     return call(
         keys_kernel,
         "keys_side",
-        [keys, values, beta_pre, decay_pre],
+        [],
         [
             ((items, PAIR, PAIR), BF),
             ((pairs, PAIR, PAIR), BF),
@@ -214,8 +230,21 @@
             ((items, CHUNK, 2 * CHUNK), BF),
             ((length, width), F32),
         ],
-        [wide, wide, wide, pltpu.VMEM((items, PAIR, CHUNK), BF)],
-        pinned=False,
+        [
+            wide,
+            wide,
+            wide,
+            pltpu.VMEM((items, PAIR, CHUNK), BF),
+            pltpu.VMEM((length, width), BF),
+            pltpu.VMEM((length, width), BF),
+            pltpu.VMEM(beta_pre.shape, F32),
+            pltpu.VMEM(beta_pre.shape, F32),
+            pltpu.SemaphoreType.DMA((2 + 2 * steps,)),
+        ],
+        far=[
+            pltpu.with_memory_space_constraint(x, pltpu.HBM)
+            for x in (keys, values, beta_pre, decay_pre)
+        ],
     )
 
 
@@ -361,7 +390,7 @@
     at_ref, o0_ref, q0_ref, o1_ref, q1_ref,
     first_ref, mine_ref, theirs_ref, gate_ref, w_ref, *rest,
 ):
-    out_refs, (mixed_ref, state_ref) = rest[:-2], rest[-2:]
+    out_ref, mixed_ref, state_ref = rest
     row, col = places()
     same = (col < HEAD_DIM) == (row < HEAD_DIM)
     ones = jnp.where(same, 1.0, 0.0).astype(BF)
@@ -381,34 +410,31 @@
         mean = half_sums(out * out, ones) * (1.0 / HEAD_DIM)
         out = out * lax.rsqrt(mean + EPSILON) * gate_ref[:, lanes]
         mixed_ref[:, lanes] = out.astype(BF)
-    size = len(out_refs)
-    block = length // size
-    for k, out_ref in enumerate(out_refs):
-        start = lax.rem(at_ref[0] + k, size) * block
-        rows = mixed_ref[pl.ds(pl.multiple_of(start, 32), block), :]
-        out_ref[...] = dot(rows, w_ref[...]).astype(out_ref.dtype)
+    for n in range(w_ref.shape[1] // STRIP):
+        here = slice(n * STRIP, (n + 1) * STRIP)
+        got = dot(mixed_ref[...], w_ref[:, here]).astype(BF)
+        block = out_ref.shape[1]
+        for k in range(out_ref.shape[0]):
+            out_ref[k, :, here] = got[k * block : (k + 1) * block, :]
 
 
 def mixed_and_projected(at, size, early, late, states, gate, w_out):
     length, width = gate.shape
-    block = (length // size, w_out.shape[1])
     return call(
         mixed_kernel,
         "mixed_and_projected",
         [*early, *late, *states, gate, w_out],
-        [(block, F32 if k == 0 else BF) for k in range(size)],
+        [((size, length // size, w_out.shape[1]), BF)],
         [pltpu.VMEM((length, width), BF), pltpu.VMEM((width // PAIR, PAIR, PAIR), BF)],
         table=at,
-    )
-
-
-def norm_kernel(stream_ref, gain_ref, *rest):
-    parts, middle_ref, normed_ref = rest[:-2], rest[-2], rest[-1]
-    total = stream_ref[...].astype(F32)
-    projected = parts[0][...].astype(F32)
-    for part in parts[1:]:
-        projected = projected + part[...].astype(F32)
-    middle = (total + projected).astype(BF)
+    )[0]
+
+
+def norm_kernel(stream_ref, gain_ref, parts_ref, middle_ref, normed_ref):
+    projected = parts_ref[0].astype(F32)
+    for k in range(1, parts_ref.shape[0]):
+        projected = projected + parts_ref[k].astype(F32)
+    middle = (stream_ref[...].astype(F32) + projected).astype(BF)
     middle_ref[...] = middle
     middle = middle.astype(F32)
     mean = jnp.mean(middle * middle, axis=-1, keepdims=True)
@@ -419,7 +445,7 @@
     return call(
         norm_kernel,
         "normed_rows",
-        [stream, gain.reshape(1, -1), *parts],
+        [stream, gain.reshape(1, -1), parts],
         [(stream.shape, BF), (stream.shape, BF)],
     )
 
@@ -437,6 +463,7 @@
 
 TILE = 128
 STRIP = 256
+AHEAD = 4
 
 
 def first_channels_kernel(count, w_ref, *rest):
@@ -444,27 +471,39 @@
     gate_ref, up_ref, down_ref, rows_ref, hidden_ref, in_sems, down_sems = rest[2 * count :]
     width, hidden = gate_ref.shape
     block = parts[0].shape[0]
-    copies, downs = [], []
+    groups = []
     for j in range(hidden // TILE):
         here = pl.ds(j * TILE, TILE)
+        group = []
         for k, ref in enumerate((gate_ref, up_ref)):
             from_ref = w_ref.at[:, pl.ds(k * hidden + j * TILE, TILE)]
-            copies.append(pltpu.make_async_copy(from_ref, ref.at[:, here], in_sems.at[k, j]))
+            group.append(pltpu.make_async_copy(from_ref, ref.at[:, here], in_sems.at[k, j]))
+        groups.append(group)
     for n in range(width // STRIP):
         here = pl.ds(n * STRIP, STRIP)
         from_ref = w_ref.at[here, pl.ds(2 * hidden, hidden)]
-        downs.append(pltpu.make_async_copy(from_ref, down_ref.at[here, :], down_sems.at[n]))
-    for copy in copies + downs:
-        copy.start()
+        groups.append([pltpu.make_async_copy(from_ref, down_ref.at[here, :], down_sems.at[n])])
+
+    def begin(g):
+        if g < len(groups):
+            for copy in groups[g]:
+                copy.start()
+
+    def arrived(g):
+        for copy in groups[g]:
+            copy.wait()
+        begin(g + AHEAD)
+
+    for g in range(AHEAD):
+        begin(g)
     for k, part in enumerate(parts):
         rows_ref[k * block : (k + 1) * block, :] = part[...]
     for j in range(hidden // TILE):
-        copies[2 * j].wait()
-        copies[2 * j + 1].wait()
+        arrived(j)
         here = slice(j * TILE, (j + 1) * TILE)
         hidden_ref[:, here] = activated(rows_ref[...], gate_ref[:, here], up_ref[:, here])
     for n in range(width // STRIP):
-        downs[n].wait()
+        arrived(hidden // TILE + n)
         here = slice(n * STRIP, (n + 1) * STRIP)
         got = product_nt(hidden_ref[...], down_ref[here, :])
         for k, out_ref in enumerate(out_refs):
@@ -490,22 +529,24 @@
     return out[:count], out[count:]
 
 
-def more_channels_kernel(rows_ref, gate_ref, up_ref, down_ref, out_ref, hidden_ref):
+def more_channels_kernel(upper_ref, lower_ref, gate_ref, up_ref, down_ref, out_ref, hidden_ref):
+    rows = jnp.concatenate([upper_ref[...], lower_ref[...]], axis=0)
     for j in range(gate_ref.shape[1] // TILE):
         here = slice(j * TILE, (j + 1) * TILE)
-        hidden_ref[:, here] = activated(rows_ref[...], gate_ref[:, here], up_ref[:, here])
+        hidden_ref[:, here] = activated(rows, gate_ref[:, here], up_ref[:, here])
     for n in range(down_ref.shape[0] // STRIP):
         here = slice(n * STRIP, (n + 1) * STRIP)
         out_ref[:, here] = product_nt(hidden_ref[...], down_ref[here, :]).astype(BF)
 
 
-def more_channels(rows, projections):
+def more_channels(halves_of_rows, projections):
+    half, width = halves_of_rows[0].shape
     return call(
         more_channels_kernel,
         "more_channels",
-        [rows, *projections],
-        [(rows.shape, BF)],
-        [pltpu.VMEM((rows.shape[0], projections[0].shape[1]), BF)],
+        [*halves_of_rows, *projections],
+        [((2 * half, width), BF)],
+        [pltpu.VMEM((2 * half, projections[0].shape[1]), BF)],
     )[0]
 
 
@@ -559,11 +600,15 @@
         lambda x: queries_side(pairs // 2, x, queries, decay, solved, before, grown),
     )
     parts = mixed_and_projected(at, size, early, late, states, gate, w_out)
-    got = [lax.ppermute(parts[k], "tp", ring(size, k)) for k in range(1, size)]
-    middle, normed = normed_rows(stream, norm_gain, [parts[0]] + got)
+    parts = lax.all_to_all(parts, "tp", 0, 0, tiled=True)
+    middle, normed = normed_rows(stream, norm_gain, parts)
     right = lax.ppermute(normed, "tp", ring(size, 1))
     left = lax.ppermute(normed, "tp", ring(size, -1))
-    across = lax.ppermute(normed, "tp", ring(size, 2))
+    half = normed.shape[0] // 2
+    across = [
+        lax.ppermute(right[:half], "tp", ring(size, 1)),
+        lax.ppermute(left[half:], "tp", ring(size, -1)),
+    ]
     sums, projections = first_channels(weights, [normed, right, left], hidden)
     back = [lax.ppermute(sums[1], "tp", ring(size, -1)), lax.ppermute(sums[2], "tp", ring(size, 1))]
     last = more_channels(across, projections)

time: 136 us -> 134 us (0.985)
  blocking collectives: 0 us -> 25.3 us
  waiting for transfers between devices: 44.9 us -> 27.5 us
  starting transfers between devices: 29.1 us -> 21.8 us
  local copies, waits for them, and re-layouts: 2.72 us -> 0.06 us
    all_to_all x0 -> x1, blocking collectives: none -> 25.3 us  [per_device(): parts = lax.all_to_all(parts, 'tp', 0, 0, tiled=True)]
    ppermute x4 -> x2, waiting for transfers between devices: 16.1 us -> 0.01 us  [the longest x1 0.01 us: per_device(): lax.ppermute(right[:half], 'tp', ring(size, 1))]
    ppermute x1, waiting for transfers between devices: 7.8 us -> 0.01 us  [per_device(): left = lax.ppermute(normed, 'tp', ring(size, -1))]
    ppermute x4 -> x2, starting transfers between devices: 7.19 us -> 3.35 us  [the longest x1 3.28 us: per_device(): lax.ppermute(left[half:], 'tp', ring(size, -1))]
    ppermute x1, starting transfers between devices: 3.73 us -> 0.11 us  [per_device(): lax.ppermute(sums[1], 'tp', ring(size, -1))]
    ppermute x1, waiting for transfers between devices: 7.76 us -> 10.9 us  [per_device(): lax.ppermute(sums[1], 'tp', ring(size, -1))]
    unnamed x20 -> x12, local copies, waits for them, and re-layouts: 2.72 us -> 0.03 us
    ppermute x1, waiting for transfers between devices: 1.16 us -> 3.38 us  [per_device(): lax.ppermute(sums[2], 'tp', ring(size, 1))]
  transfers between devices with their start and end apart: 18 -> 16, of which waited for: 10 -> 7; matrix products, arithmetic and copies ran while one was open for 0% -> 0% of each run, Pallas kernels for 31% -> 32%
where the time goes in v5:
time: 134 us
  Pallas kernels  43.4 us (32%)
  waiting for transfers between devices  27.5 us (21%)
  blocking collectives  25.3 us (19%)
  starting transfers between devices  21.8 us (16%)
  between operations  13.6 us (10%)
  other arithmetic  2.08 us (2%)
    pallas_call x11, Pallas kernels, call(): pl.pallas_call(kernel, in_specs=[TABLE] * len(tables) + [FAR] * len(far)...  42.4 us
    all_to_all x1, blocking collectives, per_device(): parts = lax.all_to_all(parts, 'tp', 0, 0, tiled=True)  25.3 us
    ppermute x1, waiting for transfers between devices, per_device(): lax.ppermute(sums[1], 'tp', ring(size, -1))  10.9 us
    ppermute x1, waiting for transfers between devices, per_device(): right = lax.ppermute(normed, 'tp', ring(size, 1))  7.77 us
    ppermute x3, starting transfers between devices, state_ahead(): planes = [lax.ppermute(whole, plane, ring(size, k)) for k in range(1, size)]  6.66 us
    ppermute x3, starting transfers between devices, state_ahead(): lax.ppermute(chip, line, ring(size, k))  6.01 us
    ppermute x1, waiting for transfers between devices, per_device(): lax.ppermute(sums[2], 'tp', ring(size, 1))  3.38 us
    ppermute x1, starting transfers between devices, per_device(): lax.ppermute(left[half:], 'tp', ring(size, -1))  3.28 us
  transfers between devices with their start and end apart: 16, of which 7 were waited for; matrix products, arithmetic and copies ran while one was open for 0% of the time, Pallas kernels for 32%

profile of v5, /device:TPU:0, one launch (start us, length us, event | category | flops | bytes accessed | tf_op | source)
XLA Modules:
  0.0 133.6 jit_solution(5037921138887273758)
XLA Ops:
  6.5 2.0 %pad_maximum_fusion = bf16[64,4224]{1,0:T(8,128)(2,1)} fusion(bf16[64,1408]{1,0:T(8,128)(2,1)} %bitcast.9, bf16[64,1408]{1,0:T(8,128)(2,1)} %param.24, bf16[64,1408]{1,0:T(8,128)(2,1)} %param.23), kind=kLoop, calls=%fused_computation | loop fusion | flops 1622016 | bytes 1081344 | tf_op jit(solution)/shard_map/concatenate | solution.py:589
  8.5 0.0 all-gather.2.cloned.1.call-update
  8.6 10.2 %keys_side.1 = (bf16[12,128,128]{2,1,0:T(8,128)(2,1)S(1)}, bf16[4,128,128]{2,1,0:T(8,128)(2,1)}, bf16[12,128,384]{2,1,0:T(8,128)(2,1)S(1)}, bf16[12,128,256]{2,1,0:T(8,128)(2,1)S(1)}, f32[384,512]{1,0:T(8,128)S(1)}) custom-call(bf16[384,512]{1,0:T(8,128)(2,1)} %k_far_ref.1, bf16[384,512]{1,0:T(8,128)(2,1)} %v_far_ref.1, f32[8,384]{1,0:T(8,128)} %beta_far_ref.1, ...), custom_call_target="tpu_custom_call" | custom-call | tf_op jit(solution)/shard_map/keys_side/pallas_call | solution.py:30
  18.8 0.1 collective-permute-start
  18.9 0.1 pad_add_fusion.at_ref
  19.0 1.6 %collective-permute-done.other_ref.first_ref = bf16[4,128,128]{2,1,0:T(8,128)(2,1)} collective-permute-done((bf16[4,128,128]{2,1,0:T(8,128)(2,1)}, bf16[4,128,128]{2,1,0:T(8,128)(2,1)}, u32[]{:S(2)}, u32[]{:S(2)}) %collective-permute-start) | collective-permute-done | bytes 131104 | tf_op jit(solution)/shard_map/ppermute | solution.py:366
  20.6 1.2 chip_total.1.after_ref.rest_0_
  21.8 1.8 %collective-permute-start.1 = (bf16[2,128,128]{2,1,0:T(8,128)(2,1)S(1)}, bf16[2,128,128]{2,1,0:T(8,128)(2,1)S(1)}, u32[]{:S(2)}, u32[]{:S(2)}) collective-permute-start(bf16[2,128,128]{2,1,0:T(8,128)(2,1)S(1)} %chip_total.1.after_ref.rest_0_), channel_id=1, source_target_pairs={{0,8},{8,16},{16,24},{24,0},{1,9},{9,17},{17,25},{25,1},{2,10},{10... | collective-permute-start | bytes 196616 | tf_op jit(solution)/shard_map/ppermute | solution.py:369
  23.6 2.9 %collective-permute-start.2 = (bf16[2,128,128]{2,1,0:T(8,128)(2,1)S(1)}, bf16[2,128,128]{2,1,0:T(8,128)(2,1)S(1)}, u32[]{:S(2)}, u32[]{:S(2)}) collective-permute-start(bf16[2,128,128]{2,1,0:T(8,128)(2,1)S(1)} %chip_total.1.after_ref.rest_0_), channel_id=1, source_target_pairs={{0,16},{8,24},{16,0},{24,8},{1,17},{9,25},{17,1},{25,9},{2,18},{10... | collective-permute-start | bytes 196616 | tf_op jit(solution)/shard_map/ppermute | solution.py:369
  26.5 1.3 %collective-permute-start.3 = (bf16[2,128,128]{2,1,0:T(8,128)(2,1)S(1)}, bf16[2,128,128]{2,1,0:T(8,128)(2,1)S(1)}, u32[]{:S(2)}, u32[]{:S(2)}) collective-permute-start(bf16[2,128,128]{2,1,0:T(8,128)(2,1)S(1)} %chip_total.1.after_ref.rest_0_), channel_id=1, source_target_pairs={{0,24},{8,0},{16,8},{24,16},{1,25},{9,1},{17,9},{25,17},{2,26},{10... | collective-permute-start | bytes 196616 | tf_op jit(solution)/shard_map/ppermute | solution.py:369
  27.8 2.9 %queries_side.2 = (f32[384,256]{1,0:T(8,128)S(1)}, bf16[384,256]{1,0:T(8,128)(2,1)S(1)}) custom-call(bf16[2,128,128]{2,1,0:T(8,128)(2,1)S(1)} %chip_total.1.after_ref.rest_0_, bf16[384,512]{1,0:T(8,128)(2,1)S(1)} %copy-done.1, bf16[12,128,256]{2,1,0:T(8,128)(2,1)S(1)} %get-tuple-element.25.d_ref, bf16[12,128,384]{2,1,0:T(8,128)(2,1)S(1)} %get-tuple-element.26.y_ref, ...), custom_call_target="tpu_custom_call" | custom-call | tf_op jit(solution)/shard_map/queries_side/pallas_call | solution.py:30
  30.7 0.0 collective-permute-done.1.rest_1_
  30.7 2.5 %collective-permute-done.2.rest_2_ = bf16[2,128,128]{2,1,0:T(8,128)(2,1)S(1)} collective-permute-done((bf16[2,128,128]{2,1,0:T(8,128)(2,1)S(1)}, bf16[2,128,128]{2,1,0:T(8,128)(2,1)S(1)}, u32[]{:S(2)}, u32[]{:S(2)}) %collective-permute-start.2) | collective-permute-done | bytes 65568 | tf_op jit(solution)/shard_map/ppermute | solution.py:369
  33.3 0.0 collective-permute-done.3.rest_3_
  33.3 1.2 line_total.1
  34.5 0.0 copy-start.2
  34.5 0.0 copy-start.5
  34.5 2.0 %collective-permute-start.4 = (bf16[2,128,128]{2,1,0:T(8,128)(2,1)S(1)}, bf16[2,128,128]{2,1,0:T(8,128)(2,1)S(1)}, u32[]{:S(2)}, u32[]{:S(2)}) collective-permute-start(bf16[2,128,128]{2,1,0:T(8,128)(2,1)S(1)} %get-tuple-element.31.after_ref), channel_id=1, source_target_pairs={{0,32},{32,64},{64,96},{96,0},{1,33},{33,65},{65,97},{97,1},{2,34}... | collective-permute-start | bytes 196616 | tf_op jit(solution)/shard_map/ppermute | solution.py:381
  36.5 3.6 %collective-permute-start.5 = (bf16[2,128,128]{2,1,0:T(8,128)(2,1)S(1)}, bf16[2,128,128]{2,1,0:T(8,128)(2,1)S(1)}, u32[]{:S(2)}, u32[]{:S(2)}) collective-permute-start(bf16[2,128,128]{2,1,0:T(8,128)(2,1)S(1)} %get-tuple-element.31.after_ref), channel_id=1, source_target_pairs={{0,64},{32,96},{64,0},{96,32},{1,65},{33,97},{65,1},{97,33},{2,66}... | collective-permute-start | bytes 196616 | tf_op jit(solution)/shard_map/ppermute | solution.py:381
  40.2 1.0 collective-permute-start.6
  41.2 2.9 %queries_side.3 = (f32[384,256]{1,0:T(8,128)S(1)}, bf16[384,256]{1,0:T(8,128)(2,1)S(1)}) custom-call(bf16[2,128,128]{2,1,0:T(8,128)(2,1)S(1)} %get-tuple-element.31.after_ref, bf16[384,512]{1,0:T(8,128)(2,1)S(1)} %copy-done.1, bf16[12,128,256]{2,1,0:T(8,128)(2,1)S(1)} %get-tuple-element.25.d_ref, bf16[12,128,384]{2,1,0:T(8,128)(2,1)S(1)} %get-tuple-element.26.y_ref, ...), custom_call_target="tpu_custom_call" | custom-call | tf_op jit(solution)/shard_map/queries_side/pallas_call | solution.py:30
  44.1 0.0 collective-permute-done.4.rest_0_
  44.1 0.0 collective-permute-done.5.rest_1_
  44.1 0.3 collective-permute-done.6.rest_2_
  44.4 1.4 %plane_state.1.mine_ref = bf16[2,128,128]{2,1,0:T(8,128)(2,1)S(1)} custom-call(s32[4]{0:T(128)S(1)} %pad_add_fusion.at_ref, bf16[384,256]{1,0:T(8,128)(2,1)S(1)} %get-tuple-element.33.after_ref.q1_ref, bf16[2,128,128]{2,1,0:T(8,128)(2,1)S(1)} %get-tuple-element.34.before_ref, bf16[2,128,128]{2,1,0:T(8,128)(2,1)S(1)} %collective-permute-done.4.rest_0_, ...), custom_call_target="tpu_custom_call" | custom-call | tf_op jit(solution)/shard_map/plane_state/pallas_call | solution.py:30
  45.9 0.1 collective-permute-start.7
  46.0 0.3 gates_side.1.gate_ref
  46.3 0.9 collective-permute-done.7.theirs_ref
  47.2 3.1 %mixed_and_projected.1 = bf16[4,96,2048]{2,1,0:T(8,128)(2,1)S(1)} custom-call(s32[4]{0:T(128)S(1)} %pad_add_fusion.at_ref, f32[384,256]{1,0:T(8,128)S(1)} %get-tuple-element.29.o0_ref, bf16[384,256]{1,0:T(8,128)(2,1)S(1)} %get-tuple-element.30.after_ref.q0_ref, f32[384,256]{1,0:T(8,128)S(1)} %get-tuple-element.32.o1_ref, ...), custom_call_target="tpu_custom_call" | custom-call | tf_op jit(solution)/shard_map/mixed_and_projected/pallas_call | solution.py:30
  50.3 0.0 copy-start.3
  50.3 0.0 copy-start.4
  50.3 25.3 %all_to_all.5.parts_ref = bf16[4,96,2048]{2,1,0:T(8,128)(2,1)S(1)} all-to-all(bf16[4,96,2048]{2,1,0:T(8,128)(2,1)S(1)} %mixed_and_projected.1), channel_id=1, replica_groups=mesh['sp_0'=4,'sp_1'=4,'sp_2'=2,'tp'=4] {'tp'}, dimensions={0} | all-to-all | bytes 3145728 | tf_op jit(solution)/shard_map/all_to_all | solution.py:603
  75.6 0.4 normed_rows.1
  76.1 0.6 collective-permute-start.8
  76.7 2.7 %collective-permute-start.9 = (bf16[96,2048]{1,0:T(8,128)(2,1)S(1)}, bf16[96,2048]{1,0:T(8,128)(2,1)S(1)}, u32[]{:S(2)}, u32[]{:S(2)}) collective-permute-start(bf16[96,2048]{1,0:T(8,128)(2,1)S(1)} %get-tuple-element.36.rest_0_), channel_id=1, source_target_pairs={{0,3},{1,0},{2,1},{3,2},{4,7},{5,4},{6,5},{7,6},{8,11},{9,8},{10,9... | collective-permute-start | bytes 1179656 | tf_op jit(solution)/shard_map/ppermute | solution.py:606
  79.4 7.8 %collective-permute-done.8.rest_1_ = bf16[96,2048]{1,0:T(8,128)(2,1)S(1)} collective-permute-done((bf16[96,2048]{1,0:T(8,128)(2,1)S(1)}, bf16[96,2048]{1,0:T(8,128)(2,1)S(1)}, u32[]{:S(2)}, u32[]{:S(2)}) %collective-permute-start.8) | collective-permute-done | bytes 393248 | tf_op jit(solution)/shard_map/ppermute | solution.py:605
  87.2 0.1 collective-permute-start.12
  87.3 3.3 %collective-permute-start.13 = (bf16[48,2048]{1,0:T(8,128)(2,1)S(1)}, bf16[48,2048]{1,0:T(8,128)(2,1)S(1)}, u32[]{:S(2)}, u32[]{:S(2)}) collective-permute-start(bf16[48,2048]{1,0:T(8,128)(2,1)S(1)} %slice.9), channel_id=1, source_target_pairs={{0,3},{1,0},{2,1},{3,2},{4,7},{5,4},{6,5},{7,6},{8,11},{9,8},{10,9... | collective-permute-start | bytes 589832 | tf_op jit(solution)/shard_map/ppermute | solution.py:610
  90.6 14.7 %first_channels.1 = (bf16[96,2048]{1,0:T(8,128)(2,1)S(1)}, bf16[96,2048]{1,0:T(8,128)(2,1)S(1)}, bf16[96,2048]{1,0:T(8,128)(2,1)S(1)}, bf16[2048,1408]{1,0:T(8,1...) custom-call(bf16[2048,4224]{1,0:T(8,128)(2,1)} %all-gather.2.cloned.1.call-done.w_ref, ...), custom_call_target="tpu_custom_call" | custom-call | tf_op jit(solution)/shard_map/first_channels/pallas_call | solution.py:30
  105.3 0.1 collective-permute-start.10
  105.4 2.0 %collective-permute-start.11 = (bf16[96,2048]{1,0:T(8,128)(2,1)S(1)}, bf16[96,2048]{1,0:T(8,128)(2,1)S(1)}, u32[]{:S(2)}, u32[]{:S(2)}) collective-permute-start(bf16[96,2048]{1,0:T(8,128)(2,1)S(1)} %get-tuple-element.39), channel_id=1, source_target_pairs={{0,1},{1,2},{2,3},{3,0},{4,5},{5,6},{6,7},{7,4},{8,9},{9,10},{10,1... | collective-permute-start | bytes 1179656 | tf_op jit(solution)/shard_map/ppermute | solution.py:613
  107.4 0.0 collective-permute-done.12.upper_ref
  107.4 4.0 %more_channels.1 = bf16[96,2048]{1,0:T(8,128)(2,1)S(1)} custom-call(bf16[48,2048]{1,0:T(8,128)(2,1)S(1)} %collective-permute-done.12.upper_ref, bf16[48,2048]{1,0:T(8,128)(2,1)S(1)} %collective-permute-done.13.lower_ref, bf16[2048,1408]{1,0:T(8,128)(2,1)S(1)} %get-tuple-element.40.gate_ref, bf16[2048,1408]{1,0:T(8,128)(2,1)S(1)} %get-tuple-element.41.up_ref, ...), custom_call_target="tpu_custom_call" | custom-call | tf_op jit(solution)/shard_map/more_channels/pallas_call | solution.py:30
  111.4 0.2 collective-permute-start.14
  111.5 10.9 %collective-permute-done.10.rest_1_ = bf16[96,2048]{1,0:T(8,128)(2,1)S(1)} collective-permute-done((bf16[96,2048]{1,0:T(8,128)(2,1)S(1)}, bf16[96,2048]{1,0:T(8,128)(2,1)S(1)}, u32[]{:S(2)}, u32[]{:S(2)}) %collective-permute-start.10) | collective-permute-done | bytes 393248 | tf_op jit(solution)/shard_map/ppermute | solution.py:613
  122.4 3.4 %collective-permute-done.11.rest_2_ = bf16[96,2048]{1,0:T(8,128)(2,1)S(1)} collective-permute-done((bf16[96,2048]{1,0:T(8,128)(2,1)S(1)}, bf16[96,2048]{1,0:T(8,128)(2,1)S(1)}, u32[]{:S(2)}, u32[]{:S(2)}) %collective-permute-start.11) | collective-permute-done | bytes 393248 | tf_op jit(solution)/shard_map/ppermute | solution.py:613
  125.8 0.0 collective-permute-done.14.rest_3_
  125.8 1.0 last_sum.1
  (14 shorter events, 0.1 us)
Async XLA Ops:
  6.5 21.3 %copy-start.1 = (bf16[384,512]{1,0:T(8,128)(2,1)S(1)}, bf16[384,512]{1,0:T(8,128)(2,1)}, u32[]{:S(2)}) copy-start(bf16[384,512]{1,0:T(8,128)(2,1)} %q_ref.3) | copy-start | bytes 1179652
  6.5 84.0 %all-gather.2.cloned.1.call-start = ((), (), s32[]{:S(2)}) async-start(), calls=%async_computation.1 | async-start | bytes 17842176 | tf_op jit(solution)/shard_map/all_gather | solution.py:590
  18.8 1.8 %collective-permute-start = (bf16[4,128,128]{2,1,0:T(8,128)(2,1)}, bf16[4,128,128]{2,1,0:T(8,128)(2,1)}, u32[]{:S(2)}, u32[]{:S(2)}) collective-permute-start(bf16[4,128,128]{2,1,0:T(8,128)(2,1)} %get-tuple-element.24.own_ref), channel_id=1, source_target_pairs={{0,4},{4,0},{1,5},{5,1},{2,6},{6,2},{3,7},{7,3},{8,12},{12,8},{9,1... | collective-permute-start | bytes 393224 | tf_op jit(solution)/shard_map/ppermute | solution.py:366
  21.8 8.9 %collective-permute-start.1 = (bf16[2,128,128]{2,1,0:T(8,128)(2,1)S(1)}, bf16[2,128,128]{2,1,0:T(8,128)(2,1)S(1)}, u32[]{:S(2)}, u32[]{:S(2)}) collective-permute-start(bf16[2,128,128]{2,1,0:T(8,128)(2,1)S(1)} %chip_total.1.after_ref.rest_0_), channel_id=1, source_target_pairs={{0,8},{8,16},{16,24},{24,0},{1,9},{9,17},{17,25},{25,1},{2,10},{10... | collective-permute-start | bytes 196616 | tf_op jit(solution)/shard_map/ppermute | solution.py:369
  23.6 9.7 %collective-permute-start.2 = (bf16[2,128,128]{2,1,0:T(8,128)(2,1)S(1)}, bf16[2,128,128]{2,1,0:T(8,128)(2,1)S(1)}, u32[]{:S(2)}, u32[]{:S(2)}) collective-permute-start(bf16[2,128,128]{2,1,0:T(8,128)(2,1)S(1)} %chip_total.1.after_ref.rest_0_), channel_id=1, source_target_pairs={{0,16},{8,24},{16,0},{24,8},{1,17},{9,25},{17,1},{25,9},{2,18},{10... | collective-permute-start | bytes 196616 | tf_op jit(solution)/shard_map/ppermute | solution.py:369
  26.5 6.8 %collective-permute-start.3 = (bf16[2,128,128]{2,1,0:T(8,128)(2,1)S(1)}, bf16[2,128,128]{2,1,0:T(8,128)(2,1)S(1)}, u32[]{:S(2)}, u32[]{:S(2)}) collective-permute-start(bf16[2,128,128]{2,1,0:T(8,128)(2,1)S(1)} %chip_total.1.after_ref.rest_0_), channel_id=1, source_target_pairs={{0,24},{8,0},{16,8},{24,16},{1,25},{9,1},{17,9},{25,17},{2,26},{10... | collective-permute-start | bytes 196616 | tf_op jit(solution)/shard_map/ppermute | solution.py:369
  34.5 11.5 %copy-start.2 = (bf16[384,512]{1,0:T(8,128)(2,1)S(1)}, bf16[384,512]{1,0:T(8,128)(2,1)}, u32[]{:S(2)}) copy-start(bf16[384,512]{1,0:T(8,128)(2,1)} %gates_ref.1) | copy-start | bytes 1179652
  34.5 11.5 %copy-start.5 = (f32[64]{0:T(128)S(1)}, f32[64]{0:T(128)}, u32[]{:S(2)}) copy-start(f32[64]{0:T(128)} %param.19) | copy-start | bytes 772
  34.5 9.6 %collective-permute-start.4 = (bf16[2,128,128]{2,1,0:T(8,128)(2,1)S(1)}, bf16[2,128,128]{2,1,0:T(8,128)(2,1)S(1)}, u32[]{:S(2)}, u32[]{:S(2)}) collective-permute-start(bf16[2,128,128]{2,1,0:T(8,128)(2,1)S(1)} %get-tuple-element.31.after_ref), channel_id=1, source_target_pairs={{0,32},{32,64},{64,96},{96,0},{1,33},{33,65},{65,97},{97,1},{2,34}... | collective-permute-start | bytes 196616 | tf_op jit(solution)/shard_map/ppermute | solution.py:381
  36.5 7.6 %collective-permute-start.5 = (bf16[2,128,128]{2,1,0:T(8,128)(2,1)S(1)}, bf16[2,128,128]{2,1,0:T(8,128)(2,1)S(1)}, u32[]{:S(2)}, u32[]{:S(2)}) collective-permute-start(bf16[2,128,128]{2,1,0:T(8,128)(2,1)S(1)} %get-tuple-element.31.after_ref), channel_id=1, source_target_pairs={{0,64},{32,96},{64,0},{96,32},{1,65},{33,97},{65,1},{97,33},{2,66}... | collective-permute-start | bytes 196616 | tf_op jit(solution)/shard_map/ppermute | solution.py:381
  40.2 4.3 %collective-permute-start.6 = (bf16[2,128,128]{2,1,0:T(8,128)(2,1)S(1)}, bf16[2,128,128]{2,1,0:T(8,128)(2,1)S(1)}, u32[]{:S(2)}, u32[]{:S(2)}) collective-permute-start(bf16[2,128,128]{2,1,0:T(8,128)(2,1)S(1)} %get-tuple-element.31.after_ref), channel_id=1, source_target_pairs={{0,96},{32,0},{64,32},{96,64},{1,97},{33,1},{65,33},{97,65},{2,98}... | collective-permute-start | bytes 196616 | tf_op jit(solution)/shard_map/ppermute | solution.py:381
  41.1 6.1 %copy-start = (bf16[512,2048]{1,0:T(8,128)(2,1)S(1)}, bf16[512,2048]{1,0:T(8,128)(2,1)}, u32[]{:S(2)}) copy-start(bf16[512,2048]{1,0:T(8,128)(2,1)} %w_ref.1) | copy-start | bytes 6291460
  45.9 1.3 collective-permute-start.7
  50.3 25.3 %copy-start.3 = (bf16[96,2048]{1,0:T(8,128)(2,1)S(1)}, bf16[96,2048]{1,0:T(8,128)(2,1)}, u32[]{:S(2)}) copy-start(bf16[96,2048]{1,0:T(8,128)(2,1)} %stream_ref.1) | copy-start | bytes 1179652
  50.3 25.3 %copy-start.4 = (f32[2048]{0:T(1024)S(1)}, f32[2048]{0:T(1024)}, u32[]{:S(2)}) copy-start(f32[2048]{0:T(1024)} %param.22) | copy-start | bytes 24580
  76.1 11.1 %collective-permute-start.8 = (bf16[96,2048]{1,0:T(8,128)(2,1)S(1)}, bf16[96,2048]{1,0:T(8,128)(2,1)S(1)}, u32[]{:S(2)}, u32[]{:S(2)}) collective-permute-start(bf16[96,2048]{1,0:T(8,128)(2,1)S(1)} %get-tuple-element.36.rest_0_), channel_id=1, source_target_pairs={{0,1},{1,2},{2,3},{3,0},{4,5},{5,6},{6,7},{7,4},{8,9},{9,10},{10,1... | collective-permute-start | bytes 1179656 | tf_op jit(solution)/shard_map/ppermute | solution.py:605
  76.7 10.5 %collective-permute-start.9 = (bf16[96,2048]{1,0:T(8,128)(2,1)S(1)}, bf16[96,2048]{1,0:T(8,128)(2,1)S(1)}, u32[]{:S(2)}, u32[]{:S(2)}) collective-permute-start(bf16[96,2048]{1,0:T(8,128)(2,1)S(1)} %get-tuple-element.36.rest_0_), channel_id=1, source_target_pairs={{0,3},{1,0},{2,1},{3,2},{4,7},{5,4},{6,5},{7,6},{8,11},{9,8},{10,9... | collective-permute-start | bytes 1179656 | tf_op jit(solution)/shard_map/ppermute | solution.py:606
  87.2 20.2 %collective-permute-start.12 = (bf16[48,2048]{1,0:T(8,128)(2,1)S(1)}, bf16[48,2048]{1,0:T(8,128)(2,1)S(1)}, u32[]{:S(2)}, u32[]{:S(2)}) collective-permute-start(bf16[48,2048]{1,0:T(8,128)(2,1)S(1)} %slice.8), channel_id=1, source_target_pairs={{0,1},{1,2},{2,3},{3,0},{4,5},{5,6},{6,7},{7,4},{8,9},{9,10},{10,1... | collective-permute-start | bytes 589832 | tf_op jit(solution)/shard_map/ppermute | solution.py:609
  87.3 20.1 %collective-permute-start.13 = (bf16[48,2048]{1,0:T(8,128)(2,1)S(1)}, bf16[48,2048]{1,0:T(8,128)(2,1)S(1)}, u32[]{:S(2)}, u32[]{:S(2)}) collective-permute-start(bf16[48,2048]{1,0:T(8,128)(2,1)S(1)} %slice.9), channel_id=1, source_target_pairs={{0,3},{1,0},{2,1},{3,2},{4,7},{5,4},{6,5},{7,6},{8,11},{9,8},{10,9... | collective-permute-start | bytes 589832 | tf_op jit(solution)/shard_map/ppermute | solution.py:610
  105.3 17.1 %collective-permute-start.10 = (bf16[96,2048]{1,0:T(8,128)(2,1)S(1)}, bf16[96,2048]{1,0:T(8,128)(2,1)S(1)}, u32[]{:S(2)}, u32[]{:S(2)}) collective-permute-start(bf16[96,2048]{1,0:T(8,128)(2,1)S(1)} %get-tuple-element.38), channel_id=1, source_target_pairs={{0,3},{1,0},{2,1},{3,2},{4,7},{5,4},{6,5},{7,6},{8,11},{9,8},{10,9... | collective-permute-start | bytes 1179656 | tf_op jit(solution)/shard_map/ppermute | solution.py:613
  105.4 20.4 %collective-permute-start.11 = (bf16[96,2048]{1,0:T(8,128)(2,1)S(1)}, bf16[96,2048]{1,0:T(8,128)(2,1)S(1)}, u32[]{:S(2)}, u32[]{:S(2)}) collective-permute-start(bf16[96,2048]{1,0:T(8,128)(2,1)S(1)} %get-tuple-element.39), channel_id=1, source_target_pairs={{0,1},{1,2},{2,3},{3,0},{4,5},{5,6},{6,7},{7,4},{8,9},{9,10},{10,1... | collective-permute-start | bytes 1179656 | tf_op jit(solution)/shard_map/ppermute | solution.py:613
  111.4 14.4 %collective-permute-start.14 = (bf16[96,2048]{1,0:T(8,128)(2,1)S(1)}, bf16[96,2048]{1,0:T(8,128)(2,1)S(1)}, u32[]{:S(2)}, u32[]{:S(2)}) collective-permute-start(bf16[96,2048]{1,0:T(8,128)(2,1)S(1)} %more_channels.1), channel_id=1, source_target_pairs={{0,2},{1,3},{2,0},{3,1},{4,6},{5,7},{6,4},{7,5},{8,10},{9,11},{10,... | collective-permute-start | bytes 1179656 | tf_op jit(solution)/shard_map/ppermute | solution.py:615
Sparse Core Ops, SparseCore 0:
  9.6 78.0 all-gather.1

commit v6 on v5

--- a/solution.py
+++ b/solution.py
@@ -7,6 +7,7 @@
 from jax.experimental.pallas import tpu as pltpu
 from jax.sharding import Mesh
 from jax.sharding import PartitionSpec as P
+
 
 HEAD_DIM = 64
 PAIR = 2 * HEAD_DIM
@@ -24,7 +25,7 @@
 TABLE = pl.BlockSpec(memory_space=pltpu.SMEM)
 
 
-def call(kernel, name, arrays, shapes, scratch=(), table=None, far=(), mib=16):
+def call(kernel, arrays, shapes, scratch=(), table=None, far=(), mib=16):
     near = [pltpu.with_memory_space_constraint(x, pltpu.VMEM) for x in arrays]
     tables = [] if table is None else [table]
     return pl.pallas_call(
@@ -34,7 +35,6 @@
         out_shape=[pltpu.VMEM(shape, dtype) for shape, dtype in shapes],
         scratch_shapes=scratch,
         compiler_params=pltpu.CompilerParams(vmem_limit_bytes=mib << 20),
-        name=name,
     )(*tables, *far, *near)
 
 
@@ -221,7 +221,6 @@
     wide = pltpu.VMEM((items, CHUNK, 2 * CHUNK), BF)
     return call(
         keys_kernel,
-        "keys_side",
         [],
         [
             ((items, PAIR, PAIR), BF),
@@ -291,9 +290,7 @@
 
 
 def gates_side(gates, gain):
-    return call(
-        gates_kernel, "gates_side", [gates, gain.reshape(1, HEAD_DIM)], [(gates.shape, F32)]
-    )[0]
+    return call(gates_kernel, [gates, gain.reshape(1, HEAD_DIM)], [(gates.shape, F32)])[0]
 
 
 def queries_side(first, after, queries, decay, solved, before, grown):
@@ -301,7 +298,6 @@
     shape = (length, width // 2)
     return call(
         functools.partial(queries_kernel, first),
-        "queries_side",
         [queries, decay, solved, before, grown],
         [(shape, F32), (shape, BF)],
         far=[after],
@@ -364,13 +360,12 @@
     swap = [(0, 1), (1, 0)]
     half = (total.shape[0] // 2, PAIR, PAIR)
     other = lax.ppermute(total, core, swap)
-    (chip,) = call(chip_kernel, "chip_total", [total, other], [(half, BF)], table=at)
+    (chip,) = call(chip_kernel, [total, other], [(half, BF)], table=at)
     size = lax.axis_size(line)
     lines = [chip] + [lax.ppermute(chip, line, ring(size, k)) for k in range(1, size)]
     early = meanwhile(chip)
     whole, before = call(
         row_kernel,
-        "line_total",
         lines,
         [(half, BF), (half, BF)],
         [pltpu.VMEM((size, *half), BF)],
@@ -380,9 +375,7 @@
     size = lax.axis_size(plane)
     planes = [lax.ppermute(whole, plane, ring(size, k)) for k in range(1, size)]
     late = then(whole)
-    (state,) = call(
-        plane_kernel, "plane_state", [before] + planes, [(half, BF)], table=at, far=[late[1]]
-    )
+    (state,) = call(plane_kernel, [before] + planes, [(half, BF)], table=at, far=[late[1]])
     return early, late, (other, state, lax.ppermute(state, core, swap))
 
 
@@ -390,7 +383,7 @@
     at_ref, o0_ref, q0_ref, o1_ref, q1_ref,
     first_ref, mine_ref, theirs_ref, gate_ref, w_ref, *rest,
 ):
-    out_ref, mixed_ref, state_ref = rest
+    out_refs, (mixed_ref, state_ref) = rest[:-2], rest[-2:]
     row, col = places()
     same = (col < HEAD_DIM) == (row < HEAD_DIM)
     ones = jnp.where(same, 1.0, 0.0).astype(BF)
@@ -410,30 +403,30 @@
         mean = half_sums(out * out, ones) * (1.0 / HEAD_DIM)
         out = out * lax.rsqrt(mean + EPSILON) * gate_ref[:, lanes]
         mixed_ref[:, lanes] = out.astype(BF)
-    for n in range(w_ref.shape[1] // STRIP):
-        here = slice(n * STRIP, (n + 1) * STRIP)
-        got = dot(mixed_ref[...], w_ref[:, here]).astype(BF)
-        block = out_ref.shape[1]
-        for k in range(out_ref.shape[0]):
-            out_ref[k, :, here] = got[k * block : (k + 1) * block, :]
+    size = len(out_refs)
+    block = length // size
+    for k, out_ref in enumerate(out_refs):
+        start = lax.rem(at_ref[0] + k, size) * block
+        rows = mixed_ref[pl.ds(pl.multiple_of(start, 32), block), :]
+        out_ref[...] = dot(rows, w_ref[...]).astype(out_ref.dtype)
 
 
 def mixed_and_projected(at, size, early, late, states, gate, w_out):
     length, width = gate.shape
     return call(
         mixed_kernel,
-        "mixed_and_projected",
         [*early, *late, *states, gate, w_out],
-        [((size, length // size, w_out.shape[1]), BF)],
+        [((length // size, w_out.shape[1]), BF if k else F32) for k in range(size)],
         [pltpu.VMEM((length, width), BF), pltpu.VMEM((width // PAIR, PAIR, PAIR), BF)],
         table=at,
-    )[0]
-
-
-def norm_kernel(stream_ref, gain_ref, parts_ref, middle_ref, normed_ref):
-    projected = parts_ref[0].astype(F32)
-    for k in range(1, parts_ref.shape[0]):
-        projected = projected + parts_ref[k].astype(F32)
+    )
+
+
+def norm_kernel(stream_ref, gain_ref, *rest):
+    parts, (middle_ref, normed_ref) = rest[:-2], rest[-2:]
+    projected = parts[0][...]
+    for part in parts[1:]:
+        projected = projected + part[...].astype(F32)
     middle = (stream_ref[...].astype(F32) + projected).astype(BF)
     middle_ref[...] = middle
     middle = middle.astype(F32)
@@ -443,10 +436,7 @@
 
 def normed_rows(stream, gain, parts):
     return call(
-        norm_kernel,
-        "normed_rows",
-        [stream, gain.reshape(1, -1), parts],
-        [(stream.shape, BF), (stream.shape, BF)],
+        norm_kernel, [stream, gain.reshape(1, -1), *parts], [(stream.shape, BF), (stream.shape, BF)]
     )
 
 
@@ -463,7 +453,9 @@
 
 TILE = 128
 STRIP = 256
-AHEAD = 4
+AHEAD = 3
+UP_GROUPS = (1, 2, 4, 4)
+DOWN_GROUPS = (8,)
 
 
 def first_channels_kernel(count, w_ref, *rest):
@@ -471,18 +463,22 @@
     gate_ref, up_ref, down_ref, rows_ref, hidden_ref, in_sems, down_sems = rest[2 * count :]
     width, hidden = gate_ref.shape
     block = parts[0].shape[0]
-    groups = []
-    for j in range(hidden // TILE):
-        here = pl.ds(j * TILE, TILE)
+    groups, spans = [], []
+    for many, spread in ((hidden // TILE, UP_GROUPS), (width // STRIP, DOWN_GROUPS)):
+        assert sum(spread) == many
+        starts = [sum(spread[:k]) for k in range(len(spread))]
+        spans.append([range(start, start + n) for start, n in zip(starts, spread)])
+    for g, tiles in enumerate(spans[0]):
+        here = pl.ds(tiles[0] * TILE, len(tiles) * TILE)
         group = []
         for k, ref in enumerate((gate_ref, up_ref)):
-            from_ref = w_ref.at[:, pl.ds(k * hidden + j * TILE, TILE)]
-            group.append(pltpu.make_async_copy(from_ref, ref.at[:, here], in_sems.at[k, j]))
+            from_ref = w_ref.at[:, pl.ds(k * hidden + tiles[0] * TILE, len(tiles) * TILE)]
+            group.append(pltpu.make_async_copy(from_ref, ref.at[:, here], in_sems.at[k, g]))
         groups.append(group)
-    for n in range(width // STRIP):
-        here = pl.ds(n * STRIP, STRIP)
+    for g, strips in enumerate(spans[1]):
+        here = pl.ds(strips[0] * STRIP, len(strips) * STRIP)
         from_ref = w_ref.at[here, pl.ds(2 * hidden, hidden)]
-        groups.append([pltpu.make_async_copy(from_ref, down_ref.at[here, :], down_sems.at[n])])
+        groups.append([pltpu.make_async_copy(from_ref, down_ref.at[here, :], down_sems.at[g])])
 
     def begin(g):
         if g < len(groups):
@@ -498,16 +494,18 @@
         begin(g)
     for k, part in enumerate(parts):
         rows_ref[k * block : (k + 1) * block, :] = part[...]
-    for j in range(hidden // TILE):
-        arrived(j)
-        here = slice(j * TILE, (j + 1) * TILE)
-        hidden_ref[:, here] = activated(rows_ref[...], gate_ref[:, here], up_ref[:, here])
-    for n in range(width // STRIP):
-        arrived(hidden // TILE + n)
-        here = slice(n * STRIP, (n + 1) * STRIP)
-        got = product_nt(hidden_ref[...], down_ref[here, :])
-        for k, out_ref in enumerate(out_refs):
-            out_ref[:, here] = got[k * block : (k + 1) * block, :].astype(BF)
+    for g, tiles in enumerate(spans[0]):
+        arrived(g)
+        for j in tiles:
+            here = slice(j * TILE, (j + 1) * TILE)
+            hidden_ref[:, here] = activated(rows_ref[...], gate_ref[:, here], up_ref[:, here])
+    for g, strips in enumerate(spans[1]):
+        arrived(len(spans[0]) + g)
+        for n in strips:
+            here = slice(n * STRIP, (n + 1) * STRIP)
+            got = product_nt(hidden_ref[...], down_ref[here, :])
+            for k, out_ref in enumerate(out_refs):
+                out_ref[:, here] = got[k * block : (k + 1) * block, :].astype(BF)
 
 
 def first_channels(weights, parts, hidden):
@@ -515,39 +513,41 @@
     count = len(parts)
     out = call(
         functools.partial(first_channels_kernel, count),
-        "first_channels",
         parts,
         [((block, width), BF)] * count + [((width, hidden), BF)] * 3,
         [
             pltpu.VMEM((block * count, width), BF),
             pltpu.VMEM((block * count, hidden), BF),
-            pltpu.SemaphoreType.DMA((2, hidden // TILE)),
-            pltpu.SemaphoreType.DMA((width // STRIP,)),
+            pltpu.SemaphoreType.DMA((2, len(UP_GROUPS))),
+            pltpu.SemaphoreType.DMA((len(DOWN_GROUPS),)),
         ],
         far=[pltpu.with_memory_space_constraint(weights, pltpu.HBM)],
     )
     return out[:count], out[count:]
 
 
-def more_channels_kernel(upper_ref, lower_ref, gate_ref, up_ref, down_ref, out_ref, hidden_ref):
-    rows = jnp.concatenate([upper_ref[...], lower_ref[...]], axis=0)
+def more_channels_kernel(own_ref, upper_ref, lower_ref, gate_ref, up_ref, down_ref, *rest):
+    out_refs, hidden_ref = rest[:-1], rest[-1]
+    block = own_ref.shape[0]
+    rows = jnp.concatenate([own_ref[...], upper_ref[...], lower_ref[...]], axis=0)
     for j in range(gate_ref.shape[1] // TILE):
         here = slice(j * TILE, (j + 1) * TILE)
         hidden_ref[:, here] = activated(rows, gate_ref[:, here], up_ref[:, here])
     for n in range(down_ref.shape[0] // STRIP):
         here = slice(n * STRIP, (n + 1) * STRIP)
-        out_ref[:, here] = product_nt(hidden_ref[...], down_ref[here, :]).astype(BF)
-
-
-def more_channels(halves_of_rows, projections):
-    half, width = halves_of_rows[0].shape
+        got = product_nt(hidden_ref[...], down_ref[here, :])
+        for k, out_ref in enumerate(out_refs):
+            out_ref[:, here] = got[k * block : (k + 1) * block, :].astype(BF)
+
+
+def more_channels(rows, projections):
+    block, width = rows[0].shape
     return call(
         more_channels_kernel,
-        "more_channels",
-        [*halves_of_rows, *projections],
-        [((2 * half, width), BF)],
-        [pltpu.VMEM((2 * half, projections[0].shape[1]), BF)],
-    )[0]
+        [*rows, *projections],
+        [((block, width), BF)] * 2,
+        [pltpu.VMEM((2 * block, projections[0].shape[1]), BF)],
+    )
 
 
 def last_kernel(middle_ref, *rest):
@@ -600,7 +600,7 @@
         lambda x: queries_side(pairs // 2, x, queries, decay, solved, before, grown),
     )
     parts = mixed_and_projected(at, size, early, late, states, gate, w_out)
-    parts = lax.all_to_all(parts, "tp", 0, 0, tiled=True)
+    parts = [parts[0]] + [lax.ppermute(parts[k], "tp", ring(size, k)) for k in (2, 1, 3)]
     middle, normed = normed_rows(stream, norm_gain, parts)
     right = lax.ppermute(normed, "tp", ring(size, 1))
     left = lax.ppermute(normed, "tp", ring(size, -1))
@@ -609,11 +609,12 @@
         lax.ppermute(right[:half], "tp", ring(size, 1)),
         lax.ppermute(left[half:], "tp", ring(size, -1)),
     ]
-    sums, projections = first_channels(weights, [normed, right, left], hidden)
-    back = [lax.ppermute(sums[1], "tp", ring(size, -1)), lax.ppermute(sums[2], "tp", ring(size, 1))]
-    last = more_channels(across, projections)
+    sums, projections = first_channels(weights, [right, left], hidden)
+    back = [lax.ppermute(sums[0], "tp", ring(size, -1))]
+    back.append(lax.ppermute(sums[1], "tp", ring(size, 1)))
+    own, last = more_channels([normed, *across], projections)
     back.append(lax.ppermute(last, "tp", ring(size, 2)))
-    return last_sum(middle, [sums[0]] + back)
+    return last_sum(middle, [own] + back)
 
 
 def solution(mesh):

time: 134 us -> 133 us (level)
  blocking collectives: 25.3 us -> 0 us
  waiting for transfers between devices: 27.5 us -> 51.3 us
  Pallas kernels: 43.4 us -> 38.6 us
  starting transfers between devices: 21.8 us -> 26.2 us
    all_to_all x1 -> x0, blocking collectives: 25.3 us -> none  [per_device(): parts = lax.all_to_all(parts, 'tp', 0, 0, tiled=True)]
    ppermute x1, waiting for transfers between devices: 0.01 us -> 11.4 us  [per_device(): back.append(lax.ppermute(last, 'tp', ring(size, 2)))]
    ppermute x2 -> x5, waiting for transfers between devices: 14.3 us -> 25.3 us  [the longest x3 19.1 us: per_device(): lax.ppermute(parts[k], 'tp', ring(size, k))]
    pallas_call x11, Pallas kernels: 42.4 us -> 37.5 us  [call(): pl.pallas_call(kernel, in_specs=[TABLE] * len(tables) + [FAR] * len(far)...]
    ppermute x2 -> x5, starting transfers between devices: 2.09 us -> 6.61 us  [the longest x3 4.52 us: per_device(): lax.ppermute(parts[k], 'tp', ring(size, k))]
    ppermute x1, waiting for transfers between devices: 7.77 us -> 9.12 us  [per_device(): right = lax.ppermute(normed, 'tp', ring(size, 1))]
  transfers between devices with their start and end apart: 16 -> 19, of which waited for: 7 -> 10; matrix products, arithmetic and copies ran while one was open for 0% -> 0% of each run, Pallas kernels for 32% -> 25%
where the time goes in v6:
time: 133 us; the launch traced here: 132 us
  waiting for transfers between devices  51.3 us (39%)
  Pallas kernels  38.6 us (29%)
  starting transfers between devices  26.2 us (20%)
  between operations  13.6 us (10%)
  other arithmetic  2.07 us (2%)
    pallas_call x11, Pallas kernels, call(): pl.pallas_call(kernel, in_specs=[TABLE] * len(tables) + [FAR] * len(far)...  37.5 us
    ppermute x3, waiting for transfers between devices, per_device(): lax.ppermute(parts[k], 'tp', ring(size, k))  19.1 us
    ppermute x1, waiting for transfers between devices, per_device(): back.append(lax.ppermute(last, 'tp', ring(size, 2)))  11.4 us
    ppermute x1, waiting for transfers between devices, per_device(): right = lax.ppermute(normed, 'tp', ring(size, 1))  9.12 us
    ppermute x3, starting transfers between devices, state_ahead(): planes = [lax.ppermute(whole, plane, ring(size, k)) for k in range(1, size)]  6.65 us
    ppermute x3, starting transfers between devices, state_ahead(): lax.ppermute(chip, line, ring(size, k))  6.01 us
    ppermute x3, starting transfers between devices, per_device(): lax.ppermute(parts[k], 'tp', ring(size, k))  4.52 us
    ppermute x1, waiting for transfers between devices, per_device(): back = [lax.ppermute(sums[0], 'tp', ring(size, -1))]  4.44 us
  transfers between devices with their start and end apart: 19, of which 10 were waited for; matrix products, arithmetic and copies ran while one was open for 0% of the time, Pallas kernels for 25%

profile of v6, /device:TPU:0, one launch (start us, length us, event | category | flops | bytes accessed | tf_op | source)
XLA Modules:
  0.0 131.8 jit_solution(11425250840245026182)
XLA Ops:
  6.5 2.0 %pad_maximum_fusion = bf16[64,4224]{1,0:T(8,128)(2,1)} fusion(bf16[64,1408]{1,0:T(8,128)(2,1)} %bitcast.9, bf16[64,1408]{1,0:T(8,128)(2,1)} %param.24, bf16[64,1408]{1,0:T(8,128)(2,1)} %param.23), kind=kLoop, calls=%fused_computation | loop fusion | flops 1622016 | bytes 1081344 | tf_op jit(solution)/shard_map/concatenate | solution.py:589
  8.5 0.0 all-gather.2.cloned.1.call-update
  8.6 10.2 %shard_map.127 = (bf16[12,128,128]{2,1,0:T(8,128)(2,1)S(1)}, bf16[4,128,128]{2,1,0:T(8,128)(2,1)}, bf16[12,128,384]{2,1,0:T(8,128)(2,1)S(1)}, bf16[12,128,256]{2,1,0:T(8,128)(2,1)S(1)}, f32[384,512]{1,0:T(8,128)S(1)}) custom-call(bf16[384,512]{1,0:T(8,128)(2,1)} %k_far_ref.1, bf16[384,512]{1,0:T(8,128)(2,1)} %v_far_ref.1, f32[8,384]{1,0:T(8,128)} %beta_far_ref.1, ...), custom_call_target="tpu_custom_call" | custom-call | tf_op jit(solution)/shard_map/pallas_call | solution.py:31
  18.8 0.1 collective-permute-start
  18.9 0.1 pad_add_fusion.at_ref
  19.0 1.6 %collective-permute-done.other_ref.first_ref = bf16[4,128,128]{2,1,0:T(8,128)(2,1)} collective-permute-done((bf16[4,128,128]{2,1,0:T(8,128)(2,1)}, bf16[4,128,128]{2,1,0:T(8,128)(2,1)}, u32[]{:S(2)}, u32[]{:S(2)}) %collective-permute-start) | collective-permute-done | bytes 131104 | tf_op jit(solution)/shard_map/ppermute | solution.py:362
  20.6 1.2 shard_map.128.after_ref.rest_0_
  21.8 1.8 %collective-permute-start.1 = (bf16[2,128,128]{2,1,0:T(8,128)(2,1)S(1)}, bf16[2,128,128]{2,1,0:T(8,128)(2,1)S(1)}, u32[]{:S(2)}, u32[]{:S(2)}) collective-permute-start(bf16[2,128,128]{2,1,0:T(8,128)(2,1)S(1)} %shard_map.128.after_ref.rest_0_), channel_id=1, source_target_pairs={{0,8},{8,16},{16,24},{24,0},{1,9},{9,17},{17,25},{25,1},{2,10},{10... | collective-permute-start | bytes 196616 | tf_op jit(solution)/shard_map/ppermute | solution.py:365
  23.5 2.9 %collective-permute-start.2 = (bf16[2,128,128]{2,1,0:T(8,128)(2,1)S(1)}, bf16[2,128,128]{2,1,0:T(8,128)(2,1)S(1)}, u32[]{:S(2)}, u32[]{:S(2)}) collective-permute-start(bf16[2,128,128]{2,1,0:T(8,128)(2,1)S(1)} %shard_map.128.after_ref.rest_0_), channel_id=1, source_target_pairs={{0,16},{8,24},{16,0},{24,8},{1,17},{9,25},{17,1},{25,9},{2,18},{10... | collective-permute-start | bytes 196616 | tf_op jit(solution)/shard_map/ppermute | solution.py:365
  26.5 1.3 %collective-permute-start.3 = (bf16[2,128,128]{2,1,0:T(8,128)(2,1)S(1)}, bf16[2,128,128]{2,1,0:T(8,128)(2,1)S(1)}, u32[]{:S(2)}, u32[]{:S(2)}) collective-permute-start(bf16[2,128,128]{2,1,0:T(8,128)(2,1)S(1)} %shard_map.128.after_ref.rest_0_), channel_id=1, source_target_pairs={{0,24},{8,0},{16,8},{24,16},{1,25},{9,1},{17,9},{25,17},{2,26},{10... | collective-permute-start | bytes 196616 | tf_op jit(solution)/shard_map/ppermute | solution.py:365
  27.8 2.9 %shard_map.129 = (f32[384,256]{1,0:T(8,128)S(1)}, bf16[384,256]{1,0:T(8,128)(2,1)S(1)}) custom-call(bf16[2,128,128]{2,1,0:T(8,128)(2,1)S(1)} %shard_map.128.after_ref.rest_0_, bf16[384,512]{1,0:T(8,128)(2,1)S(1)} %copy-done.1, bf16[12,128,256]{2,1,0:T(8,128)(2,1)S(1)} %get-tuple-element.30.d_ref, bf16[12,128,384]{2,1,0:T(8,128)(2,1)S(1)} %get-tuple-element.31.y_ref, ...), custom_call_target="tpu_custom_call" | custom-call | tf_op jit(solution)/shard_map/pallas_call | solution.py:31
  30.7 0.0 collective-permute-done.1.rest_1_
  30.7 2.5 %collective-permute-done.2.rest_2_ = bf16[2,128,128]{2,1,0:T(8,128)(2,1)S(1)} collective-permute-done((bf16[2,128,128]{2,1,0:T(8,128)(2,1)S(1)}, bf16[2,128,128]{2,1,0:T(8,128)(2,1)S(1)}, u32[]{:S(2)}, u32[]{:S(2)}) %collective-permute-start.2) | collective-permute-done | bytes 65568 | tf_op jit(solution)/shard_map/ppermute | solution.py:365
  33.3 1.2 shard_map.130
  34.5 0.0 copy-start.3
  34.5 0.0 copy-start.5
  34.5 2.0 %collective-permute-start.4 = (bf16[2,128,128]{2,1,0:T(8,128)(2,1)S(1)}, bf16[2,128,128]{2,1,0:T(8,128)(2,1)S(1)}, u32[]{:S(2)}, u32[]{:S(2)}) collective-permute-start(bf16[2,128,128]{2,1,0:T(8,128)(2,1)S(1)} %get-tuple-element.36.after_ref), channel_id=1, source_target_pairs={{0,32},{32,64},{64,96},{96,0},{1,33},{33,65},{65,97},{97,1},{2,34}... | collective-permute-start | bytes 196616 | tf_op jit(solution)/shard_map/ppermute | solution.py:376
  36.5 3.6 %collective-permute-start.5 = (bf16[2,128,128]{2,1,0:T(8,128)(2,1)S(1)}, bf16[2,128,128]{2,1,0:T(8,128)(2,1)S(1)}, u32[]{:S(2)}, u32[]{:S(2)}) collective-permute-start(bf16[2,128,128]{2,1,0:T(8,128)(2,1)S(1)} %get-tuple-element.36.after_ref), channel_id=1, source_target_pairs={{0,64},{32,96},{64,0},{96,32},{1,65},{33,97},{65,1},{97,33},{2,66}... | collective-permute-start | bytes 196616 | tf_op jit(solution)/shard_map/ppermute | solution.py:376
  40.2 1.0 collective-permute-start.6
  41.2 2.9 %shard_map.131 = (f32[384,256]{1,0:T(8,128)S(1)}, bf16[384,256]{1,0:T(8,128)(2,1)S(1)}) custom-call(bf16[2,128,128]{2,1,0:T(8,128)(2,1)S(1)} %get-tuple-element.36.after_ref, bf16[384,512]{1,0:T(8,128)(2,1)S(1)} %copy-done.1, bf16[12,128,256]{2,1,0:T(8,128)(2,1)S(1)} %get-tuple-element.30.d_ref, bf16[12,128,384]{2,1,0:T(8,128)(2,1)S(1)} %get-tuple-element.31.y_ref, ...), custom_call_target="tpu_custom_call" | custom-call | tf_op jit(solution)/shard_map/pallas_call | solution.py:31
  44.1 0.0 collective-permute-done.4.rest_0_
  44.1 0.3 collective-permute-done.6.rest_2_
  44.4 1.4 %shard_map.132.mine_ref = bf16[2,128,128]{2,1,0:T(8,128)(2,1)S(1)} custom-call(s32[4]{0:T(128)S(1)} %pad_add_fusion.at_ref, bf16[384,256]{1,0:T(8,128)(2,1)S(1)} %get-tuple-element.38.after_ref.q1_ref, bf16[2,128,128]{2,1,0:T(8,128)(2,1)S(1)} %get-tuple-element.39.before_ref, bf16[2,128,128]{2,1,0:T(8,128)(2,1)S(1)} %collective-permute-done.4.rest_0_, ...), custom_call_target="tpu_custom_call" | custom-call | tf_op jit(solution)/shard_map/pallas_call | solution.py:31
  45.9 0.1 collective-permute-start.7
  46.0 0.3 shard_map.133.gate_ref
  46.3 0.9 collective-permute-done.7.theirs_ref
  47.2 3.8 %shard_map.134 = (f32[96,2048]{1,0:T(8,128)S(1)}, bf16[96,2048]{1,0:T(8,128)(2,1)S(1)}, bf16[96,2048]{1,0:T(8,128)(2,1)S(1)}, bf16[96,2048]{1,0:T(8,128)(2,1)S(1)}) custom-call(s32[4]{0:T(128)S(1)} %pad_add_fusion.at_ref, f32[384,256]{1,0:T(8,128)S(1)} %get-tuple-element.34.o0_ref, bf16[384,256]{1,0:T(8,128)(2,1)S(1)} %get-tuple-element.35.after_ref.q0_ref, ...), custom_call_target="tpu_custom_call" | custom-call | tf_op jit(solution)/shard_map/pallas_call | solution.py:31
  51.0 2.8 %collective-permute-start.10 = (bf16[96,2048]{1,0:T(8,128)(2,1)S(1)}, bf16[96,2048]{1,0:T(8,128)(2,1)S(1)}, u32[]{:S(2)}, u32[]{:S(2)}) collective-permute-start(bf16[96,2048]{1,0:T(8,128)(2,1)S(1)} %get-tuple-element.43), channel_id=1, source_target_pairs={{0,3},{1,0},{2,1},{3,2},{4,7},{5,4},{6,5},{7,6},{8,11},{9,8},{10,9... | collective-permute-start | bytes 1179656 | tf_op jit(solution)/shard_map/ppermute | solution.py:603
  53.8 0.8 collective-permute-start.8
  54.6 0.9 collective-permute-start.9
  55.5 15.5 %collective-permute-done.10.rest_3_ = bf16[96,2048]{1,0:T(8,128)(2,1)S(1)} collective-permute-done((bf16[96,2048]{1,0:T(8,128)(2,1)S(1)}, bf16[96,2048]{1,0:T(8,128)(2,1)S(1)}, u32[]{:S(2)}, u32[]{:S(2)}) %collective-permute-start.10) | collective-permute-done | bytes 393248 | tf_op jit(solution)/shard_map/ppermute | solution.py:603
  71.0 3.7 %collective-permute-done.9.rest_2_ = bf16[96,2048]{1,0:T(8,128)(2,1)S(1)} collective-permute-done((bf16[96,2048]{1,0:T(8,128)(2,1)S(1)}, bf16[96,2048]{1,0:T(8,128)(2,1)S(1)}, u32[]{:S(2)}, u32[]{:S(2)}) %collective-permute-start.9) | collective-permute-done | bytes 393248 | tf_op jit(solution)/shard_map/ppermute | solution.py:603
  74.7 0.4 shard_map.135
  75.1 0.1 collective-permute-start.11
  75.2 3.2 %collective-permute-start.13 = (bf16[96,2048]{1,0:T(8,128)(2,1)S(1)}, bf16[96,2048]{1,0:T(8,128)(2,1)S(1)}, u32[]{:S(2)}, u32[]{:S(2)}) collective-permute-start(bf16[96,2048]{1,0:T(8,128)(2,1)S(1)} %get-tuple-element.45.own_ref), channel_id=1, source_target_pairs={{0,3},{1,0},{2,1},{3,2},{4,7},{5,4},{6,5},{7,6},{8,11},{9,8},{10,9... | collective-permute-start | bytes 1179656 | tf_op jit(solution)/shard_map/ppermute | solution.py:606
  78.4 9.1 %collective-permute-done.11.rest_0_ = bf16[96,2048]{1,0:T(8,128)(2,1)S(1)} collective-permute-done((bf16[96,2048]{1,0:T(8,128)(2,1)S(1)}, bf16[96,2048]{1,0:T(8,128)(2,1)S(1)}, u32[]{:S(2)}, u32[]{:S(2)}) %collective-permute-start.11) | collective-permute-done | bytes 393248 | tf_op jit(solution)/shard_map/ppermute | solution.py:605
  87.5 0.1 collective-permute-start.12
  87.6 0.0 collective-permute-done.13.rest_1_
  87.7 3.3 %collective-permute-start.14 = (bf16[48,2048]{1,0:T(8,128)(2,1)S(1)}, bf16[48,2048]{1,0:T(8,128)(2,1)S(1)}, u32[]{:S(2)}, u32[]{:S(2)}) collective-permute-start(bf16[48,2048]{1,0:T(8,128)(2,1)S(1)} %slice.9), channel_id=1, source_target_pairs={{0,3},{1,0},{2,1},{3,2},{4,7},{5,4},{6,5},{7,6},{8,11},{9,8},{10,9... | collective-permute-start | bytes 589832 | tf_op jit(solution)/shard_map/ppermute | solution.py:610
  90.9 8.5 %shard_map.136 = (bf16[96,2048]{1,0:T(8,128)(2,1)S(1)}, bf16[96,2048]{1,0:T(8,128)(2,1)S(1)}, bf16[2048,1408]{1,0:T(8,128)(2,1)S(1)}, bf16[2048,1408]{1,0:T(8,128)(2,1)S(1)}, bf16[2048,1408]{1,0:T(8,128)(2,1)S(1)}) custom-call(bf16[2048,4224]{1,0:T(8,128)(2,1)} %all-gather.2.cloned.1.call-done.w_ref, bf16[96,2048]{1,0:T(8,128)(2,1)S(1)} %collective-permute-done.11.rest_0_, ...), custom_call_target="tpu_custom_call" | custom-call | tf_op jit(solution)/shard_map/pallas_call | solution.py:31
  99.4 4.7 %shard_map.137 = (bf16[96,2048]{1,0:T(8,128)(2,1)S(1)}, bf16[96,2048]{1,0:T(8,128)(2,1)S(1)}) custom-call(bf16[96,2048]{1,0:T(8,128)(2,1)S(1)} %get-tuple-element.45.own_ref, bf16[48,2048]{1,0:T(8,128)(2,1)S(1)} %collective-permute-done.12.upper_ref, bf16[48,2048]{1,0:T(8,128)(2,1)S(1)} %collective-permute-done.14.lower_ref, ...), custom_call_target="tpu_custom_call" | custom-call | tf_op jit(solution)/shard_map/pallas_call | solution.py:31
  104.2 0.1 collective-permute-start.17
  104.2 1.5 %collective-permute-start.15 = (bf16[96,2048]{1,0:T(8,128)(2,1)S(1)}, bf16[96,2048]{1,0:T(8,128)(2,1)S(1)}, u32[]{:S(2)}, u32[]{:S(2)}) collective-permute-start(bf16[96,2048]{1,0:T(8,128)(2,1)S(1)} %get-tuple-element.50), channel_id=1, source_target_pairs={{0,3},{1,0},{2,1},{3,2},{4,7},{5,4},{6,5},{7,6},{8,11},{9,8},{10,9... | collective-permute-start | bytes 1179656 | tf_op jit(solution)/shard_map/ppermute | solution.py:613
  105.7 0.6 collective-permute-start.16
  106.3 11.4 %collective-permute-done.17.rest_3_ = bf16[96,2048]{1,0:T(8,128)(2,1)S(1)} collective-permute-done((bf16[96,2048]{1,0:T(8,128)(2,1)S(1)}, bf16[96,2048]{1,0:T(8,128)(2,1)S(1)}, u32[]{:S(2)}, u32[]{:S(2)}) %collective-permute-start.17) | collective-permute-done | bytes 393248 | tf_op jit(solution)/shard_map/ppermute | solution.py:616
  117.8 4.4 %collective-permute-done.15.rest_1_ = bf16[96,2048]{1,0:T(8,128)(2,1)S(1)} collective-permute-done((bf16[96,2048]{1,0:T(8,128)(2,1)S(1)}, bf16[96,2048]{1,0:T(8,128)(2,1)S(1)}, u32[]{:S(2)}, u32[]{:S(2)}) %collective-permute-start.15) | collective-permute-done | bytes 393248 | tf_op jit(solution)/shard_map/ppermute | solution.py:613
  122.2 1.7 %collective-permute-done.16.rest_2_ = bf16[96,2048]{1,0:T(8,128)(2,1)S(1)} collective-permute-done((bf16[96,2048]{1,0:T(8,128)(2,1)S(1)}, bf16[96,2048]{1,0:T(8,128)(2,1)S(1)}, u32[]{:S(2)}, u32[]{:S(2)}) %collective-permute-start.16) | collective-permute-done | bytes 393248 | tf_op jit(solution)/shard_map/ppermute | solution.py:614
  123.9 1.0 last_sum.1
  (19 shorter events, 0.1 us)
Async XLA Ops:
  6.5 84.4 %all-gather.2.cloned.1.call-start = ((), (), s32[]{:S(2)}) async-start(), calls=%async_computation | async-start | bytes 17842176 | tf_op jit(solution)/shard_map/all_gather | solution.py:590
  6.5 21.3 %copy-start.1 = (bf16[384,512]{1,0:T(8,128)(2,1)S(1)}, bf16[384,512]{1,0:T(8,128)(2,1)}, u32[]{:S(2)}) copy-start(bf16[384,512]{1,0:T(8,128)(2,1)} %q_ref.3) | copy-start | bytes 1179652
  18.8 1.8 %collective-permute-start = (bf16[4,128,128]{2,1,0:T(8,128)(2,1)}, bf16[4,128,128]{2,1,0:T(8,128)(2,1)}, u32[]{:S(2)}, u32[]{:S(2)}) collective-permute-start(bf16[4,128,128]{2,1,0:T(8,128)(2,1)} %get-tuple-element.29.own_ref), channel_id=1, source_target_pairs={{0,4},{4,0},{1,5},{5,1},{2,6},{6,2},{3,7},{7,3},{8,12},{12,8},{9,1... | collective-permute-start | bytes 393224 | tf_op jit(solution)/shard_map/ppermute | solution.py:362
  21.8 8.9 %collective-permute-start.1 = (bf16[2,128,128]{2,1,0:T(8,128)(2,1)S(1)}, bf16[2,128,128]{2,1,0:T(8,128)(2,1)S(1)}, u32[]{:S(2)}, u32[]{:S(2)}) collective-permute-start(bf16[2,128,128]{2,1,0:T(8,128)(2,1)S(1)} %shard_map.128.after_ref.rest_0_), channel_id=1, source_target_pairs={{0,8},{8,16},{16,24},{24,0},{1,9},{9,17},{17,25},{25,1},{2,10},{10... | collective-permute-start | bytes 196616 | tf_op jit(solution)/shard_map/ppermute | solution.py:365
  23.5 9.7 %collective-permute-start.2 = (bf16[2,128,128]{2,1,0:T(8,128)(2,1)S(1)}, bf16[2,128,128]{2,1,0:T(8,128)(2,1)S(1)}, u32[]{:S(2)}, u32[]{:S(2)}) collective-permute-start(bf16[2,128,128]{2,1,0:T(8,128)(2,1)S(1)} %shard_map.128.after_ref.rest_0_), channel_id=1, source_target_pairs={{0,16},{8,24},{16,0},{24,8},{1,17},{9,25},{17,1},{25,9},{2,18},{10... | collective-permute-start | bytes 196616 | tf_op jit(solution)/shard_map/ppermute | solution.py:365
  26.5 6.8 %collective-permute-start.3 = (bf16[2,128,128]{2,1,0:T(8,128)(2,1)S(1)}, bf16[2,128,128]{2,1,0:T(8,128)(2,1)S(1)}, u32[]{:S(2)}, u32[]{:S(2)}) collective-permute-start(bf16[2,128,128]{2,1,0:T(8,128)(2,1)S(1)} %shard_map.128.after_ref.rest_0_), channel_id=1, source_target_pairs={{0,24},{8,0},{16,8},{24,16},{1,25},{9,1},{17,9},{25,17},{2,26},{10... | collective-permute-start | bytes 196616 | tf_op jit(solution)/shard_map/ppermute | solution.py:365
  34.5 11.5 %copy-start.3 = (bf16[384,512]{1,0:T(8,128)(2,1)S(1)}, bf16[384,512]{1,0:T(8,128)(2,1)}, u32[]{:S(2)}) copy-start(bf16[384,512]{1,0:T(8,128)(2,1)} %gates_ref.1) | copy-start | bytes 1179652
  34.5 11.5 %copy-start.5 = (f32[64]{0:T(128)S(1)}, f32[64]{0:T(128)}, u32[]{:S(2)}) copy-start(f32[64]{0:T(128)} %param.19) | copy-start | bytes 772
  34.5 9.6 %collective-permute-start.4 = (bf16[2,128,128]{2,1,0:T(8,128)(2,1)S(1)}, bf16[2,128,128]{2,1,0:T(8,128)(2,1)S(1)}, u32[]{:S(2)}, u32[]{:S(2)}) collective-permute-start(bf16[2,128,128]{2,1,0:T(8,128)(2,1)S(1)} %get-tuple-element.36.after_ref), channel_id=1, source_target_pairs={{0,32},{32,64},{64,96},{96,0},{1,33},{33,65},{65,97},{97,1},{2,34}... | collective-permute-start | bytes 196616 | tf_op jit(solution)/shard_map/ppermute | solution.py:376
  36.5 7.6 %collective-permute-start.5 = (bf16[2,128,128]{2,1,0:T(8,128)(2,1)S(1)}, bf16[2,128,128]{2,1,0:T(8,128)(2,1)S(1)}, u32[]{:S(2)}, u32[]{:S(2)}) collective-permute-start(bf16[2,128,128]{2,1,0:T(8,128)(2,1)S(1)} %get-tuple-element.36.after_ref), channel_id=1, source_target_pairs={{0,64},{32,96},{64,0},{96,32},{1,65},{33,97},{65,1},{97,33},{2,66}... | collective-permute-start | bytes 196616 | tf_op jit(solution)/shard_map/ppermute | solution.py:376
  40.2 4.3 %collective-permute-start.6 = (bf16[2,128,128]{2,1,0:T(8,128)(2,1)S(1)}, bf16[2,128,128]{2,1,0:T(8,128)(2,1)S(1)}, u32[]{:S(2)}, u32[]{:S(2)}) collective-permute-start(bf16[2,128,128]{2,1,0:T(8,128)(2,1)S(1)} %get-tuple-element.36.after_ref), channel_id=1, source_target_pairs={{0,96},{32,0},{64,32},{96,64},{1,97},{33,1},{65,33},{97,65},{2,98}... | collective-permute-start | bytes 196616 | tf_op jit(solution)/shard_map/ppermute | solution.py:376
  41.1 6.1 %copy-start = (bf16[512,2048]{1,0:T(8,128)(2,1)S(1)}, bf16[512,2048]{1,0:T(8,128)(2,1)}, u32[]{:S(2)}) copy-start(bf16[512,2048]{1,0:T(8,128)(2,1)} %w_ref.1) | copy-start | bytes 6291460
  45.9 1.3 %collective-permute-start.7 = (bf16[2,128,128]{2,1,0:T(8,128)(2,1)S(1)}, bf16[2,128,128]{2,1,0:T(8,128)(2,1)S(1)}, u32[]{:S(2)}, u32[]{:S(2)}) collective-permute-start(bf16[2,128,128]{2,1,0:T(8,128)(2,1)S(1)} %shard_map.132.mine_ref), channel_id=1, source_target_pairs={{0,4},{4,0},{1,5},{5,1},{2,6},{6,2},{3,7},{7,3},{8,12},{12,8},{9,1... | collective-permute-start | bytes 196616 | tf_op jit(solution)/shard_map/ppermute | solution.py:379
  47.2 27.5 %copy-start.2 = (bf16[96,2048]{1,0:T(8,128)(2,1)S(1)}, bf16[96,2048]{1,0:T(8,128)(2,1)}, u32[]{:S(2)}) copy-start(bf16[96,2048]{1,0:T(8,128)(2,1)} %stream_ref.1) | copy-start | bytes 1179652
  47.2 27.5 %copy-start.4 = (f32[2048]{0:T(1024)S(1)}, f32[2048]{0:T(1024)}, u32[]{:S(2)}) copy-start(f32[2048]{0:T(1024)} %param.22) | copy-start | bytes 24580
  51.0 20.0 %collective-permute-start.10 = (bf16[96,2048]{1,0:T(8,128)(2,1)S(1)}, bf16[96,2048]{1,0:T(8,128)(2,1)S(1)}, u32[]{:S(2)}, u32[]{:S(2)}) collective-permute-start(bf16[96,2048]{1,0:T(8,128)(2,1)S(1)} %get-tuple-element.43), channel_id=1, source_target_pairs={{0,3},{1,0},{2,1},{3,2},{4,7},{5,4},{6,5},{7,6},{8,11},{9,8},{10,9... | collective-permute-start | bytes 1179656 | tf_op jit(solution)/shard_map/ppermute | solution.py:603
  53.8 17.2 %collective-permute-start.8 = (bf16[96,2048]{1,0:T(8,128)(2,1)S(1)}, bf16[96,2048]{1,0:T(8,128)(2,1)S(1)}, u32[]{:S(2)}, u32[]{:S(2)}) collective-permute-start(bf16[96,2048]{1,0:T(8,128)(2,1)S(1)} %get-tuple-element.41), channel_id=1, source_target_pairs={{0,2},{1,3},{2,0},{3,1},{4,6},{5,7},{6,4},{7,5},{8,10},{9,11},{10,... | collective-permute-start | bytes 1179656 | tf_op jit(solution)/shard_map/ppermute | solution.py:603
  54.6 20.0 %collective-permute-start.9 = (bf16[96,2048]{1,0:T(8,128)(2,1)S(1)}, bf16[96,2048]{1,0:T(8,128)(2,1)S(1)}, u32[]{:S(2)}, u32[]{:S(2)}) collective-permute-start(bf16[96,2048]{1,0:T(8,128)(2,1)S(1)} %get-tuple-element.42), channel_id=1, source_target_pairs={{0,1},{1,2},{2,3},{3,0},{4,5},{5,6},{6,7},{7,4},{8,9},{9,10},{10,1... | collective-permute-start | bytes 1179656 | tf_op jit(solution)/shard_map/ppermute | solution.py:603
  75.1 12.4 %collective-permute-start.11 = (bf16[96,2048]{1,0:T(8,128)(2,1)S(1)}, bf16[96,2048]{1,0:T(8,128)(2,1)S(1)}, u32[]{:S(2)}, u32[]{:S(2)}) collective-permute-start(bf16[96,2048]{1,0:T(8,128)(2,1)S(1)} %get-tuple-element.45.own_ref), channel_id=1, source_target_pairs={{0,1},{1,2},{2,3},{3,0},{4,5},{5,6},{6,7},{7,4},{8,9},{9,10},{10,1... | collective-permute-start | bytes 1179656 | tf_op jit(solution)/shard_map/ppermute | solution.py:605
  75.2 12.4 %collective-permute-start.13 = (bf16[96,2048]{1,0:T(8,128)(2,1)S(1)}, bf16[96,2048]{1,0:T(8,128)(2,1)S(1)}, u32[]{:S(2)}, u32[]{:S(2)}) collective-permute-start(bf16[96,2048]{1,0:T(8,128)(2,1)S(1)} %get-tuple-element.45.own_ref), channel_id=1, source_target_pairs={{0,3},{1,0},{2,1},{3,2},{4,7},{5,4},{6,5},{7,6},{8,11},{9,8},{10,9... | collective-permute-start | bytes 1179656 | tf_op jit(solution)/shard_map/ppermute | solution.py:606
  87.5 11.9 %collective-permute-start.12 = (bf16[48,2048]{1,0:T(8,128)(2,1)S(1)}, bf16[48,2048]{1,0:T(8,128)(2,1)S(1)}, u32[]{:S(2)}, u32[]{:S(2)}) collective-permute-start(bf16[48,2048]{1,0:T(8,128)(2,1)S(1)} %slice.8), channel_id=1, source_target_pairs={{0,1},{1,2},{2,3},{3,0},{4,5},{5,6},{6,7},{7,4},{8,9},{9,10},{10,1... | collective-permute-start | bytes 589832 | tf_op jit(solution)/shard_map/ppermute | solution.py:609
  87.7 11.8 %collective-permute-start.14 = (bf16[48,2048]{1,0:T(8,128)(2,1)S(1)}, bf16[48,2048]{1,0:T(8,128)(2,1)S(1)}, u32[]{:S(2)}, u32[]{:S(2)}) collective-permute-start(bf16[48,2048]{1,0:T(8,128)(2,1)S(1)} %slice.9), channel_id=1, source_target_pairs={{0,3},{1,0},{2,1},{3,2},{4,7},{5,4},{6,5},{7,6},{8,11},{9,8},{10,9... | collective-permute-start | bytes 589832 | tf_op jit(solution)/shard_map/ppermute | solution.py:610
  104.2 13.6 %collective-permute-start.17 = (bf16[96,2048]{1,0:T(8,128)(2,1)S(1)}, bf16[96,2048]{1,0:T(8,128)(2,1)S(1)}, u32[]{:S(2)}, u32[]{:S(2)}) collective-permute-start(bf16[96,2048]{1,0:T(8,128)(2,1)S(1)} %get-tuple-element.52), channel_id=1, source_target_pairs={{0,2},{1,3},{2,0},{3,1},{4,6},{5,7},{6,4},{7,5},{8,10},{9,11},{10,... | collective-permute-start | bytes 1179656 | tf_op jit(solution)/shard_map/ppermute | solution.py:616
  104.2 18.0 %collective-permute-start.15 = (bf16[96,2048]{1,0:T(8,128)(2,1)S(1)}, bf16[96,2048]{1,0:T(8,128)(2,1)S(1)}, u32[]{:S(2)}, u32[]{:S(2)}) collective-permute-start(bf16[96,2048]{1,0:T(8,128)(2,1)S(1)} %get-tuple-element.50), channel_id=1, source_target_pairs={{0,3},{1,0},{2,1},{3,2},{4,7},{5,4},{6,5},{7,6},{8,11},{9,8},{10,9... | collective-permute-start | bytes 1179656 | tf_op jit(solution)/shard_map/ppermute | solution.py:613
  105.7 18.2 %collective-permute-start.16 = (bf16[96,2048]{1,0:T(8,128)(2,1)S(1)}, bf16[96,2048]{1,0:T(8,128)(2,1)S(1)}, u32[]{:S(2)}, u32[]{:S(2)}) collective-permute-start(bf16[96,2048]{1,0:T(8,128)(2,1)S(1)} %get-tuple-element.51), channel_id=1, source_target_pairs={{0,1},{1,2},{2,3},{3,0},{4,5},{5,6},{6,7},{7,4},{8,9},{9,10},{10,1... | collective-permute-start | bytes 1179656 | tf_op jit(solution)/shard_map/ppermute | solution.py:614
Sparse Core Ops, SparseCore 0:
  9.6 78.0 all-gather.1

commit v7 on v6

--- a/solution.py
+++ b/solution.py
@@ -22,20 +22,18 @@
 
 FULL = pl.BlockSpec(memory_space=pltpu.VMEM)
 FAR = pl.BlockSpec(memory_space=pl.ANY)
-TABLE = pl.BlockSpec(memory_space=pltpu.SMEM)
-
-
-def call(kernel, arrays, shapes, scratch=(), table=None, far=(), mib=16):
+
+
+def call(kernel, arrays, shapes, scratch=(), far=(), mib=16):
     near = [pltpu.with_memory_space_constraint(x, pltpu.VMEM) for x in arrays]
-    tables = [] if table is None else [table]
     return pl.pallas_call(
         kernel,
-        in_specs=[TABLE] * len(tables) + [FAR] * len(far) + [FULL] * len(near),
+        in_specs=[FAR] * len(far) + [FULL] * len(near),
         out_specs=[FULL] * len(shapes),
         out_shape=[pltpu.VMEM(shape, dtype) for shape, dtype in shapes],
         scratch_shapes=scratch,
         compiler_params=pltpu.CompilerParams(vmem_limit_bytes=mib << 20),
-    )(*tables, *far, *near)
+    )(*far, *near)
 
 
 def ring(size, k):
@@ -92,6 +90,33 @@
 
 def halves(x):
     return x[:, :CHUNK], x[:, CHUNK:]
+
+
+def packing_kernel(*rest):
+    from_refs, packed_ref, sems = rest[:-2], rest[-2], rest[-1]
+    hidden = from_refs[0].shape[1]
+    copies = []
+    for k, ref in enumerate(from_refs):
+        here = packed_ref.at[:, pl.ds(k * hidden, hidden)]
+        copies.append(pltpu.make_async_copy(ref, here, sems.at[k]))
+    for copy in copies:
+        copy.start()
+    for copy in copies:
+        copy.wait()
+
+
+def packed(weights):
+    rows, hidden = weights[0].shape
+    far = [pltpu.with_memory_space_constraint(x, pltpu.HBM) for x in weights]
+    return pl.pallas_call(
+        packing_kernel,
+        in_specs=[FAR] * len(far),
+        out_specs=FAR,
+        out_shape=pltpu.HBM((rows, len(weights) * hidden), BF),
+        scratch_shapes=[pltpu.SemaphoreType.DMA((len(far),))],
+        compiler_params=pltpu.CompilerParams(vmem_limit_bytes=16 << 20),
+        name="packed",
+    )(*far)
 
 
 def keys_kernel(
@@ -129,7 +154,7 @@
     def stacked(x):
         return jnp.concatenate([x[:, c * CHUNK : (c + 1) * CHUNK] for c in range(steps)], axis=0)
 
-    for copy in rate_copies:
+    for copy in rate_copies + row_copies:
         copy.wait()
     rates = split_three(stacked(-softplus(decay_ref[...])))
     strength = split_three(stacked(1.0 / (1.0 + jnp.exp(-beta_ref[...]))))
@@ -144,8 +169,6 @@
     ends = []
     for c in range(steps):
         rows = slice(c * CHUNK, (c + 1) * CHUNK)
-        row_copies[2 * c].wait()
-        row_copies[2 * c + 1].wait()
         for p in range(pairs):
             lanes = slice(p * PAIR, (p + 1) * PAIR)
             item = c * pairs + p
@@ -181,7 +204,7 @@
 
     items = steps * pairs
 
-    def level(power, carry):
+    for power in range(1, 7):
         mask = jnp.where((differ >> power) == 1, 1.0, 0.0).astype(BF)
         parts = []
         for i in range(items):
@@ -190,9 +213,6 @@
         for i in range(items):
             x = x_ref[i]
             x_ref[i] = x - dot(parts[i], side_by_side(halves(x))).astype(BF)
-        return carry
-
-    lax.fori_loop(1, 7, level, 0)
 
     runs = [None] * pairs
     for c in range(steps):
@@ -310,10 +330,11 @@
     return dot(step, earlier.astype(BF)) + jnp.where(same, later, 0.0)
 
 
-def chip_kernel(at_ref, own_ref, other_ref, out_ref):
+def chip_kernel(own_ref, other_ref, out_ref, kept_ref):
+    kept_ref[...] = other_ref[...]
     row, col = places()
     same = (col < HEAD_DIM) == (row < HEAD_DIM)
-    core = at_ref[1]
+    core = lax.axis_index(SP[2])
     count = out_ref.shape[0]
     for p in range(count):
         mine = own_ref[core * count + p]
@@ -323,11 +344,11 @@
         out_ref[p] = chained(first, second, same).astype(BF)
 
 
-def row_kernel(at_ref, after_ref, *rest):
+def row_kernel(after_ref, *rest):
     parts, (total_ref, before_ref, all_ref) = rest[:-3], rest[-3:]
     row, col = places()
     same = (col < HEAD_DIM) == (row < HEAD_DIM)
-    place = at_ref[2]
+    place = lax.axis_index(SP[1])
     size = len(parts)
     for k, part in enumerate(parts):
         all_ref[lax.rem(place - k + size, size)] = part[...]
@@ -341,11 +362,11 @@
         total_ref[p] = run.astype(BF)
 
 
-def plane_kernel(at_ref, after_ref, before_ref, *rest):
+def plane_kernel(after_ref, before_ref, *rest):
     parts, out_ref = rest[:-1], rest[-1]
     row, col = places()
     same = (col < HEAD_DIM) == (row < HEAD_DIM)
-    place = at_ref[3]
+    place = lax.axis_index(SP[0])
     for p in range(out_ref.shape[0]):
         state = jnp.zeros((PAIR, PAIR), F32)
         for k in range(len(parts), 0, -1):
@@ -355,32 +376,27 @@
         out_ref[p] = jnp.where(same, state, 0.0).astype(BF)
 
 
-def state_ahead(at, total, meanwhile, then):
+def state_ahead(total, meanwhile, then):
     plane, line, core = SP
     swap = [(0, 1), (1, 0)]
     half = (total.shape[0] // 2, PAIR, PAIR)
     other = lax.ppermute(total, core, swap)
-    (chip,) = call(chip_kernel, [total, other], [(half, BF)], table=at)
+    chip, other = call(chip_kernel, [total, other], [(half, BF), (total.shape, BF)])
     size = lax.axis_size(line)
     lines = [chip] + [lax.ppermute(chip, line, ring(size, k)) for k in range(1, size)]
     early = meanwhile(chip)
     whole, before = call(
-        row_kernel,
-        lines,
-        [(half, BF), (half, BF)],
-        [pltpu.VMEM((size, *half), BF)],
-        table=at,
-        far=[early[1]],
+        row_kernel, lines, [(half, BF), (half, BF)], [pltpu.VMEM((size, *half), BF)], far=[early[1]]
     )
     size = lax.axis_size(plane)
     planes = [lax.ppermute(whole, plane, ring(size, k)) for k in range(1, size)]
     late = then(whole)
-    (state,) = call(plane_kernel, [before] + planes, [(half, BF)], table=at, far=[late[1]])
+    (state,) = call(plane_kernel, [before] + planes, [(half, BF)], far=[late[1]])
     return early, late, (other, state, lax.ppermute(state, core, swap))
 
 
 def mixed_kernel(
-    at_ref, o0_ref, q0_ref, o1_ref, q1_ref,
+    o0_ref, q0_ref, o1_ref, q1_ref,
     first_ref, mine_ref, theirs_ref, gate_ref, w_ref, *rest,
 ):
     out_refs, (mixed_ref, state_ref) = rest[:-2], rest[-2:]
@@ -388,7 +404,10 @@
     same = (col < HEAD_DIM) == (row < HEAD_DIM)
     ones = jnp.where(same, 1.0, 0.0).astype(BF)
     length, width = gate_ref.shape
-    core = at_ref[1]
+    size = len(out_refs)
+    block = length // size
+    core = lax.axis_index(SP[2])
+    turn = lax.axis_index("tp")
     half = mine_ref.shape[0]
     state_ref[pl.ds(core * half, half)] = mine_ref[...]
     state_ref[pl.ds((1 - core) * half, half)] = theirs_ref[...]
@@ -401,24 +420,24 @@
         place = slice((p % half) * PAIR, (p % half + 1) * PAIR)
         out = o_ref[:, place] + dot(q_ref[:, place], state)
         mean = half_sums(out * out, ones) * (1.0 / HEAD_DIM)
-        out = out * lax.rsqrt(mean + EPSILON) * gate_ref[:, lanes]
-        mixed_ref[:, lanes] = out.astype(BF)
-    size = len(out_refs)
-    block = length // size
-    for k, out_ref in enumerate(out_refs):
-        start = lax.rem(at_ref[0] + k, size) * block
-        rows = mixed_ref[pl.ds(pl.multiple_of(start, 32), block), :]
-        out_ref[...] = dot(rows, w_ref[...]).astype(out_ref.dtype)
-
-
-def mixed_and_projected(at, size, early, late, states, gate, w_out):
+        out = (out * lax.rsqrt(mean + EPSILON) * gate_ref[:, lanes]).astype(BF)
+        for k in range(size):
+            start = pl.multiple_of(lax.rem(k - turn + size, size) * block, 32)
+            mixed_ref[pl.ds(start, block), lanes] = out[k * block : (k + 1) * block, :]
+    for n in range(w_ref.shape[1] // STRIP):
+        here = slice(n * STRIP, (n + 1) * STRIP)
+        got = dot(mixed_ref[...], w_ref[:, here])
+        for k, out_ref in enumerate(out_refs):
+            out_ref[:, here] = got[k * block : (k + 1) * block, :].astype(out_ref.dtype)
+
+
+def mixed_and_projected(size, early, late, states, gate, w_out):
     length, width = gate.shape
     return call(
         mixed_kernel,
         [*early, *late, *states, gate, w_out],
         [((length // size, w_out.shape[1]), BF if k else F32) for k in range(size)],
         [pltpu.VMEM((length, width), BF), pltpu.VMEM((width // PAIR, PAIR, PAIR), BF)],
-        table=at,
     )
 
 
@@ -586,21 +605,19 @@
     w_down,
 ):
     hidden = w_gate.shape[1]
-    weights = jnp.concatenate([w_gate, w_up, w_down.T], axis=1)
+    weights = packed([w_gate, w_up, w_down.T])
     weights = lax.all_gather(weights, SP, axis=0, tiled=True)
     size = lax.axis_size("tp")
-    at = jnp.stack([lax.axis_index(a).astype(jnp.int32) for a in ("tp", *reversed(SP))])
     before, total, solved, decay, grown = keys_side(keys, values, beta_pre, decay_pre)
     gate = gates_side(gates, out_gain)
     pairs = queries.shape[1] // PAIR
     early, late, states = state_ahead(
-        at,
         total,
         lambda x: queries_side(0, x, queries, decay, solved, before, grown),
         lambda x: queries_side(pairs // 2, x, queries, decay, solved, before, grown),
     )
-    parts = mixed_and_projected(at, size, early, late, states, gate, w_out)
-    parts = [parts[0]] + [lax.ppermute(parts[k], "tp", ring(size, k)) for k in (2, 1, 3)]
+    parts = mixed_and_projected(size, early, late, states, gate, w_out)
+    parts = [parts[0]] + [lax.ppermute(parts[k], "tp", ring(size, k)) for k in (1, 2, 3)]
     middle, normed = normed_rows(stream, norm_gain, parts)
     right = lax.ppermute(normed, "tp", ring(size, 1))
     left = lax.ppermute(normed, "tp", ring(size, -1))

time: 133 us -> 146 us (1.098)
  Pallas kernels: 38.6 us -> 50.3 us
  starting transfers between devices: 26.2 us -> 30.1 us
  other arithmetic: 2.07 us -> 0 us
    pallas_call x11 -> x12, Pallas kernels: 37.5 us -> 49.3 us  [the longest x11 31.8 us: call(): pl.pallas_call(kernel, in_specs=[FAR] * len(far) + [FULL] * len(near), ou...]
    all_gather x1, waiting for transfers between devices: 0.01 us -> 4.55 us  [per_device(): weights = lax.all_gather(weights, SP, axis=0, tiled=True)]
    ppermute x1, waiting for transfers between devices: 4.44 us -> 7.73 us  [per_device(): back = [lax.ppermute(sums[0], 'tp', ring(size, -1))]]
    ppermute x1, starting transfers between devices: 0.09 us -> 3.06 us  [per_device(): back.append(lax.ppermute(last, 'tp', ring(size, 2)))]
    ppermute x1, waiting for transfers between devices: 11.4 us -> 8.53 us  [per_device(): back.append(lax.ppermute(last, 'tp', ring(size, 2)))]
    ppermute x1, waiting for transfers between devices: 9.12 us -> 7.11 us  [per_device(): right = lax.ppermute(normed, 'tp', ring(size, 1))]
    concatenate x1 -> x0, other arithmetic: 2 us -> none  [per_device(): weights = jnp.concatenate([w_gate, w_up, w_down.T], axis=1)]
    ppermute x3, waiting for transfers between devices: 2.55 us -> 0.63 us  [state_ahead(): lax.ppermute(chip, line, ring(size, k))]
  transfers between devices with their start and end apart: 19 -> 19, of which waited for: 10 -> 11; matrix products, arithmetic and copies ran while one was open for 0% -> 0% of each run, Pallas kernels for 25% -> 19%
where the time goes in v7:
time: 146 us; the launch traced here: 145 us
  waiting for transfers between devices  50.4 us (35%)
  Pallas kernels  50.3 us (34%)
  starting transfers between devices  30.1 us (21%)
  between operations  13.6 us (9%)
    pallas_call x11, Pallas kernels, call(): pl.pallas_call(kernel, in_specs=[FAR] * len(far) + [FULL] * len(near), ou...  31.8 us
    ppermute x3, waiting for transfers between devices, per_device(): lax.ppermute(parts[k], 'tp', ring(size, k))  18.2 us
    pallas_call x1, Pallas kernels, packed(): pl.pallas_call(packing_kernel, in_specs=[FAR] * len(far), out_specs=FAR,...  17.5 us
    ppermute x1, waiting for transfers between devices, per_device(): back.append(lax.ppermute(last, 'tp', ring(size, 2)))  8.53 us
    ppermute x1, waiting for transfers between devices, per_device(): back = [lax.ppermute(sums[0], 'tp', ring(size, -1))]  7.73 us
    ppermute x1, waiting for transfers between devices, per_device(): right = lax.ppermute(normed, 'tp', ring(size, 1))  7.11 us
    ppermute x3, starting transfers between devices, state_ahead(): planes = [lax.ppermute(whole, plane, ring(size, k)) for k in range(1, size)]  6.87 us
    ppermute x3, starting transfers between devices, state_ahead(): lax.ppermute(chip, line, ring(size, k))  6 us
  transfers between devices with their start and end apart: 19, of which 11 were waited for; matrix products, arithmetic and copies ran while one was open for 0% of the time, Pallas kernels for 19%

profile of v7, /device:TPU:0, one launch (start us, length us, event | category | flops | bytes accessed | tf_op | source)
XLA Modules:
  0.0 145.5 jit_solution(4616542103650810346)
XLA Ops:
  6.5 17.5 %packed.1 = bf16[64,4224]{1,0:T(8,128)(2,1)} custom-call(bf16[64,1408]{1,0:T(8,128)(2,1)} %rest_0_.1, bf16[64,1408]{1,0:T(8,128)(2,1)} %rest_1_.1, bf16[64,1408]{1,0:T(8,128)(2,1)} %bitcast.5), custom_call_target="tpu_custom_call" | custom-call | tf_op jit(solution)/shard_map/packed/pallas_call | solution.py:111
  24.1 0.0 copy-start
  24.1 0.0 all-gather.2.cloned.1.call-update
  24.1 8.2 %shard_map.127 = (bf16[12,128,128]{2,1,0:T(8,128)(2,1)S(1)}, bf16[4,128,128]{2,1,0:T(8,128)(2,1)S(1)}, bf16[12,128,384]{2,1,0:T(8,128)(2,1)S(1)}, bf16[12,128,256]{2,1,0:T(8,128)(2,1)S(1)}, f32[384,512]{1,0:T(8,128)S(1)}) custom-call(bf16[384,512]{1,0:T(8,128)(2,1)} %k_far_ref.1, bf16[384,512]{1,0:T(8,128)(2,1)} %v_far_ref.1, f32[8,384]{1,0:T(8,128)} %beta_far_ref.1, ...), custom_call_target="tpu_custom_call" | custom-call | tf_op jit(solution)/shard_map/pallas_call | solution.py:29
  32.3 0.1 collective-permute-start
  32.4 1.3 collective-permute-done.other_ref
  33.7 0.2 shard_map.128
  34.0 1.7 %collective-permute-start.1 = (bf16[2,128,128]{2,1,0:T(8,128)(2,1)S(1)}, bf16[2,128,128]{2,1,0:T(8,128)(2,1)S(1)}, u32[]{:S(2)}, u32[]{:S(2)}) collective-permute-start(bf16[2,128,128]{2,1,0:T(8,128)(2,1)S(1)} %get-tuple-element.32.after_ref.rest_0_), channel_id=1, source_target_pairs={{0,8},{8,16},{16,24},{24,0},{1,9},{9,17},{17,25},{25,1},{2,10},{10... | collective-permute-start | bytes 196616 | tf_op jit(solution)/shard_map/ppermute | solution.py:386
  35.7 2.9 %collective-permute-start.2 = (bf16[2,128,128]{2,1,0:T(8,128)(2,1)S(1)}, bf16[2,128,128]{2,1,0:T(8,128)(2,1)S(1)}, u32[]{:S(2)}, u32[]{:S(2)}) collective-permute-start(bf16[2,128,128]{2,1,0:T(8,128)(2,1)S(1)} %get-tuple-element.32.after_ref.rest_0_), channel_id=1, source_target_pairs={{0,16},{8,24},{16,0},{24,8},{1,17},{9,25},{17,1},{25,9},{2,18},{10... | collective-permute-start | bytes 196616 | tf_op jit(solution)/shard_map/ppermute | solution.py:386
  38.6 1.3 collective-permute-start.3
  40.0 1.0 copy-done.1
  41.0 2.9 %shard_map.129 = (f32[384,256]{1,0:T(8,128)S(1)}, bf16[384,256]{1,0:T(8,128)(2,1)S(1)}) custom-call(bf16[2,128,128]{2,1,0:T(8,128)(2,1)S(1)} %get-tuple-element.32.after_ref.rest_0_, bf16[384,512]{1,0:T(8,128)(2,1)S(1)} %copy-done.1, bf16[12,128,256]{2,1,0:T(8,128)(2,1)S(1)} %get-tuple-element.33.d_ref, bf16[12,128,384]{2,1,0:T(8,128)(2,1)S(1)} %get-tuple-element.34.y_ref, ...), custom_call_target="tpu_custom_call" | custom-call | tf_op jit(solution)/shard_map/pallas_call | solution.py:29
  43.9 0.0 copy-start.3
  43.9 0.0 copy-start.5
  43.9 0.2 collective-permute-done.2.rest_2_
  44.1 0.5 collective-permute-done.3.rest_3_
  44.5 0.6 shard_map.130
  45.2 2.1 %collective-permute-start.4 = (bf16[2,128,128]{2,1,0:T(8,128)(2,1)S(1)}, bf16[2,128,128]{2,1,0:T(8,128)(2,1)S(1)}, u32[]{:S(2)}, u32[]{:S(2)}) collective-permute-start(bf16[2,128,128]{2,1,0:T(8,128)(2,1)S(1)} %get-tuple-element.39.after_ref), channel_id=1, source_target_pairs={{0,32},{32,64},{64,96},{96,0},{1,33},{33,65},{65,97},{97,1},{2,34}... | collective-permute-start | bytes 196616 | tf_op jit(solution)/shard_map/ppermute | solution.py:392
  47.3 3.9 %collective-permute-start.5 = (bf16[2,128,128]{2,1,0:T(8,128)(2,1)S(1)}, bf16[2,128,128]{2,1,0:T(8,128)(2,1)S(1)}, u32[]{:S(2)}, u32[]{:S(2)}) collective-permute-start(bf16[2,128,128]{2,1,0:T(8,128)(2,1)S(1)} %get-tuple-element.39.after_ref), channel_id=1, source_target_pairs={{0,64},{32,96},{64,0},{96,32},{1,65},{33,97},{65,1},{97,33},{2,66}... | collective-permute-start | bytes 196616 | tf_op jit(solution)/shard_map/ppermute | solution.py:392
  51.2 0.9 collective-permute-start.6
  52.1 2.9 %shard_map.131 = (f32[384,256]{1,0:T(8,128)S(1)}, bf16[384,256]{1,0:T(8,128)(2,1)S(1)}) custom-call(bf16[2,128,128]{2,1,0:T(8,128)(2,1)S(1)} %get-tuple-element.39.after_ref, bf16[384,512]{1,0:T(8,128)(2,1)S(1)} %copy-done.2, bf16[12,128,256]{2,1,0:T(8,128)(2,1)S(1)} %get-tuple-element.33.d_ref, bf16[12,128,384]{2,1,0:T(8,128)(2,1)S(1)} %get-tuple-element.34.y_ref, ...), custom_call_target="tpu_custom_call" | custom-call | tf_op jit(solution)/shard_map/pallas_call | solution.py:29
  55.0 0.0 collective-permute-done.4.rest_0_
  55.0 1.3 collective-permute-done.5.rest_1_
  56.3 0.0 collective-permute-done.6.rest_2_
  56.3 0.9 shard_map.132.mine_ref
  57.2 0.3 collective-permute-start.7
  57.5 0.3 shard_map.133.gate_ref
  57.8 0.9 collective-permute-done.7.theirs_ref
  58.7 2.1 %shard_map.134 = (f32[96,2048]{1,0:T(8,128)S(1)}, bf16[96,2048]{1,0:T(8,128)(2,1)S(1)}, bf16[96,2048]{1,0:T(8,128)(2,1)S(1)}, bf16[96,2048]{1,0:T(8,128)(2,1)S(1)}) custom-call(f32[384,256]{1,0:T(8,128)S(1)} %get-tuple-element.37.o0_ref, bf16[384,256]{1,0:T(8,128)(2,1)S(1)} %get-tuple-element.38.after_ref.q0_ref, f32[384,256]{1,0:T(8,128)S(1)} %get-tuple-element.40.o1_ref, ...), custom_call_target="tpu_custom_call" | custom-call | tf_op jit(solution)/shard_map/pallas_call | solution.py:29
  60.9 2.8 %collective-permute-start.10 = (bf16[96,2048]{1,0:T(8,128)(2,1)S(1)}, bf16[96,2048]{1,0:T(8,128)(2,1)S(1)}, u32[]{:S(2)}, u32[]{:S(2)}) collective-permute-start(bf16[96,2048]{1,0:T(8,128)(2,1)S(1)} %get-tuple-element.47), channel_id=1, source_target_pairs={{0,3},{1,0},{2,1},{3,2},{4,7},{5,4},{6,5},{7,6},{8,11},{9,8},{10,9... | collective-permute-start | bytes 1179656 | tf_op jit(solution)/shard_map/ppermute | solution.py:620
  63.7 2.3 %collective-permute-start.9 = (bf16[96,2048]{1,0:T(8,128)(2,1)S(1)}, bf16[96,2048]{1,0:T(8,128)(2,1)S(1)}, u32[]{:S(2)}, u32[]{:S(2)}) collective-permute-start(bf16[96,2048]{1,0:T(8,128)(2,1)S(1)} %get-tuple-element.46), channel_id=1, source_target_pairs={{0,2},{1,3},{2,0},{3,1},{4,6},{5,7},{6,4},{7,5},{8,10},{9,11},{10,... | collective-permute-start | bytes 1179656 | tf_op jit(solution)/shard_map/ppermute | solution.py:620
  66.0 14.9 %collective-permute-done.10.rest_3_ = bf16[96,2048]{1,0:T(8,128)(2,1)S(1)} collective-permute-done((bf16[96,2048]{1,0:T(8,128)(2,1)S(1)}, bf16[96,2048]{1,0:T(8,128)(2,1)S(1)}, u32[]{:S(2)}, u32[]{:S(2)}) %collective-permute-start.10) | collective-permute-done | bytes 393248 | tf_op jit(solution)/shard_map/ppermute | solution.py:620
  80.9 3.4 %collective-permute-done.8.rest_1_ = bf16[96,2048]{1,0:T(8,128)(2,1)S(1)} collective-permute-done((bf16[96,2048]{1,0:T(8,128)(2,1)S(1)}, bf16[96,2048]{1,0:T(8,128)(2,1)S(1)}, u32[]{:S(2)}, u32[]{:S(2)}) %collective-permute-start.8) | collective-permute-done | bytes 393248 | tf_op jit(solution)/shard_map/ppermute | solution.py:620
  84.3 0.4 shard_map.135
  84.7 0.1 collective-permute-start.11
  84.8 3.2 %collective-permute-start.13 = (bf16[96,2048]{1,0:T(8,128)(2,1)S(1)}, bf16[96,2048]{1,0:T(8,128)(2,1)S(1)}, u32[]{:S(2)}, u32[]{:S(2)}) collective-permute-start(bf16[96,2048]{1,0:T(8,128)(2,1)S(1)} %get-tuple-element.49.own_ref), channel_id=1, source_target_pairs={{0,3},{1,0},{2,1},{3,2},{4,7},{5,4},{6,5},{7,6},{8,11},{9,8},{10,9... | collective-permute-start | bytes 1179656 | tf_op jit(solution)/shard_map/ppermute | solution.py:623
  88.0 7.1 %collective-permute-done.11.rest_0_ = bf16[96,2048]{1,0:T(8,128)(2,1)S(1)} collective-permute-done((bf16[96,2048]{1,0:T(8,128)(2,1)S(1)}, bf16[96,2048]{1,0:T(8,128)(2,1)S(1)}, u32[]{:S(2)}, u32[]{:S(2)}) %collective-permute-start.11) | collective-permute-done | bytes 393248 | tf_op jit(solution)/shard_map/ppermute | solution.py:622
  95.1 0.1 collective-permute-start.12
  95.2 3.3 %collective-permute-start.14 = (bf16[48,2048]{1,0:T(8,128)(2,1)S(1)}, bf16[48,2048]{1,0:T(8,128)(2,1)S(1)}, u32[]{:S(2)}, u32[]{:S(2)}) collective-permute-start(bf16[48,2048]{1,0:T(8,128)(2,1)S(1)} %slice.9), channel_id=1, source_target_pairs={{0,3},{1,0},{2,1},{3,2},{4,7},{5,4},{6,5},{7,6},{8,11},{9,8},{10,9... | collective-permute-start | bytes 589832 | tf_op jit(solution)/shard_map/ppermute | solution.py:627
  98.5 4.5 %all-gather.2.cloned.1.call-done.w_ref = bf16[2048,4224]{1,0:T(8,128)(2,1)} async-done(((bf16[64,4224]{1,0:T(8,128)(2,1)}), bf16[2048,4224]{1,0:T(8,128)(2,1)}) %all-gather.2.cloned.1.call-update) | async-done | bytes 17301520 | tf_op jit(solution)/shard_map/all_gather | solution.py:609
  103.1 8.5 %shard_map.136 = (bf16[96,2048]{1,0:T(8,128)(2,1)S(1)}, bf16[96,2048]{1,0:T(8,128)(2,1)S(1)}, bf16[2048,1408]{1,0:T(8,128)(2,1)S(1)}, bf16[2048,1408]{1,0:T(8,128)(2,1)S(1)}, bf16[2048,1408]{1,0:T(8,128)(2,1)S(1)}) custom-call(bf16[2048,4224]{1,0:T(8,128)(2,1)} %all-gather.2.cloned.1.call-done.w_ref, bf16[96,2048]{1,0:T(8,128)(2,1)S(1)} %collective-permute-done.11.rest_0_, ...), custom_call_target="tpu_custom_call" | custom-call | tf_op jit(solution)/shard_map/pallas_call | solution.py:29
  111.5 4.7 %shard_map.137 = (bf16[96,2048]{1,0:T(8,128)(2,1)S(1)}, bf16[96,2048]{1,0:T(8,128)(2,1)S(1)}) custom-call(bf16[96,2048]{1,0:T(8,128)(2,1)S(1)} %get-tuple-element.49.own_ref, bf16[48,2048]{1,0:T(8,128)(2,1)S(1)} %collective-permute-done.12.upper_ref, bf16[48,2048]{1,0:T(8,128)(2,1)S(1)} %collective-permute-done.14.lower_ref, ...), custom_call_target="tpu_custom_call" | custom-call | tf_op jit(solution)/shard_map/pallas_call | solution.py:29
  116.3 3.1 %collective-permute-start.17 = (bf16[96,2048]{1,0:T(8,128)(2,1)S(1)}, bf16[96,2048]{1,0:T(8,128)(2,1)S(1)}, u32[]{:S(2)}, u32[]{:S(2)}) collective-permute-start(bf16[96,2048]{1,0:T(8,128)(2,1)S(1)} %get-tuple-element.56), channel_id=1, source_target_pairs={{0,2},{1,3},{2,0},{3,1},{4,6},{5,7},{6,4},{7,5},{8,10},{9,11},{10,... | collective-permute-start | bytes 1179656 | tf_op jit(solution)/shard_map/ppermute | solution.py:633
  119.3 1.2 collective-permute-start.15
  120.5 0.9 collective-permute-start.16
  121.4 8.5 %collective-permute-done.17.rest_3_ = bf16[96,2048]{1,0:T(8,128)(2,1)S(1)} collective-permute-done((bf16[96,2048]{1,0:T(8,128)(2,1)S(1)}, bf16[96,2048]{1,0:T(8,128)(2,1)S(1)}, u32[]{:S(2)}, u32[]{:S(2)}) %collective-permute-start.17) | collective-permute-done | bytes 393248 | tf_op jit(solution)/shard_map/ppermute | solution.py:633
  129.9 7.7 %collective-permute-done.15.rest_1_ = bf16[96,2048]{1,0:T(8,128)(2,1)S(1)} collective-permute-done((bf16[96,2048]{1,0:T(8,128)(2,1)S(1)}, bf16[96,2048]{1,0:T(8,128)(2,1)S(1)}, u32[]{:S(2)}, u32[]{:S(2)}) %collective-permute-start.15) | collective-permute-done | bytes 393248 | tf_op jit(solution)/shard_map/ppermute | solution.py:630
  137.6 1.0 last_sum.1
  (20 shorter events, 0.1 us)
Async XLA Ops:
  6.5 45.5 %copy-start.2 = (bf16[384,512]{1,0:T(8,128)(2,1)S(1)}, bf16[384,512]{1,0:T(8,128)(2,1)}, u32[]{:S(2)}) copy-start(bf16[384,512]{1,0:T(8,128)(2,1)} %q_ref.3) | copy-start | bytes 1179652
  6.5 51.0 %copy-start.6 = (f32[64]{0:T(128)S(1)}, f32[64]{0:T(128)}, u32[]{:S(2)}) copy-start(f32[64]{0:T(128)} %param.19) | copy-start | bytes 772
  6.5 51.0 %copy-start.4 = (bf16[384,512]{1,0:T(8,128)(2,1)S(1)}, bf16[384,512]{1,0:T(8,128)(2,1)}, u32[]{:S(2)}) copy-start(bf16[384,512]{1,0:T(8,128)(2,1)} %gates_ref.1) | copy-start | bytes 1179652
  6.5 96.5 %all-gather.2.cloned.1.call-start = ((), (), s32[]{:S(2)}) async-start(), calls=%async_computation | async-start | bytes 17842176 | tf_op jit(solution)/shard_map/all_gather | solution.py:609
  24.1 34.7 %copy-start = (bf16[512,2048]{1,0:T(8,128)(2,1)S(1)}, bf16[512,2048]{1,0:T(8,128)(2,1)}, u32[]{:S(2)}) copy-start(bf16[512,2048]{1,0:T(8,128)(2,1)} %w_ref.1) | copy-start | bytes 6291460
  32.3 1.4 collective-permute-start
  34.0 9.9 %collective-permute-start.1 = (bf16[2,128,128]{2,1,0:T(8,128)(2,1)S(1)}, bf16[2,128,128]{2,1,0:T(8,128)(2,1)S(1)}, u32[]{:S(2)}, u32[]{:S(2)}) collective-permute-start(bf16[2,128,128]{2,1,0:T(8,128)(2,1)S(1)} %get-tuple-element.32.after_ref.rest_0_), channel_id=1, source_target_pairs={{0,8},{8,16},{16,24},{24,0},{1,9},{9,17},{17,25},{25,1},{2,10},{10... | collective-permute-start | bytes 196616 | tf_op jit(solution)/shard_map/ppermute | solution.py:386
  35.7 8.4 %collective-permute-start.2 = (bf16[2,128,128]{2,1,0:T(8,128)(2,1)S(1)}, bf16[2,128,128]{2,1,0:T(8,128)(2,1)S(1)}, u32[]{:S(2)}, u32[]{:S(2)}) collective-permute-start(bf16[2,128,128]{2,1,0:T(8,128)(2,1)S(1)} %get-tuple-element.32.after_ref.rest_0_), channel_id=1, source_target_pairs={{0,16},{8,24},{16,0},{24,8},{1,17},{9,25},{17,1},{25,9},{2,18},{10... | collective-permute-start | bytes 196616 | tf_op jit(solution)/shard_map/ppermute | solution.py:386
  38.6 5.9 %collective-permute-start.3 = (bf16[2,128,128]{2,1,0:T(8,128)(2,1)S(1)}, bf16[2,128,128]{2,1,0:T(8,128)(2,1)S(1)}, u32[]{:S(2)}, u32[]{:S(2)}) collective-permute-start(bf16[2,128,128]{2,1,0:T(8,128)(2,1)S(1)} %get-tuple-element.32.after_ref.rest_0_), channel_id=1, source_target_pairs={{0,24},{8,0},{16,8},{24,16},{1,25},{9,1},{17,9},{25,17},{2,26},{10... | collective-permute-start | bytes 196616 | tf_op jit(solution)/shard_map/ppermute | solution.py:386
  40.0 1.0 copy-start.1
  43.9 40.4 %copy-start.3 = (bf16[96,2048]{1,0:T(8,128)(2,1)S(1)}, bf16[96,2048]{1,0:T(8,128)(2,1)}, u32[]{:S(2)}) copy-start(bf16[96,2048]{1,0:T(8,128)(2,1)} %stream_ref.1) | copy-start | bytes 1179652
  43.9 40.4 %copy-start.5 = (f32[2048]{0:T(1024)S(1)}, f32[2048]{0:T(1024)}, u32[]{:S(2)}) copy-start(f32[2048]{0:T(1024)} %param.22) | copy-start | bytes 24580
  45.2 9.8 %collective-permute-start.4 = (bf16[2,128,128]{2,1,0:T(8,128)(2,1)S(1)}, bf16[2,128,128]{2,1,0:T(8,128)(2,1)S(1)}, u32[]{:S(2)}, u32[]{:S(2)}) collective-permute-start(bf16[2,128,128]{2,1,0:T(8,128)(2,1)S(1)} %get-tuple-element.39.after_ref), channel_id=1, source_target_pairs={{0,32},{32,64},{64,96},{96,0},{1,33},{33,65},{65,97},{97,1},{2,34}... | collective-permute-start | bytes 196616 | tf_op jit(solution)/shard_map/ppermute | solution.py:392
  47.3 9.1 %collective-permute-start.5 = (bf16[2,128,128]{2,1,0:T(8,128)(2,1)S(1)}, bf16[2,128,128]{2,1,0:T(8,128)(2,1)S(1)}, u32[]{:S(2)}, u32[]{:S(2)}) collective-permute-start(bf16[2,128,128]{2,1,0:T(8,128)(2,1)S(1)} %get-tuple-element.39.after_ref), channel_id=1, source_target_pairs={{0,64},{32,96},{64,0},{96,32},{1,65},{33,97},{65,1},{97,33},{2,66}... | collective-permute-start | bytes 196616 | tf_op jit(solution)/shard_map/ppermute | solution.py:392
  51.2 5.1 %collective-permute-start.6 = (bf16[2,128,128]{2,1,0:T(8,128)(2,1)S(1)}, bf16[2,128,128]{2,1,0:T(8,128)(2,1)S(1)}, u32[]{:S(2)}, u32[]{:S(2)}) collective-permute-start(bf16[2,128,128]{2,1,0:T(8,128)(2,1)S(1)} %get-tuple-element.39.after_ref), channel_id=1, source_target_pairs={{0,96},{32,0},{64,32},{96,64},{1,97},{33,1},{65,33},{97,65},{2,98}... | collective-permute-start | bytes 196616 | tf_op jit(solution)/shard_map/ppermute | solution.py:392
  57.2 1.5 %collective-permute-start.7 = (bf16[2,128,128]{2,1,0:T(8,128)(2,1)S(1)}, bf16[2,128,128]{2,1,0:T(8,128)(2,1)S(1)}, u32[]{:S(2)}, u32[]{:S(2)}) collective-permute-start(bf16[2,128,128]{2,1,0:T(8,128)(2,1)S(1)} %shard_map.132.mine_ref), channel_id=1, source_target_pairs={{0,4},{4,0},{1,5},{5,1},{2,6},{6,2},{3,7},{7,3},{8,12},{12,8},{9,1... | collective-permute-start | bytes 196616 | tf_op jit(solution)/shard_map/ppermute | solution.py:395
  60.9 20.0 %collective-permute-start.10 = (bf16[96,2048]{1,0:T(8,128)(2,1)S(1)}, bf16[96,2048]{1,0:T(8,128)(2,1)S(1)}, u32[]{:S(2)}, u32[]{:S(2)}) collective-permute-start(bf16[96,2048]{1,0:T(8,128)(2,1)S(1)} %get-tuple-element.47), channel_id=1, source_target_pairs={{0,3},{1,0},{2,1},{3,2},{4,7},{5,4},{6,5},{7,6},{8,11},{9,8},{10,9... | collective-permute-start | bytes 1179656 | tf_op jit(solution)/shard_map/ppermute | solution.py:620
  63.7 20.5 %collective-permute-start.8 = (bf16[96,2048]{1,0:T(8,128)(2,1)S(1)}, bf16[96,2048]{1,0:T(8,128)(2,1)S(1)}, u32[]{:S(2)}, u32[]{:S(2)}) collective-permute-start(bf16[96,2048]{1,0:T(8,128)(2,1)S(1)} %get-tuple-element.45), channel_id=1, source_target_pairs={{0,1},{1,2},{2,3},{3,0},{4,5},{5,6},{6,7},{7,4},{8,9},{9,10},{10,1... | collective-permute-start | bytes 1179656 | tf_op jit(solution)/shard_map/ppermute | solution.py:620
  63.7 20.5 %collective-permute-start.9 = (bf16[96,2048]{1,0:T(8,128)(2,1)S(1)}, bf16[96,2048]{1,0:T(8,128)(2,1)S(1)}, u32[]{:S(2)}, u32[]{:S(2)}) collective-permute-start(bf16[96,2048]{1,0:T(8,128)(2,1)S(1)} %get-tuple-element.46), channel_id=1, source_target_pairs={{0,2},{1,3},{2,0},{3,1},{4,6},{5,7},{6,4},{7,5},{8,10},{9,11},{10,... | collective-permute-start | bytes 1179656 | tf_op jit(solution)/shard_map/ppermute | solution.py:620
  84.7 10.4 %collective-permute-start.11 = (bf16[96,2048]{1,0:T(8,128)(2,1)S(1)}, bf16[96,2048]{1,0:T(8,128)(2,1)S(1)}, u32[]{:S(2)}, u32[]{:S(2)}) collective-permute-start(bf16[96,2048]{1,0:T(8,128)(2,1)S(1)} %get-tuple-element.49.own_ref), channel_id=1, source_target_pairs={{0,1},{1,2},{2,3},{3,0},{4,5},{5,6},{6,7},{7,4},{8,9},{9,10},{10,1... | collective-permute-start | bytes 1179656 | tf_op jit(solution)/shard_map/ppermute | solution.py:622
  84.8 10.4 %collective-permute-start.13 = (bf16[96,2048]{1,0:T(8,128)(2,1)S(1)}, bf16[96,2048]{1,0:T(8,128)(2,1)S(1)}, u32[]{:S(2)}, u32[]{:S(2)}) collective-permute-start(bf16[96,2048]{1,0:T(8,128)(2,1)S(1)} %get-tuple-element.49.own_ref), channel_id=1, source_target_pairs={{0,3},{1,0},{2,1},{3,2},{4,7},{5,4},{6,5},{7,6},{8,11},{9,8},{10,9... | collective-permute-start | bytes 1179656 | tf_op jit(solution)/shard_map/ppermute | solution.py:623
  95.1 16.4 %collective-permute-start.12 = (bf16[48,2048]{1,0:T(8,128)(2,1)S(1)}, bf16[48,2048]{1,0:T(8,128)(2,1)S(1)}, u32[]{:S(2)}, u32[]{:S(2)}) collective-permute-start(bf16[48,2048]{1,0:T(8,128)(2,1)S(1)} %slice.8), channel_id=1, source_target_pairs={{0,1},{1,2},{2,3},{3,0},{4,5},{5,6},{6,7},{7,4},{8,9},{9,10},{10,1... | collective-permute-start | bytes 589832 | tf_op jit(solution)/shard_map/ppermute | solution.py:626
  95.2 16.3 %collective-permute-start.14 = (bf16[48,2048]{1,0:T(8,128)(2,1)S(1)}, bf16[48,2048]{1,0:T(8,128)(2,1)S(1)}, u32[]{:S(2)}, u32[]{:S(2)}) collective-permute-start(bf16[48,2048]{1,0:T(8,128)(2,1)S(1)} %slice.9), channel_id=1, source_target_pairs={{0,3},{1,0},{2,1},{3,2},{4,7},{5,4},{6,5},{7,6},{8,11},{9,8},{10,9... | collective-permute-start | bytes 589832 | tf_op jit(solution)/shard_map/ppermute | solution.py:627
  116.3 13.6 %collective-permute-start.17 = (bf16[96,2048]{1,0:T(8,128)(2,1)S(1)}, bf16[96,2048]{1,0:T(8,128)(2,1)S(1)}, u32[]{:S(2)}, u32[]{:S(2)}) collective-permute-start(bf16[96,2048]{1,0:T(8,128)(2,1)S(1)} %get-tuple-element.56), channel_id=1, source_target_pairs={{0,2},{1,3},{2,0},{3,1},{4,6},{5,7},{6,4},{7,5},{8,10},{9,11},{10,... | collective-permute-start | bytes 1179656 | tf_op jit(solution)/shard_map/ppermute | solution.py:633
  119.3 18.3 %collective-permute-start.15 = (bf16[96,2048]{1,0:T(8,128)(2,1)S(1)}, bf16[96,2048]{1,0:T(8,128)(2,1)S(1)}, u32[]{:S(2)}, u32[]{:S(2)}) collective-permute-start(bf16[96,2048]{1,0:T(8,128)(2,1)S(1)} %get-tuple-element.54), channel_id=1, source_target_pairs={{0,3},{1,0},{2,1},{3,2},{4,7},{5,4},{6,5},{7,6},{8,11},{9,8},{10,9... | collective-permute-start | bytes 1179656 | tf_op jit(solution)/shard_map/ppermute | solution.py:630
  120.5 17.1 %collective-permute-start.16 = (bf16[96,2048]{1,0:T(8,128)(2,1)S(1)}, bf16[96,2048]{1,0:T(8,128)(2,1)S(1)}, u32[]{:S(2)}, u32[]{:S(2)}) collective-permute-start(bf16[96,2048]{1,0:T(8,128)(2,1)S(1)} %get-tuple-element.55), channel_id=1, source_target_pairs={{0,1},{1,2},{2,3},{3,0},{4,5},{5,6},{6,7},{7,4},{8,9},{9,10},{10,1... | collective-permute-start | bytes 1179656 | tf_op jit(solution)/shard_map/ppermute | solution.py:631
Sparse Core Ops, SparseCore 0:
  24.2 78.8 all-gather.1

commit v8 on v7

--- a/solution.py
+++ b/solution.py
@@ -90,33 +90,6 @@
 
 def halves(x):
     return x[:, :CHUNK], x[:, CHUNK:]
-
-
-def packing_kernel(*rest):
-    from_refs, packed_ref, sems = rest[:-2], rest[-2], rest[-1]
-    hidden = from_refs[0].shape[1]
-    copies = []
-    for k, ref in enumerate(from_refs):
-        here = packed_ref.at[:, pl.ds(k * hidden, hidden)]
-        copies.append(pltpu.make_async_copy(ref, here, sems.at[k]))
-    for copy in copies:
-        copy.start()
-    for copy in copies:
-        copy.wait()
-
-
-def packed(weights):
-    rows, hidden = weights[0].shape
-    far = [pltpu.with_memory_space_constraint(x, pltpu.HBM) for x in weights]
-    return pl.pallas_call(
-        packing_kernel,
-        in_specs=[FAR] * len(far),
-        out_specs=FAR,
-        out_shape=pltpu.HBM((rows, len(weights) * hidden), BF),
-        scratch_shapes=[pltpu.SemaphoreType.DMA((len(far),))],
-        compiler_params=pltpu.CompilerParams(vmem_limit_bytes=16 << 20),
-        name="packed",
-    )(*far)
 
 
 def keys_kernel(
@@ -605,7 +578,7 @@
     w_down,
 ):
     hidden = w_gate.shape[1]
-    weights = packed([w_gate, w_up, w_down.T])
+    weights = jnp.concatenate([w_gate, w_up, w_down.T], axis=1)
     weights = lax.all_gather(weights, SP, axis=0, tiled=True)
     size = lax.axis_size("tp")
     before, total, solved, decay, grown = keys_side(keys, values, beta_pre, decay_pre)

time: 146 us -> 132 us (0.904)
  Pallas kernels: 50.3 us -> 32.7 us
  waiting for transfers between devices: 50.4 us -> 52.6 us
  other arithmetic: 0 us -> 2 us
    pallas_call x1 -> x0, Pallas kernels: 17.5 us -> none  [packed(): pl.pallas_call(packing_kernel, in_specs=[FAR] * len(far), out_specs=FAR,...]
    concatenate x0 -> x1, other arithmetic: none -> 2 us  [per_device(): weights = jnp.concatenate([w_gate, w_up, w_down.T], axis=1)]
  transfers between devices with their start and end apart: 19 -> 19, of which waited for: 11 -> 10; matrix products, arithmetic and copies ran while one was open for 0% -> 0% of each run, Pallas kernels for 19% -> 21%
where the time goes in v8:
time: 132 us; the launch traced here: 131 us
  waiting for transfers between devices  52.6 us (40%)
  Pallas kernels  32.7 us (25%)
  starting transfers between devices  29.9 us (23%)
  between operations  13.6 us (10%)
  other arithmetic  2 us (2%)
    pallas_call x11, Pallas kernels, call(): pl.pallas_call(kernel, in_specs=[FAR] * len(far) + [FULL] * len(near), ou...  31.7 us
    ppermute x3, waiting for transfers between devices, per_device(): lax.ppermute(parts[k], 'tp', ring(size, k))  18.2 us
    ppermute x1, waiting for transfers between devices, per_device(): back.append(lax.ppermute(last, 'tp', ring(size, 2)))  8.53 us
    ppermute x1, waiting for transfers between devices, per_device(): back = [lax.ppermute(sums[0], 'tp', ring(size, -1))]  7.72 us
    ppermute x1, waiting for transfers between devices, per_device(): right = lax.ppermute(normed, 'tp', ring(size, 1))  7.1 us
    ppermute x3, starting transfers between devices, state_ahead(): planes = [lax.ppermute(whole, plane, ring(size, k)) for k in range(1, size)]  6.69 us
    ppermute x3, starting transfers between devices, state_ahead(): lax.ppermute(chip, line, ring(size, k))  6 us
    all_gather x1, waiting for transfers between devices, per_device(): weights = lax.all_gather(weights, SP, axis=0, tiled=True)  5.28 us
  transfers between devices with their start and end apart: 19, of which 10 were waited for; matrix products, arithmetic and copies ran while one was open for 0% of the time, Pallas kernels for 21%

profile of v8, /device:TPU:0, one launch (start us, length us, event | category | flops | bytes accessed | tf_op | source)
XLA Modules:
  0.0 130.8 jit_solution(14559153050019587304)
XLA Ops:
  6.5 2.0 %pad_maximum_fusion = bf16[64,4224]{1,0:T(8,128)(2,1)} fusion(bf16[64,1408]{1,0:T(8,128)(2,1)} %bitcast.5, bf16[64,1408]{1,0:T(8,128)(2,1)} %param.24, bf16[64,1408]{1,0:T(8,128)(2,1)} %param.23), kind=kLoop, calls=%fused_computation | loop fusion | flops 1622016 | bytes 1081344 | tf_op jit(solution)/shard_map/concatenate | solution.py:581
  8.5 0.0 all-gather.2.cloned.1.call-update
  8.6 8.1 %shard_map.127 = (bf16[12,128,128]{2,1,0:T(8,128)(2,1)S(1)}, bf16[4,128,128]{2,1,0:T(8,128)(2,1)S(1)}, bf16[12,128,384]{2,1,0:T(8,128)(2,1)S(1)}, bf16[12,128,256]{2,1,0:T(8,128)(2,1)S(1)}, f32[384,512]{1,0:T(8,128)S(1)}) custom-call(bf16[384,512]{1,0:T(8,128)(2,1)} %k_far_ref.1, bf16[384,512]{1,0:T(8,128)(2,1)} %v_far_ref.1, f32[8,384]{1,0:T(8,128)} %beta_far_ref.1, ...), custom_call_target="tpu_custom_call" | custom-call | tf_op jit(solution)/shard_map/pallas_call | solution.py:29
  16.6 0.1 collective-permute-start
  16.7 1.3 %collective-permute-done.other_ref = bf16[4,128,128]{2,1,0:T(8,128)(2,1)S(1)} collective-permute-done((bf16[4,128,128]{2,1,0:T(8,128)(2,1)S(1)}, bf16[4,128,128]{2,1,0:T(8,128)(2,1)S(1)}, u32[]{:S(2)}, u32[]{:S(2)}) %collective-permute-start) | collective-permute-done | bytes 131104 | tf_op jit(solution)/shard_map/ppermute | solution.py:356
  18.1 0.2 shard_map.128
  18.3 1.7 %collective-permute-start.1 = (bf16[2,128,128]{2,1,0:T(8,128)(2,1)S(1)}, bf16[2,128,128]{2,1,0:T(8,128)(2,1)S(1)}, u32[]{:S(2)}, u32[]{:S(2)}) collective-permute-start(bf16[2,128,128]{2,1,0:T(8,128)(2,1)S(1)} %get-tuple-element.32.after_ref.rest_0_), channel_id=1, source_target_pairs={{0,8},{8,16},{16,24},{24,0},{1,9},{9,17},{17,25},{25,1},{2,10},{10... | collective-permute-start | bytes 196616 | tf_op jit(solution)/shard_map/ppermute | solution.py:359
  20.0 2.9 %collective-permute-start.2 = (bf16[2,128,128]{2,1,0:T(8,128)(2,1)S(1)}, bf16[2,128,128]{2,1,0:T(8,128)(2,1)S(1)}, u32[]{:S(2)}, u32[]{:S(2)}) collective-permute-start(bf16[2,128,128]{2,1,0:T(8,128)(2,1)S(1)} %get-tuple-element.32.after_ref.rest_0_), channel_id=1, source_target_pairs={{0,16},{8,24},{16,0},{24,8},{1,17},{9,25},{17,1},{25,9},{2,18},{10... | collective-permute-start | bytes 196616 | tf_op jit(solution)/shard_map/ppermute | solution.py:359
  22.9 1.3 %collective-permute-start.3 = (bf16[2,128,128]{2,1,0:T(8,128)(2,1)S(1)}, bf16[2,128,128]{2,1,0:T(8,128)(2,1)S(1)}, u32[]{:S(2)}, u32[]{:S(2)}) collective-permute-start(bf16[2,128,128]{2,1,0:T(8,128)(2,1)S(1)} %get-tuple-element.32.after_ref.rest_0_), channel_id=1, source_target_pairs={{0,24},{8,0},{16,8},{24,16},{1,25},{9,1},{17,9},{25,17},{2,26},{10... | collective-permute-start | bytes 196616 | tf_op jit(solution)/shard_map/ppermute | solution.py:359
  24.3 2.9 %shard_map.129 = (f32[384,256]{1,0:T(8,128)S(1)}, bf16[384,256]{1,0:T(8,128)(2,1)S(1)}) custom-call(bf16[2,128,128]{2,1,0:T(8,128)(2,1)S(1)} %get-tuple-element.32.after_ref.rest_0_, bf16[384,512]{1,0:T(8,128)(2,1)S(1)} %copy-done.1, bf16[12,128,256]{2,1,0:T(8,128)(2,1)S(1)} %get-tuple-element.33.d_ref, bf16[12,128,384]{2,1,0:T(8,128)(2,1)S(1)} %get-tuple-element.34.y_ref, ...), custom_call_target="tpu_custom_call" | custom-call | tf_op jit(solution)/shard_map/pallas_call | solution.py:29
  27.2 0.0 collective-permute-done.1.rest_1_
  27.2 0.0 collective-permute-done.2.rest_2_
  27.2 1.5 %collective-permute-done.3.rest_3_ = bf16[2,128,128]{2,1,0:T(8,128)(2,1)S(1)} collective-permute-done((bf16[2,128,128]{2,1,0:T(8,128)(2,1)S(1)}, bf16[2,128,128]{2,1,0:T(8,128)(2,1)S(1)}, u32[]{:S(2)}, u32[]{:S(2)}) %collective-permute-start.3) | collective-permute-done | bytes 65568 | tf_op jit(solution)/shard_map/ppermute | solution.py:359
  28.8 0.6 shard_map.130
  29.4 0.0 copy-start.3
  29.4 0.0 copy-start.5
  29.4 2.0 %collective-permute-start.4 = (bf16[2,128,128]{2,1,0:T(8,128)(2,1)S(1)}, bf16[2,128,128]{2,1,0:T(8,128)(2,1)S(1)}, u32[]{:S(2)}, u32[]{:S(2)}) collective-permute-start(bf16[2,128,128]{2,1,0:T(8,128)(2,1)S(1)} %get-tuple-element.39.after_ref), channel_id=1, source_target_pairs={{0,32},{32,64},{64,96},{96,0},{1,33},{33,65},{65,97},{97,1},{2,34}... | collective-permute-start | bytes 196616 | tf_op jit(solution)/shard_map/ppermute | solution.py:365
  31.4 3.6 %collective-permute-start.5 = (bf16[2,128,128]{2,1,0:T(8,128)(2,1)S(1)}, bf16[2,128,128]{2,1,0:T(8,128)(2,1)S(1)}, u32[]{:S(2)}, u32[]{:S(2)}) collective-permute-start(bf16[2,128,128]{2,1,0:T(8,128)(2,1)S(1)} %get-tuple-element.39.after_ref), channel_id=1, source_target_pairs={{0,64},{32,96},{64,0},{96,32},{1,65},{33,97},{65,1},{97,33},{2,66}... | collective-permute-start | bytes 196616 | tf_op jit(solution)/shard_map/ppermute | solution.py:365
  35.1 1.0 collective-permute-start.6
  36.1 2.9 %shard_map.131 = (f32[384,256]{1,0:T(8,128)S(1)}, bf16[384,256]{1,0:T(8,128)(2,1)S(1)}) custom-call(bf16[2,128,128]{2,1,0:T(8,128)(2,1)S(1)} %get-tuple-element.39.after_ref, bf16[384,512]{1,0:T(8,128)(2,1)S(1)} %copy-done.1, bf16[12,128,256]{2,1,0:T(8,128)(2,1)S(1)} %get-tuple-element.33.d_ref, bf16[12,128,384]{2,1,0:T(8,128)(2,1)S(1)} %get-tuple-element.34.y_ref, ...), custom_call_target="tpu_custom_call" | custom-call | tf_op jit(solution)/shard_map/pallas_call | solution.py:29
  39.0 1.9 %collective-permute-done.5.rest_1_ = bf16[2,128,128]{2,1,0:T(8,128)(2,1)S(1)} collective-permute-done((bf16[2,128,128]{2,1,0:T(8,128)(2,1)S(1)}, bf16[2,128,128]{2,1,0:T(8,128)(2,1)S(1)}, u32[]{:S(2)}, u32[]{:S(2)}) %collective-permute-start.5) | collective-permute-done | bytes 65568 | tf_op jit(solution)/shard_map/ppermute | solution.py:365
  40.9 0.9 shard_map.132.mine_ref
  41.8 0.3 collective-permute-start.7
  42.1 0.3 shard_map.133.gate_ref
  42.4 0.9 collective-permute-done.7.theirs_ref
  43.4 2.1 %shard_map.134 = (f32[96,2048]{1,0:T(8,128)S(1)}, bf16[96,2048]{1,0:T(8,128)(2,1)S(1)}, bf16[96,2048]{1,0:T(8,128)(2,1)S(1)}, bf16[96,2048]{1,0:T(8,128)(2,1)S(1)}) custom-call(f32[384,256]{1,0:T(8,128)S(1)} %get-tuple-element.37.o0_ref, bf16[384,256]{1,0:T(8,128)(2,1)S(1)} %get-tuple-element.38.after_ref.q0_ref, f32[384,256]{1,0:T(8,128)S(1)} %get-tuple-element.40.o1_ref, ...), custom_call_target="tpu_custom_call" | custom-call | tf_op jit(solution)/shard_map/pallas_call | solution.py:29
  45.5 2.8 %collective-permute-start.10 = (bf16[96,2048]{1,0:T(8,128)(2,1)S(1)}, bf16[96,2048]{1,0:T(8,128)(2,1)S(1)}, u32[]{:S(2)}, u32[]{:S(2)}) collective-permute-start(bf16[96,2048]{1,0:T(8,128)(2,1)S(1)} %get-tuple-element.47), channel_id=1, source_target_pairs={{0,3},{1,0},{2,1},{3,2},{4,7},{5,4},{6,5},{7,6},{8,11},{9,8},{10,9... | collective-permute-start | bytes 1179656 | tf_op jit(solution)/shard_map/ppermute | solution.py:593
  48.3 2.3 %collective-permute-start.9 = (bf16[96,2048]{1,0:T(8,128)(2,1)S(1)}, bf16[96,2048]{1,0:T(8,128)(2,1)S(1)}, u32[]{:S(2)}, u32[]{:S(2)}) collective-permute-start(bf16[96,2048]{1,0:T(8,128)(2,1)S(1)} %get-tuple-element.46), channel_id=1, source_target_pairs={{0,2},{1,3},{2,0},{3,1},{4,6},{5,7},{6,4},{7,5},{8,10},{9,11},{10,... | collective-permute-start | bytes 1179656 | tf_op jit(solution)/shard_map/ppermute | solution.py:593
  50.6 14.9 %collective-permute-done.10.rest_3_ = bf16[96,2048]{1,0:T(8,128)(2,1)S(1)} collective-permute-done((bf16[96,2048]{1,0:T(8,128)(2,1)S(1)}, bf16[96,2048]{1,0:T(8,128)(2,1)S(1)}, u32[]{:S(2)}, u32[]{:S(2)}) %collective-permute-start.10) | collective-permute-done | bytes 393248 | tf_op jit(solution)/shard_map/ppermute | solution.py:593
  65.5 3.4 %collective-permute-done.8.rest_1_ = bf16[96,2048]{1,0:T(8,128)(2,1)S(1)} collective-permute-done((bf16[96,2048]{1,0:T(8,128)(2,1)S(1)}, bf16[96,2048]{1,0:T(8,128)(2,1)S(1)}, u32[]{:S(2)}, u32[]{:S(2)}) %collective-permute-start.8) | collective-permute-done | bytes 393248 | tf_op jit(solution)/shard_map/ppermute | solution.py:593
  68.8 0.0 collective-permute-done.9.rest_2_
  68.8 0.4 shard_map.135
  69.3 0.1 collective-permute-start.11
  69.4 3.2 %collective-permute-start.13 = (bf16[96,2048]{1,0:T(8,128)(2,1)S(1)}, bf16[96,2048]{1,0:T(8,128)(2,1)S(1)}, u32[]{:S(2)}, u32[]{:S(2)}) collective-permute-start(bf16[96,2048]{1,0:T(8,128)(2,1)S(1)} %get-tuple-element.49.own_ref), channel_id=1, source_target_pairs={{0,3},{1,0},{2,1},{3,2},{4,7},{5,4},{6,5},{7,6},{8,11},{9,8},{10,9... | collective-permute-start | bytes 1179656 | tf_op jit(solution)/shard_map/ppermute | solution.py:596
  72.6 7.1 %collective-permute-done.11.rest_0_ = bf16[96,2048]{1,0:T(8,128)(2,1)S(1)} collective-permute-done((bf16[96,2048]{1,0:T(8,128)(2,1)S(1)}, bf16[96,2048]{1,0:T(8,128)(2,1)S(1)}, u32[]{:S(2)}, u32[]{:S(2)}) %collective-permute-start.11) | collective-permute-done | bytes 393248 | tf_op jit(solution)/shard_map/ppermute | solution.py:595
  79.7 0.1 collective-permute-start.12
  79.8 3.3 %collective-permute-start.14 = (bf16[48,2048]{1,0:T(8,128)(2,1)S(1)}, bf16[48,2048]{1,0:T(8,128)(2,1)S(1)}, u32[]{:S(2)}, u32[]{:S(2)}) collective-permute-start(bf16[48,2048]{1,0:T(8,128)(2,1)S(1)} %slice.9), channel_id=1, source_target_pairs={{0,3},{1,0},{2,1},{3,2},{4,7},{5,4},{6,5},{7,6},{8,11},{9,8},{10,9... | collective-permute-start | bytes 589832 | tf_op jit(solution)/shard_map/ppermute | solution.py:600
  83.1 5.3 %all-gather.2.cloned.1.call-done.w_ref = bf16[2048,4224]{1,0:T(8,128)(2,1)} async-done(((bf16[64,4224]{1,0:T(8,128)(2,1)}), bf16[2048,4224]{1,0:T(8,128)(2,1)}) %all-gather.2.cloned.1.call-update) | async-done | bytes 17301520 | tf_op jit(solution)/shard_map/all_gather | solution.py:582
  88.4 8.5 %shard_map.136 = (bf16[96,2048]{1,0:T(8,128)(2,1)S(1)}, bf16[96,2048]{1,0:T(8,128)(2,1)S(1)}, bf16[2048,1408]{1,0:T(8,128)(2,1)S(1)}, bf16[2048,1408]{1,0:T(8,128)(2,1)S(1)}, bf16[2048,1408]{1,0:T(8,128)(2,1)S(1)}) custom-call(bf16[2048,4224]{1,0:T(8,128)(2,1)} %all-gather.2.cloned.1.call-done.w_ref, bf16[96,2048]{1,0:T(8,128)(2,1)S(1)} %collective-permute-done.11.rest_0_, ...), custom_call_target="tpu_custom_call" | custom-call | tf_op jit(solution)/shard_map/pallas_call | solution.py:29
  96.9 0.0 collective-permute-done.14.lower_ref
  96.9 4.7 %shard_map.137 = (bf16[96,2048]{1,0:T(8,128)(2,1)S(1)}, bf16[96,2048]{1,0:T(8,128)(2,1)S(1)}) custom-call(bf16[96,2048]{1,0:T(8,128)(2,1)S(1)} %get-tuple-element.49.own_ref, bf16[48,2048]{1,0:T(8,128)(2,1)S(1)} %collective-permute-done.12.upper_ref, bf16[48,2048]{1,0:T(8,128)(2,1)S(1)} %collective-permute-done.14.lower_ref, ...), custom_call_target="tpu_custom_call" | custom-call | tf_op jit(solution)/shard_map/pallas_call | solution.py:29
  101.6 3.1 %collective-permute-start.17 = (bf16[96,2048]{1,0:T(8,128)(2,1)S(1)}, bf16[96,2048]{1,0:T(8,128)(2,1)S(1)}, u32[]{:S(2)}, u32[]{:S(2)}) collective-permute-start(bf16[96,2048]{1,0:T(8,128)(2,1)S(1)} %get-tuple-element.56), channel_id=1, source_target_pairs={{0,2},{1,3},{2,0},{3,1},{4,6},{5,7},{6,4},{7,5},{8,10},{9,11},{10,... | collective-permute-start | bytes 1179656 | tf_op jit(solution)/shard_map/ppermute | solution.py:606
  104.7 1.2 collective-permute-start.15
  105.8 0.9 collective-permute-start.16
  106.7 8.5 %collective-permute-done.17.rest_3_ = bf16[96,2048]{1,0:T(8,128)(2,1)S(1)} collective-permute-done((bf16[96,2048]{1,0:T(8,128)(2,1)S(1)}, bf16[96,2048]{1,0:T(8,128)(2,1)S(1)}, u32[]{:S(2)}, u32[]{:S(2)}) %collective-permute-start.17) | collective-permute-done | bytes 393248 | tf_op jit(solution)/shard_map/ppermute | solution.py:606
  115.2 7.7 %collective-permute-done.15.rest_1_ = bf16[96,2048]{1,0:T(8,128)(2,1)S(1)} collective-permute-done((bf16[96,2048]{1,0:T(8,128)(2,1)S(1)}, bf16[96,2048]{1,0:T(8,128)(2,1)S(1)}, u32[]{:S(2)}, u32[]{:S(2)}) %collective-permute-start.15) | collective-permute-done | bytes 393248 | tf_op jit(solution)/shard_map/ppermute | solution.py:603
  122.9 0.0 collective-permute-done.16.rest_2_
  122.9 1.0 last_sum.1
  (18 shorter events, 0.1 us)
Async XLA Ops:
  6.5 81.9 %all-gather.2.cloned.1.call-start = ((), (), s32[]{:S(2)}) async-start(), calls=%async_computation | async-start | bytes 17842176 | tf_op jit(solution)/shard_map/all_gather | solution.py:582
  6.5 17.7 %copy-start.1 = (bf16[384,512]{1,0:T(8,128)(2,1)S(1)}, bf16[384,512]{1,0:T(8,128)(2,1)}, u32[]{:S(2)}) copy-start(bf16[384,512]{1,0:T(8,128)(2,1)} %q_ref.3) | copy-start | bytes 1179652
  16.6 1.4 %collective-permute-start = (bf16[4,128,128]{2,1,0:T(8,128)(2,1)S(1)}, bf16[4,128,128]{2,1,0:T(8,128)(2,1)S(1)}, u32[]{:S(2)}, u32[]{:S(2)}) collective-permute-start(bf16[4,128,128]{2,1,0:T(8,128)(2,1)S(1)} %get-tuple-element.31.own_ref), channel_id=1, source_target_pairs={{0,4},{4,0},{1,5},{5,1},{2,6},{6,2},{3,7},{7,3},{8,12},{12,8},{9,1... | collective-permute-start | bytes 393224 | tf_op jit(solution)/shard_map/ppermute | solution.py:356
  18.3 8.9 %collective-permute-start.1 = (bf16[2,128,128]{2,1,0:T(8,128)(2,1)S(1)}, bf16[2,128,128]{2,1,0:T(8,128)(2,1)S(1)}, u32[]{:S(2)}, u32[]{:S(2)}) collective-permute-start(bf16[2,128,128]{2,1,0:T(8,128)(2,1)S(1)} %get-tuple-element.32.after_ref.rest_0_), channel_id=1, source_target_pairs={{0,8},{8,16},{16,24},{24,0},{1,9},{9,17},{17,25},{25,1},{2,10},{10... | collective-permute-start | bytes 196616 | tf_op jit(solution)/shard_map/ppermute | solution.py:359
  20.0 7.2 %collective-permute-start.2 = (bf16[2,128,128]{2,1,0:T(8,128)(2,1)S(1)}, bf16[2,128,128]{2,1,0:T(8,128)(2,1)S(1)}, u32[]{:S(2)}, u32[]{:S(2)}) collective-permute-start(bf16[2,128,128]{2,1,0:T(8,128)(2,1)S(1)} %get-tuple-element.32.after_ref.rest_0_), channel_id=1, source_target_pairs={{0,16},{8,24},{16,0},{24,8},{1,17},{9,25},{17,1},{25,9},{2,18},{10... | collective-permute-start | bytes 196616 | tf_op jit(solution)/shard_map/ppermute | solution.py:359
  22.9 5.8 %collective-permute-start.3 = (bf16[2,128,128]{2,1,0:T(8,128)(2,1)S(1)}, bf16[2,128,128]{2,1,0:T(8,128)(2,1)S(1)}, u32[]{:S(2)}, u32[]{:S(2)}) collective-permute-start(bf16[2,128,128]{2,1,0:T(8,128)(2,1)S(1)} %get-tuple-element.32.after_ref.rest_0_), channel_id=1, source_target_pairs={{0,24},{8,0},{16,8},{24,16},{1,25},{9,1},{17,9},{25,17},{2,26},{10... | collective-permute-start | bytes 196616 | tf_op jit(solution)/shard_map/ppermute | solution.py:359
  29.4 12.7 %copy-start.3 = (bf16[384,512]{1,0:T(8,128)(2,1)S(1)}, bf16[384,512]{1,0:T(8,128)(2,1)}, u32[]{:S(2)}) copy-start(bf16[384,512]{1,0:T(8,128)(2,1)} %gates_ref.1) | copy-start | bytes 1179652
  29.4 12.7 %copy-start.5 = (f32[64]{0:T(128)S(1)}, f32[64]{0:T(128)}, u32[]{:S(2)}) copy-start(f32[64]{0:T(128)} %param.19) | copy-start | bytes 772
  29.4 9.6 %collective-permute-start.4 = (bf16[2,128,128]{2,1,0:T(8,128)(2,1)S(1)}, bf16[2,128,128]{2,1,0:T(8,128)(2,1)S(1)}, u32[]{:S(2)}, u32[]{:S(2)}) collective-permute-start(bf16[2,128,128]{2,1,0:T(8,128)(2,1)S(1)} %get-tuple-element.39.after_ref), channel_id=1, source_target_pairs={{0,32},{32,64},{64,96},{96,0},{1,33},{33,65},{65,97},{97,1},{2,34}... | collective-permute-start | bytes 196616 | tf_op jit(solution)/shard_map/ppermute | solution.py:365
  31.4 9.5 %collective-permute-start.5 = (bf16[2,128,128]{2,1,0:T(8,128)(2,1)S(1)}, bf16[2,128,128]{2,1,0:T(8,128)(2,1)S(1)}, u32[]{:S(2)}, u32[]{:S(2)}) collective-permute-start(bf16[2,128,128]{2,1,0:T(8,128)(2,1)S(1)} %get-tuple-element.39.after_ref), channel_id=1, source_target_pairs={{0,64},{32,96},{64,0},{96,32},{1,65},{33,97},{65,1},{97,33},{2,66}... | collective-permute-start | bytes 196616 | tf_op jit(solution)/shard_map/ppermute | solution.py:365
  35.1 5.9 %collective-permute-start.6 = (bf16[2,128,128]{2,1,0:T(8,128)(2,1)S(1)}, bf16[2,128,128]{2,1,0:T(8,128)(2,1)S(1)}, u32[]{:S(2)}, u32[]{:S(2)}) collective-permute-start(bf16[2,128,128]{2,1,0:T(8,128)(2,1)S(1)} %get-tuple-element.39.after_ref), channel_id=1, source_target_pairs={{0,96},{32,0},{64,32},{96,64},{1,97},{33,1},{65,33},{97,65},{2,98}... | collective-permute-start | bytes 196616 | tf_op jit(solution)/shard_map/ppermute | solution.py:365
  36.1 7.2 %copy-start = (bf16[512,2048]{1,0:T(8,128)(2,1)S(1)}, bf16[512,2048]{1,0:T(8,128)(2,1)}, u32[]{:S(2)}) copy-start(bf16[512,2048]{1,0:T(8,128)(2,1)} %w_ref.1) | copy-start | bytes 6291460
  41.8 1.5 %collective-permute-start.7 = (bf16[2,128,128]{2,1,0:T(8,128)(2,1)S(1)}, bf16[2,128,128]{2,1,0:T(8,128)(2,1)S(1)}, u32[]{:S(2)}, u32[]{:S(2)}) collective-permute-start(bf16[2,128,128]{2,1,0:T(8,128)(2,1)S(1)} %shard_map.132.mine_ref), channel_id=1, source_target_pairs={{0,4},{4,0},{1,5},{5,1},{2,6},{6,2},{3,7},{7,3},{8,12},{12,8},{9,1... | collective-permute-start | bytes 196616 | tf_op jit(solution)/shard_map/ppermute | solution.py:368
  43.4 25.5 %copy-start.2 = (bf16[96,2048]{1,0:T(8,128)(2,1)S(1)}, bf16[96,2048]{1,0:T(8,128)(2,1)}, u32[]{:S(2)}) copy-start(bf16[96,2048]{1,0:T(8,128)(2,1)} %stream_ref.1) | copy-start | bytes 1179652
  43.4 25.5 %copy-start.4 = (f32[2048]{0:T(1024)S(1)}, f32[2048]{0:T(1024)}, u32[]{:S(2)}) copy-start(f32[2048]{0:T(1024)} %param.22) | copy-start | bytes 24580
  45.5 20.0 %collective-permute-start.10 = (bf16[96,2048]{1,0:T(8,128)(2,1)S(1)}, bf16[96,2048]{1,0:T(8,128)(2,1)S(1)}, u32[]{:S(2)}, u32[]{:S(2)}) collective-permute-start(bf16[96,2048]{1,0:T(8,128)(2,1)S(1)} %get-tuple-element.47), channel_id=1, source_target_pairs={{0,3},{1,0},{2,1},{3,2},{4,7},{5,4},{6,5},{7,6},{8,11},{9,8},{10,9... | collective-permute-start | bytes 1179656 | tf_op jit(solution)/shard_map/ppermute | solution.py:593
  48.3 20.5 %collective-permute-start.8 = (bf16[96,2048]{1,0:T(8,128)(2,1)S(1)}, bf16[96,2048]{1,0:T(8,128)(2,1)S(1)}, u32[]{:S(2)}, u32[]{:S(2)}) collective-permute-start(bf16[96,2048]{1,0:T(8,128)(2,1)S(1)} %get-tuple-element.45), channel_id=1, source_target_pairs={{0,1},{1,2},{2,3},{3,0},{4,5},{5,6},{6,7},{7,4},{8,9},{9,10},{10,1... | collective-permute-start | bytes 1179656 | tf_op jit(solution)/shard_map/ppermute | solution.py:593
  48.3 20.5 %collective-permute-start.9 = (bf16[96,2048]{1,0:T(8,128)(2,1)S(1)}, bf16[96,2048]{1,0:T(8,128)(2,1)S(1)}, u32[]{:S(2)}, u32[]{:S(2)}) collective-permute-start(bf16[96,2048]{1,0:T(8,128)(2,1)S(1)} %get-tuple-element.46), channel_id=1, source_target_pairs={{0,2},{1,3},{2,0},{3,1},{4,6},{5,7},{6,4},{7,5},{8,10},{9,11},{10,... | collective-permute-start | bytes 1179656 | tf_op jit(solution)/shard_map/ppermute | solution.py:593
  69.3 10.4 %collective-permute-start.11 = (bf16[96,2048]{1,0:T(8,128)(2,1)S(1)}, bf16[96,2048]{1,0:T(8,128)(2,1)S(1)}, u32[]{:S(2)}, u32[]{:S(2)}) collective-permute-start(bf16[96,2048]{1,0:T(8,128)(2,1)S(1)} %get-tuple-element.49.own_ref), channel_id=1, source_target_pairs={{0,1},{1,2},{2,3},{3,0},{4,5},{5,6},{6,7},{7,4},{8,9},{9,10},{10,1... | collective-permute-start | bytes 1179656 | tf_op jit(solution)/shard_map/ppermute | solution.py:595
  69.4 10.4 %collective-permute-start.13 = (bf16[96,2048]{1,0:T(8,128)(2,1)S(1)}, bf16[96,2048]{1,0:T(8,128)(2,1)S(1)}, u32[]{:S(2)}, u32[]{:S(2)}) collective-permute-start(bf16[96,2048]{1,0:T(8,128)(2,1)S(1)} %get-tuple-element.49.own_ref), channel_id=1, source_target_pairs={{0,3},{1,0},{2,1},{3,2},{4,7},{5,4},{6,5},{7,6},{8,11},{9,8},{10,9... | collective-permute-start | bytes 1179656 | tf_op jit(solution)/shard_map/ppermute | solution.py:596
  79.7 17.1 %collective-permute-start.12 = (bf16[48,2048]{1,0:T(8,128)(2,1)S(1)}, bf16[48,2048]{1,0:T(8,128)(2,1)S(1)}, u32[]{:S(2)}, u32[]{:S(2)}) collective-permute-start(bf16[48,2048]{1,0:T(8,128)(2,1)S(1)} %slice.8), channel_id=1, source_target_pairs={{0,1},{1,2},{2,3},{3,0},{4,5},{5,6},{6,7},{7,4},{8,9},{9,10},{10,1... | collective-permute-start | bytes 589832 | tf_op jit(solution)/shard_map/ppermute | solution.py:599
  79.8 17.0 %collective-permute-start.14 = (bf16[48,2048]{1,0:T(8,128)(2,1)S(1)}, bf16[48,2048]{1,0:T(8,128)(2,1)S(1)}, u32[]{:S(2)}, u32[]{:S(2)}) collective-permute-start(bf16[48,2048]{1,0:T(8,128)(2,1)S(1)} %slice.9), channel_id=1, source_target_pairs={{0,3},{1,0},{2,1},{3,2},{4,7},{5,4},{6,5},{7,6},{8,11},{9,8},{10,9... | collective-permute-start | bytes 589832 | tf_op jit(solution)/shard_map/ppermute | solution.py:600
  101.6 13.6 %collective-permute-start.17 = (bf16[96,2048]{1,0:T(8,128)(2,1)S(1)}, bf16[96,2048]{1,0:T(8,128)(2,1)S(1)}, u32[]{:S(2)}, u32[]{:S(2)}) collective-permute-start(bf16[96,2048]{1,0:T(8,128)(2,1)S(1)} %get-tuple-element.56), channel_id=1, source_target_pairs={{0,2},{1,3},{2,0},{3,1},{4,6},{5,7},{6,4},{7,5},{8,10},{9,11},{10,... | collective-permute-start | bytes 1179656 | tf_op jit(solution)/shard_map/ppermute | solution.py:606
  104.7 18.3 %collective-permute-start.15 = (bf16[96,2048]{1,0:T(8,128)(2,1)S(1)}, bf16[96,2048]{1,0:T(8,128)(2,1)S(1)}, u32[]{:S(2)}, u32[]{:S(2)}) collective-permute-start(bf16[96,2048]{1,0:T(8,128)(2,1)S(1)} %get-tuple-element.54), channel_id=1, source_target_pairs={{0,3},{1,0},{2,1},{3,2},{4,7},{5,4},{6,5},{7,6},{8,11},{9,8},{10,9... | collective-permute-start | bytes 1179656 | tf_op jit(solution)/shard_map/ppermute | solution.py:603
  105.8 17.1 %collective-permute-start.16 = (bf16[96,2048]{1,0:T(8,128)(2,1)S(1)}, bf16[96,2048]{1,0:T(8,128)(2,1)S(1)}, u32[]{:S(2)}, u32[]{:S(2)}) collective-permute-start(bf16[96,2048]{1,0:T(8,128)(2,1)S(1)} %get-tuple-element.55), channel_id=1, source_target_pairs={{0,1},{1,2},{2,3},{3,0},{4,5},{5,6},{6,7},{7,4},{8,9},{9,10},{10,1... | collective-permute-start | bytes 1179656 | tf_op jit(solution)/shard_map/ppermute | solution.py:604
Sparse Core Ops, SparseCore 0:
  9.6 78.7 all-gather.1

commit v9 on v8

--- a/solution.py
+++ b/solution.py
@@ -432,6 +432,55 @@
     )
 
 
+def tail_kernel(after_ref, far_ref, out_ref, sem):
+    head = far_ref.shape[1] - out_ref.shape[1]
+    copy = pltpu.make_async_copy(far_ref.at[:, pl.ds(head, out_ref.shape[1])], out_ref, sem)
+    copy.start()
+    copy.wait()
+
+
+def planes_kernel(*refs):
+    parts, out_ref = refs[:-1], refs[-1]
+    place = lax.axis_index(SP[0])
+    size = len(parts)
+    for k, part in enumerate(parts):
+        out_ref[lax.rem(place - k + size, size)] = part[...]
+
+
+def lines_kernel(*refs):
+    parts, out_ref = refs[:-1], refs[-1]
+    place = lax.axis_index(SP[1])
+    size = len(parts)
+    for k, part in enumerate(parts):
+        for plane in range(part.shape[0]):
+            out_ref[plane, lax.rem(place - k + size, size)] = part[plane]
+
+
+def tails_of_all(after, down):
+    plane, line, core = SP
+    shape = (down.shape[0], TAIL)
+    far = [after, pltpu.with_memory_space_constraint(down, pltpu.HBM)]
+    (tail,) = call(tail_kernel, [], [(shape, BF)], [pltpu.SemaphoreType.DMA(())], far=far)
+    size = lax.axis_size(plane)
+    parts = [tail] + [lax.ppermute(tail, plane, ring(size, k)) for k in range(1, size)]
+    (tail,) = call(planes_kernel, parts, [((size, *shape), BF)])
+    size = lax.axis_size(line)
+    parts = [tail] + [lax.ppermute(tail, line, ring(size, k)) for k in range(1, size)]
+    shape = (tail.shape[0], size, *shape)
+    (tail,) = call(lines_kernel, parts, [(shape, BF)])
+    return tail, lax.ppermute(tail, core, [(0, 1), (1, 0)])
+
+
+def half_kernel(which, rows_ref, out_ref):
+    half = out_ref.shape[0]
+    out_ref[...] = rows_ref[which * half : (which + 1) * half, :]
+
+
+def half_of(rows, which):
+    shape = (rows.shape[0] // 2, rows.shape[1])
+    return call(functools.partial(half_kernel, which), [rows], [(shape, BF)])[0]
+
+
 def activated(rows, gate, up):
     got = dot(rows, jnp.concatenate([gate, up], axis=1))
     width = gate.shape[1]
@@ -448,12 +497,14 @@
 AHEAD = 3
 UP_GROUPS = (1, 2, 4, 4)
 DOWN_GROUPS = (8,)
+TAIL = 512
 
 
 def first_channels_kernel(count, w_ref, *rest):
-    parts, out_refs = rest[:count], rest[count : 2 * count]
-    gate_ref, up_ref, down_ref, rows_ref, hidden_ref, in_sems, down_sems = rest[2 * count :]
+    parts, tails, out_refs = rest[:count], rest[count : count + 2], rest[count + 2 : 2 * count + 2]
+    gate_ref, up_ref, down_ref, rows_ref, hidden_ref, in_sems, down_sems = rest[2 * count + 2 :]
     width, hidden = gate_ref.shape
+    head = hidden - TAIL
     block = parts[0].shape[0]
     groups, spans = [], []
     for many, spread in ((hidden // TILE, UP_GROUPS), (width // STRIP, DOWN_GROUPS)):
@@ -469,8 +520,9 @@
         groups.append(group)
     for g, strips in enumerate(spans[1]):
         here = pl.ds(strips[0] * STRIP, len(strips) * STRIP)
-        from_ref = w_ref.at[here, pl.ds(2 * hidden, hidden)]
-        groups.append([pltpu.make_async_copy(from_ref, down_ref.at[here, :], down_sems.at[g])])
+        from_ref = w_ref.at[here, pl.ds(2 * hidden, head)]
+        to_ref = down_ref.at[here, pl.ds(0, head)]
+        groups.append([pltpu.make_async_copy(from_ref, to_ref, down_sems.at[g])])
 
     def begin(g):
         if g < len(groups):
@@ -484,6 +536,12 @@
 
     for g in range(AHEAD):
         begin(g)
+    core = lax.axis_index(SP[2])
+    for c, tail in enumerate(tails):
+        planes, lines, rows, _ = tail.shape
+        for i in range(planes * lines):
+            start = pl.multiple_of((2 * i + (core if c == 0 else 1 - core)) * rows, rows)
+            down_ref[pl.ds(start, rows), head:] = tail[i // lines, i % lines]
     for k, part in enumerate(parts):
         rows_ref[k * block : (k + 1) * block, :] = part[...]
     for g, tiles in enumerate(spans[0]):
@@ -500,12 +558,12 @@
                 out_ref[:, here] = got[k * block : (k + 1) * block, :].astype(BF)
 
 
-def first_channels(weights, parts, hidden):
+def first_channels(weights, parts, tails, hidden):
     block, width = parts[0].shape
     count = len(parts)
     out = call(
         functools.partial(first_channels_kernel, count),
-        parts,
+        [*parts, *tails],
         [((block, width), BF)] * count + [((width, hidden), BF)] * 3,
         [
             pltpu.VMEM((block * count, width), BF),
@@ -578,7 +636,8 @@
     w_down,
 ):
     hidden = w_gate.shape[1]
-    weights = jnp.concatenate([w_gate, w_up, w_down.T], axis=1)
+    down = w_down.T
+    weights = jnp.concatenate([w_gate, w_up, down[:, : hidden - TAIL]], axis=1)
     weights = lax.all_gather(weights, SP, axis=0, tiled=True)
     size = lax.axis_size("tp")
     before, total, solved, decay, grown = keys_side(keys, values, beta_pre, decay_pre)
@@ -590,16 +649,24 @@
         lambda x: queries_side(pairs // 2, x, queries, decay, solved, before, grown),
     )
     parts = mixed_and_projected(size, early, late, states, gate, w_out)
-    parts = [parts[0]] + [lax.ppermute(parts[k], "tp", ring(size, k)) for k in (1, 2, 3)]
-    middle, normed = normed_rows(stream, norm_gain, parts)
+    return feed_forward(
+        parts, size, stream, norm_gain, weights, down, hidden
+    )
+
+
+def feed_forward(parts, size, stream, norm_gain, weights, down, hidden):
+    got = [parts[0]]
+    for k in range(1, size):
+        got.append(lax.ppermute(parts[k], "tp", ring(size, k)))
+    tails = tails_of_all(parts[1], down)
+    middle, normed = normed_rows(stream, norm_gain, got)
     right = lax.ppermute(normed, "tp", ring(size, 1))
     left = lax.ppermute(normed, "tp", ring(size, -1))
-    half = normed.shape[0] // 2
     across = [
-        lax.ppermute(right[:half], "tp", ring(size, 1)),
-        lax.ppermute(left[half:], "tp", ring(size, -1)),
+        lax.ppermute(half_of(right, 0), "tp", ring(size, 1)),
+        lax.ppermute(half_of(left, 1), "tp", ring(size, -1)),
     ]
-    sums, projections = first_channels(weights, [right, left], hidden)
+    sums, projections = first_channels(weights, [right, left], tails, hidden)
     back = [lax.ppermute(sums[0], "tp", ring(size, -1))]
     back.append(lax.ppermute(sums[1], "tp", ring(size, 1)))
     own, last = more_channels([normed, *across], projections)

time: 132 us -> 166 us (1.26)
  waiting for transfers between devices: 52.6 us -> 74.3 us
  starting transfers between devices: 29.9 us -> 37.3 us
  Pallas kernels: 32.7 us -> 35.5 us
  local copies, waits for them, and re-layouts: 0.06 us -> 1.99 us
    ppermute x10 -> x17, waiting for transfers between devices: 41.6 us -> 71 us  [the longest x3 21.6 us: tails_of_all(): lax.ppermute(tail, line, ring(size, k))]
    ppermute x10 -> x17, starting transfers between devices: 16.8 us -> 24 us  [the longest x3 5.9 us: tails_of_all(): lax.ppermute(tail, line, ring(size, k))]
    all_gather x1, waiting for transfers between devices: 5.28 us -> 0.01 us  [per_device(): weights = lax.all_gather(weights, SP, axis=0, tiled=True)]
    pallas_call x11 -> x16, Pallas kernels: 31.7 us -> 34.5 us  [call(): pl.pallas_call(kernel, in_specs=[FAR] * len(far) + [FULL] * len(near), ou...]
  transfers between devices with their start and end apart: 19 -> 26, of which waited for: 10 -> 16; matrix products, arithmetic and copies ran while one was open for 0% -> 0% of each run, Pallas kernels for 21% -> 18%
where the time goes in v9:
time: 166 us; the launch traced here: 165 us
  waiting for transfers between devices  74.3 us (45%)
  starting transfers between devices  37.3 us (22%)
  Pallas kernels  35.5 us (21%)
  between operations  13.6 us (8%)
  local copies, waits for them, and re-layouts  1.99 us (1%)
  other arithmetic  1.99 us (1%)
    pallas_call x16, Pallas kernels, call(): pl.pallas_call(kernel, in_specs=[FAR] * len(far) + [FULL] * len(near), ou...  34.5 us
    ppermute x3, waiting for transfers between devices, tails_of_all(): lax.ppermute(tail, line, ring(size, k))  21.6 us
    ppermute x3, waiting for transfers between devices, feed_forward(): got.append(lax.ppermute(parts[k], 'tp', ring(size, k)))  17 us
    ppermute x1, waiting for transfers between devices, feed_forward(): back.append(lax.ppermute(last, 'tp', ring(size, 2)))  11.4 us
    ppermute x1, waiting for transfers between devices, feed_forward(): right = lax.ppermute(normed, 'tp', ring(size, 1))  8.57 us
    ppermute x3, starting transfers between devices, state_ahead(): planes = [lax.ppermute(whole, plane, ring(size, k)) for k in range(1, size)]  6.98 us
    ppermute x3, waiting for transfers between devices, tails_of_all(): lax.ppermute(tail, plane, ring(size, k))  6.78 us
    ppermute x3, starting transfers between devices, state_ahead(): lax.ppermute(chip, line, ring(size, k))  6 us
  transfers between devices with their start and end apart: 26, of which 16 were waited for; matrix products, arithmetic and copies ran while one was open for 0% of the time, Pallas kernels for 18%

profile of v9, /device:TPU:0, one launch (start us, length us, event | category | flops | bytes accessed | tf_op | source)
XLA Modules:
  0.0 164.7 jit_solution(2936082168329184988)
XLA Ops:
  6.5 1.0 slice.4
  7.5 2.0 %pad_maximum_fusion = bf16[64,3712]{1,0:T(8,128)(2,1)} fusion(bf16[64,896]{1,0:T(8,128)(2,1)S(1)} %slice.4, bf16[64,1408]{1,0:T(8,128)(2,1)} %param.24, bf16[64,1408]{1,0:T(8,128)(2,1)} %param.23), kind=kLoop, calls=%fused_computation | loop fusion | flops 1425408 | bytes 950272 | tf_op jit(solution)/shard_map/concatenate | solution.py:640
  9.5 8.1 %shard_map.127 = (bf16[12,128,128]{2,1,0:T(8,128)(2,1)S(1)}, bf16[4,128,128]{2,1,0:T(8,128)(2,1)S(1)}, bf16[12,128,384]{2,1,0:T(8,128)(2,1)S(1)}, bf16[12,128,256]{2,1,0:T(8,128)(2,1)S(1)}, f32[384,512]{1,0:T(8,128)S(1)}) custom-call(bf16[384,512]{1,0:T(8,128)(2,1)} %k_far_ref.1, bf16[384,512]{1,0:T(8,128)(2,1)} %v_far_ref.1, f32[8,384]{1,0:T(8,128)} %beta_far_ref.1, ...), custom_call_target="tpu_custom_call" | custom-call | tf_op jit(solution)/shard_map/pallas_call | solution.py:29
  17.7 1.3 collective-permute-done.other_ref
  19.3 1.7 %collective-permute-start.1 = (bf16[2,128,128]{2,1,0:T(8,128)(2,1)S(1)}, bf16[2,128,128]{2,1,0:T(8,128)(2,1)S(1)}, u32[]{:S(2)}, u32[]{:S(2)}) collective-permute-start(bf16[2,128,128]{2,1,0:T(8,128)(2,1)S(1)} %get-tuple-element.32.after_ref.rest_0_), channel_id=1, source_target_pairs={{0,8},{8,16},{16,24},{24,0},{1,9},{9,17},{17,25},{25,1},{2,10},{10... | collective-permute-start | bytes 196616 | tf_op jit(solution)/shard_map/ppermute | solution.py:359
  21.0 2.9 %collective-permute-start.2 = (bf16[2,128,128]{2,1,0:T(8,128)(2,1)S(1)}, bf16[2,128,128]{2,1,0:T(8,128)(2,1)S(1)}, u32[]{:S(2)}, u32[]{:S(2)}) collective-permute-start(bf16[2,128,128]{2,1,0:T(8,128)(2,1)S(1)} %get-tuple-element.32.after_ref.rest_0_), channel_id=1, source_target_pairs={{0,16},{8,24},{16,0},{24,8},{1,17},{9,25},{17,1},{25,9},{2,18},{10... | collective-permute-start | bytes 196616 | tf_op jit(solution)/shard_map/ppermute | solution.py:359
  23.9 1.3 collective-permute-start.3
  25.3 1.0 copy-done.1
  26.2 2.9 %shard_map.129 = (f32[384,256]{1,0:T(8,128)S(1)}, bf16[384,256]{1,0:T(8,128)(2,1)S(1)}) custom-call(bf16[2,128,128]{2,1,0:T(8,128)(2,1)S(1)} %get-tuple-element.32.after_ref.rest_0_, bf16[384,512]{1,0:T(8,128)(2,1)S(1)} %copy-done.1, bf16[12,128,256]{2,1,0:T(8,128)(2,1)S(1)} %get-tuple-element.33.d_ref, bf16[12,128,384]{2,1,0:T(8,128)(2,1)S(1)} %get-tuple-element.34.y_ref, ...), custom_call_target="tpu_custom_call" | custom-call | tf_op jit(solution)/shard_map/pallas_call | solution.py:29
  30.3 2.2 %collective-permute-start.4 = (bf16[2,128,128]{2,1,0:T(8,128)(2,1)S(1)}, bf16[2,128,128]{2,1,0:T(8,128)(2,1)S(1)}, u32[]{:S(2)}, u32[]{:S(2)}) collective-permute-start(bf16[2,128,128]{2,1,0:T(8,128)(2,1)S(1)} %get-tuple-element.39.after_ref), channel_id=1, source_target_pairs={{0,32},{32,64},{64,96},{96,0},{1,33},{33,65},{65,97},{97,1},{2,34}... | collective-permute-start | bytes 196616 | tf_op jit(solution)/shard_map/ppermute | solution.py:365
  32.4 4.0 %collective-permute-start.5 = (bf16[2,128,128]{2,1,0:T(8,128)(2,1)S(1)}, bf16[2,128,128]{2,1,0:T(8,128)(2,1)S(1)}, u32[]{:S(2)}, u32[]{:S(2)}) collective-permute-start(bf16[2,128,128]{2,1,0:T(8,128)(2,1)S(1)} %get-tuple-element.39.after_ref), channel_id=1, source_target_pairs={{0,64},{32,96},{64,0},{96,32},{1,65},{33,97},{65,1},{97,33},{2,66}... | collective-permute-start | bytes 196616 | tf_op jit(solution)/shard_map/ppermute | solution.py:365
  36.4 0.8 collective-permute-start.6
  37.3 2.9 %shard_map.131 = (f32[384,256]{1,0:T(8,128)S(1)}, bf16[384,256]{1,0:T(8,128)(2,1)S(1)}) custom-call(bf16[2,128,128]{2,1,0:T(8,128)(2,1)S(1)} %get-tuple-element.39.after_ref, bf16[384,512]{1,0:T(8,128)(2,1)S(1)} %copy-done.2, bf16[12,128,256]{2,1,0:T(8,128)(2,1)S(1)} %get-tuple-element.33.d_ref, bf16[12,128,384]{2,1,0:T(8,128)(2,1)S(1)} %get-tuple-element.34.y_ref, ...), custom_call_target="tpu_custom_call" | custom-call | tf_op jit(solution)/shard_map/pallas_call | solution.py:29
  40.7 0.9 shard_map.132.mine_ref
  42.2 0.9 collective-permute-done.7.theirs_ref
  43.2 2.1 %shard_map.134 = (f32[96,2048]{1,0:T(8,128)S(1)}, bf16[96,2048]{1,0:T(8,128)(2,1)S(1)}, bf16[96,2048]{1,0:T(8,128)(2,1)S(1)}, bf16[96,2048]{1,0:T(8,128)(2,1)S(1)}) custom-call(f32[384,256]{1,0:T(8,128)S(1)} %get-tuple-element.37.o0_ref, bf16[384,256]{1,0:T(8,128)(2,1)S(1)} %get-tuple-element.38.after_ref.q0_ref, f32[384,256]{1,0:T(8,128)S(1)} %get-tuple-element.40.o1_ref, ...), custom_call_target="tpu_custom_call" | custom-call | tf_op jit(solution)/shard_map/pallas_call | solution.py:29
  45.3 0.9 shard_map.138.refs_0_
  46.2 0.9 collective-permute-start.15
  47.0 2.6 %collective-permute-start.16 = (bf16[64,512]{1,0:T(8,128)(2,1)S(1)}, bf16[64,512]{1,0:T(8,128)(2,1)S(1)}, u32[]{:S(2)}, u32[]{:S(2)}) collective-permute-start(bf16[64,512]{1,0:T(8,128)(2,1)S(1)} %shard_map.138.refs_0_), channel_id=1, source_target_pairs={{0,64},{32,96},{64,0},{96,32},{1,65},{33,97},{65,1},{97,33},{2,66}... | collective-permute-start | bytes 196616 | tf_op jit(solution)/shard_map/ppermute | solution.py:465
  49.7 0.7 collective-permute-start.17
  50.4 3.1 %collective-permute-done.15.refs_1_ = bf16[64,512]{1,0:T(8,128)(2,1)S(1)} collective-permute-done((bf16[64,512]{1,0:T(8,128)(2,1)S(1)}, bf16[64,512]{1,0:T(8,128)(2,1)S(1)}, u32[]{:S(2)}, u32[]{:S(2)}) %collective-permute-start.15) | collective-permute-done | bytes 65568 | tf_op jit(solution)/shard_map/ppermute | solution.py:465
  53.5 2.6 %collective-permute-done.16.refs_2_ = bf16[64,512]{1,0:T(8,128)(2,1)S(1)} collective-permute-done((bf16[64,512]{1,0:T(8,128)(2,1)S(1)}, bf16[64,512]{1,0:T(8,128)(2,1)S(1)}, u32[]{:S(2)}, u32[]{:S(2)}) %collective-permute-start.16) | collective-permute-done | bytes 65568 | tf_op jit(solution)/shard_map/ppermute | solution.py:465
  56.2 1.0 collective-permute-done.17.refs_3_
  57.2 1.8 %collective-permute-start.18 = (bf16[4,64,512]{2,1,0:T(8,128)(2,1)S(1)}, bf16[4,64,512]{2,1,0:T(8,128)(2,1)S(1)}, u32[]{:S(2)}, u32[]{:S(2)}) collective-permute-start(bf16[4,64,512]{2,1,0:T(8,128)(2,1)S(1)} %shard_map.139.refs_0_), channel_id=1, source_target_pairs={{0,8},{8,16},{16,24},{24,0},{1,9},{9,17},{17,25},{25,1},{2,10},{10... | collective-permute-start | bytes 786440 | tf_op jit(solution)/shard_map/ppermute | solution.py:468
  58.9 1.6 collective-permute-start.19
  60.5 2.5 %collective-permute-start.20 = (bf16[4,64,512]{2,1,0:T(8,128)(2,1)S(1)}, bf16[4,64,512]{2,1,0:T(8,128)(2,1)S(1)}, u32[]{:S(2)}, u32[]{:S(2)}) collective-permute-start(bf16[4,64,512]{2,1,0:T(8,128)(2,1)S(1)} %shard_map.139.refs_0_), channel_id=1, source_target_pairs={{0,24},{8,0},{16,8},{24,16},{1,25},{9,1},{17,9},{25,17},{2,26},{10... | collective-permute-start | bytes 786440 | tf_op jit(solution)/shard_map/ppermute | solution.py:468
  63.1 10.0 %collective-permute-done.18.refs_1_ = bf16[4,64,512]{2,1,0:T(8,128)(2,1)S(1)} collective-permute-done((bf16[4,64,512]{2,1,0:T(8,128)(2,1)S(1)}, bf16[4,64,512]{2,1,0:T(8,128)(2,1)S(1)}, u32[]{:S(2)}, u32[]{:S(2)}) %collective-permute-start.18) | collective-permute-done | bytes 262176 | tf_op jit(solution)/shard_map/ppermute | solution.py:468
  73.1 10.9 %collective-permute-done.19.refs_2_ = bf16[4,64,512]{2,1,0:T(8,128)(2,1)S(1)} collective-permute-done((bf16[4,64,512]{2,1,0:T(8,128)(2,1)S(1)}, bf16[4,64,512]{2,1,0:T(8,128)(2,1)S(1)}, u32[]{:S(2)}, u32[]{:S(2)}) %collective-permute-start.19) | collective-permute-done | bytes 262176 | tf_op jit(solution)/shard_map/ppermute | solution.py:468
  84.0 0.7 collective-permute-done.20.refs_3_
  84.9 1.5 collective-permute-start.8
  86.4 1.8 %collective-permute-start.10 = (bf16[96,2048]{1,0:T(8,128)(2,1)S(1)}, bf16[96,2048]{1,0:T(8,128)(2,1)S(1)}, u32[]{:S(2)}, u32[]{:S(2)}) collective-permute-start(bf16[96,2048]{1,0:T(8,128)(2,1)S(1)} %get-tuple-element.47), channel_id=1, source_target_pairs={{0,3},{1,0},{2,1},{3,2},{4,7},{5,4},{6,5},{7,6},{8,11},{9,8},{10,9... | collective-permute-start | bytes 1179656 | tf_op jit(solution)/shard_map/ppermute | solution.py:660
  88.2 1.8 %collective-permute-start.9 = (bf16[96,2048]{1,0:T(8,128)(2,1)S(1)}, bf16[96,2048]{1,0:T(8,128)(2,1)S(1)}, u32[]{:S(2)}, u32[]{:S(2)}) collective-permute-start(bf16[96,2048]{1,0:T(8,128)(2,1)S(1)} %get-tuple-element.46), channel_id=1, source_target_pairs={{0,2},{1,3},{2,0},{3,1},{4,6},{5,7},{6,4},{7,5},{8,10},{9,11},{10,... | collective-permute-start | bytes 1179656 | tf_op jit(solution)/shard_map/ppermute | solution.py:660
  90.0 15.3 %collective-permute-done.10.rest_3_ = bf16[96,2048]{1,0:T(8,128)(2,1)S(1)} collective-permute-done((bf16[96,2048]{1,0:T(8,128)(2,1)S(1)}, bf16[96,2048]{1,0:T(8,128)(2,1)S(1)}, u32[]{:S(2)}, u32[]{:S(2)}) %collective-permute-start.10) | collective-permute-done | bytes 393248 | tf_op jit(solution)/shard_map/ppermute | solution.py:660
  105.3 1.7 %collective-permute-done.9.rest_2_ = bf16[96,2048]{1,0:T(8,128)(2,1)S(1)} collective-permute-done((bf16[96,2048]{1,0:T(8,128)(2,1)S(1)}, bf16[96,2048]{1,0:T(8,128)(2,1)S(1)}, u32[]{:S(2)}, u32[]{:S(2)}) %collective-permute-start.9) | collective-permute-done | bytes 393248 | tf_op jit(solution)/shard_map/ppermute | solution.py:660
  107.5 1.2 collective-permute-start.11
  108.7 2.1 %collective-permute-start.13 = (bf16[96,2048]{1,0:T(8,128)(2,1)S(1)}, bf16[96,2048]{1,0:T(8,128)(2,1)S(1)}, u32[]{:S(2)}, u32[]{:S(2)}) collective-permute-start(bf16[96,2048]{1,0:T(8,128)(2,1)S(1)} %get-tuple-element.49.own_ref), channel_id=1, source_target_pairs={{0,3},{1,0},{2,1},{3,2},{4,7},{5,4},{6,5},{7,6},{8,11},{9,8},{10,9... | collective-permute-start | bytes 1179656 | tf_op jit(solution)/shard_map/ppermute | solution.py:664
  110.8 8.6 %collective-permute-done.11.rows_ref.rest_0_ = bf16[96,2048]{1,0:T(8,128)(2,1)S(1)} collective-permute-done((bf16[96,2048]{1,0:T(8,128)(2,1)S(1)}, bf16[96,2048]{1,0:T(8,128)(2,1)S(1)}, u32[]{:S(2)}, u32[]{:S(2)}) %collective-permute-start.11) | collective-permute-done | bytes 393248 | tf_op jit(solution)/shard_map/ppermute | solution.py:663
  119.3 0.7 shard_map.136
  120.0 0.7 shard_map.137
  120.8 3.2 %collective-permute-start.14 = (bf16[48,2048]{1,0:T(8,128)(2,1)}, bf16[48,2048]{1,0:T(8,128)(2,1)}, u32[]{:S(2)}, u32[]{:S(2)}) collective-permute-start(bf16[48,2048]{1,0:T(8,128)(2,1)} %shard_map.137), channel_id=1, source_target_pairs={{0,3},{1,0},{2,1},{3,2},{4,7},{5,4},{6,5},{7,6},{8,11},{9,8},{10,9... | collective-permute-start | bytes 589832 | tf_op jit(solution)/shard_map/ppermute | solution.py:667
  124.0 8.0 %shard_map.141 = (bf16[96,2048]{1,0:T(8,128)(2,1)S(1)}, bf16[96,2048]{1,0:T(8,128)(2,1)S(1)}, bf16[2048,1408]{1,0:T(8,128)(2,1)S(1)}, bf16[2048,1408]{1,0:T(8,128)(2,1)S(1)}, bf16[2048,1408]{1,0:T(8,128)(2,1)S(1)}) custom-call(bf16[2048,3712]{1,0:T(8,128)(2,1)} %all-gather.2.cloned.1.call-done.w_ref, ...), custom_call_target="tpu_custom_call" | custom-call | tf_op jit(solution)/shard_map/pallas_call | solution.py:29
  132.0 5.6 %shard_map.142 = (bf16[96,2048]{1,0:T(8,128)(2,1)S(1)}, bf16[96,2048]{1,0:T(8,128)(2,1)S(1)}) custom-call(bf16[96,2048]{1,0:T(8,128)(2,1)S(1)} %copy-done.6, bf16[48,2048]{1,0:T(8,128)(2,1)S(1)} %collective-permute-done.12.upper_ref, bf16[48,2048]{1,0:T(8,128)(2,1)} %collective-permute-done.14.lower_ref, bf16[2048,1408]{1,0:T(8,128)(2,1)S(1)} %get-tuple-element.50.gate_ref, ...), custom_call_target="tpu_custom_call" | custom-call | tf_op jit(solution)/shard_map/pallas_call | solution.py:29
  137.8 1.4 collective-permute-start.22
  139.2 0.6 collective-permute-start.23
  139.9 11.4 %collective-permute-done.24.rest_3_ = bf16[96,2048]{1,0:T(8,128)(2,1)S(1)} collective-permute-done((bf16[96,2048]{1,0:T(8,128)(2,1)S(1)}, bf16[96,2048]{1,0:T(8,128)(2,1)S(1)}, u32[]{:S(2)}, u32[]{:S(2)}) %collective-permute-start.24) | collective-permute-done | bytes 393248 | tf_op jit(solution)/shard_map/ppermute | solution.py:673
  151.3 3.3 %collective-permute-done.22.rest_1_ = bf16[96,2048]{1,0:T(8,128)(2,1)S(1)} collective-permute-done((bf16[96,2048]{1,0:T(8,128)(2,1)S(1)}, bf16[96,2048]{1,0:T(8,128)(2,1)S(1)}, u32[]{:S(2)}, u32[]{:S(2)}) %collective-permute-start.22) | collective-permute-done | bytes 393248 | tf_op jit(solution)/shard_map/ppermute | solution.py:670
  154.6 2.3 %collective-permute-done.23.rest_2_ = bf16[96,2048]{1,0:T(8,128)(2,1)S(1)} collective-permute-done((bf16[96,2048]{1,0:T(8,128)(2,1)S(1)}, bf16[96,2048]{1,0:T(8,128)(2,1)S(1)}, u32[]{:S(2)}, u32[]{:S(2)}) %collective-permute-start.23) | collective-permute-done | bytes 393248 | tf_op jit(solution)/shard_map/ppermute | solution.py:671
  156.9 1.0 last_sum.1
  (42 shorter events, 3.3 us)
Async XLA Ops:
  6.5 30.7 %copy-start.2 = (bf16[384,512]{1,0:T(8,128)(2,1)S(1)}, bf16[384,512]{1,0:T(8,128)(2,1)}, u32[]{:S(2)}) copy-start(bf16[384,512]{1,0:T(8,128)(2,1)} %q_ref.3) | copy-start | bytes 1179652
  6.5 35.4 %copy-start.8 = (f32[64]{0:T(128)S(1)}, f32[64]{0:T(128)}, u32[]{:S(2)}) copy-start(f32[64]{0:T(128)} %param.19) | copy-start | bytes 772
  6.5 117.5 %all-gather.2.cloned.1.call-start = ((), (), s32[]{:S(2)}) async-start(), calls=%async_computation | async-start | bytes 15679488 | tf_op jit(solution)/shard_map/all_gather | solution.py:641
  7.5 35.7 %copy-start = (bf16[512,2048]{1,0:T(8,128)(2,1)S(1)}, bf16[512,2048]{1,0:T(8,128)(2,1)}, u32[]{:S(2)}) copy-start(bf16[512,2048]{1,0:T(8,128)(2,1)} %w_ref.1) | copy-start | bytes 6291460
  17.6 1.4 collective-permute-start
  19.3 9.9 %collective-permute-start.1 = (bf16[2,128,128]{2,1,0:T(8,128)(2,1)S(1)}, bf16[2,128,128]{2,1,0:T(8,128)(2,1)S(1)}, u32[]{:S(2)}, u32[]{:S(2)}) collective-permute-start(bf16[2,128,128]{2,1,0:T(8,128)(2,1)S(1)} %get-tuple-element.32.after_ref.rest_0_), channel_id=1, source_target_pairs={{0,8},{8,16},{16,24},{24,0},{1,9},{9,17},{17,25},{25,1},{2,10},{10... | collective-permute-start | bytes 196616 | tf_op jit(solution)/shard_map/ppermute | solution.py:359
  21.0 8.2 %collective-permute-start.2 = (bf16[2,128,128]{2,1,0:T(8,128)(2,1)S(1)}, bf16[2,128,128]{2,1,0:T(8,128)(2,1)S(1)}, u32[]{:S(2)}, u32[]{:S(2)}) collective-permute-start(bf16[2,128,128]{2,1,0:T(8,128)(2,1)S(1)} %get-tuple-element.32.after_ref.rest_0_), channel_id=1, source_target_pairs={{0,16},{8,24},{16,0},{24,8},{1,17},{9,25},{17,1},{25,9},{2,18},{10... | collective-permute-start | bytes 196616 | tf_op jit(solution)/shard_map/ppermute | solution.py:359
  23.9 5.7 %collective-permute-start.3 = (bf16[2,128,128]{2,1,0:T(8,128)(2,1)S(1)}, bf16[2,128,128]{2,1,0:T(8,128)(2,1)S(1)}, u32[]{:S(2)}, u32[]{:S(2)}) collective-permute-start(bf16[2,128,128]{2,1,0:T(8,128)(2,1)S(1)} %get-tuple-element.32.after_ref.rest_0_), channel_id=1, source_target_pairs={{0,24},{8,0},{16,8},{24,16},{1,25},{9,1},{17,9},{25,17},{2,26},{10... | collective-permute-start | bytes 196616 | tf_op jit(solution)/shard_map/ppermute | solution.py:359
  25.3 1.0 copy-start.1
  26.2 15.7 %copy-start.4 = (bf16[384,512]{1,0:T(8,128)(2,1)S(1)}, bf16[384,512]{1,0:T(8,128)(2,1)}, u32[]{:S(2)}) copy-start(bf16[384,512]{1,0:T(8,128)(2,1)} %gates_ref.1) | copy-start | bytes 1179652
  30.2 76.8 %copy-start.3 = (bf16[96,2048]{1,0:T(8,128)(2,1)S(1)}, bf16[96,2048]{1,0:T(8,128)(2,1)}, u32[]{:S(2)}) copy-start(bf16[96,2048]{1,0:T(8,128)(2,1)} %stream_ref.1) | copy-start | bytes 1179652
  30.3 76.8 %copy-start.7 = (f32[2048]{0:T(1024)S(1)}, f32[2048]{0:T(1024)}, u32[]{:S(2)}) copy-start(f32[2048]{0:T(1024)} %param.22) | copy-start | bytes 24580
  30.3 9.9 %collective-permute-start.4 = (bf16[2,128,128]{2,1,0:T(8,128)(2,1)S(1)}, bf16[2,128,128]{2,1,0:T(8,128)(2,1)S(1)}, u32[]{:S(2)}, u32[]{:S(2)}) collective-permute-start(bf16[2,128,128]{2,1,0:T(8,128)(2,1)S(1)} %get-tuple-element.39.after_ref), channel_id=1, source_target_pairs={{0,32},{32,64},{64,96},{96,0},{1,33},{33,65},{65,97},{97,1},{2,34}... | collective-permute-start | bytes 196616 | tf_op jit(solution)/shard_map/ppermute | solution.py:365
  32.4 8.3 %collective-permute-start.5 = (bf16[2,128,128]{2,1,0:T(8,128)(2,1)S(1)}, bf16[2,128,128]{2,1,0:T(8,128)(2,1)S(1)}, u32[]{:S(2)}, u32[]{:S(2)}) collective-permute-start(bf16[2,128,128]{2,1,0:T(8,128)(2,1)S(1)} %get-tuple-element.39.after_ref), channel_id=1, source_target_pairs={{0,64},{32,96},{64,0},{96,32},{1,65},{33,97},{65,1},{97,33},{2,66}... | collective-permute-start | bytes 196616 | tf_op jit(solution)/shard_map/ppermute | solution.py:365
  36.4 4.3 %collective-permute-start.6 = (bf16[2,128,128]{2,1,0:T(8,128)(2,1)S(1)}, bf16[2,128,128]{2,1,0:T(8,128)(2,1)S(1)}, u32[]{:S(2)}, u32[]{:S(2)}) collective-permute-start(bf16[2,128,128]{2,1,0:T(8,128)(2,1)S(1)} %get-tuple-element.39.after_ref), channel_id=1, source_target_pairs={{0,96},{32,0},{64,32},{96,64},{1,97},{33,1},{65,33},{97,65},{2,98}... | collective-permute-start | bytes 196616 | tf_op jit(solution)/shard_map/ppermute | solution.py:365
  41.6 1.5 collective-permute-start.7
  46.2 7.3 %collective-permute-start.15 = (bf16[64,512]{1,0:T(8,128)(2,1)S(1)}, bf16[64,512]{1,0:T(8,128)(2,1)S(1)}, u32[]{:S(2)}, u32[]{:S(2)}) collective-permute-start(bf16[64,512]{1,0:T(8,128)(2,1)S(1)} %shard_map.138.refs_0_), channel_id=1, source_target_pairs={{0,32},{32,64},{64,96},{96,0},{1,33},{33,65},{65,97},{97,1},{2,34}... | collective-permute-start | bytes 196616 | tf_op jit(solution)/shard_map/ppermute | solution.py:465
  47.0 9.1 %collective-permute-start.16 = (bf16[64,512]{1,0:T(8,128)(2,1)S(1)}, bf16[64,512]{1,0:T(8,128)(2,1)S(1)}, u32[]{:S(2)}, u32[]{:S(2)}) collective-permute-start(bf16[64,512]{1,0:T(8,128)(2,1)S(1)} %shard_map.138.refs_0_), channel_id=1, source_target_pairs={{0,64},{32,96},{64,0},{96,32},{1,65},{33,97},{65,1},{97,33},{2,66}... | collective-permute-start | bytes 196616 | tf_op jit(solution)/shard_map/ppermute | solution.py:465
  49.7 7.5 %collective-permute-start.17 = (bf16[64,512]{1,0:T(8,128)(2,1)S(1)}, bf16[64,512]{1,0:T(8,128)(2,1)S(1)}, u32[]{:S(2)}, u32[]{:S(2)}) collective-permute-start(bf16[64,512]{1,0:T(8,128)(2,1)S(1)} %shard_map.138.refs_0_), channel_id=1, source_target_pairs={{0,96},{32,0},{64,32},{96,64},{1,97},{33,1},{65,33},{97,65},{2,98}... | collective-permute-start | bytes 196616 | tf_op jit(solution)/shard_map/ppermute | solution.py:465
  57.2 15.9 %collective-permute-start.18 = (bf16[4,64,512]{2,1,0:T(8,128)(2,1)S(1)}, bf16[4,64,512]{2,1,0:T(8,128)(2,1)S(1)}, u32[]{:S(2)}, u32[]{:S(2)}) collective-permute-start(bf16[4,64,512]{2,1,0:T(8,128)(2,1)S(1)} %shard_map.139.refs_0_), channel_id=1, source_target_pairs={{0,8},{8,16},{16,24},{24,0},{1,9},{9,17},{17,25},{25,1},{2,10},{10... | collective-permute-start | bytes 786440 | tf_op jit(solution)/shard_map/ppermute | solution.py:468
  58.9 25.1 %collective-permute-start.19 = (bf16[4,64,512]{2,1,0:T(8,128)(2,1)S(1)}, bf16[4,64,512]{2,1,0:T(8,128)(2,1)S(1)}, u32[]{:S(2)}, u32[]{:S(2)}) collective-permute-start(bf16[4,64,512]{2,1,0:T(8,128)(2,1)S(1)} %shard_map.139.refs_0_), channel_id=1, source_target_pairs={{0,16},{8,24},{16,0},{24,8},{1,17},{9,25},{17,1},{25,9},{2,18},{10... | collective-permute-start | bytes 786440 | tf_op jit(solution)/shard_map/ppermute | solution.py:468
  60.5 24.2 %collective-permute-start.20 = (bf16[4,64,512]{2,1,0:T(8,128)(2,1)S(1)}, bf16[4,64,512]{2,1,0:T(8,128)(2,1)S(1)}, u32[]{:S(2)}, u32[]{:S(2)}) collective-permute-start(bf16[4,64,512]{2,1,0:T(8,128)(2,1)S(1)} %shard_map.139.refs_0_), channel_id=1, source_target_pairs={{0,24},{8,0},{16,8},{24,16},{1,25},{9,1},{17,9},{25,17},{2,26},{10... | collective-permute-start | bytes 786440 | tf_op jit(solution)/shard_map/ppermute | solution.py:468
  84.8 39.2 %collective-permute-start.21 = (bf16[4,4,64,512]{3,2,1,0:T(8,128)(2,1)S(1)}, bf16[4,4,64,512]{3,2,1,0:T(8,128)(2,1)S(1)}, u32[]{:S(2)}, u32[]{:S(2)}) collective-permute-start(bf16[4,4,64,512]{3,2,1,0:T(8,128)(2,1)S(1)} %shard_map.140.rest_2_), channel_id=1, source_target_pairs={{0,4},{4,0},{1,5},{5,1},{2,6},{6,2},{3,7},{7,3},{8,12},{12,8},{9,1... | collective-permute-start | bytes 3145736 | tf_op jit(solution)/shard_map/ppermute | solution.py:471
  84.9 20.5 %collective-permute-start.8 = (bf16[96,2048]{1,0:T(8,128)(2,1)S(1)}, bf16[96,2048]{1,0:T(8,128)(2,1)S(1)}, u32[]{:S(2)}, u32[]{:S(2)}) collective-permute-start(bf16[96,2048]{1,0:T(8,128)(2,1)S(1)} %get-tuple-element.45.after_ref), channel_id=1, source_target_pairs={{0,1},{1,2},{2,3},{3,0},{4,5},{5,6},{6,7},{7,4},{8,9},{9,10},{10,1... | collective-permute-start | bytes 1179656 | tf_op jit(solution)/shard_map/ppermute | solution.py:660
  86.4 18.9 %collective-permute-start.10 = (bf16[96,2048]{1,0:T(8,128)(2,1)S(1)}, bf16[96,2048]{1,0:T(8,128)(2,1)S(1)}, u32[]{:S(2)}, u32[]{:S(2)}) collective-permute-start(bf16[96,2048]{1,0:T(8,128)(2,1)S(1)} %get-tuple-element.47), channel_id=1, source_target_pairs={{0,3},{1,0},{2,1},{3,2},{4,7},{5,4},{6,5},{7,6},{8,11},{9,8},{10,9... | collective-permute-start | bytes 1179656 | tf_op jit(solution)/shard_map/ppermute | solution.py:660
  88.2 18.8 %collective-permute-start.9 = (bf16[96,2048]{1,0:T(8,128)(2,1)S(1)}, bf16[96,2048]{1,0:T(8,128)(2,1)S(1)}, u32[]{:S(2)}, u32[]{:S(2)}) collective-permute-start(bf16[96,2048]{1,0:T(8,128)(2,1)S(1)} %get-tuple-element.46), channel_id=1, source_target_pairs={{0,2},{1,3},{2,0},{3,1},{4,6},{5,7},{6,4},{7,5},{8,10},{9,11},{10,... | collective-permute-start | bytes 1179656 | tf_op jit(solution)/shard_map/ppermute | solution.py:660
  107.5 13.3 %copy-start.5 = (bf16[96,2048]{1,0:T(8,128)(2,1)}, bf16[96,2048]{1,0:T(8,128)(2,1)S(1)}, u32[]{:S(2)}) copy-start(bf16[96,2048]{1,0:T(8,128)(2,1)S(1)} %get-tuple-element.49.own_ref) | copy-start | bytes 1179652
  107.5 11.9 %collective-permute-start.11 = (bf16[96,2048]{1,0:T(8,128)(2,1)S(1)}, bf16[96,2048]{1,0:T(8,128)(2,1)S(1)}, u32[]{:S(2)}, u32[]{:S(2)}) collective-permute-start(bf16[96,2048]{1,0:T(8,128)(2,1)S(1)} %get-tuple-element.49.own_ref), channel_id=1, source_target_pairs={{0,1},{1,2},{2,3},{3,0},{4,5},{5,6},{6,7},{7,4},{8,9},{9,10},{10,1... | collective-permute-start | bytes 1179656 | tf_op jit(solution)/shard_map/ppermute | solution.py:663
  108.7 11.3 %collective-permute-start.13 = (bf16[96,2048]{1,0:T(8,128)(2,1)S(1)}, bf16[96,2048]{1,0:T(8,128)(2,1)S(1)}, u32[]{:S(2)}, u32[]{:S(2)}) collective-permute-start(bf16[96,2048]{1,0:T(8,128)(2,1)S(1)} %get-tuple-element.49.own_ref), channel_id=1, source_target_pairs={{0,3},{1,0},{2,1},{3,2},{4,7},{5,4},{6,5},{7,6},{8,11},{9,8},{10,9... | collective-permute-start | bytes 1179656 | tf_op jit(solution)/shard_map/ppermute | solution.py:664
  120.0 12.0 %collective-permute-start.12 = (bf16[48,2048]{1,0:T(8,128)(2,1)}, bf16[48,2048]{1,0:T(8,128)(2,1)S(1)}, u32[]{:S(2)}, u32[]{:S(2)}) collective-permute-start(bf16[48,2048]{1,0:T(8,128)(2,1)} %shard_map.136), channel_id=1, source_target_pairs={{0,1},{1,2},{2,3},{3,0},{4,5},{5,6},{6,7},{7,4},{8,9},{9,10},{10,1... | collective-permute-start | bytes 589832 | tf_op jit(solution)/shard_map/ppermute | solution.py:666
  120.8 11.3 %collective-permute-start.14 = (bf16[48,2048]{1,0:T(8,128)(2,1)}, bf16[48,2048]{1,0:T(8,128)(2,1)}, u32[]{:S(2)}, u32[]{:S(2)}) collective-permute-start(bf16[48,2048]{1,0:T(8,128)(2,1)} %shard_map.137), channel_id=1, source_target_pairs={{0,3},{1,0},{2,1},{3,2},{4,7},{5,4},{6,5},{7,6},{8,11},{9,8},{10,9... | collective-permute-start | bytes 589832 | tf_op jit(solution)/shard_map/ppermute | solution.py:667
  124.0 8.0 %copy-start.6 = (bf16[96,2048]{1,0:T(8,128)(2,1)S(1)}, bf16[96,2048]{1,0:T(8,128)(2,1)}, u32[]{:S(2)}) copy-start(bf16[96,2048]{1,0:T(8,128)(2,1)} %copy-done.5) | copy-start | bytes 1179652
  137.7 13.6 %collective-permute-start.24 = (bf16[96,2048]{1,0:T(8,128)(2,1)S(1)}, bf16[96,2048]{1,0:T(8,128)(2,1)S(1)}, u32[]{:S(2)}, u32[]{:S(2)}) collective-permute-start(bf16[96,2048]{1,0:T(8,128)(2,1)S(1)} %get-tuple-element.56), channel_id=1, source_target_pairs={{0,2},{1,3},{2,0},{3,1},{4,6},{5,7},{6,4},{7,5},{8,10},{9,11},{10,... | collective-permute-start | bytes 1179656 | tf_op jit(solution)/shard_map/ppermute | solution.py:673
  137.8 16.8 %collective-permute-start.22 = (bf16[96,2048]{1,0:T(8,128)(2,1)S(1)}, bf16[96,2048]{1,0:T(8,128)(2,1)S(1)}, u32[]{:S(2)}, u32[]{:S(2)}) collective-permute-start(bf16[96,2048]{1,0:T(8,128)(2,1)S(1)} %get-tuple-element.54), channel_id=1, source_target_pairs={{0,3},{1,0},{2,1},{3,2},{4,7},{5,4},{6,5},{7,6},{8,11},{9,8},{10,9... | collective-permute-start | bytes 1179656 | tf_op jit(solution)/shard_map/ppermute | solution.py:670
  139.2 17.6 %collective-permute-start.23 = (bf16[96,2048]{1,0:T(8,128)(2,1)S(1)}, bf16[96,2048]{1,0:T(8,128)(2,1)S(1)}, u32[]{:S(2)}, u32[]{:S(2)}) collective-permute-start(bf16[96,2048]{1,0:T(8,128)(2,1)S(1)} %get-tuple-element.55), channel_id=1, source_target_pairs={{0,1},{1,2},{2,3},{3,0},{4,5},{5,6},{6,7},{7,4},{8,9},{9,10},{10,1... | collective-permute-start | bytes 1179656 | tf_op jit(solution)/shard_map/ppermute | solution.py:671
Sparse Core Ops, SparseCore 0:
  9.6 84.2 all-gather.1

commit v10 on v8

--- a/solution.py
+++ b/solution.py
@@ -7,7 +7,6 @@
 from jax.experimental.pallas import tpu as pltpu
 from jax.sharding import Mesh
 from jax.sharding import PartitionSpec as P
-
 
 HEAD_DIM = 64
 PAIR = 2 * HEAD_DIM
@@ -24,7 +23,7 @@
 FAR = pl.BlockSpec(memory_space=pl.ANY)
 
 
-def call(kernel, arrays, shapes, scratch=(), far=(), mib=16):
+def call(kernel, name, arrays, shapes, scratch=(), far=(), mib=16):
     near = [pltpu.with_memory_space_constraint(x, pltpu.VMEM) for x in arrays]
     return pl.pallas_call(
         kernel,
@@ -33,6 +32,7 @@
         out_shape=[pltpu.VMEM(shape, dtype) for shape, dtype in shapes],
         scratch_shapes=scratch,
         compiler_params=pltpu.CompilerParams(vmem_limit_bytes=mib << 20),
+        name=name,
     )(*far, *near)
 
 
@@ -214,6 +214,7 @@
     wide = pltpu.VMEM((items, CHUNK, 2 * CHUNK), BF)
     return call(
         keys_kernel,
+        "keys_side",
         [],
         [
             ((items, PAIR, PAIR), BF),
@@ -283,7 +284,9 @@
 
 
 def gates_side(gates, gain):
-    return call(gates_kernel, [gates, gain.reshape(1, HEAD_DIM)], [(gates.shape, F32)])[0]
+    return call(
+        gates_kernel, "gates_side", [gates, gain.reshape(1, HEAD_DIM)], [(gates.shape, F32)]
+    )[0]
 
 
 def queries_side(first, after, queries, decay, solved, before, grown):
@@ -291,6 +294,7 @@
     shape = (length, width // 2)
     return call(
         functools.partial(queries_kernel, first),
+        "queries_side",
         [queries, decay, solved, before, grown],
         [(shape, F32), (shape, BF)],
         far=[after],
@@ -354,17 +358,26 @@
     swap = [(0, 1), (1, 0)]
     half = (total.shape[0] // 2, PAIR, PAIR)
     other = lax.ppermute(total, core, swap)
-    chip, other = call(chip_kernel, [total, other], [(half, BF), (total.shape, BF)])
+    chip, other = call(
+        chip_kernel, "chip_total", [total, other], [(half, BF), (total.shape, BF)]
+    )
     size = lax.axis_size(line)
     lines = [chip] + [lax.ppermute(chip, line, ring(size, k)) for k in range(1, size)]
     early = meanwhile(chip)
     whole, before = call(
-        row_kernel, lines, [(half, BF), (half, BF)], [pltpu.VMEM((size, *half), BF)], far=[early[1]]
+        row_kernel,
+        "line_total",
+        lines,
+        [(half, BF), (half, BF)],
+        [pltpu.VMEM((size, *half), BF)],
+        far=[early[1]],
     )
     size = lax.axis_size(plane)
     planes = [lax.ppermute(whole, plane, ring(size, k)) for k in range(1, size)]
     late = then(whole)
-    (state,) = call(plane_kernel, [before] + planes, [(half, BF)], far=[late[1]])
+    (state,) = call(
+        plane_kernel, "plane_state", [before] + planes, [(half, BF)], far=[late[1]]
+    )
     return early, late, (other, state, lax.ppermute(state, core, swap))
 
 
@@ -408,6 +421,7 @@
     length, width = gate.shape
     return call(
         mixed_kernel,
+        "mixed_and_projected",
         [*early, *late, *states, gate, w_out],
         [((length // size, w_out.shape[1]), BF if k else F32) for k in range(size)],
         [pltpu.VMEM((length, width), BF), pltpu.VMEM((width // PAIR, PAIR, PAIR), BF)],
@@ -428,7 +442,10 @@
 
 def normed_rows(stream, gain, parts):
     return call(
-        norm_kernel, [stream, gain.reshape(1, -1), *parts], [(stream.shape, BF), (stream.shape, BF)]
+        norm_kernel,
+        "normed_rows",
+        [stream, gain.reshape(1, -1), *parts],
+        [(stream.shape, BF), (stream.shape, BF)],
     )
 
 
@@ -450,11 +467,11 @@
 DOWN_GROUPS = (8,)
 
 
-def first_channels_kernel(count, w_ref, *rest):
-    parts, out_refs = rest[:count], rest[count : 2 * count]
-    gate_ref, up_ref, down_ref, rows_ref, hidden_ref, in_sems, down_sems = rest[2 * count :]
+def channels_kernel(w_ref, *rest):
+    own_ref, right_ref, left_ref, upper_ref, lower_ref, out_ref = rest[:6]
+    gate_ref, up_ref, down_ref, rows_ref, hidden_ref, in_sems, down_sems = rest[6:]
     width, hidden = gate_ref.shape
-    block = parts[0].shape[0]
+    size, block = out_ref.shape[:2]
     groups, spans = [], []
     for many, spread in ((hidden // TILE, UP_GROUPS), (width // STRIP, DOWN_GROUPS)):
         assert sum(spread) == many
@@ -484,8 +501,14 @@
 
     for g in range(AHEAD):
         begin(g)
-    for k, part in enumerate(parts):
-        rows_ref[k * block : (k + 1) * block, :] = part[...]
+    rows_ref[:block, :] = own_ref[...]
+    rows_ref[block : 2 * block, :] = right_ref[...]
+    rows_ref[2 * block : 3 * block, :] = left_ref[...]
+    half = block // 2
+    rows_ref[3 * block : 3 * block + half, :] = upper_ref[...]
+    rows_ref[3 * block + half :, :] = lower_ref[...]
+    place = lax.axis_index("tp")
+    owners = [lax.rem(place + k, size) for k in (0, size - 1, 1, 2)]
     for g, tiles in enumerate(spans[0]):
         arrived(g)
         for j in tiles:
@@ -495,63 +518,42 @@
         arrived(len(spans[0]) + g)
         for n in strips:
             here = slice(n * STRIP, (n + 1) * STRIP)
-            got = product_nt(hidden_ref[...], down_ref[here, :])
-            for k, out_ref in enumerate(out_refs):
-                out_ref[:, here] = got[k * block : (k + 1) * block, :].astype(BF)
-
-
-def first_channels(weights, parts, hidden):
+            got = product_nt(hidden_ref[...], down_ref[here, :]).astype(BF)
+            for k, owner in enumerate(owners):
+                out_ref[owner, :, here] = got[k * block : (k + 1) * block, :]
+
+
+def channel_sums(weights, parts, hidden, size):
     block, width = parts[0].shape
-    count = len(parts)
-    out = call(
-        functools.partial(first_channels_kernel, count),
+    weight = pltpu.VMEM((width, hidden), BF)
+    return call(
+        channels_kernel,
+        "channel_sums",
         parts,
-        [((block, width), BF)] * count + [((width, hidden), BF)] * 3,
+        [((size, block, width), BF)],
         [
-            pltpu.VMEM((block * count, width), BF),
-            pltpu.VMEM((block * count, hidden), BF),
+            weight,
+            weight,
+            weight,
+            pltpu.VMEM((block * size, width), BF),
+            pltpu.VMEM((block * size, hidden), BF),
             pltpu.SemaphoreType.DMA((2, len(UP_GROUPS))),
             pltpu.SemaphoreType.DMA((len(DOWN_GROUPS),)),
         ],
         far=[pltpu.with_memory_space_constraint(weights, pltpu.HBM)],
-    )
-    return out[:count], out[count:]
-
-
-def more_channels_kernel(own_ref, upper_ref, lower_ref, gate_ref, up_ref, down_ref, *rest):
-    out_refs, hidden_ref = rest[:-1], rest[-1]
-    block = own_ref.shape[0]
-    rows = jnp.concatenate([own_ref[...], upper_ref[...], lower_ref[...]], axis=0)
-    for j in range(gate_ref.shape[1] // TILE):
-        here = slice(j * TILE, (j + 1) * TILE)
-        hidden_ref[:, here] = activated(rows, gate_ref[:, here], up_ref[:, here])
-    for n in range(down_ref.shape[0] // STRIP):
-        here = slice(n * STRIP, (n + 1) * STRIP)
-        got = product_nt(hidden_ref[...], down_ref[here, :])
-        for k, out_ref in enumerate(out_refs):
-            out_ref[:, here] = got[k * block : (k + 1) * block, :].astype(BF)
-
-
-def more_channels(rows, projections):
-    block, width = rows[0].shape
-    return call(
-        more_channels_kernel,
-        [*rows, *projections],
-        [((block, width), BF)] * 2,
-        [pltpu.VMEM((2 * block, projections[0].shape[1]), BF)],
-    )
-
-
-def last_kernel(middle_ref, *rest):
-    parts, out_ref = rest[:-1], rest[-1]
-    total = parts[0][...].astype(F32)
-    for part in parts[1:]:
-        total = total + part[...].astype(F32)
+        mib=32,
+    )[0]
+
+
+def last_kernel(middle_ref, parts_ref, out_ref):
+    total = parts_ref[0].astype(F32)
+    for k in range(1, parts_ref.shape[0]):
+        total = total + parts_ref[k].astype(F32)
     out_ref[...] = (middle_ref[...].astype(F32) + 0.5 * total).astype(BF)
 
 
 def last_sum(middle, parts):
-    near = [pltpu.with_memory_space_constraint(x, pltpu.VMEM) for x in [middle, *parts]]
+    near = [pltpu.with_memory_space_constraint(x, pltpu.VMEM) for x in (middle, parts)]
     return pl.pallas_call(
         last_kernel,
         in_specs=[FULL] * len(near),
@@ -599,12 +601,9 @@
         lax.ppermute(right[:half], "tp", ring(size, 1)),
         lax.ppermute(left[half:], "tp", ring(size, -1)),
     ]
-    sums, projections = first_channels(weights, [right, left], hidden)
-    back = [lax.ppermute(sums[0], "tp", ring(size, -1))]
-    back.append(lax.ppermute(sums[1], "tp", ring(size, 1)))
-    own, last = more_channels([normed, *across], projections)
-    back.append(lax.ppermute(last, "tp", ring(size, 2)))
-    return last_sum(middle, [own] + back)
+    sums = channel_sums(weights, [normed, right, left, *across], hidden, size)
+    sums = lax.all_to_all(sums, "tp", 0, 0, tiled=True)
+    return last_sum(middle, sums)
 
 
 def solution(mesh):

time: 132 us -> 132 us (level)
  blocking collectives: 0 us -> 25.2 us
  waiting for transfers between devices: 52.6 us -> 35.8 us
  starting transfers between devices: 29.9 us -> 25.4 us
  Pallas kernels: 32.7 us -> 29.8 us
    all_to_all x0 -> x1, blocking collectives: none -> 25.2 us  [per_device(): sums = lax.all_to_all(sums, 'tp', 0, 0, tiled=True)]
    ppermute x3 -> x0, waiting for transfers between devices: 16.3 us -> none  [the longest x1 8.53 us: per_device(): back.append(lax.ppermute(last, 'tp', ring(size, 2)))]
    ppermute x3 -> x0, starting transfers between devices: 5.09 us -> none  [the longest x1 3.06 us: per_device(): back.append(lax.ppermute(last, 'tp', ring(size, 2)))]
    ppermute x1, waiting for transfers between devices: 0.01 us -> 3.55 us  [per_device(): lax.ppermute(right[:half], 'tp', ring(size, 1))]
    all_gather x1, waiting for transfers between devices: 5.28 us -> 1.87 us  [per_device(): weights = lax.all_gather(weights, SP, axis=0, tiled=True)]
    pallas_call x11 -> x10, Pallas kernels: 31.7 us -> 28.8 us  [call(): pl.pallas_call(kernel, in_specs=[FAR] * len(far) + [FULL] * len(near), ou...]
    ppermute x3, waiting for transfers between devices: 18.2 us -> 16.1 us  [per_device(): lax.ppermute(parts[k], 'tp', ring(size, k))]
    ppermute x1, starting transfers between devices: 0.07 us -> 1.44 us  [per_device(): right = lax.ppermute(normed, 'tp', ring(size, 1))]
  transfers between devices with their start and end apart: 19 -> 16, of which waited for: 10 -> 9; matrix products, arithmetic and copies ran while one was open for 0% -> 0% of each run, Pallas kernels for 21% -> 14%
where the time goes in v10:
time: 132 us
  waiting for transfers between devices  35.8 us (27%)
  Pallas kernels  29.8 us (23%)
  starting transfers between devices  25.4 us (19%)
  blocking collectives  25.2 us (19%)
  between operations  13.5 us (10%)
  other arithmetic  2.01 us (2%)
    pallas_call x10, Pallas kernels, call(): pl.pallas_call(kernel, in_specs=[FAR] * len(far) + [FULL] * len(near), ou...  28.8 us
    all_to_all x1, blocking collectives, per_device(): sums = lax.all_to_all(sums, 'tp', 0, 0, tiled=True)  25.2 us
    ppermute x3, waiting for transfers between devices, per_device(): lax.ppermute(parts[k], 'tp', ring(size, k))  16.1 us
    ppermute x1, waiting for transfers between devices, per_device(): right = lax.ppermute(normed, 'tp', ring(size, 1))  8.46 us
    ppermute x3, starting transfers between devices, state_ahead(): planes = [lax.ppermute(whole, plane, ring(size, k)) for k in range(1, size)]  6.67 us
    ppermute x3, starting transfers between devices, state_ahead(): lax.ppermute(chip, line, ring(size, k))  6 us
    ppermute x3, starting transfers between devices, per_device(): lax.ppermute(parts[k], 'tp', ring(size, k))  5.69 us
    ppermute x1, waiting for transfers between devices, per_device(): lax.ppermute(right[:half], 'tp', ring(size, 1))  3.55 us
  transfers between devices with their start and end apart: 16, of which 9 were waited for; matrix products, arithmetic and copies ran while one was open for 0% of the time, Pallas kernels for 14%

profile of v10, /device:TPU:0, one launch (start us, length us, event | category | flops | bytes accessed | tf_op | source)
XLA Modules:
  0.0 131.8 jit_solution(5846022949424615590)
XLA Ops:
  6.5 2.0 %pad_maximum_fusion = bf16[64,4224]{1,0:T(8,128)(2,1)} fusion(bf16[64,1408]{1,0:T(8,128)(2,1)} %bitcast.5, bf16[64,1408]{1,0:T(8,128)(2,1)} %param.24, bf16[64,1408]{1,0:T(8,128)(2,1)} %param.23), kind=kLoop, calls=%fused_computation | loop fusion | flops 1622016 | bytes 1081344 | tf_op jit(solution)/shard_map/concatenate | solution.py:583
  8.5 0.0 all-gather.2.cloned.1.call-update
  8.6 8.1 %keys_side.1 = (bf16[12,128,128]{2,1,0:T(8,128)(2,1)S(1)}, bf16[4,128,128]{2,1,0:T(8,128)(2,1)S(1)}, bf16[12,128,384]{2,1,0:T(8,128)(2,1)S(1)}, bf16[12,128,256]{2,1,0:T(8,128)(2,1)S(1)}, f32[384,512]{1,0:T(8,128)S(1)}) custom-call(bf16[384,512]{1,0:T(8,128)(2,1)} %k_far_ref.1, bf16[384,512]{1,0:T(8,128)(2,1)} %v_far_ref.1, f32[8,384]{1,0:T(8,128)} %beta_far_ref.1, ...), custom_call_target="tpu_custom_call" | custom-call | tf_op jit(solution)/shard_map/keys_side/pallas_call | solution.py:28
  16.6 0.1 collective-permute-start
  16.7 1.3 %collective-permute-done.other_ref = bf16[4,128,128]{2,1,0:T(8,128)(2,1)S(1)} collective-permute-done((bf16[4,128,128]{2,1,0:T(8,128)(2,1)S(1)}, bf16[4,128,128]{2,1,0:T(8,128)(2,1)S(1)}, u32[]{:S(2)}, u32[]{:S(2)}) %collective-permute-start) | collective-permute-done | bytes 131104 | tf_op jit(solution)/shard_map/ppermute | solution.py:360
  18.1 0.2 chip_total.1
  18.3 1.8 %collective-permute-start.1 = (bf16[2,128,128]{2,1,0:T(8,128)(2,1)S(1)}, bf16[2,128,128]{2,1,0:T(8,128)(2,1)S(1)}, u32[]{:S(2)}, u32[]{:S(2)}) collective-permute-start(bf16[2,128,128]{2,1,0:T(8,128)(2,1)S(1)} %get-tuple-element.25.after_ref.rest_0_), channel_id=1, source_target_pairs={{0,8},{8,16},{16,24},{24,0},{1,9},{9,17},{17,25},{25,1},{2,10},{10... | collective-permute-start | bytes 196616 | tf_op jit(solution)/shard_map/ppermute | solution.py:365
  20.0 2.9 %collective-permute-start.2 = (bf16[2,128,128]{2,1,0:T(8,128)(2,1)S(1)}, bf16[2,128,128]{2,1,0:T(8,128)(2,1)S(1)}, u32[]{:S(2)}, u32[]{:S(2)}) collective-permute-start(bf16[2,128,128]{2,1,0:T(8,128)(2,1)S(1)} %get-tuple-element.25.after_ref.rest_0_), channel_id=1, source_target_pairs={{0,16},{8,24},{16,0},{24,8},{1,17},{9,25},{17,1},{25,9},{2,18},{10... | collective-permute-start | bytes 196616 | tf_op jit(solution)/shard_map/ppermute | solution.py:365
  22.9 1.3 %collective-permute-start.3 = (bf16[2,128,128]{2,1,0:T(8,128)(2,1)S(1)}, bf16[2,128,128]{2,1,0:T(8,128)(2,1)S(1)}, u32[]{:S(2)}, u32[]{:S(2)}) collective-permute-start(bf16[2,128,128]{2,1,0:T(8,128)(2,1)S(1)} %get-tuple-element.25.after_ref.rest_0_), channel_id=1, source_target_pairs={{0,24},{8,0},{16,8},{24,16},{1,25},{9,1},{17,9},{25,17},{2,26},{10... | collective-permute-start | bytes 196616 | tf_op jit(solution)/shard_map/ppermute | solution.py:365
  24.3 2.9 %queries_side.2 = (f32[384,256]{1,0:T(8,128)S(1)}, bf16[384,256]{1,0:T(8,128)(2,1)S(1)}) custom-call(bf16[2,128,128]{2,1,0:T(8,128)(2,1)S(1)} %get-tuple-element.25.after_ref.rest_0_, bf16[384,512]{1,0:T(8,128)(2,1)S(1)} %copy-done.1, bf16[12,128,256]{2,1,0:T(8,128)(2,1)S(1)} %get-tuple-element.26.d_ref, bf16[12,128,384]{2,1,0:T(8,128)(2,1)S(1)} %get-tuple-element.27.y_ref, ...), custom_call_target="tpu_custom_call" | custom-call | tf_op jit(solution)/shard_map/queries_side/pallas_call | solution.py:28
  27.2 0.0 collective-permute-done.1.rest_1_
  27.2 0.0 collective-permute-done.2.rest_2_
  27.2 1.5 %collective-permute-done.3.rest_3_ = bf16[2,128,128]{2,1,0:T(8,128)(2,1)S(1)} collective-permute-done((bf16[2,128,128]{2,1,0:T(8,128)(2,1)S(1)}, bf16[2,128,128]{2,1,0:T(8,128)(2,1)S(1)}, u32[]{:S(2)}, u32[]{:S(2)}) %collective-permute-start.3) | collective-permute-done | bytes 65568 | tf_op jit(solution)/shard_map/ppermute | solution.py:365
  28.8 0.6 line_total.1
  29.4 0.0 copy-start.3
  29.4 0.0 copy-start.5
  29.5 2.0 %collective-permute-start.4 = (bf16[2,128,128]{2,1,0:T(8,128)(2,1)S(1)}, bf16[2,128,128]{2,1,0:T(8,128)(2,1)S(1)}, u32[]{:S(2)}, u32[]{:S(2)}) collective-permute-start(bf16[2,128,128]{2,1,0:T(8,128)(2,1)S(1)} %get-tuple-element.32.after_ref), channel_id=1, source_target_pairs={{0,32},{32,64},{64,96},{96,0},{1,33},{33,65},{65,97},{97,1},{2,34}... | collective-permute-start | bytes 196616 | tf_op jit(solution)/shard_map/ppermute | solution.py:376
  31.4 3.6 %collective-permute-start.5 = (bf16[2,128,128]{2,1,0:T(8,128)(2,1)S(1)}, bf16[2,128,128]{2,1,0:T(8,128)(2,1)S(1)}, u32[]{:S(2)}, u32[]{:S(2)}) collective-permute-start(bf16[2,128,128]{2,1,0:T(8,128)(2,1)S(1)} %get-tuple-element.32.after_ref), channel_id=1, source_target_pairs={{0,64},{32,96},{64,0},{96,32},{1,65},{33,97},{65,1},{97,33},{2,66}... | collective-permute-start | bytes 196616 | tf_op jit(solution)/shard_map/ppermute | solution.py:376
  35.1 1.1 collective-permute-start.6
  36.1 2.9 %queries_side.3 = (f32[384,256]{1,0:T(8,128)S(1)}, bf16[384,256]{1,0:T(8,128)(2,1)S(1)}) custom-call(bf16[2,128,128]{2,1,0:T(8,128)(2,1)S(1)} %get-tuple-element.32.after_ref, bf16[384,512]{1,0:T(8,128)(2,1)S(1)} %copy-done.1, bf16[12,128,256]{2,1,0:T(8,128)(2,1)S(1)} %get-tuple-element.26.d_ref, bf16[12,128,384]{2,1,0:T(8,128)(2,1)S(1)} %get-tuple-element.27.y_ref, ...), custom_call_target="tpu_custom_call" | custom-call | tf_op jit(solution)/shard_map/queries_side/pallas_call | solution.py:28
  39.0 0.0 collective-permute-done.4.rest_0_
  39.1 1.9 %collective-permute-done.5.rest_1_ = bf16[2,128,128]{2,1,0:T(8,128)(2,1)S(1)} collective-permute-done((bf16[2,128,128]{2,1,0:T(8,128)(2,1)S(1)}, bf16[2,128,128]{2,1,0:T(8,128)(2,1)S(1)}, u32[]{:S(2)}, u32[]{:S(2)}) %collective-permute-start.5) | collective-permute-done | bytes 65568 | tf_op jit(solution)/shard_map/ppermute | solution.py:376
  40.9 0.0 collective-permute-done.6.rest_2_
  40.9 0.9 plane_state.1.mine_ref
  41.8 0.3 collective-permute-start.7
  42.1 0.0 copy-done.3
  42.1 0.3 gates_side.1.gate_ref
  42.4 0.9 collective-permute-done.7.theirs_ref
  43.4 2.1 %mixed_and_projected.1 = (f32[96,2048]{1,0:T(8,128)S(1)}, bf16[96,2048]{1,0:T(8,128)(2,1)S(1)}, bf16[96,2048]{1,0:T(8,128)(2,1)S(1)}, bf16[96,2048]{1,0:T(8,128)(2,1)S(1)}) custom-call(f32[384,256]{1,0:T(8,128)S(1)} %get-tuple-element.30.o0_ref, bf16[384,256]{1,0:T(8,128)(2,1)S(1)} %get-tuple-element.31.after_ref.q0_ref, ...), custom_call_target="tpu_custom_call" | custom-call | tf_op jit(solution)/shard_map/mixed_and_projected/pallas_call | solution.py:28
  45.5 1.5 %collective-permute-start.8 = (bf16[96,2048]{1,0:T(8,128)(2,1)S(1)}, bf16[96,2048]{1,0:T(8,128)(2,1)S(1)}, u32[]{:S(2)}, u32[]{:S(2)}) collective-permute-start(bf16[96,2048]{1,0:T(8,128)(2,1)S(1)} %get-tuple-element.38), channel_id=1, source_target_pairs={{0,1},{1,2},{2,3},{3,0},{4,5},{5,6},{6,7},{7,4},{8,9},{9,10},{10,1... | collective-permute-start | bytes 1179656 | tf_op jit(solution)/shard_map/ppermute | solution.py:595
  47.0 2.7 %collective-permute-start.9 = (bf16[96,2048]{1,0:T(8,128)(2,1)S(1)}, bf16[96,2048]{1,0:T(8,128)(2,1)S(1)}, u32[]{:S(2)}, u32[]{:S(2)}) collective-permute-start(bf16[96,2048]{1,0:T(8,128)(2,1)S(1)} %get-tuple-element.39), channel_id=1, source_target_pairs={{0,2},{1,3},{2,0},{3,1},{4,6},{5,7},{6,4},{7,5},{8,10},{9,11},{10,... | collective-permute-start | bytes 1179656 | tf_op jit(solution)/shard_map/ppermute | solution.py:595
  49.8 1.4 %collective-permute-start.10 = (bf16[96,2048]{1,0:T(8,128)(2,1)S(1)}, bf16[96,2048]{1,0:T(8,128)(2,1)S(1)}, u32[]{:S(2)}, u32[]{:S(2)}) collective-permute-start(bf16[96,2048]{1,0:T(8,128)(2,1)S(1)} %get-tuple-element.40), channel_id=1, source_target_pairs={{0,3},{1,0},{2,1},{3,2},{4,7},{5,4},{6,5},{7,6},{8,11},{9,8},{10,9... | collective-permute-start | bytes 1179656 | tf_op jit(solution)/shard_map/ppermute | solution.py:595
  51.2 6.8 %collective-permute-done.8.rest_1_ = bf16[96,2048]{1,0:T(8,128)(2,1)S(1)} collective-permute-done((bf16[96,2048]{1,0:T(8,128)(2,1)S(1)}, bf16[96,2048]{1,0:T(8,128)(2,1)S(1)}, u32[]{:S(2)}, u32[]{:S(2)}) %collective-permute-start.8) | collective-permute-done | bytes 393248 | tf_op jit(solution)/shard_map/ppermute | solution.py:595
  58.0 9.4 %collective-permute-done.9.rest_2_ = bf16[96,2048]{1,0:T(8,128)(2,1)S(1)} collective-permute-done((bf16[96,2048]{1,0:T(8,128)(2,1)S(1)}, bf16[96,2048]{1,0:T(8,128)(2,1)S(1)}, u32[]{:S(2)}, u32[]{:S(2)}) %collective-permute-start.9) | collective-permute-done | bytes 393248 | tf_op jit(solution)/shard_map/ppermute | solution.py:595
  67.3 0.0 collective-permute-done.10.rest_3_
  67.4 0.4 normed_rows.1
  67.8 1.4 %collective-permute-start.11 = (bf16[96,2048]{1,0:T(8,128)(2,1)S(1)}, bf16[96,2048]{1,0:T(8,128)(2,1)S(1)}, u32[]{:S(2)}, u32[]{:S(2)}) collective-permute-start(bf16[96,2048]{1,0:T(8,128)(2,1)S(1)} %get-tuple-element.42.rest_0_), channel_id=1, source_target_pairs={{0,1},{1,2},{2,3},{3,0},{4,5},{5,6},{6,7},{7,4},{8,9},{9,10},{10,1... | collective-permute-start | bytes 1179656 | tf_op jit(solution)/shard_map/ppermute | solution.py:597
  69.2 1.9 %collective-permute-start.12 = (bf16[96,2048]{1,0:T(8,128)(2,1)S(1)}, bf16[96,2048]{1,0:T(8,128)(2,1)S(1)}, u32[]{:S(2)}, u32[]{:S(2)}) collective-permute-start(bf16[96,2048]{1,0:T(8,128)(2,1)S(1)} %get-tuple-element.42.rest_0_), channel_id=1, source_target_pairs={{0,3},{1,0},{2,1},{3,2},{4,7},{5,4},{6,5},{7,6},{8,11},{9,8},{10,9... | collective-permute-start | bytes 1179656 | tf_op jit(solution)/shard_map/ppermute | solution.py:598
  71.1 8.5 %collective-permute-done.11.rest_1_ = bf16[96,2048]{1,0:T(8,128)(2,1)S(1)} collective-permute-done((bf16[96,2048]{1,0:T(8,128)(2,1)S(1)}, bf16[96,2048]{1,0:T(8,128)(2,1)S(1)}, u32[]{:S(2)}, u32[]{:S(2)}) %collective-permute-start.11) | collective-permute-done | bytes 393248 | tf_op jit(solution)/shard_map/ppermute | solution.py:597
  79.6 0.2 collective-permute-start.13
  79.8 0.0 collective-permute-done.12.rest_2_
  79.9 3.1 %collective-permute-start.14 = (bf16[48,2048]{1,0:T(8,128)(2,1)S(1)}, bf16[48,2048]{1,0:T(8,128)(2,1)S(1)}, u32[]{:S(2)}, u32[]{:S(2)}) collective-permute-start(bf16[48,2048]{1,0:T(8,128)(2,1)S(1)} %slice.9), channel_id=1, source_target_pairs={{0,3},{1,0},{2,1},{3,2},{4,7},{5,4},{6,5},{7,6},{8,11},{9,8},{10,9... | collective-permute-start | bytes 589832 | tf_op jit(solution)/shard_map/ppermute | solution.py:602
  83.0 3.6 %collective-permute-done.13.rest_3_ = bf16[48,2048]{1,0:T(8,128)(2,1)S(1)} collective-permute-done((bf16[48,2048]{1,0:T(8,128)(2,1)S(1)}, bf16[48,2048]{1,0:T(8,128)(2,1)S(1)}, u32[]{:S(2)}, u32[]{:S(2)}) %collective-permute-start.13) | collective-permute-done | bytes 196640 | tf_op jit(solution)/shard_map/ppermute | solution.py:601
  86.5 0.0 collective-permute-done.14.rest_4_
  86.5 1.9 %all-gather.2.cloned.1.call-done.w_ref = bf16[2048,4224]{1,0:T(8,128)(2,1)} async-done(((bf16[64,4224]{1,0:T(8,128)(2,1)}), bf16[2048,4224]{1,0:T(8,128)(2,1)}) %all-gather.2.cloned.1.call-update) | async-done | bytes 17301520 | tf_op jit(solution)/shard_map/all_gather | solution.py:584
  88.4 10.3 %channel_sums.1 = bf16[4,96,2048]{2,1,0:T(8,128)(2,1)S(1)} custom-call(bf16[2048,4224]{1,0:T(8,128)(2,1)} %all-gather.2.cloned.1.call-done.w_ref, bf16[96,2048]{1,0:T(8,128)(2,1)S(1)} %get-tuple-element.42.rest_0_, bf16[96,2048]{1,0:T(8,128)(2,1)S(1)} %collective-permute-done.11.rest_1_, bf16[96,2048]{1,0:T(8,128)(2,1)S(1)} %collective-permute-done.12.rest_2_, ...), custom_call_target="tpu_custom_call" | custom-call | tf_op jit(solution)/shard_map/channel_sums/pallas_call | solution.py:28
  98.7 25.2 %all_to_all.5.parts_ref = bf16[4,96,2048]{2,1,0:T(8,128)(2,1)S(1)} all-to-all(bf16[4,96,2048]{2,1,0:T(8,128)(2,1)S(1)} %channel_sums.1), channel_id=1, replica_groups=mesh['sp_0'=4,'sp_1'=4,'sp_2'=2,'tp'=4] {'tp'}, dimensions={0} | all-to-all | bytes 3145728 | tf_op jit(solution)/shard_map/all_to_all | solution.py:605
  123.9 1.0 last_sum.1
  (12 shorter events, 0.0 us)
Async XLA Ops:
  6.5 81.9 %all-gather.2.cloned.1.call-start = ((), (), s32[]{:S(2)}) async-start(), calls=%async_computation.1 | async-start | bytes 17842176 | tf_op jit(solution)/shard_map/all_gather | solution.py:584
  6.5 17.8 %copy-start.1 = (bf16[384,512]{1,0:T(8,128)(2,1)S(1)}, bf16[384,512]{1,0:T(8,128)(2,1)}, u32[]{:S(2)}) copy-start(bf16[384,512]{1,0:T(8,128)(2,1)} %q_ref.3) | copy-start | bytes 1179652
  16.6 1.4 %collective-permute-start = (bf16[4,128,128]{2,1,0:T(8,128)(2,1)S(1)}, bf16[4,128,128]{2,1,0:T(8,128)(2,1)S(1)}, u32[]{:S(2)}, u32[]{:S(2)}) collective-permute-start(bf16[4,128,128]{2,1,0:T(8,128)(2,1)S(1)} %get-tuple-element.24.own_ref), channel_id=1, source_target_pairs={{0,4},{4,0},{1,5},{5,1},{2,6},{6,2},{3,7},{7,3},{8,12},{12,8},{9,1... | collective-permute-start | bytes 393224 | tf_op jit(solution)/shard_map/ppermute | solution.py:360
  18.3 8.9 %collective-permute-start.1 = (bf16[2,128,128]{2,1,0:T(8,128)(2,1)S(1)}, bf16[2,128,128]{2,1,0:T(8,128)(2,1)S(1)}, u32[]{:S(2)}, u32[]{:S(2)}) collective-permute-start(bf16[2,128,128]{2,1,0:T(8,128)(2,1)S(1)} %get-tuple-element.25.after_ref.rest_0_), channel_id=1, source_target_pairs={{0,8},{8,16},{16,24},{24,0},{1,9},{9,17},{17,25},{25,1},{2,10},{10... | collective-permute-start | bytes 196616 | tf_op jit(solution)/shard_map/ppermute | solution.py:365
  20.0 7.2 %collective-permute-start.2 = (bf16[2,128,128]{2,1,0:T(8,128)(2,1)S(1)}, bf16[2,128,128]{2,1,0:T(8,128)(2,1)S(1)}, u32[]{:S(2)}, u32[]{:S(2)}) collective-permute-start(bf16[2,128,128]{2,1,0:T(8,128)(2,1)S(1)} %get-tuple-element.25.after_ref.rest_0_), channel_id=1, source_target_pairs={{0,16},{8,24},{16,0},{24,8},{1,17},{9,25},{17,1},{25,9},{2,18},{10... | collective-permute-start | bytes 196616 | tf_op jit(solution)/shard_map/ppermute | solution.py:365
  22.9 5.8 %collective-permute-start.3 = (bf16[2,128,128]{2,1,0:T(8,128)(2,1)S(1)}, bf16[2,128,128]{2,1,0:T(8,128)(2,1)S(1)}, u32[]{:S(2)}, u32[]{:S(2)}) collective-permute-start(bf16[2,128,128]{2,1,0:T(8,128)(2,1)S(1)} %get-tuple-element.25.after_ref.rest_0_), channel_id=1, source_target_pairs={{0,24},{8,0},{16,8},{24,16},{1,25},{9,1},{17,9},{25,17},{2,26},{10... | collective-permute-start | bytes 196616 | tf_op jit(solution)/shard_map/ppermute | solution.py:365
  29.4 12.7 %copy-start.3 = (bf16[384,512]{1,0:T(8,128)(2,1)S(1)}, bf16[384,512]{1,0:T(8,128)(2,1)}, u32[]{:S(2)}) copy-start(bf16[384,512]{1,0:T(8,128)(2,1)} %gates_ref.1) | copy-start | bytes 1179652
  29.4 12.7 %copy-start.5 = (f32[64]{0:T(128)S(1)}, f32[64]{0:T(128)}, u32[]{:S(2)}) copy-start(f32[64]{0:T(128)} %param.19) | copy-start | bytes 772
  29.5 9.6 %collective-permute-start.4 = (bf16[2,128,128]{2,1,0:T(8,128)(2,1)S(1)}, bf16[2,128,128]{2,1,0:T(8,128)(2,1)S(1)}, u32[]{:S(2)}, u32[]{:S(2)}) collective-permute-start(bf16[2,128,128]{2,1,0:T(8,128)(2,1)S(1)} %get-tuple-element.32.after_ref), channel_id=1, source_target_pairs={{0,32},{32,64},{64,96},{96,0},{1,33},{33,65},{65,97},{97,1},{2,34}... | collective-permute-start | bytes 196616 | tf_op jit(solution)/shard_map/ppermute | solution.py:376
  31.4 9.5 %collective-permute-start.5 = (bf16[2,128,128]{2,1,0:T(8,128)(2,1)S(1)}, bf16[2,128,128]{2,1,0:T(8,128)(2,1)S(1)}, u32[]{:S(2)}, u32[]{:S(2)}) collective-permute-start(bf16[2,128,128]{2,1,0:T(8,128)(2,1)S(1)} %get-tuple-element.32.after_ref), channel_id=1, source_target_pairs={{0,64},{32,96},{64,0},{96,32},{1,65},{33,97},{65,1},{97,33},{2,66}... | collective-permute-start | bytes 196616 | tf_op jit(solution)/shard_map/ppermute | solution.py:376
  35.1 5.9 %collective-permute-start.6 = (bf16[2,128,128]{2,1,0:T(8,128)(2,1)S(1)}, bf16[2,128,128]{2,1,0:T(8,128)(2,1)S(1)}, u32[]{:S(2)}, u32[]{:S(2)}) collective-permute-start(bf16[2,128,128]{2,1,0:T(8,128)(2,1)S(1)} %get-tuple-element.32.after_ref), channel_id=1, source_target_pairs={{0,96},{32,0},{64,32},{96,64},{1,97},{33,1},{65,33},{97,65},{2,98}... | collective-permute-start | bytes 196616 | tf_op jit(solution)/shard_map/ppermute | solution.py:376
  36.1 7.2 %copy-start = (bf16[512,2048]{1,0:T(8,128)(2,1)S(1)}, bf16[512,2048]{1,0:T(8,128)(2,1)}, u32[]{:S(2)}) copy-start(bf16[512,2048]{1,0:T(8,128)(2,1)} %w_ref.1) | copy-start | bytes 6291460
  41.8 1.5 %collective-permute-start.7 = (bf16[2,128,128]{2,1,0:T(8,128)(2,1)S(1)}, bf16[2,128,128]{2,1,0:T(8,128)(2,1)S(1)}, u32[]{:S(2)}, u32[]{:S(2)}) collective-permute-start(bf16[2,128,128]{2,1,0:T(8,128)(2,1)S(1)} %plane_state.1.mine_ref), channel_id=1, source_target_pairs={{0,4},{4,0},{1,5},{5,1},{2,6},{6,2},{3,7},{7,3},{8,12},{12,8},{9,1... | collective-permute-start | bytes 196616 | tf_op jit(solution)/shard_map/ppermute | solution.py:381
  43.4 24.0 %copy-start.2 = (bf16[96,2048]{1,0:T(8,128)(2,1)S(1)}, bf16[96,2048]{1,0:T(8,128)(2,1)}, u32[]{:S(2)}) copy-start(bf16[96,2048]{1,0:T(8,128)(2,1)} %stream_ref.1) | copy-start | bytes 1179652
  43.4 24.0 %copy-start.4 = (f32[2048]{0:T(1024)S(1)}, f32[2048]{0:T(1024)}, u32[]{:S(2)}) copy-start(f32[2048]{0:T(1024)} %param.22) | copy-start | bytes 24580
  45.5 12.5 %collective-permute-start.8 = (bf16[96,2048]{1,0:T(8,128)(2,1)S(1)}, bf16[96,2048]{1,0:T(8,128)(2,1)S(1)}, u32[]{:S(2)}, u32[]{:S(2)}) collective-permute-start(bf16[96,2048]{1,0:T(8,128)(2,1)S(1)} %get-tuple-element.38), channel_id=1, source_target_pairs={{0,1},{1,2},{2,3},{3,0},{4,5},{5,6},{6,7},{7,4},{8,9},{9,10},{10,1... | collective-permute-start | bytes 1179656 | tf_op jit(solution)/shard_map/ppermute | solution.py:595
  47.0 20.3 %collective-permute-start.9 = (bf16[96,2048]{1,0:T(8,128)(2,1)S(1)}, bf16[96,2048]{1,0:T(8,128)(2,1)S(1)}, u32[]{:S(2)}, u32[]{:S(2)}) collective-permute-start(bf16[96,2048]{1,0:T(8,128)(2,1)S(1)} %get-tuple-element.39), channel_id=1, source_target_pairs={{0,2},{1,3},{2,0},{3,1},{4,6},{5,7},{6,4},{7,5},{8,10},{9,11},{10,... | collective-permute-start | bytes 1179656 | tf_op jit(solution)/shard_map/ppermute | solution.py:595
  49.8 17.6 %collective-permute-start.10 = (bf16[96,2048]{1,0:T(8,128)(2,1)S(1)}, bf16[96,2048]{1,0:T(8,128)(2,1)S(1)}, u32[]{:S(2)}, u32[]{:S(2)}) collective-permute-start(bf16[96,2048]{1,0:T(8,128)(2,1)S(1)} %get-tuple-element.40), channel_id=1, source_target_pairs={{0,3},{1,0},{2,1},{3,2},{4,7},{5,4},{6,5},{7,6},{8,11},{9,8},{10,9... | collective-permute-start | bytes 1179656 | tf_op jit(solution)/shard_map/ppermute | solution.py:595
  67.8 11.8 %collective-permute-start.11 = (bf16[96,2048]{1,0:T(8,128)(2,1)S(1)}, bf16[96,2048]{1,0:T(8,128)(2,1)S(1)}, u32[]{:S(2)}, u32[]{:S(2)}) collective-permute-start(bf16[96,2048]{1,0:T(8,128)(2,1)S(1)} %get-tuple-element.42.rest_0_), channel_id=1, source_target_pairs={{0,1},{1,2},{2,3},{3,0},{4,5},{5,6},{6,7},{7,4},{8,9},{9,10},{10,1... | collective-permute-start | bytes 1179656 | tf_op jit(solution)/shard_map/ppermute | solution.py:597
  69.2 10.6 %collective-permute-start.12 = (bf16[96,2048]{1,0:T(8,128)(2,1)S(1)}, bf16[96,2048]{1,0:T(8,128)(2,1)S(1)}, u32[]{:S(2)}, u32[]{:S(2)}) collective-permute-start(bf16[96,2048]{1,0:T(8,128)(2,1)S(1)} %get-tuple-element.42.rest_0_), channel_id=1, source_target_pairs={{0,3},{1,0},{2,1},{3,2},{4,7},{5,4},{6,5},{7,6},{8,11},{9,8},{10,9... | collective-permute-start | bytes 1179656 | tf_op jit(solution)/shard_map/ppermute | solution.py:598
  79.6 6.9 %collective-permute-start.13 = (bf16[48,2048]{1,0:T(8,128)(2,1)S(1)}, bf16[48,2048]{1,0:T(8,128)(2,1)S(1)}, u32[]{:S(2)}, u32[]{:S(2)}) collective-permute-start(bf16[48,2048]{1,0:T(8,128)(2,1)S(1)} %slice.8), channel_id=1, source_target_pairs={{0,1},{1,2},{2,3},{3,0},{4,5},{5,6},{6,7},{7,4},{8,9},{9,10},{10,1... | collective-permute-start | bytes 589832 | tf_op jit(solution)/shard_map/ppermute | solution.py:601
  79.9 6.7 %collective-permute-start.14 = (bf16[48,2048]{1,0:T(8,128)(2,1)S(1)}, bf16[48,2048]{1,0:T(8,128)(2,1)S(1)}, u32[]{:S(2)}, u32[]{:S(2)}) collective-permute-start(bf16[48,2048]{1,0:T(8,128)(2,1)S(1)} %slice.9), channel_id=1, source_target_pairs={{0,3},{1,0},{2,1},{3,2},{4,7},{5,4},{6,5},{7,6},{8,11},{9,8},{10,9... | collective-permute-start | bytes 589832 | tf_op jit(solution)/shard_map/ppermute | solution.py:602
Sparse Core Ops, SparseCore 0:
  9.6 78.7 all-gather.1
